TPU v7x, 512 devices: a whole 4x8x8 slice. The times are simulated.
512 devices in a mesh: sp: 32 (over z, x), tp: 16 (over y, core).
Axes of the slice: x: 4, y: 8, z: 8, core: 2. Of those that a mesh axis runs over, the one named last changes fastest.
Arguments:
- latent: bfloat16 [8192, 2048], P(('sp', 'tp')), may hold values from -6 to 6
- cond: float32 [2048], replicated, may hold values from -6 to 6
- ctx_mod: float32 [2048], replicated, may hold values from -6 to 6
- context: bfloat16 [512, 2048], P(('sp', 'tp')), may hold values from -6 to 6
- shift_w: float32 [2048, 2048], P('sp', 'tp'), may hold values from -0.125 to 0.125
- scale_w: float32 [2048, 2048], P('sp', 'tp'), may hold values from -0.125 to 0.125
- gate_w: float32 [2048, 2048], P('sp', 'tp'), may hold values from -0.125 to 0.125
- norm_gain: float32 [2048], replicated, may hold values from 0.1 to 1.9
- w_qn: bfloat16 [2048, 2048], P(None, 'tp'), may hold values from -0.125 to 0.125
- w_qr: bfloat16 [2048, 1024], P(None, 'tp'), may hold values from -0.13258252 to 0.13258252
- w_kv_down: bfloat16 [2048, 512], replicated, may hold values from -0.125 to 0.125
- w_rope_key: bfloat16 [2048, 64], replicated, may hold values from -0.13258252 to 0.13258252
- kv_gain: float32 [512], replicated, may hold values from 0.1 to 1.9
- w_key_up: bfloat16 [512, 2048], P(None, 'tp'), may hold values from -0.66015625 to 0.66015625
- w_value_up: bfloat16 [512, 2048], P(None, 'tp'), may hold values from -0.25 to 0.25
- ctx_bias: float32 [16], P('tp'), may hold values from 2 to 3.5
- w_out: bfloat16 [2048, 2048], P('tp'), may hold values from -0.52734375 to 0.52734375
Outputs:
- mixed: bfloat16 [8192, 2048], P(('sp', 'tp'))
All inputs are finite; a program needn't handle non-finite values.
Results may differ from a plain program's by a relative error of at most 0.018.
Values may be sent and summed in bfloat16 or wider, within the bound.
No kernel may reach another device: no remote copies, remote signals or barrier semaphores. Data moves between devices by JAX's collectives and lax.ppermute only.
A program may use at most 64 MiB of HBM per device.

v0:
```python
import jax
import jax.numpy as jnp
from jax import lax
from jax.sharding import PartitionSpec as P

GRID_W = 128


EPS = 1e-06
ROPE_BASE = 10000.0


def sent_to_all(array, axis):
    devices = lax.axis_size(axis)
    return lax.all_to_all(
        jnp.broadcast_to(array[None], (devices, *array.shape)), axis, 0, 0, tiled=True
    )


def taken_together(array, axis):
    everything = sent_to_all(array, axis)
    return jnp.sum(everything, axis=0)


def packed_total(arrays, axis):
    line, at, outs = (jnp.concatenate([a.reshape(-1) for a in arrays]), 0, [])
    so_far = taken_together(line, axis)
    for a in arrays:
        outs.append(so_far[at : at + a.size].reshape(a.shape))
        at += a.size
    return tuple(outs)


def sent_together(arrays, axis, dim, along):
    both = jnp.concatenate(arrays, axis=along)
    result, at, outs = (lax.all_gather(both, axis, axis=dim, tiled=True), 0, [])
    for a in arrays:
        outs.append(lax.slice_in_dim(result, at, at + a.shape[along], axis=along))
        at += a.shape[along]
    return tuple(outs)


def in_order(pieces, dim):
    pieces = jnp.moveaxis(pieces, 0, dim)
    dims = pieces.shape
    return pieces.reshape(*dims[:dim], dims[dim] * dims[dim + 1], *dims[dim + 2 :])


def gathered_copies(array, axis, dim):
    return in_order(sent_to_all(array, axis), dim)


def cut_along(array, dim, devices):
    before, after = (array.shape[:dim], array.shape[dim + 1 :])
    return jnp.moveaxis(array.reshape(*before, devices, -1, *after), dim, 0)


def sum_at_owner(array, axis, dim):
    devices = lax.axis_size(axis)
    pieces = lax.all_to_all(cut_along(array, dim, devices), axis, 0, 0, tiled=True)
    return jnp.sum(pieces.astype(jnp.float32), axis=0)


def modulate(rows_in, gain, shift, scale):
    values = rows_in.astype(jnp.float32)
    normed = values * lax.rsqrt(jnp.mean(values * values, axis=-1, keepdims=True) + EPS)
    return (normed * gain * (1.0 + scale) + shift).astype(jnp.bfloat16)


def compress(rows_in, w_kv_down, kv_gain):
    inner = jnp.dot(rows_in, w_kv_down, preferred_element_type=jnp.float32)
    normed = inner * lax.rsqrt(jnp.mean(inner * inner, axis=-1, keepdims=True) + EPS)
    return (normed * kv_gain).astype(jnp.bfloat16)


def angles(positions, rope_dim):
    quarter = rope_dim // 4
    inverse = ROPE_BASE ** (-jnp.arange(quarter, dtype=jnp.float32) / quarter)
    row = (positions // GRID_W).astype(jnp.float32)
    column = (positions % GRID_W).astype(jnp.float32)
    return jnp.concatenate(
        [row[:, None] * inverse[None, :], column[:, None] * inverse[None, :]], axis=-1
    )


def rotate(values, angle):
    pairs = values.reshape(values.shape[:-1] + (values.shape[-1] // 2, 2))
    first = pairs[..., 0]
    second = pairs[..., 1]
    cosine = jnp.cos(angle)
    sine = jnp.sin(angle)
    turned = jnp.stack([first * cosine - second * sine, first * sine + second * cosine], axis=-1)
    return turned.reshape(values.shape)


def body(
    latent,
    cond,
    ctx_mod,
    context,
    shift_w,
    scale_w,
    gate_w,
    norm_gain,
    w_qn,
    w_qr,
    w_kv_down,
    w_rope_key,
    kv_gain,
    w_key_up,
    w_value_up,
    ctx_bias,
    w_out,
):
    n_tp = lax.axis_size("tp")
    sp_index = lax.axis_index("sp")
    tp_index = lax.axis_index("tp")
    rows = latent.shape[0]
    ctx_rows = context.shape[0]
    tok_dev = rows * n_tp
    heads_dev = ctx_bias.shape[0]
    nope = w_key_up.shape[1] // heads_dev
    vsize = w_value_up.shape[1] // heads_dev
    rope = w_rope_key.shape[1]
    period = rows + ctx_rows
    factor = (nope + rope) ** (-0.5)
    pair = jnp.stack([jax.nn.silu(cond), jax.nn.silu(ctx_mod)])
    feat_block = shift_w.shape[0]
    pair_block = lax.dynamic_slice_in_dim(pair, sp_index * feat_block, feat_block, 1)
    partials = tuple(
        (
            jnp.dot(pair_block, weight, precision=lax.Precision.HIGHEST)
            for weight in (shift_w, scale_w, gate_w)
        )
    )
    summed = packed_total((partials[0], partials[1], partials[2]), "sp")
    shift, scale, gate = sent_together((summed[0], summed[1], summed[2]), "tp", 1, 0)
    h_rows = modulate(latent, norm_gain, shift[0], scale[0])
    h_ctx = modulate(context, norm_gain, shift[1], scale[1])
    own_positions = sp_index * tok_dev + tp_index * rows + jnp.arange(rows, dtype=jnp.int32)
    own_latents = jnp.concatenate(
        [compress(h_rows, w_kv_down, kv_gain), compress(h_ctx, w_kv_down, kv_gain)], axis=0
    )
    rope_rows = rotate(
        jnp.dot(h_rows, w_rope_key, preferred_element_type=jnp.float32), angles(own_positions, rope)
    ).astype(jnp.bfloat16)
    rope_ctx = jnp.dot(h_ctx, w_rope_key, preferred_element_type=jnp.float32).astype(jnp.bfloat16)
    own_rope = jnp.concatenate([rope_rows, rope_ctx], axis=0)
    piece = gathered_copies(h_rows, "tp", 0)
    count = piece.shape[0]
    nope_part = jnp.dot(piece, w_qn, preferred_element_type=jnp.float32).astype(jnp.bfloat16)
    places = sp_index * tok_dev + jnp.arange(count, dtype=jnp.int32)
    rope_part = jnp.dot(piece, w_qr, preferred_element_type=jnp.float32).reshape(
        count, heads_dev, rope
    )
    rope_part = rotate(rope_part, angles(places, rope)[:, None, :]).reshape(count, heads_dev * rope)
    queries = jnp.concatenate([nope_part, rope_part.astype(jnp.bfloat16)], axis=1)
    query_nope = queries[:, : heads_dev * nope].reshape(tok_dev, heads_dev, nope)
    query_rope = queries[:, heads_dev * nope :].reshape(tok_dev, heads_dev, rope)
    seq_latents, seq_rope = sent_together((own_latents, own_rope), "tp", 0, 1)
    head_nope = jnp.dot(seq_latents, w_key_up, preferred_element_type=jnp.float32).astype(
        jnp.bfloat16
    )
    head_values = jnp.dot(seq_latents, w_value_up, preferred_element_type=jnp.float32).astype(
        jnp.bfloat16
    )
    pieces = sent_together((head_nope, head_values, seq_rope), "sp", 0, 1)
    keys = pieces[0]
    values = pieces[1]
    rope_keys = pieces[2]
    best = jnp.full((heads_dev, tok_dev), -1e30, jnp.float32)
    count = rope_keys.shape[0]
    keys = keys.reshape(count, heads_dev, nope)
    values = values.reshape(count, heads_dev, vsize)
    scores = jnp.einsum("qhd,khd->hqk", query_nope, keys, preferred_element_type=jnp.float32)
    scores = scores + jnp.einsum(
        "qhr,kr->hqk", query_rope, rope_keys, preferred_element_type=jnp.float32
    )
    index = jnp.arange(count, dtype=jnp.int32)
    is_ctx = (index % period >= rows).astype(jnp.float32)
    scores = scores * factor + ctx_bias[:, None, None] * is_ctx[None, None, :]
    new_best = jnp.maximum(best, jnp.max(scores, axis=-1))
    weights = jnp.exp(scores - new_best[..., None])
    total = jnp.sum(weights, axis=-1)
    accum = jnp.einsum(
        "hqk,khd->hqd", weights.astype(jnp.bfloat16), values, preferred_element_type=jnp.float32
    )
    best, total, accum = (new_best, total, accum)
    attended = (accum / total[..., None]).astype(jnp.bfloat16)
    attended = jnp.transpose(attended, (1, 0, 2)).reshape(tok_dev, heads_dev * vsize)
    branch = sum_at_owner(
        jnp.dot(attended, w_out, preferred_element_type=jnp.float32).astype(jnp.bfloat16), "tp", 0
    )
    return (latent.astype(jnp.float32) + gate[0] * branch).astype(jnp.bfloat16)


def solution(mesh):
    placed = (
        P(("sp", "tp"), None),
        P(),
        P(),
        P(("sp", "tp"), None),
        P("sp", "tp"),
        P("sp", "tp"),
        P("sp", "tp"),
        P(),
        P(None, "tp"),
        P(None, "tp"),
        P(),
        P(),
        P(),
        P(None, "tp"),
        P(None, "tp"),
        P("tp"),
        P("tp", None),
    )
    return jax.shard_map(
        body, mesh=mesh, in_specs=placed, out_specs=P(("sp", "tp"), None), check_vma=False
    )
```

profile of v0, /device:TPU:1, one launch (start us, length us, event | category | flops | bytes accessed | tf_op | source)
XLA Modules:
  0.0 238.9 jit_solution(6771261742470312171)
XLA Ops:
  6.5 0.0 copy-start
  6.5 0.0 copy-start.2
  6.5 0.0 copy-start.3
  6.5 0.9 divide_multiply_fusion.1
  7.4 0.7 divide_multiply_fusion
  8.1 1.0 convolution_bitcast_fusion.3
  9.1 1.0 convolution_bitcast_fusion.4
  10.0 1.0 convolution_bitcast_fusion.5
  11.0 0.7 broadcast_in_dim.8
  11.7 13.7 %all-to-all-start = ((f32[32,1,768]{2,1,0:T(1,128)}), f32[32,1,768]{2,1,0:T(1,128)S(1)}, u32[]{:S(2)}, u32[]{:S(2)}) async-start(f32[32,1,768]{2,1,0:T(1,128)} %broadcast_in_dim.8), calls=%async_computation | async-start | bytes 196608 | tf_op jit(solution)/shard_map/all_to_all | solution.py:15
  25.4 0.0 all-gather.3.cloned.1.call-start
  25.5 1.0 fusion.31
  26.5 1.3 multiply_reduce_fusion.1
  28.5 0.1 multiply_bitcast_fusion.3
  28.6 6.0 %all-to-all-done = f32[32,1,768]{2,1,0:T(1,128)S(1)} async-done(((f32[32,1,768]{2,1,0:T(1,128)}), f32[32,1,768]{2,1,0:T(1,128)S(1)}, u32[]{:S(2)}, u32[]{:S(2)}) %all-to-all-start) | async-done | bytes 98336 | tf_op jit(solution)/shard_map/all_to_all | solution.py:15
  34.5 0.1 reduce_sum.63
  34.6 19.7 %all_gather.9 = f32[6,2048]{1,0:T(8,128)S(1)} all-gather(f32[6,128]{1,0:T(8,128)S(1)} %pad_maximum_fusion.6), channel_id=1, replica_groups=mesh['sp'=32,'tp'=16] {'tp'}, dimensions={1}, use_global_device_ids=true | all-gather | bytes 52224 | tf_op jit(solution)/shard_map/all_gather | solution.py:36
  54.3 0.9 fusion.35
  55.3 0.0 copy-done
  55.3 0.5 multiply_reduce_fusion
  55.8 1.2 fusion.65
  56.9 1.1 fusion.60
  58.0 1.2 fusion.13
  59.2 0.1 copy.65
  59.3 0.1 copy.66
  59.4 0.1 subtract_convert_fusion.1
  59.5 0.1 copy.54
  59.6 0.1 copy.55
  59.7 0.6 multiply_reduce_fusion.2
  61.0 0.7 multiply_convert_fusion.1
  61.7 0.8 multiply_convert_fusion
  62.5 16.3 %all-gather = bf16[16,17,576]{2,1,0:T(8,128)(2,1)S(1)} all-gather(bf16[1,17,576]{2,1,0:T(8,128)(2,1)S(1)} %maximum_bitcast_fusion), channel_id=1, replica_groups=mesh['sp'=32,'tp'=16] {'tp'}, dimensions={0}, use_global_device_ids=true | all-gather | bytes 332928 | tf_op jit(solution)/shard_map/all_gather | solution.py:36
  78.8 0.2 reshape.561
  78.9 0.0 copy-done.2
  79.0 0.2 convolution_convert_fusion.1
  79.2 0.0 copy-done.3
  79.2 0.2 convolution_convert_fusion.2
  79.4 0.7 pad_maximum_fusion
  80.2 0.0 all-gather.3.cloned.1.call-update
  80.2 1.1 broadcast_in_dim.9
  81.3 5.0 %all-to-all-start.1 = ((bf16[16,16,2048]{2,1,0:T(8,128)(2,1)}), bf16[16,16,2048]{2,1,0:T(8,128)(2,1)S(1)}, u32[]{:S(2)}, u32[]{:S(2)}) async-start(bf16[16,16,2048]{2,1,0:T(8,128)(2,1)} %broadcast_in_dim.9), calls=%async_computation.1 | async-start | bytes 2097152 | tf_op jit(solution)/shard_map/all_to_all | solution.py:15
  86.3 1.1 reshape.557
  88.1 0.1 multiply_bitcast_fusion.1
  88.2 26.1 %all-to-all-done.1 = bf16[16,16,2048]{2,1,0:T(8,128)(2,1)S(1)} async-done(((bf16[16,16,2048]{2,1,0:T(8,128)(2,1)}), bf16[16,16,2048]{2,1,0:T(8,128)(2,1)S(1)}, u32[]{:S(2)}, u32[]{:S(2)}) %all-to-all-start.1) | async-done | bytes 1048608 | tf_op jit(solution)/shard_map/all_to_all | solution.py:15
  114.3 0.4 convolution_bitcast_fusion.2
  114.8 0.1 subtract_convert_fusion
  115.0 53.2 %all-gather.3.cloned.1.call-done = bf16[8704,320]{1,0:T(8,128)(2,1)} async-done(((bf16[272,320]{1,0:T(8,128)(2,1)}), bf16[8704,320]{1,0:T(8,128)(2,1)}) %all-gather.3.cloned.1.call-update) | async-done | bytes 5570576 | tf_op jit(solution)/shard_map/all_gather | solution.py:36
  168.2 6.4 %convolution_bitcast_fusion = f32[1,256,8704]{2,1,0:T(8,128)} fusion(bf16[256,64]{0,1:T(8,128)(2,1)S(1)} %convert_element_type.110, bf16[8704,320]{1,0:T(8,128)(2,1)} %all-gather.3.cloned.1.call-done), kind=kOutput, calls=%fused_computation | convolution fusion | flops 285212672 | bytes 11173888 | tf_op jit(solution)/shard_map/qhr,kr->hqk/dot_general | solution.py:176
  174.6 9.5 %fusion.64 = (f32[256]{0:T(256)S(1)}, f32[1,256,8704]{2,1,0:T(8,128)}) fusion(f32[8704]{0:T(1024)S(1)} %fusion.42, f32[1,256,8704]{2,1,0:T(8,128)} %convolution_bitcast_fusion, bf16[8704,320]{1,0:T(8,128)(2,1)} %all-gather.3.cloned.1.call-done, bf16[256,2048]{1,0:T(8,128)(2,1)S(1)} %bitcast.92, bf16[2048,128]{1,0:T(8,128)(2,1)} %param.25), kind=kOutput, calls=%fused_computation.112 | convolution fusion | flops 713588480 | bytes 21662720 | tf_op jit(solution)/shard_map/qhd,khd->hqk/dot_general | solution.py:175
  184.1 4.9 %fusion.3 = f32[256]{0:T(256)S(1)} fusion(f32[1,256,8704]{2,1,0:T(8,128)} %get-tuple-element.24, f32[256]{0:T(256)S(1)} %broadcast_maximum_fusion), kind=kLoop, calls=%fused_computation.6 | loop fusion | flops 4456192 | bytes 8914944 | tf_op jit(solution)/shard_map/reduce_sum | solution.py:184
  189.0 0.0 copy-start.1
  189.0 6.1 %convolution_convert_fusion = bf16[256,2048]{1,0:T(8,128)(2,1)S(1)} fusion(bf16[128,2048]{1,0:T(8,128)(2,1)} %param.33, bf16[8704,320]{1,0:T(8,128)(2,1)} %all-gather.3.cloned.1.call-done, f32[1,256,8704]{2,1,0:T(8,128)} %get-tuple-element.24, f32[256]{0:T(256)S(1)} %broadcast_maximum_fusion, f32[256]{0:T(256)S(1)} %fusion.3), kind=kOutput, calls=%fused_computation.11 | convolution fusion | flops 709689344 | bytes 12716032 | tf_op jit(solution)/shard_map/dot_general | solution.py:192
  195.1 36.1 %all_to_all.16 = bf16[16,16,2048]{2,1,0:T(8,128)(2,1)S(1)} all-to-all(bf16[16,16,2048]{2,1,0:T(8,128)(2,1)S(1)} %bitcast.93), channel_id=1, replica_groups=mesh['sp'=32,'tp'=16] {'tp'}, dimensions={0} | all-to-all | bytes 2097152 | tf_op jit(solution)/shard_map/all_to_all | solution.py:60
  231.2 0.1 convert_reduce_fusion
  231.3 0.0 copy-done.1
  231.4 0.6 fusion.36
  (19 shorter events, 0.3 us)
Async XLA Ops:
  6.5 48.7 %copy-start = (bf16[2048,512]{1,0:T(8,128)(2,1)S(1)}, bf16[2048,512]{1,0:T(8,128)(2,1)}, u32[]{:S(2)}) copy-start(bf16[2048,512]{1,0:T(8,128)(2,1)} %param.27) | copy-start | bytes 6291460
  6.5 72.4 %copy-start.2 = (bf16[512,128]{1,0:T(8,128)(2,1)S(1)}, bf16[512,128]{1,0:T(8,128)(2,1)}, u32[]{:S(2)}) copy-start(bf16[512,128]{1,0:T(8,128)(2,1)} %param.31) | copy-start | bytes 393220
  6.5 72.6 %copy-start.3 = (bf16[512,128]{1,0:T(8,128)(2,1)S(1)}, bf16[512,128]{1,0:T(8,128)(2,1)}, u32[]{:S(2)}) copy-start(bf16[512,128]{1,0:T(8,128)(2,1)} %param.30) | copy-start | bytes 393220
  11.7 22.8 %all-to-all-start = ((f32[32,1,768]{2,1,0:T(1,128)}), f32[32,1,768]{2,1,0:T(1,128)S(1)}, u32[]{:S(2)}, u32[]{:S(2)}) async-start(f32[32,1,768]{2,1,0:T(1,128)} %broadcast_in_dim.8), calls=%async_computation | async-start | bytes 196608 | tf_op jit(solution)/shard_map/all_to_all | solution.py:15
  25.4 142.8 %all-gather.3.cloned.1.call-start = ((), (), s32[]{:S(2)}) async-start(), calls=%async_computation.3 | async-start | bytes 6893568 | tf_op jit(solution)/shard_map/all_gather | solution.py:36
  81.3 33.0 %all-to-all-start.1 = ((bf16[16,16,2048]{2,1,0:T(8,128)(2,1)}), bf16[16,16,2048]{2,1,0:T(8,128)(2,1)S(1)}, u32[]{:S(2)}, u32[]{:S(2)}) async-start(bf16[16,16,2048]{2,1,0:T(8,128)(2,1)} %broadcast_in_dim.9), calls=%async_computation.1 | async-start | bytes 2097152 | tf_op jit(solution)/shard_map/all_to_all | solution.py:15
  189.0 42.4 %copy-start.1 = (bf16[16,2048]{1,0:T(8,128)(2,1)S(1)}, bf16[16,2048]{1,0:T(8,128)(2,1)}, u32[]{:S(2)}) copy-start(bf16[16,2048]{1,0:T(8,128)(2,1)} %param.17) | copy-start | bytes 196612
Sparse Core Ops, SparseCore 0:
  80.3 87.8 all-gather.2
where the time goes:
time: 240 us; the launch traced here: 239 us
  waiting for transfers between devices  85.3 us (36%)
  blocking collectives  72 us (30%)
  matrix products  29.8 us (12%)
  starting transfers between devices  18.8 us (8%)
  between operations  15.6 us (6%)
  other arithmetic  13.9 us (6%)
  local copies, waits for them, and re-layouts  3.53 us (1%)
    all_gather x1, waiting for transfers between devices, sent_together(): result, at, outs = (lax.all_gather(both, axis, axis=dim, tiled=True), 0, [])  53.2 us
    all_to_all x1, blocking collectives, sum_at_owner(): lax.all_to_all(cut_along(array, dim, devices), axis, 0, 0, tiled=True)  36.1 us
    all_gather x2, blocking collectives, sent_together(): result, at, outs = (lax.all_gather(both, axis, axis=dim, tiled=True), 0, [])  35.9 us
    all_to_all x2, waiting for transfers between devices, sent_to_all(): lax.all_to_all(jnp.broadcast_to(array[None], (devices, *array.shape)), ax...  32 us
    all_to_all x2, starting transfers between devices, sent_to_all(): lax.all_to_all(jnp.broadcast_to(array[None], (devices, *array.shape)), ax...  18.7 us
    dot_general x1, matrix products, body(): jnp.einsum('qhd,khd->hqk', query_nope, keys, preferred_element_type=jnp.f...  9.54 us
    dot_general x1, matrix products, body(): jnp.einsum('qhr,kr->hqk', query_rope, rope_keys, preferred_element_type=j...  6.4 us
    dot_general x1, matrix products, body(): jnp.dot(attended, w_out, preferred_element_type=jnp.float32)  6.12 us
  transfers between devices with their start and end apart: 3, of which 3 were waited for; matrix products, arithmetic and copies ran while one was open for 2% of the time, Pallas kernels for 0%

commit v1 on v0

v1 whole, which is shorter than its diff:
```python
import functools

import jax
import jax.numpy as jnp
from jax import lax
from jax.experimental import pallas as pl
from jax.experimental.pallas import tpu as pltpu
from jax.sharding import Mesh
from jax.sharding import PartitionSpec as P

GRID_W = 128
EPS = 1e-06
ROPE_BASE = 10000.0
LOG2E = 1.4426950408889634
F32 = jnp.float32
BF16 = jnp.bfloat16
SP = ("za", "zb", "x")
TP = ("y", "c")
CORE_FIRST = ("c", "y")
KV_AXES = ("zb", "x")
Q_AXES = ("za",)


def copies(array, axes):
    n = lax.axis_size(axes)
    return lax.all_to_all(jnp.broadcast_to(array[None], (n, *array.shape)), axes, 0, 0, tiled=True)


def exchanged(array, axes):
    return lax.all_to_all(array, axes, 0, 0, tiled=True)


def modulate(rows_in, gain, shift, scale):
    values = rows_in.astype(F32)
    normed = values * lax.rsqrt(jnp.mean(values * values, axis=-1, keepdims=True) + EPS)
    return (normed * gain * (1.0 + scale) + shift).astype(BF16)


def angles(positions, rope_dim):
    quarter = rope_dim // 4
    inverse = ROPE_BASE ** (-jnp.arange(quarter, dtype=F32) / quarter)
    row = (positions // GRID_W).astype(F32)
    column = (positions % GRID_W).astype(F32)
    return jnp.concatenate([row[:, None] * inverse[None, :], column[:, None] * inverse[None, :]], axis=-1)


def split_pairs(weight):
    return jnp.concatenate([weight[:, 0::2], weight[:, 1::2]], axis=1)


def rotate_halves(values, cosine, sine):
    half = values.shape[-1] // 2
    first = values[:, :half]
    second = values[:, half:]
    return jnp.concatenate([first * cosine - second * sine, first * sine + second * cosine], axis=-1)


def attend_kernel(q_ref, k_ref, v_ref, b_ref, o_ref, s_ref, *, factor, latents):
    q = q_ref[...]
    dims = (((1,), (1,)), ((), ()))
    bias = b_ref[0, 0] * LOG2E
    main = lax.dot_general(q, k_ref[:latents], dims, preferred_element_type=F32) * (factor * LOG2E)
    side = lax.dot_general(q, k_ref[latents:], dims, preferred_element_type=F32) * (factor * LOG2E) + bias
    top = jnp.maximum(jnp.max(main, axis=1, keepdims=True), jnp.max(side, axis=1, keepdims=True))
    main = jnp.exp2(main - top)
    side = jnp.exp2(side - top)
    total = jnp.sum(main, axis=1, keepdims=True) + jnp.sum(side, axis=1, keepdims=True)
    out = jnp.dot(main.astype(BF16), v_ref[:latents], preferred_element_type=F32)
    out = out + jnp.dot(side.astype(BF16), v_ref[latents:], preferred_element_type=F32)
    o_ref[...] = (out / total).astype(BF16)
    s_ref[...] = top + jnp.log2(total)


def attend(queries, keys, values, bias, factor, latents):
    tile = 256
    count, width = queries.shape
    n_keys = keys.shape[0]
    vsize = values.shape[1]
    return pl.pallas_call(
        functools.partial(attend_kernel, factor=factor, latents=latents),
        grid=(count // tile,),
        in_specs=[
            pl.BlockSpec((tile, width), lambda i: (i, 0)),
            pl.BlockSpec((n_keys, width), lambda i: (0, 0)),
            pl.BlockSpec((n_keys, vsize), lambda i: (0, 0)),
            pl.BlockSpec((1, 1), lambda i: (0, 0), memory_space=pltpu.SMEM),
        ],
        out_specs=[pl.BlockSpec((tile, vsize), lambda i: (i, 0)), pl.BlockSpec((tile, 1), lambda i: (i, 0))],
        out_shape=[jax.ShapeDtypeStruct((count, vsize), BF16), jax.ShapeDtypeStruct((count, 1), F32)],
        name="attend",
    )(queries, keys, values, bias)


def three_parts(value):
    high = value.astype(BF16)
    rest = value - high.astype(F32)
    middle = rest.astype(BF16)
    low = (rest - middle.astype(F32)).astype(BF16)
    return jnp.stack([high, middle, low], axis=-2)


def body(
    latent, cond, ctx_mod, context, shift_w, scale_w, gate_w, norm_gain, w_qn, w_qr, w_kv_down, w_rope_key, kv_gain,
    w_key_up, w_value_up, ctx_bias, w_out,
):
    n_tp = lax.axis_size(TP)
    n_c = lax.axis_size("c")
    n_y = lax.axis_size("y")
    sp_index = lax.axis_index(SP)
    rows, width = latent.shape
    lanes = width // rows
    tok = rows * n_tp
    nope = w_key_up.shape[1]
    vsize = w_value_up.shape[1]
    rope = w_rope_key.shape[1]
    rank = w_kv_down.shape[1]
    factor = (nope + rope) ** (-0.5)

    raw = copies(jnp.concatenate([latent, context.reshape(rows, lanes)], axis=1), CORE_FIRST)

    feat = shift_w.shape[0]
    own = jnp.stack([lax.dynamic_slice_in_dim(v, sp_index * feat, feat) for v in (cond, ctx_mod)])
    own = jax.nn.silu(own)
    parts = [jnp.sum(own[i][:, None] * w, axis=0) for w, i in ((shift_w, 0), (shift_w, 1), (scale_w, 0), (scale_w, 1), (gate_w, 0))]
    summed = jnp.sum(copies(jnp.stack(parts), SP), axis=0)
    vectors = copies(summed, TP)
    vectors = jnp.moveaxis(vectors, 0, 1).reshape(5, width)
    gate = vectors[4]

    w_pair = copies(w_out, ("c",)).reshape(n_c * vsize, width)

    rows_all = raw[:, :, :width].reshape(tok, width)
    ctx_all = raw[:, :, width:].reshape(n_tp, width)
    h_rows = modulate(rows_all, norm_gain, vectors[0], vectors[2])
    h_ctx = modulate(ctx_all, norm_gain, vectors[1], vectors[3])
    h = jnp.concatenate([h_rows, h_ctx], axis=0)

    place = jnp.arange(tok, dtype=jnp.int32)
    place = (place // rows % n_y * n_c + place // (rows * n_y)) * rows + place % rows
    turn = angles(sp_index * tok + place, rope)
    cosine = jnp.cos(turn)
    sine = jnp.sin(turn)
    q_nope = jnp.dot(h_rows, w_qn, preferred_element_type=F32).astype(BF16)
    q_rope = rotate_halves(jnp.dot(h_rows, split_pairs(w_qr), preferred_element_type=F32), cosine, sine).astype(BF16)
    queries = copies(jnp.concatenate([q_nope, q_rope], axis=1), Q_AXES)
    n_q = queries.shape[0]
    queries = queries.reshape(n_q * tok, nope + rope)

    inner = jnp.dot(h, w_kv_down, preferred_element_type=F32)
    inner = (inner * lax.rsqrt(jnp.mean(inner * inner, axis=-1, keepdims=True) + EPS) * kv_gain).astype(BF16)
    k_rope = jnp.dot(h, split_pairs(w_rope_key), preferred_element_type=F32)
    k_rope = jnp.concatenate([rotate_halves(k_rope[:tok], cosine, sine), k_rope[tok:]], axis=0).astype(BF16)
    k_nope = jnp.dot(inner, w_key_up, preferred_element_type=F32).astype(BF16)
    value = jnp.dot(inner, w_value_up, preferred_element_type=F32).astype(BF16)
    kv = copies(jnp.concatenate([k_nope, k_rope, value], axis=1), KV_AXES)
    kv = jnp.concatenate([kv[:, :tok].reshape(-1, kv.shape[2]), kv[:, tok:].reshape(-1, kv.shape[2])], axis=0)
    n_keys = kv.shape[0]
    latents = n_keys // (tok + n_tp) * tok

    out, lse = attend(queries, kv[:, : nope + rope], kv[:, nope + rope :], ctx_bias.reshape(1, 1), factor, latents)

    half = tok // n_c
    out = out.reshape(n_q * n_c, half, vsize)
    stats = three_parts(lse.reshape(n_q * n_c, half))
    stats = jnp.pad(stats, ((0, 0), (0, 16 - stats.shape[1]), (0, vsize - half)))
    got = exchanged(jnp.concatenate([out, stats], axis=1), (*Q_AXES, "c")).reshape(n_q, n_c, half + 16, vsize)
    lse = jnp.sum(got[:, :, half : half + 3, :half].astype(F32), axis=2)
    share = jnp.exp2(lse - jnp.max(lse, axis=0))
    share = share / jnp.sum(share, axis=0)
    attended = jnp.sum(got[:, :, :half].astype(F32) * share[..., None], axis=0).astype(BF16)
    attended = jnp.moveaxis(attended, 0, 1).reshape(half, n_c * vsize)

    term = jnp.dot(attended, w_pair, preferred_element_type=F32).astype(BF16)
    branch = jnp.sum(exchanged(term.reshape(n_y, rows, width), ("y",)).astype(F32), axis=0)
    return (latent.astype(F32) + gate * branch).astype(BF16)


def solution(mesh):
    fine = Mesh(mesh.devices.reshape(4, 2, 4, 8, 2), ("za", "zb", "x", "y", "c"))
    row = P((*SP, *TP), None)
    placed = (
        row, P(), P(), row, P(SP, TP), P(SP, TP), P(SP, TP), P(), P(None, TP), P(None, TP), P(), P(), P(), P(None, TP),
        P(None, TP), P(TP), P(TP, None),
    )
    return jax.shard_map(body, mesh=fine, in_specs=placed, out_specs=row, check_vma=False)
```

time: 240 us -> 187 us (0.78)
  blocking collectives: 72 us -> 38.1 us
  matrix products: 29.8 us -> 4.39 us
  starting transfers between devices: 18.8 us -> 39.2 us
  waiting for transfers between devices: 85.3 us -> 70.2 us
  between operations: 15.6 us -> 1.07 us
  local copies, waits for them, and re-layouts: 3.53 us -> 14.4 us
  Pallas kernels: 0 us -> 7.26 us
  other arithmetic: 13.9 us -> 11.4 us
    all_gather x1 -> x0, waiting for transfers between devices: 53.2 us -> none  [sent_together(): result, at, outs = (lax.all_gather(both, axis, axis=dim, tiled=True), 0, [])]
    all_to_all x2 -> x6, waiting for transfers between devices: 32 us -> 70.2 us  [copies(): lax.all_to_all(jnp.broadcast_to(array[None], (n, *array.shape)), axes, 0,...]
    all_gather x2 -> x0, blocking collectives: 35.9 us -> none  [sent_together(): result, at, outs = (lax.all_gather(both, axis, axis=dim, tiled=True), 0, [])]
    dot_general x13 -> x7, matrix products: 29.8 us -> 4.39 us  [the longest x1 1.71 us: body(): q_nope = jnp.dot(h_rows, w_qn, preferred_element_type=F32).astype(BF16)]
    all_to_all x2 -> x6, starting transfers between devices: 18.7 us -> 39.2 us  [copies(): lax.all_to_all(jnp.broadcast_to(array[None], (n, *array.shape)), axes, 0,...]
    pallas_call x0 -> x1, Pallas kernels: none -> 7.26 us  [attend(): pl.pallas_call(functools.partial(attend_kernel, factor=factor, latents=la...]
    slice x3 -> x7, local copies, waits for them, and re-layouts: 0.05 us -> 6.13 us  [the longest x4 3.62 us: split_pairs(): return jnp.concatenate([weight[:, 0::2], weight[:, 1::2]], axis=1)]
    reduce_sum x4 -> x6, other arithmetic: 5.7 us -> 1.25 us  [the longest x1 0.89 us: body(): jnp.sum(own[i][:, None] * w, axis=0)]
  transfers between devices with their start and end apart: 3 -> 6, of which waited for: 3 -> 6; matrix products, arithmetic and copies ran while one was open for 2% -> 5% of each run, Pallas kernels for 0% -> 0%
where the time goes in v1:
time: 187 us; the launch traced here: 186 us
  waiting for transfers between devices  70.2 us (38%)
  starting transfers between devices  39.2 us (21%)
  blocking collectives  38.1 us (20%)
  local copies, waits for them, and re-layouts  14.4 us (8%)
  other arithmetic  11.4 us (6%)
  Pallas kernels  7.26 us (4%)
  matrix products  4.39 us (2%)
    all_to_all x6, waiting for transfers between devices, copies(): lax.all_to_all(jnp.broadcast_to(array[None], (n, *array.shape)), axes, 0,...  70.2 us
    all_to_all x6, starting transfers between devices, copies(): lax.all_to_all(jnp.broadcast_to(array[None], (n, *array.shape)), axes, 0,...  39.2 us
    all_to_all x2, blocking collectives, exchanged(): return lax.all_to_all(array, axes, 0, 0, tiled=True)  38.1 us
    pallas_call x1, Pallas kernels, attend(): pl.pallas_call(functools.partial(attend_kernel, factor=factor, latents=la...  7.26 us
    broadcast_in_dim x6, local copies, waits for them, and re-layouts, copies(): jnp.broadcast_to(array[None], (n, *array.shape))  5.56 us
  transfers between devices with their start and end apart: 6, of which 6 were waited for; matrix products, arithmetic and copies ran while one was open for 5% of the time, Pallas kernels for 0%

profile of v1, /device:TPU:1, one launch (start us, length us, event | category | flops | bytes accessed | tf_op | source)
XLA Modules:
  0.0 186.1 jit_solution(5762420442273971455)
XLA Ops:
  0.0 0.9 dynamic-slice_bitcast_fusion
  1.0 0.9 multiply_reduce_fusion.7
  1.9 0.7 broadcast_in_dim.12
  2.5 13.7 %all-to-all-start = ((f32[32,5,128]{2,1,0:T(8,128)}), f32[32,5,128]{2,1,0:T(8,128)S(1)}, u32[]{:S(2)}, u32[]{:S(2)}) async-start(f32[32,5,128]{2,1,0:T(8,128)} %broadcast_in_dim.12), calls=%async_computation | async-start | bytes 262144 | tf_op jit(solution)/shard_map/all_to_all | solution.py:26
  16.2 0.7 reduce.2
  17.0 8.6 %all-to-all-done = f32[32,5,128]{2,1,0:T(8,128)S(1)} async-done(((f32[32,5,128]{2,1,0:T(8,128)}), f32[32,5,128]{2,1,0:T(8,128)S(1)}, u32[]{:S(2)}, u32[]{:S(2)}) %all-to-all-start) | async-done | bytes 81952 | tf_op jit(solution)/shard_map/all_to_all | solution.py:26
  25.6 0.6 broadcast_in_dim.13
  26.3 9.2 %all-to-all-start.1 = ((f32[16,5,128]{2,1,0:T(8,128)}), f32[16,5,128]{2,1,0:T(8,128)S(1)}, u32[]{:S(2)}, u32[]{:S(2)}) async-start(f32[16,5,128]{2,1,0:T(8,128)} %broadcast_in_dim.13), calls=%async_computation.1 | async-start | bytes 131072 | tf_op jit(solution)/shard_map/all_to_all | solution.py:26
  35.4 0.8 pad_maximum_fusion.6
  36.3 6.9 %all-to-all-done.1 = f32[16,5,128]{2,1,0:T(8,128)S(1)} async-done(((f32[16,5,128]{2,1,0:T(8,128)}), f32[16,5,128]{2,1,0:T(8,128)S(1)}, u32[]{:S(2)}, u32[]{:S(2)}) %all-to-all-start.1) | async-done | bytes 40992 | tf_op jit(solution)/shard_map/all_to_all | solution.py:26
  43.2 1.1 broadcast_in_dim.14
  44.3 3.7 %all-to-all-start.2 = ((bf16[16,16,2176]{2,1,0:T(8,128)(2,1)}), bf16[16,16,2176]{2,1,0:T(8,128)(2,1)S(1)}, u32[]{:S(2)}, u32[]{:S(2)}) async-start(bf16[16,16,2176]{2,1,0:T(8,128)(2,1)} %broadcast_in_dim.14), calls=%async_computation.2 | async-start | bytes 2228224 | tf_op jit(solution)/shard_map/all_to_all | solution.py:26
  47.9 0.8 slice.97
  48.7 0.8 slice.98
  49.5 1.0 slice.90
  50.5 1.0 slice.91
  51.6 0.7 broadcast_multiply_fusion.1
  52.3 0.6 fusion.41
  52.9 22.9 %all-to-all-done.2 = bf16[16,16,2176]{2,1,0:T(8,128)(2,1)S(1)} async-done(((bf16[16,16,2176]{2,1,0:T(8,128)(2,1)}), bf16[16,16,2176]{2,1,0:T(8,128)(2,1)S(1)}, u32[]{:S(2)}, u32[]{:S(2)}) %all-to-all-start.2) | async-done | bytes 1114144 | tf_op jit(solution)/shard_map/all_to_all | solution.py:26
  75.9 0.3 multiply_reduce_fusion
  76.2 0.1 rsqrt.28
  76.2 0.2 multiply_reduce_fusion.3
  76.5 0.2 slice_convert_fusion
  76.7 0.1 copy-done.11
  76.8 0.0 copy-done.13
  76.9 0.0 copy-done.14
  76.9 0.4 fusion.4
  77.3 0.3 copy-done.12
  77.6 0.0 copy-done.15
  77.6 0.0 copy-done.16
  77.6 0.1 fusion.20
  77.7 0.9 multiply_reduce_fusion.1
  78.6 0.6 add_rsqrt_fusion.1
  79.2 0.5 fusion.6
  79.8 0.4 fusion.10
  80.2 0.1 subtract_convert_fusion
  80.4 0.1 copy.32
  80.5 1.7 convolution_convert_fusion.2
  82.3 0.8 broadcast_in_dim.15
  83.1 3.5 %all-to-all-start.3 = ((bf16[4,256,192]{1,2,0:T(8,128)(2,1)}), bf16[4,256,192]{1,2,0:T(8,128)(2,1)S(1)}, u32[]{:S(2)}, u32[]{:S(2)}) async-start(bf16[4,256,192]{1,2,0:T(8,128)(2,1)} %broadcast_in_dim.15), calls=%async_computation.3 | async-start | bytes 786432 | tf_op jit(solution)/shard_map/all_to_all | solution.py:26
  86.6 0.3 convolution_convert_fusion.1
  86.8 0.3 convolution_convert_fusion
  87.1 0.1 pad_maximum_fusion.4
  87.2 10.9 %all-to-all-done.3 = bf16[4,256,192]{1,2,0:T(8,128)(2,1)S(1)} async-done(((bf16[4,256,192]{1,2,0:T(8,128)(2,1)}), bf16[4,256,192]{1,2,0:T(8,128)(2,1)S(1)}, u32[]{:S(2)}, u32[]{:S(2)}) %all-to-all-start.3) | async-done | bytes 393248 | tf_op jit(solution)/shard_map/all_to_all | solution.py:26
  98.1 1.3 broadcast_in_dim.16
  99.4 5.0 %all-to-all-start.4 = ((bf16[8,272,320]{2,1,0:T(8,128)(2,1)}), bf16[8,272,320]{2,1,0:T(8,128)(2,1)}, u32[]{:S(2)}, u32[]{:S(2)}) async-start(bf16[8,272,320]{2,1,0:T(8,128)(2,1)} %broadcast_in_dim.16), calls=%async_computation.4 | async-start | bytes 3342336 | tf_op jit(solution)/shard_map/all_to_all | solution.py:26
  105.1 1.0 copy.31
  106.1 19.5 %all-to-all-done.4 = bf16[8,272,320]{2,1,0:T(8,128)(2,1)} async-done(((bf16[8,272,320]{2,1,0:T(8,128)(2,1)}), bf16[8,272,320]{2,1,0:T(8,128)(2,1)}, u32[]{:S(2)}, u32[]{:S(2)}) %all-to-all-start.4) | async-done | bytes 1392672 | tf_op jit(solution)/shard_map/all_to_all | solution.py:26
  125.6 1.6 slice.120
  127.2 0.9 slice.121
  128.1 1.1 pad_maximum_fusion.3.v_ref
  129.2 1.1 fusion.5.k_ref
  130.2 7.3 %attend.1 = (bf16[1024,128]{1,0:T(8,128)(2,1)}, f32[1024,1]{1,0:T(8,128)}) custom-call(bf16[1024,192]{1,0:T(8,128)(2,1)} %bitcast.78, bf16[2176,192]{1,0:T(8,128)(2,1)} %fusion.5.k_ref, bf16[2176,128]{1,0:T(8,128)(2,1)} %pad_maximum_fusion.3.v_ref, f32[1,1]{1,0:T(1,128)} %bitcast.75.b_ref), custom_call_target="tpu_custom_call" | custom-call | tf_op jit(solution)/shard_map/attend/pallas_call | solution.py:79
  137.5 1.2 reduce.3
  138.8 1.0 fusion.9
  139.8 18.3 %all_to_all.40 = bf16[8,144,128]{2,1,0:T(8,128)(2,1)S(1)} all-to-all(bf16[8,144,128]{2,1,0:T(8,128)(2,1)S(1)} %fusion.9), channel_id=1, replica_groups=mesh['za'=4,'zb'=2,'x'=4,'y'=8,'c'=2] {'za','c'}, dimensions={0} | all-to-all | bytes 589824 | tf_op jit(solution)/shard_map/all_to_all | solution.py:30
  158.1 1.1 broadcast_in_dim.17
  159.2 4.2 %all-to-all-start.6 = ((bf16[2,128,2048]{2,1,0:T(8,128)(2,1)}), bf16[2,128,2048]{2,1,0:T(8,128)(2,1)S(1)}, u32[]{:S(2)}, u32[]{:S(2)}) async-start(bf16[2,128,2048]{2,1,0:T(8,128)(2,1)} %broadcast_in_dim.17), calls=%async_computation.6 | async-start | bytes 2097152 | tf_op jit(solution)/shard_map/all_to_all | solution.py:26
  163.5 0.2 multiply_reduce_fusion.2
  163.8 1.4 all-to-all-done.6
  165.2 0.3 fusion
  165.5 19.8 %all_to_all.41 = bf16[8,16,2048]{2,1,0:T(8,128)(2,1)S(1)} all-to-all(bf16[8,16,2048]{2,1,0:T(8,128)(2,1)S(1)} %bitcast.79), channel_id=1, replica_groups=mesh['za'=4,'zb'=2,'x'=4,'y'=8,'c'=2] {'y'}, dimensions={0} | all-to-all | bytes 1048576 | tf_op jit(solution)/shard_map/all_to_all | solution.py:30
  185.3 0.1 convert_reduce_fusion
  185.4 0.7 add_convert_fusion
  (54 shorter events, 0.3 us)
Async XLA Ops:
  0.0 77.7 %copy-start = (bf16[2048,512]{1,0:T(8,128)(2,1)S(1)}, bf16[2048,512]{1,0:T(8,128)(2,1)}, u32[]{:S(2)}) copy-start(bf16[2048,512]{1,0:T(8,128)(2,1)} %param.27) | copy-start | bytes 6291460
  2.5 23.1 %all-to-all-start = ((f32[32,5,128]{2,1,0:T(8,128)}), f32[32,5,128]{2,1,0:T(8,128)S(1)}, u32[]{:S(2)}, u32[]{:S(2)}) async-start(f32[32,5,128]{2,1,0:T(8,128)} %broadcast_in_dim.12), calls=%async_computation | async-start | bytes 262144 | tf_op jit(solution)/shard_map/all_to_all | solution.py:26
  26.3 16.9 %all-to-all-start.1 = ((f32[16,5,128]{2,1,0:T(8,128)}), f32[16,5,128]{2,1,0:T(8,128)S(1)}, u32[]{:S(2)}, u32[]{:S(2)}) async-start(f32[16,5,128]{2,1,0:T(8,128)} %broadcast_in_dim.13), calls=%async_computation.1 | async-start | bytes 131072 | tf_op jit(solution)/shard_map/all_to_all | solution.py:26
  36.3 11.6 %copy-start.4 = (bf16[2048,64]{0,1:T(8,128)(2,1)S(1)}, bf16[2048,64]{0,1:T(8,128)(2,1)}, u32[]{:S(2)}) copy-start(bf16[2048,64]{0,1:T(8,128)(2,1)} %param.28) | copy-start | bytes 786436
  44.3 31.6 %all-to-all-start.2 = ((bf16[16,16,2176]{2,1,0:T(8,128)(2,1)}), bf16[16,16,2176]{2,1,0:T(8,128)(2,1)S(1)}, u32[]{:S(2)}, u32[]{:S(2)}) async-start(bf16[16,16,2176]{2,1,0:T(8,128)(2,1)} %broadcast_in_dim.14), calls=%async_computation.2 | async-start | bytes 2228224 | tf_op jit(solution)/shard_map/all_to_all | solution.py:26
  76.1 0.7 copy-start.11
  76.1 0.7 copy-start.13
  76.1 0.7 copy-start.14
  76.9 0.7 copy-start.12
  76.9 0.7 copy-start.15
  76.9 0.7 copy-start.16
  77.3 2.5 %copy-start.1 = (bf16[256,2048]{1,0:T(8,128)(2,1)}, bf16[256,2048]{1,0:T(8,128)(2,1)S(1)}, u32[]{:S(2)}) copy-start(bf16[256,2048]{1,0:T(8,128)(2,1)S(1)} %fusion.4) | copy-start | bytes 3145732
  77.7 1.5 copy-start.6
  77.7 1.5 copy-start.7
  79.2 1.0 copy-start.10
  79.2 1.3 copy-start.2
  80.4 6.2 %copy-start.8 = (bf16[512,128]{1,0:T(8,128)(2,1)S(1)}, bf16[512,128]{1,0:T(8,128)(2,1)}, u32[]{:S(2)}) copy-start(bf16[512,128]{1,0:T(8,128)(2,1)} %param.30) | copy-start | bytes 393220
  80.4 6.2 %copy-start.18 = (f32[272]{0:T(512)S(1)}, f32[272]{0:T(512)}, u32[]{:S(2)}) copy-start(f32[272]{0:T(512)} %add_rsqrt_fusion.1) | copy-start | bytes 3268
  80.4 6.2 %copy-start.19 = (f32[512]{0:T(512)S(1)}, f32[512]{0:T(512)}, u32[]{:S(2)}) copy-start(f32[512]{0:T(512)} %param.29) | copy-start | bytes 6148
  82.3 4.6 %copy-start.9 = (bf16[512,128]{1,0:T(8,128)(2,1)S(1)}, bf16[512,128]{1,0:T(8,128)(2,1)}, u32[]{:S(2)}) copy-start(bf16[512,128]{1,0:T(8,128)(2,1)} %param.31) | copy-start | bytes 393220
  83.1 15.1 %all-to-all-start.3 = ((bf16[4,256,192]{1,2,0:T(8,128)(2,1)}), bf16[4,256,192]{1,2,0:T(8,128)(2,1)S(1)}, u32[]{:S(2)}, u32[]{:S(2)}) async-start(bf16[4,256,192]{1,2,0:T(8,128)(2,1)} %broadcast_in_dim.15), calls=%async_computation.3 | async-start | bytes 786432 | tf_op jit(solution)/shard_map/all_to_all | solution.py:26
  99.4 26.1 %all-to-all-start.4 = ((bf16[8,272,320]{2,1,0:T(8,128)(2,1)}), bf16[8,272,320]{2,1,0:T(8,128)(2,1)}, u32[]{:S(2)}, u32[]{:S(2)}) async-start(bf16[8,272,320]{2,1,0:T(8,128)(2,1)} %broadcast_in_dim.16), calls=%async_computation.4 | async-start | bytes 3342336 | tf_op jit(solution)/shard_map/all_to_all | solution.py:26
  130.2 27.9 %copy-start.3 = (bf16[128,2048]{1,0:T(8,128)(2,1)S(1)}, bf16[128,2048]{1,0:T(8,128)(2,1)}, u32[]{:S(2)}) copy-start(bf16[128,2048]{1,0:T(8,128)(2,1)} %param.33) | copy-start | bytes 1572868
  159.2 6.0 %all-to-all-start.6 = ((bf16[2,128,2048]{2,1,0:T(8,128)(2,1)}), bf16[2,128,2048]{2,1,0:T(8,128)(2,1)S(1)}, u32[]{:S(2)}, u32[]{:S(2)}) async-start(bf16[2,128,2048]{2,1,0:T(8,128)(2,1)} %broadcast_in_dim.17), calls=%async_computation.6 | async-start | bytes 2097152 | tf_op jit(solution)/shard_map/all_to_all | solution.py:26
  163.7 21.7 %copy-start.5 = (bf16[16,2048]{1,0:T(8,128)(2,1)S(1)}, bf16[16,2048]{1,0:T(8,128)(2,1)}, u32[]{:S(2)}) copy-start(bf16[16,2048]{1,0:T(8,128)(2,1)} %param.17) | copy-start | bytes 196612
  163.7 21.7 %copy-start.17 = (f32[1,16,128]{2,0,1:T(1,128)S(1)}, f32[1,16,128]{2,0,1:T(1,128)}, u32[]{:S(2)}) copy-start(f32[1,16,128]{2,0,1:T(1,128)} %get-tuple-element.20) | copy-start | bytes 24580

commit v2 on v1

v2 whole, which is shorter than its diff:
```python
import functools

import jax
import jax.numpy as jnp
from jax import lax
from jax.experimental import pallas as pl
from jax.experimental.pallas import tpu as pltpu
from jax.sharding import Mesh
from jax.sharding import PartitionSpec as P

GRID_W = 128
EPS = 1e-06
ROPE_BASE = 10000.0
LOG2E = 1.4426950408889634
F32 = jnp.float32
BF16 = jnp.bfloat16
SP = ("za", "zb", "x")
TP = ("y", "c")
CORE_FIRST = ("c", "y")
KV_AXES = ("zb", "x")
Q_AXIS = "za"


def copies(array, axes):
    n = lax.axis_size(axes)
    return lax.all_to_all(jnp.broadcast_to(array[None], (n, *array.shape)), axes, 0, 0, tiled=True)


def exchanged(array, axes):
    return lax.all_to_all(array, axes, 0, 0, tiled=True)


def angles(positions, rope_dim):
    quarter = rope_dim // 4
    inverse = ROPE_BASE ** (-jnp.arange(quarter, dtype=F32) / quarter)
    row = (positions // GRID_W).astype(F32)
    column = (positions % GRID_W).astype(F32)
    return jnp.concatenate([row[:, None] * inverse[None, :], column[:, None] * inverse[None, :]], axis=-1)


def split_pairs(weight):
    return jnp.concatenate([weight[:, 0::2], weight[:, 1::2]], axis=1)


def shifted(array, axis, k):
    n = lax.axis_size(axis)
    return lax.ppermute(array, axis, [(i, (i + k) % n) for i in range(n)])


def three_parts(value):
    high = lax.reduce_precision(value, 8, 7)
    middle = lax.reduce_precision(value - high, 8, 7)
    return jnp.concatenate([high, middle, value - high - middle], axis=0).astype(BF16)


def project_kernel(raw_ref, gain_ref, kv_gain_ref, turn_ref, w_side_ref, w_down_ref, w_up_ref, q_ref, kv_ref, ctx_ref, h_ref, *, n_y, n_c):
    n_tp, rows, _ = raw_ref.shape
    tok = n_tp * rows
    width = gain_ref.shape[1]
    lanes = width // n_tp
    order = [c * n_y + y for y in range(n_y) for c in range(n_c)]
    vectors = []
    for j in range(5):
        pieces = []
        for t in order:
            part = [raw_ref[t, :, width + lanes :].astype(F32)[p * 5 + j : p * 5 + j + 1] for p in range(3)]
            pieces.append(part[0] + part[1] + part[2])
        vectors.append(jnp.concatenate(pieces, axis=1))
    gain = gain_ref[...]
    for t in range(n_tp):
        ctx_ref[t * rows : (t + 1) * rows, :] = raw_ref[t, :, width : width + lanes].astype(F32)
    context = jnp.concatenate([ctx_ref[pl.ds(i, n_tp, stride=rows), :] for i in range(rows)], axis=1)

    def modulated(values, shift, scale):
        normed = values * lax.rsqrt(jnp.mean(values * values, axis=1, keepdims=True) + EPS)
        return (normed * (gain * (1.0 + scale)) + shift).astype(BF16)

    for t in range(n_tp):
        h_ref[t * rows : (t + 1) * rows, :] = modulated(raw_ref[t, :, :width].astype(F32), vectors[0], vectors[2])
    h_ref[tok:, :] = modulated(context, vectors[1], vectors[3])
    h = h_ref[...]
    side = jnp.dot(h, w_side_ref[...], preferred_element_type=F32)
    q_ref[:tok, :] = side[:tok, :lanes].astype(BF16)
    pair = side[:, lanes:]
    own = pair[:tok]
    lane = lax.broadcasted_iota(jnp.int32, own.shape, 1)
    other = jnp.where(lane % (lanes // 2) < lanes // 4, pltpu.roll(own, lanes - lanes // 4, 1), pltpu.roll(own, lanes // 4, 1))
    turned = own * turn_ref[:, :lanes] + other * turn_ref[:, lanes:]
    half = tok // 2
    swapped = pltpu.roll(turned, lanes // 2, 1)
    low = lax.broadcasted_iota(jnp.int32, (half, lanes), 1) < lanes // 2
    q_ref[tok:, :] = jnp.where(low, turned[:half], swapped[half:]).astype(BF16)
    inner = jnp.dot(h, w_down_ref[...], preferred_element_type=F32)
    inner = inner * lax.rsqrt(jnp.mean(inner * inner, axis=1, keepdims=True) + EPS) * kv_gain_ref[...]
    both = jnp.dot(inner.astype(BF16), w_up_ref[...], preferred_element_type=F32).astype(BF16)
    count = tok + n_tp
    kv_ref[:count, :] = both[:, :lanes]
    kv_ref[count : 2 * count, :] = both[:, lanes:]
    kv_ref[2 * count : 2 * count + half, :] = jnp.where(low, swapped[:half], turned[half:]).astype(BF16)
    kv_ref[2 * count + half :, :] = pltpu.roll(pair[tok:], lanes // 2, 1).astype(BF16)


def attend_kernel(place_ref, bias_ref, q0, q1, q2, q3, kv_ref, o_ref, k_ref, kc_ref, vc_ref, *, factor, tok, n_ctx):
    n_blocks, _, lanes = kv_ref.shape
    count = tok + n_ctx
    half = tok // 2
    rope = lanes // 2
    for i in range(n_blocks):
        k_ref[i, :, :lanes] = kv_ref[i, :tok]
        k_ref[i, :half, lanes:] = kv_ref[i, 2 * count : 2 * count + half, :rope]
        k_ref[i, half:, lanes:] = kv_ref[i, 2 * count : 2 * count + half, rope:]
        at = slice(i * n_ctx, (i + 1) * n_ctx)
        kc_ref[at, :lanes] = kv_ref[i, tok:count]
        kc_ref[at, lanes:] = kv_ref[i, 2 * count + half :, :rope]
        vc_ref[at, :] = kv_ref[i, count + tok : 2 * count]
    dims = (((1,), (1,)), ((), ()))
    step = factor * LOG2E
    bias = bias_ref[0, 0] * LOG2E
    blocks = (q0, q1, q2, q3)
    for k, block in enumerate(blocks):
        to = (place_ref[0, 0] + (len(blocks) - k)) % len(blocks)
        for part in range(2):
            rows = slice(part * half, (part + 1) * half)
            q = jnp.concatenate([block[rows, :], block[tok:, part * rope : (part + 1) * rope]], axis=1)
            scores = [lax.dot_general(q, k_ref[i], dims, preferred_element_type=F32) * step for i in range(n_blocks)]
            scores.append(lax.dot_general(q, kc_ref[...], dims, preferred_element_type=F32) * step + bias)
            tops = [jnp.max(s, axis=1, keepdims=True) for s in scores]
            top = functools.reduce(jnp.maximum, tops)
            weights = [jnp.exp2(s - top) for s in scores]
            total = functools.reduce(jnp.add, [jnp.sum(w, axis=1, keepdims=True) for w in weights])
            values = [kv_ref[i, count : count + tok] for i in range(n_blocks)] + [vc_ref[...]]
            out = functools.reduce(
                jnp.add, [jnp.dot(w.astype(BF16), v, preferred_element_type=F32) for w, v in zip(weights, values, strict=True)]
            )
            o_ref[to, part, :half, :] = (out / total).astype(BF16)
            lse = jnp.transpose(jnp.broadcast_to(top + jnp.log2(total), (half, lanes)))[:16]
            high = lse.astype(BF16).astype(F32)
            middle = (lse - high).astype(BF16).astype(F32)
            row = lax.broadcasted_iota(jnp.int32, lse.shape, 0)
            stats = jnp.where(row == 0, high, jnp.where(row == 1, middle, jnp.where(row == 2, lse - high - middle, 0.0)))
            o_ref[to, part, half:, :] = stats.astype(BF16)


def body(
    latent, cond, ctx_mod, context, shift_w, scale_w, gate_w, norm_gain, w_qn, w_qr, w_kv_down, w_rope_key, kv_gain,
    w_key_up, w_value_up, ctx_bias, w_out,
):
    n_tp = lax.axis_size(TP)
    n_c = lax.axis_size("c")
    n_y = lax.axis_size("y")
    n_q = lax.axis_size(Q_AXIS)
    sp_index = lax.axis_index(SP)
    rows, width = latent.shape
    lanes = width // rows
    tok = rows * n_tp
    half = tok // n_c
    nope = w_key_up.shape[1]
    vsize = w_value_up.shape[1]
    rope = w_rope_key.shape[1]
    factor = (nope + rope) ** (-0.5)

    feat = shift_w.shape[0]
    own = jnp.stack([lax.dynamic_slice_in_dim(v, sp_index * feat, feat) for v in (cond, ctx_mod)])
    own = jax.nn.silu(own)
    parts = [jnp.sum(own[i][:, None] * w, axis=0) for w, i in ((shift_w, 0), (shift_w, 1), (scale_w, 0), (scale_w, 1), (gate_w, 0))]
    summed = jnp.sum(copies(jnp.stack(parts), SP), axis=0)

    w_other = shifted(w_out, "c", 1)
    first = lax.axis_index("c") == 0
    w_pair = jnp.concatenate([jnp.where(first, w_out, w_other), jnp.where(first, w_other, w_out)], axis=0)

    w_side = jnp.concatenate([w_qn, split_pairs(w_qr), split_pairs(w_rope_key)], axis=1)
    w_up = jnp.concatenate([w_key_up, w_value_up], axis=1)
    place = jnp.arange(tok, dtype=jnp.int32)
    place = (place // rows % n_y * n_c + place // (rows * n_y)) * rows + place % rows
    turn = angles(sp_index * tok + place, rope)
    cosine = jnp.cos(turn)
    sine = jnp.sin(turn)
    turn = jnp.concatenate([cosine] * 4 + [-sine, sine] * 2, axis=1)

    message = jnp.concatenate(
        [latent, context.reshape(rows, lanes), jnp.pad(three_parts(summed), ((0, rows - 15), (0, 0)))], axis=1
    )
    message, w_pair, w_side, w_up, turn = lax.optimization_barrier((message, w_pair, w_side, w_up, turn))
    raw = copies(message, CORE_FIRST)
    columns = raw[:, :15, width + lanes :].astype(F32).reshape(n_c, n_y, 3, 5, lanes)[:, :, :, 4]
    gate = jnp.transpose(jnp.sum(columns, axis=2), (1, 0, 2)).reshape(width)

    q_own, kv_own = pl.pallas_call(
        functools.partial(project_kernel, n_y=n_y, n_c=n_c),
        out_shape=[
            jax.ShapeDtypeStruct((tok + tok // 2, lanes), BF16),
            jax.ShapeDtypeStruct((2 * (tok + n_tp) + tok // 2 + n_tp, lanes), BF16),
        ],
        scratch_shapes=[pltpu.VMEM((tok, lanes), F32), pltpu.VMEM((tok + n_tp, width), BF16)],
        name="project",
    )(raw, norm_gain.reshape(1, width), kv_gain.reshape(1, -1), turn, w_side, w_kv_down, w_up)

    queries = [q_own] + [shifted(q_own, Q_AXIS, k) for k in range(1, n_q)]
    kv = copies(kv_own, KV_AXES)
    n_kv = kv.shape[0]
    vmem = pl.BlockSpec(memory_space=pltpu.VMEM)
    smem = pl.BlockSpec(memory_space=pltpu.SMEM)
    out = pl.pallas_call(
        functools.partial(attend_kernel, factor=factor, tok=tok, n_ctx=n_tp),
        in_specs=[smem, smem] + [vmem] * 5,
        out_specs=vmem,
        out_shape=jax.ShapeDtypeStruct((n_q, n_c, half + 16, vsize), BF16),
        scratch_shapes=[
            pltpu.VMEM((n_kv, tok, nope + rope), BF16),
            pltpu.VMEM((n_kv * n_tp, nope + rope), BF16),
            pltpu.VMEM((n_kv * n_tp, vsize), BF16),
        ],
        name="attend",
    )(lax.axis_index(Q_AXIS).astype(jnp.int32).reshape(1, 1), ctx_bias.reshape(1, 1), *queries, kv)

    got = exchanged(out.reshape(n_q * n_c, half + 16, vsize), (Q_AXIS, "c")).reshape(n_q, n_c, half + 16, vsize)
    lse = jnp.sum(got[:, :, half : half + 3, :half].astype(F32), axis=2)
    share = jnp.exp2(lse - jnp.max(lse, axis=0))
    share = share / jnp.sum(share, axis=0)
    attended = jnp.sum(got[:, :, :half].astype(F32) * share[..., None], axis=0).astype(BF16)
    attended = jnp.moveaxis(attended, 0, 1).reshape(half, n_c * vsize)

    term = jnp.dot(attended, w_pair, preferred_element_type=F32).astype(BF16)
    branch = jnp.sum(exchanged(term.reshape(n_y, rows, width), ("y",)).astype(F32), axis=0)
    return (latent.astype(F32) + gate * branch).astype(BF16)


def solution(mesh):
    fine = Mesh(mesh.devices.reshape(4, 2, 4, 8, 2), ("za", "zb", "x", "y", "c"))
    row = P((*SP, *TP), None)
    placed = (
        row, P(), P(), row, P(SP, TP), P(SP, TP), P(SP, TP), P(), P(None, TP), P(None, TP), P(), P(), P(), P(None, TP),
        P(None, TP), P(TP), P(TP, None),
    )
    return jax.shard_map(body, mesh=fine, in_specs=placed, out_specs=row, check_vma=False)
```

time: 187 us -> 160 us (0.86)
  waiting for transfers between devices: 70.2 us -> 28.3 us
  blocking collectives: 38.1 us -> 58 us
  other arithmetic: 11.4 us -> 5.09 us
  Pallas kernels: 7.26 us -> 12.9 us
  matrix products: 4.39 us -> 1.15 us
    all_to_all x6 -> x2, waiting for transfers between devices: 70.2 us -> 0.01 us  [copies(): lax.all_to_all(jnp.broadcast_to(array[None], (n, *array.shape)), axes, 0,...]
    all_to_all x0 -> x1, blocking collectives: none -> 37.3 us  [copies(): lax.all_to_all(jnp.broadcast_to(array[None], (n, *array.shape)), axes, 0,...]
    all_to_all x6 -> x2, starting transfers between devices: 39.2 us -> 18.9 us  [copies(): lax.all_to_all(jnp.broadcast_to(array[None], (n, *array.shape)), axes, 0,...]
    all_to_all x2 -> x1, blocking collectives: 38.1 us -> 20.7 us  [exchanged(): return lax.all_to_all(array, axes, 0, 0, tiled=True)]
    all_to_all x0 -> x1, waiting for transfers between devices: none -> 17 us  [exchanged(): return lax.all_to_all(array, axes, 0, 0, tiled=True)]
    ppermute x0 -> x4, starting transfers between devices: none -> 15.2 us  [shifted(): return lax.ppermute(array, axis, [(i, (i + k) % n) for i in range(n)])]
    ppermute x0 -> x4, waiting for transfers between devices: none -> 11.4 us  [shifted(): return lax.ppermute(array, axis, [(i, (i + k) % n) for i in range(n)])]
    pallas_call x1 -> x2, Pallas kernels: 7.26 us -> 12.9 us  [the longest x1 8.13 us: body(): pl.pallas_call(functools.partial(attend_kernel, factor=factor, tok=tok, n...]
  transfers between devices with their start and end apart: 6 -> 7, of which waited for: 6 -> 3; matrix products, arithmetic and copies ran while one was open for 5% -> 7% of each run, Pallas kernels for 0% -> 0%
where the time goes in v2:
time: 160 us; the launch traced here: 159 us
  blocking collectives  58 us (36%)
  starting transfers between devices  37.6 us (24%)
  waiting for transfers between devices  28.3 us (18%)
  local copies, waits for them, and re-layouts  14.6 us (9%)
  Pallas kernels  12.9 us (8%)
  other arithmetic  5.09 us (3%)
    all_to_all x1, blocking collectives, copies(): lax.all_to_all(jnp.broadcast_to(array[None], (n, *array.shape)), axes, 0,...  37.3 us
    all_to_all x1, blocking collectives, exchanged(): return lax.all_to_all(array, axes, 0, 0, tiled=True)  20.7 us
    all_to_all x2, starting transfers between devices, copies(): lax.all_to_all(jnp.broadcast_to(array[None], (n, *array.shape)), axes, 0,...  18.9 us
    all_to_all x1, waiting for transfers between devices, exchanged(): return lax.all_to_all(array, axes, 0, 0, tiled=True)  17 us
    ppermute x4, starting transfers between devices, shifted(): return lax.ppermute(array, axis, [(i, (i + k) % n) for i in range(n)])  15.2 us
    ppermute x4, waiting for transfers between devices, shifted(): return lax.ppermute(array, axis, [(i, (i + k) % n) for i in range(n)])  11.4 us
    pallas_call x1, Pallas kernels, body(): pl.pallas_call(functools.partial(attend_kernel, factor=factor, tok=tok, n...  8.13 us
    pallas_call x1, Pallas kernels, body(): pl.pallas_call(functools.partial(project_kernel, n_y=n_y, n_c=n_c), out_s...  4.72 us
  transfers between devices with their start and end apart: 7, of which 3 were waited for; matrix products, arithmetic and copies ran while one was open for 7% of the time, Pallas kernels for 0%

profile of v2, /device:TPU:1, one launch (start us, length us, event | category | flops | bytes accessed | tf_op | source)
XLA Modules:
  0.0 158.6 jit_solution(18093320570309248658)
XLA Ops:
  0.0 0.8 dynamic-slice_bitcast_fusion
  0.8 0.9 multiply_reduce_fusion.4
  1.7 0.6 broadcast_in_dim.6
  2.4 13.8 %all-to-all-start = ((f32[32,5,128]{2,1,0:T(8,128)}), f32[32,5,128]{2,1,0:T(8,128)}, u32[]{:S(2)}, u32[]{:S(2)}) async-start(f32[32,5,128]{2,1,0:T(8,128)} %broadcast_in_dim.6), calls=%async_computation | async-start | bytes 262144 | tf_op jit(solution)/shard_map/all_to_all | solution.py:26
  16.2 2.9 %collective-permute-start = (bf16[128,2048]{1,0:T(8,128)(2,1)}, bf16[128,2048]{1,0:T(8,128)(2,1)}, u32[]{:S(2)}, u32[]{:S(2)}) collective-permute-start(bf16[128,2048]{1,0:T(8,128)(2,1)} %param.33), channel_id=1, source_target_pairs={{0,1},{1,0},{2,3},{3,2},{4,5},{5,4},{6,7},{7,6},{8,9},{9,8},{10,11... | collective-permute-start | bytes 1572872 | tf_op jit(solution)/shard_map/ppermute | solution.py:47
  19.1 0.1 broadcast_multiply_fusion.1
  19.2 0.1 fusion
  19.3 0.0 copy-start.11
  19.4 1.0 slice.38
  20.4 1.0 slice.39
  21.5 1.0 slice.40
  22.5 1.0 slice.41
  23.6 0.1 copy.60
  23.7 0.0 copy-start.1
  23.7 0.1 copy.61
  23.8 0.3 copy.74
  24.1 0.3 copy.73
  24.4 0.3 copy.72
  24.6 0.3 copy.71
  24.9 0.0 copy-done.11
  25.0 1.0 concatenate.28.turn_ref
  25.9 0.0 copy-done.1
  25.9 0.0 copy-start.5
  26.0 0.0 copy-start.2
  26.0 2.3 %concatenate.25.w_side_ref = bf16[2048,256]{1,0:T(8,128)(2,1)} concatenate(bf16[2048,128]{1,0:T(8,128)(2,1)S(1)} %copy-done.1, bf16[2048,32]{1,0:T(8,128)(2,1)S(1)} %copy.71, bf16[2048,32]{1,0:T(8,128)(2,1)S(1)} %copy.72, bf16[2048,32]{1,0:T(8,128)(2,1)S(1)} %copy.73, bf16[2048,32]{1,0:T(8,128)(2,1)S(1)} %copy.74), dimensions={1} | concatenate | bytes 2097152 | tf_op jit(solution)/shard_map/concatenate | solution.py:172
  28.2 0.0 copy-done.5
  28.2 0.0 copy-done.6
  28.2 0.7 pad_maximum_fusion.1.w_up_ref
  29.0 0.0 all-to-all-done
  29.0 0.9 reduce_sum.104
  29.9 0.0 copy-done.3
  29.9 0.0 collective-permute-done
  30.0 0.0 copy-done.2
  30.0 1.1 broadcast_select_fusion.1
  31.1 0.1 pad_maximum_fusion
  31.2 0.1 broadcast_in_dim.7
  31.3 37.3 %all_to_all.25.raw_ref = bf16[16,16,2304]{2,1,0:T(8,128)(2,1)} all-to-all(bf16[16,16,2304]{2,1,0:T(8,128)(2,1)S(1)} %broadcast_in_dim.7), channel_id=1, replica_groups=mesh['za'=4,'zb'=2,'x'=4,'y'=8,'c'=2] {'c','y'}, dimensions={0} | all-to-all | bytes 2359296 | tf_op jit(solution)/shard_map/all_to_all | solution.py:26
  68.6 4.7 %project.1 = (bf16[384,128]{1,0:T(8,128)(2,1)}, bf16[688,128]{1,0:T(8,128)(2,1)}) custom-call(bf16[16,16,2304]{2,1,0:T(8,128)(2,1)} %all_to_all.25.raw_ref, f32[1,2048]{1,0:T(1,128)} %bitcast.40, f32[1,512]{1,0:T(1,128)} %bitcast.41, f32[256,256]{1,0:T(8,128)} %concatenate.28.turn_ref, bf16[2048,256]{1,0:T(8,128)(2,1)} %concatenate.25.w_side_ref, ...), custom_call_target="tpu_custom_call" | custom-call | tf_op jit(solution)/shard_map/project/pallas_call | solution.py:189
  73.3 2.2 %broadcast_in_dim.8 = bf16[8,688,128]{2,1,0:T(8,128)(2,1)} broadcast(bf16[688,128]{1,0:T(8,128)(2,1)} %get-tuple-element.17), dimensions={1,2} | broadcast | bytes 1585152 | tf_op jit(solution)/shard_map/broadcast_in_dim | solution.py:26
  75.5 5.1 %all-to-all-start.2 = ((bf16[8,688,128]{2,1,0:T(8,128)(2,1)}), bf16[8,688,128]{2,1,0:T(8,128)(2,1)S(1)}, u32[]{:S(2)}, u32[]{:S(2)}) async-start(bf16[8,688,128]{2,1,0:T(8,128)(2,1)} %broadcast_in_dim.8), calls=%async_computation.2 | async-start | bytes 2818048 | tf_op jit(solution)/shard_map/all_to_all | solution.py:26
  80.6 0.0 copy-done.7
  80.6 4.4 %collective-permute-start.3 = (bf16[384,128]{1,0:T(8,128)(2,1)S(1)}, bf16[384,128]{1,0:T(8,128)(2,1)S(1)}, u32[]{:S(2)}, u32[]{:S(2)}) collective-permute-start(bf16[384,128]{1,0:T(8,128)(2,1)S(1)} %copy-done.7), channel_id=1, source_target_pairs={{0,384},{128,0},{256,128},{384,256},{1,385},{129,1},{257,129},{385... | collective-permute-start | bytes 294920 | tf_op jit(solution)/shard_map/ppermute | solution.py:47
  85.0 4.8 %collective-permute-start.2 = (bf16[384,128]{1,0:T(8,128)(2,1)S(1)}, bf16[384,128]{1,0:T(8,128)(2,1)S(1)}, u32[]{:S(2)}, u32[]{:S(2)}) collective-permute-start(bf16[384,128]{1,0:T(8,128)(2,1)S(1)} %copy-done.7), channel_id=1, source_target_pairs={{0,256},{128,384},{256,0},{384,128},{1,257},{129,385},{257,1},{385... | collective-permute-start | bytes 294920 | tf_op jit(solution)/shard_map/ppermute | solution.py:47
  89.8 3.1 %collective-permute-start.1 = (bf16[384,128]{1,0:T(8,128)(2,1)S(1)}, bf16[384,128]{1,0:T(8,128)(2,1)S(1)}, u32[]{:S(2)}, u32[]{:S(2)}) collective-permute-start(bf16[384,128]{1,0:T(8,128)(2,1)S(1)} %copy-done.7), channel_id=1, source_target_pairs={{0,128},{128,256},{256,384},{384,0},{1,129},{129,257},{257,385},{3... | collective-permute-start | bytes 294920 | tf_op jit(solution)/shard_map/ppermute | solution.py:47
  93.6 0.0 collective-permute-done.3.q3
  93.6 0.0 copy-start.8
  93.6 10.2 %collective-permute-done.2.q2 = bf16[384,128]{1,0:T(8,128)(2,1)S(1)} collective-permute-done((bf16[384,128]{1,0:T(8,128)(2,1)S(1)}, bf16[384,128]{1,0:T(8,128)(2,1)S(1)}, u32[]{:S(2)}, u32[]{:S(2)}) %collective-permute-start.2) | collective-permute-done | bytes 98336 | tf_op jit(solution)/shard_map/ppermute | solution.py:47
  103.8 1.2 collective-permute-done.1.q1
  105.0 0.0 all-to-all-done.2.kv_ref
  105.0 0.0 copy-done.8
  105.0 0.0 copy-done.9
  105.0 0.6 copy-done.10
  105.6 0.5 copy-done
  106.1 8.1 %attend.1 = bf16[4,2,144,128]{3,2,1,0:T(8,128)(2,1)} custom-call(s32[1,1]{1,0:T(1,128)} %bitcast.12.place_ref, f32[1,1]{1,0:T(1,128)} %bitcast.30.bias_ref, bf16[384,128]{1,0:T(8,128)(2,1)} %get-tuple-element.16.q0, bf16[384,128]{1,0:T(8,128)(2,1)} %copy-done.10, bf16[384,128]{1,0:T(8,128)(2,1)} %copy-done.9, bf16[384,128]{1,0:T(8,128)(2,1)} %copy-done.8, ...), custom_call_target="tpu_custom_call" | custom-call | tf_op jit(solution)/shard_map/attend/pallas_call | solution.py:204
  114.2 20.7 %all_to_all.26 = bf16[8,144,128]{2,1,0:T(8,128)(2,1)S(1)} all-to-all(bf16[8,144,128]{2,1,0:T(8,128)(2,1)} %bitcast.31), channel_id=1, replica_groups=mesh['za'=4,'zb'=2,'x'=4,'y'=8,'c'=2] {'za','c'}, dimensions={0} | all-to-all | bytes 589824 | tf_op jit(solution)/shard_map/all_to_all | solution.py:30
  135.0 0.2 multiply_reduce_fusion
  135.3 0.1 copy.69
  135.4 1.2 convolution_convert_fusion
  136.5 3.5 %all-to-all-start.4 = ((bf16[8,16,2048]{2,1,0:T(8,128)(2,1)}), bf16[8,16,2048]{2,1,0:T(8,128)(2,1)S(1)}, u32[]{:S(2)}, u32[]{:S(2)}) async-start(bf16[8,16,2048]{2,1,0:T(8,128)(2,1)} %bitcast.20), calls=%async_computation.4 | async-start | bytes 1048576 | tf_op jit(solution)/shard_map/all_to_all | solution.py:30
  140.0 0.8 slice.47
  140.9 17.0 %all-to-all-done.4 = bf16[8,16,2048]{2,1,0:T(8,128)(2,1)S(1)} async-done(((bf16[8,16,2048]{2,1,0:T(8,128)(2,1)}), bf16[8,16,2048]{2,1,0:T(8,128)(2,1)S(1)}, u32[]{:S(2)}, u32[]{:S(2)}) %all-to-all-start.4) | async-done | bytes 524320 | tf_op jit(solution)/shard_map/all_to_all | solution.py:30
  157.9 0.1 convert_reduce_fusion
  158.0 0.0 copy-done.4
  158.0 0.7 add_convert_fusion
  (24 shorter events, 0.3 us)
Async XLA Ops:
  2.4 26.6 %all-to-all-start = ((f32[32,5,128]{2,1,0:T(8,128)}), f32[32,5,128]{2,1,0:T(8,128)}, u32[]{:S(2)}, u32[]{:S(2)}) async-start(f32[32,5,128]{2,1,0:T(8,128)} %broadcast_in_dim.6), calls=%async_computation | async-start | bytes 262144 | tf_op jit(solution)/shard_map/all_to_all | solution.py:26
  16.2 13.7 %collective-permute-start = (bf16[128,2048]{1,0:T(8,128)(2,1)}, bf16[128,2048]{1,0:T(8,128)(2,1)}, u32[]{:S(2)}, u32[]{:S(2)}) collective-permute-start(bf16[128,2048]{1,0:T(8,128)(2,1)} %param.33), channel_id=1, source_target_pairs={{0,1},{1,0},{2,3},{3,2},{4,5},{5,4},{6,7},{7,6},{8,9},{9,8},{10,11... | collective-permute-start | bytes 1572872 | tf_op jit(solution)/shard_map/ppermute | solution.py:47
  19.3 5.6 %copy-start.11 = (bf16[1,2048]{1,0:T(2,128)(2,1)S(1)}, bf16[1,2048]{1,0:T(2,128)(2,1)}, u32[]{:S(2)}) copy-start(bf16[1,2048]{1,0:T(2,128)(2,1)} %param.20) | copy-start | bytes 12292
  23.7 2.3 %copy-start.1 = (bf16[2048,128]{1,0:T(8,128)(2,1)S(1)}, bf16[2048,128]{1,0:T(8,128)(2,1)}, u32[]{:S(2)}) copy-start(bf16[2048,128]{1,0:T(8,128)(2,1)} %param.25) | copy-start | bytes 1572868
  25.9 2.3 %copy-start.5 = (bf16[512,128]{1,0:T(8,128)(2,1)S(1)}, bf16[512,128]{1,0:T(8,128)(2,1)}, u32[]{:S(2)}) copy-start(bf16[512,128]{1,0:T(8,128)(2,1)} %param.31) | copy-start | bytes 393220
  25.9 2.3 %copy-start.6 = (bf16[512,128]{1,0:T(8,128)(2,1)S(1)}, bf16[512,128]{1,0:T(8,128)(2,1)}, u32[]{:S(2)}) copy-start(bf16[512,128]{1,0:T(8,128)(2,1)} %param.30) | copy-start | bytes 393220
  25.9 4.0 %copy-start.3 = (bf16[16,2048]{1,0:T(8,128)(2,1)S(1)}, bf16[16,2048]{1,0:T(8,128)(2,1)}, u32[]{:S(2)}) copy-start(bf16[16,2048]{1,0:T(8,128)(2,1)} %param.17) | copy-start | bytes 196612
  26.0 4.0 %copy-start.2 = (bf16[128,2048]{1,0:T(8,128)(2,1)S(1)}, bf16[128,2048]{1,0:T(8,128)(2,1)}, u32[]{:S(2)}) copy-start(bf16[128,2048]{1,0:T(8,128)(2,1)} %param.33) | copy-start | bytes 1572868
  73.3 7.3 %copy-start.7 = (bf16[384,128]{1,0:T(8,128)(2,1)S(1)}, bf16[384,128]{1,0:T(8,128)(2,1)}, u32[]{:S(2)}) copy-start(bf16[384,128]{1,0:T(8,128)(2,1)} %get-tuple-element.16.q0) | copy-start | bytes 294916
  75.5 29.5 %all-to-all-start.2 = ((bf16[8,688,128]{2,1,0:T(8,128)(2,1)}), bf16[8,688,128]{2,1,0:T(8,128)(2,1)S(1)}, u32[]{:S(2)}, u32[]{:S(2)}) async-start(bf16[8,688,128]{2,1,0:T(8,128)(2,1)} %broadcast_in_dim.8), calls=%async_computation.2 | async-start | bytes 2818048 | tf_op jit(solution)/shard_map/all_to_all | solution.py:26
  80.6 13.0 %collective-permute-start.3 = (bf16[384,128]{1,0:T(8,128)(2,1)S(1)}, bf16[384,128]{1,0:T(8,128)(2,1)S(1)}, u32[]{:S(2)}, u32[]{:S(2)}) collective-permute-start(bf16[384,128]{1,0:T(8,128)(2,1)S(1)} %copy-done.7), channel_id=1, source_target_pairs={{0,384},{128,0},{256,128},{384,256},{1,385},{129,1},{257,129},{385... | collective-permute-start | bytes 294920 | tf_op jit(solution)/shard_map/ppermute | solution.py:47
  85.0 18.8 %collective-permute-start.2 = (bf16[384,128]{1,0:T(8,128)(2,1)S(1)}, bf16[384,128]{1,0:T(8,128)(2,1)S(1)}, u32[]{:S(2)}, u32[]{:S(2)}) collective-permute-start(bf16[384,128]{1,0:T(8,128)(2,1)S(1)} %copy-done.7), channel_id=1, source_target_pairs={{0,256},{128,384},{256,0},{384,128},{1,257},{129,385},{257,1},{385... | collective-permute-start | bytes 294920 | tf_op jit(solution)/shard_map/ppermute | solution.py:47
  89.8 15.1 %collective-permute-start.1 = (bf16[384,128]{1,0:T(8,128)(2,1)S(1)}, bf16[384,128]{1,0:T(8,128)(2,1)S(1)}, u32[]{:S(2)}, u32[]{:S(2)}) collective-permute-start(bf16[384,128]{1,0:T(8,128)(2,1)S(1)} %copy-done.7), channel_id=1, source_target_pairs={{0,128},{128,256},{256,384},{384,0},{1,129},{129,257},{257,385},{3... | collective-permute-start | bytes 294920 | tf_op jit(solution)/shard_map/ppermute | solution.py:47
  93.6 11.4 %copy-start.8 = (bf16[384,128]{1,0:T(8,128)(2,1)}, bf16[384,128]{1,0:T(8,128)(2,1)S(1)}, u32[]{:S(2)}) copy-start(bf16[384,128]{1,0:T(8,128)(2,1)S(1)} %collective-permute-done.3.q3) | copy-start | bytes 294916
  103.8 1.2 copy-start.9
  105.0 0.6 copy-start.10
  105.0 1.1 copy-start
  135.0 23.0 %copy-start.4 = (bf16[16,2048]{1,0:T(8,128)(2,1)S(1)}, bf16[16,2048]{1,0:T(8,128)(2,1)}, u32[]{:S(2)}) copy-start(bf16[16,2048]{1,0:T(8,128)(2,1)} %param.17) | copy-start | bytes 196612
  136.5 21.4 %all-to-all-start.4 = ((bf16[8,16,2048]{2,1,0:T(8,128)(2,1)}), bf16[8,16,2048]{2,1,0:T(8,128)(2,1)S(1)}, u32[]{:S(2)}, u32[]{:S(2)}) async-start(bf16[8,16,2048]{2,1,0:T(8,128)(2,1)} %bitcast.20), calls=%async_computation.4 | async-start | bytes 1048576 | tf_op jit(solution)/shard_map/all_to_all | solution.py:30

commit v3 on v2

v3 whole, which is shorter than its diff:
```python
import functools

import jax
import jax.numpy as jnp
from jax import lax
from jax.experimental import pallas as pl
from jax.experimental.pallas import tpu as pltpu
from jax.sharding import Mesh
from jax.sharding import PartitionSpec as P


GRID_W = 128
EPS = 1e-06
ROPE_BASE = 10000.0
LOG2E = 1.4426950408889634
F32 = jnp.float32
BF16 = jnp.bfloat16
SP = ("za", "zb", "x")
TP = ("y", "c")
KV_AXES = ("zb", "x")
Q_AXIS = "za"


def copies(array, axes):
    n = lax.axis_size(axes)
    return lax.all_to_all(jnp.broadcast_to(array[None], (n, *array.shape)), axes, 0, 0, tiled=True)


def exchanged(array, axes):
    return lax.all_to_all(array, axes, 0, 0, tiled=True)


def turn_table(positions, rope_dim, lanes):
    quarter = rope_dim // 4
    lane = jnp.arange(lanes, dtype=jnp.int32) % rope_dim
    inverse = ROPE_BASE ** (-(lane // 2 % quarter).astype(F32) / quarter)
    by_row = jnp.where(lane < rope_dim // 2, inverse, 0.0)
    by_column = jnp.where(lane < rope_dim // 2, 0.0, inverse)
    row = (positions // GRID_W).astype(F32)
    column = (positions % GRID_W).astype(F32)
    angle = row[:, None] * by_row[None, :] + column[:, None] * by_column[None, :]
    sign = jnp.where(lane % 2 == 0, -1.0, 1.0)
    return jnp.cos(angle), jnp.sin(angle) * sign[None, :]


def shifted(array, axis, k):
    n = lax.axis_size(axis)
    return lax.ppermute(array, axis, [(i, (i + k) % n) for i in range(n)])


def project_kernel(
    at_ref, own_ref, other_ref, vec_ref, gain_ref, kv_gain_ref, cos_ref, sin_ref, w_qn_ref, w_turn_ref, w_down_ref, w_key_ref, w_value_ref,
    q_ref, kv_ref, ctx_ref, h_ref,
):
    n_y, rows, _ = own_ref.shape
    tok = 2 * n_y * rows
    width = gain_ref.shape[1]
    lanes = width // rows
    n_ctx = 2 * n_y
    columns = jnp.concatenate([vec_ref[t] for t in range(vec_ref.shape[0])], axis=1)
    shift, shift_ctx, scale, scale_ctx = (columns[j : j + 1] for j in range(4))
    gain = gain_ref[...]

    def modulated(values, shift, scale):
        normed = values * lax.rsqrt(jnp.mean(values * values, axis=1, keepdims=True) + EPS)
        return (normed * (gain * (1.0 + scale)) + shift).astype(BF16)

    for side, ref in enumerate((own_ref, other_ref)):
        core = (at_ref[0, 1] + side) % 2
        for k in range(n_y):
            block = core * n_y + (at_ref[0, 0] + (n_y - k)) % n_y
            h_ref[pl.ds(pl.multiple_of(block * rows, rows), rows), :] = modulated(ref[k, :, :width].astype(F32), shift, scale)
            t = side * n_y + k
            ctx_ref[t * rows : (t + 1) * rows, :] = ref[k, :, width:].astype(F32)
    context = jnp.concatenate([ctx_ref[pl.ds(i, n_ctx, stride=rows), :] for i in range(rows)], axis=1)
    h_ref[tok:, :] = modulated(context, shift_ctx, scale_ctx)
    h = h_ref[...]
    q_ref[:tok, :] = jnp.dot(h[:tok], w_qn_ref[...], preferred_element_type=F32).astype(BF16)
    pair = lax.dot_general(h, w_turn_ref[...], (((1,), (1,)), ((), ())), preferred_element_type=F32)
    own = pair[:tok]
    lane = lax.broadcasted_iota(jnp.int32, own.shape, 1)
    other = jnp.where(lane % 2 == 0, pltpu.roll(own, lanes - 1, 1), pltpu.roll(own, 1, 1))
    turned = own * cos_ref[...] + other * sin_ref[...]
    half = tok // 2
    swapped = pltpu.roll(turned, lanes // 2, 1)
    low = lax.broadcasted_iota(jnp.int32, (half, lanes), 1) < lanes // 2
    q_ref[tok:, :] = jnp.where(low, turned[:half], swapped[half:]).astype(BF16)
    inner = jnp.dot(h, w_down_ref[...], preferred_element_type=F32)
    inner = (inner * lax.rsqrt(jnp.mean(inner * inner, axis=1, keepdims=True) + EPS) * kv_gain_ref[...]).astype(BF16)
    keys = jnp.dot(inner, w_key_ref[...], preferred_element_type=F32).astype(BF16)
    values = jnp.dot(inner, w_value_ref[...], preferred_element_type=F32).astype(BF16)
    turned = jnp.where(low, swapped[:half], turned[half:]).astype(BF16)
    still = pltpu.roll(pair[tok:], lanes // 2, 1).astype(BF16)
    count = tok + n_ctx
    for i in range(kv_ref.shape[0]):
        kv_ref[i, :count, :] = keys
        kv_ref[i, count : 2 * count, :] = values
        kv_ref[i, 2 * count : 2 * count + half, :] = turned
        kv_ref[i, 2 * count + half :, :] = still


def attend_kernel(place_ref, bias_ref, q0, q1, q2, q3, kv_ref, o_ref, k_ref, kc_ref, vc_ref, *, factor, tok, n_ctx):
    n_blocks, _, lanes = kv_ref.shape
    count = tok + n_ctx
    half = tok // 2
    rope = lanes // 2
    for i in range(n_blocks):
        k_ref[i, :, :lanes] = kv_ref[i, :tok]
        k_ref[i, :half, lanes:] = kv_ref[i, 2 * count : 2 * count + half, :rope]
        k_ref[i, half:, lanes:] = kv_ref[i, 2 * count : 2 * count + half, rope:]
        at = slice(i * n_ctx, (i + 1) * n_ctx)
        kc_ref[at, :lanes] = kv_ref[i, tok:count]
        kc_ref[at, lanes:] = kv_ref[i, 2 * count + half :, :rope]
        vc_ref[at, :] = kv_ref[i, count + tok : 2 * count]
    dims = (((1,), (1,)), ((), ()))
    step = factor * LOG2E
    bias = bias_ref[0, 0] * LOG2E
    blocks = (q0, q1, q2, q3)
    for k, block in enumerate(blocks):
        to = (place_ref[0, 0] + (len(blocks) - k)) % len(blocks)
        for part in range(2):
            rows = slice(part * half, (part + 1) * half)
            q = jnp.concatenate([block[rows, :], block[tok:, part * rope : (part + 1) * rope]], axis=1)
            scores = [lax.dot_general(q, k_ref[i], dims, preferred_element_type=F32) * step for i in range(n_blocks)]
            scores.append(lax.dot_general(q, kc_ref[...], dims, preferred_element_type=F32) * step + bias)
            tops = [jnp.max(s, axis=1, keepdims=True) for s in scores]
            top = functools.reduce(jnp.maximum, tops)
            weights = [jnp.exp2(s - top) for s in scores]
            total = functools.reduce(jnp.add, [jnp.sum(w, axis=1, keepdims=True) for w in weights])
            values = [kv_ref[i, count : count + tok] for i in range(n_blocks)] + [vc_ref[...]]
            out = functools.reduce(
                jnp.add, [jnp.dot(w.astype(BF16), v, preferred_element_type=F32) for w, v in zip(weights, values, strict=True)]
            )
            o_ref[to, part, :half, :] = (out / total).astype(BF16)
            lse = jnp.transpose(jnp.broadcast_to(top + jnp.log2(total), (half, lanes)))[:16]
            high = lse.astype(BF16).astype(F32)
            middle = (lse - high).astype(BF16).astype(F32)
            row = lax.broadcasted_iota(jnp.int32, lse.shape, 0)
            stats = jnp.where(row == 0, high, jnp.where(row == 1, middle, jnp.where(row == 2, lse - high - middle, 0.0)))
            o_ref[to, part, half:, :] = stats.astype(BF16)


def merge_kernel(at_ref, got_ref, w_own_ref, w_other_ref, o_ref):
    n_q, _, height, lanes = got_ref.shape
    half = height - 16
    n_y, rows, width = o_ref.shape
    term = None
    for side, w_ref in enumerate((w_own_ref, w_other_ref)):
        core = (at_ref[0, 0] + side) % 2
        lse = [jnp.sum(got_ref[i, core, half:, :].astype(F32), axis=0, keepdims=True) for i in range(n_q)]
        top = functools.reduce(jnp.maximum, lse)
        shares = [jnp.exp2(v - top) for v in lse]
        total = functools.reduce(jnp.add, shares)
        mixed = None
        for i in range(n_q):
            share = jnp.transpose(jnp.broadcast_to(shares[i] / total, (lanes, half)))
            piece = got_ref[i, core, :half, :].astype(F32) * share
            mixed = piece if mixed is None else mixed + piece
        out = jnp.dot(mixed.astype(BF16), w_ref[...], preferred_element_type=F32)
        term = out if term is None else term + out
    o_ref[...] = term.astype(BF16).reshape(n_y, rows, width)


def step(
    latent, cond, ctx_mod, context, shift_w, scale_w, gate_w, norm_gain, w_qn, w_qr, w_kv_down, w_rope_key, kv_gain,
    w_key_up, w_value_up, ctx_bias, w_out,
):
    n_tp = lax.axis_size(TP)
    n_c = lax.axis_size("c")
    n_y = lax.axis_size("y")
    n_q = lax.axis_size(Q_AXIS)
    sp_index = lax.axis_index(SP)
    rows, width = latent.shape
    lanes = width // rows
    tok = rows * n_tp
    half = tok // n_c
    nope = w_key_up.shape[1]
    vsize = w_value_up.shape[1]
    rope = w_rope_key.shape[1]
    factor = (nope + rope) ** (-0.5)

    block = jnp.concatenate([latent, context.reshape(rows, lanes)], axis=1)
    moved = [shifted(block, "y", k) for k in range(1, n_y)]
    mine = jnp.stack([block] + moved)
    other = shifted(mine, "c", 1)

    feat = shift_w.shape[0]
    own = jnp.stack([lax.dynamic_slice_in_dim(v, sp_index * feat, feat) for v in (cond, ctx_mod)])
    own = jax.nn.silu(own)
    parts = [jnp.sum(own[i][:, None] * w, axis=0) for w, i in ((shift_w, 0), (shift_w, 1), (scale_w, 0), (scale_w, 1), (gate_w, 0))]
    summed = copies(jnp.stack(parts), SP)
    summed = jnp.sum(summed, axis=0)
    vectors = copies(summed, TP)
    gate = vectors[:, 4].reshape(width)

    w_other = shifted(w_out, "c", 1)
    w_turn = jnp.concatenate([w_qr.T, w_rope_key.T], axis=0)
    place = jnp.arange(tok, dtype=jnp.int32)
    place = (place // rows % n_y * n_c + place // (rows * n_y)) * rows + place % rows
    cosine, sine = turn_table(sp_index * tok + place, rope, lanes)
    vectors, w_turn, cosine, sine, w_other = lax.optimization_barrier((vectors, w_turn, cosine, sine, w_other))

    at = jnp.stack([lax.axis_index("y"), lax.axis_index("c")]).astype(jnp.int32).reshape(1, 2)
    smem = pl.BlockSpec(memory_space=pltpu.SMEM)
    vmem = pl.BlockSpec(memory_space=pltpu.VMEM)
    q_own, kv_copies = pl.pallas_call(
        project_kernel,
        in_specs=[smem] + [vmem] * 12,
        out_specs=[vmem, vmem],
        out_shape=[
            jax.ShapeDtypeStruct((tok + tok // 2, lanes), BF16),
            jax.ShapeDtypeStruct((lax.axis_size(KV_AXES), 2 * (tok + n_tp) + tok // 2 + n_tp, lanes), BF16),
        ],
        scratch_shapes=[pltpu.VMEM((tok, lanes), F32), pltpu.VMEM((tok + n_tp, width), BF16)],
        name="project",
    )(
        at, mine, other, vectors, norm_gain.reshape(1, width), kv_gain.reshape(1, -1), cosine, sine, w_qn, w_turn, w_kv_down, w_key_up,
        w_value_up,
    )

    queries = [q_own] + [shifted(q_own, Q_AXIS, k) for k in range(1, n_q)]
    kv = exchanged(kv_copies, KV_AXES)
    n_kv = kv.shape[0]
    out = pl.pallas_call(
        functools.partial(attend_kernel, factor=factor, tok=tok, n_ctx=n_tp),
        in_specs=[smem, smem] + [vmem] * 5,
        out_specs=vmem,
        out_shape=jax.ShapeDtypeStruct((n_q, n_c, half + 16, vsize), BF16),
        scratch_shapes=[
            pltpu.VMEM((n_kv, tok, nope + rope), BF16),
            pltpu.VMEM((n_kv * n_tp, nope + rope), BF16),
            pltpu.VMEM((n_kv * n_tp, vsize), BF16),
        ],
        name="attend",
    )(lax.axis_index(Q_AXIS).astype(jnp.int32).reshape(1, 1), ctx_bias.reshape(1, 1), *queries, kv)

    got = exchanged(out.reshape(n_q * n_c, half + 16, vsize), (Q_AXIS, "c")).reshape(n_q, n_c, half + 16, vsize)
    term = pl.pallas_call(
        merge_kernel,
        in_specs=[smem] + [vmem] * 3,
        out_specs=vmem,
        out_shape=jax.ShapeDtypeStruct((n_y, rows, width), BF16),
        name="merge",
    )(lax.axis_index("c").astype(jnp.int32).reshape(1, 1), got, w_out, w_other)
    branch = jnp.sum(exchanged(term, ("y",)).astype(F32), axis=0)
    return (latent.astype(F32) + gate * branch).astype(BF16)


def solution(mesh):
    fine = Mesh(mesh.devices.reshape(4, 2, 4, 8, 2), ("za", "zb", "x", "y", "c"))
    row = P((*SP, *TP), None)
    placed = (
        row, P(), P(), row, P(SP, TP), P(SP, TP), P(SP, TP), P(), P(None, TP), P(None, TP), P(), P(), P(), P(None, TP),
        P(None, TP), P(TP), P(TP, None),
    )
    return jax.shard_map(step, mesh=fine, in_specs=placed, out_specs=row, check_vma=False)
```

time: 160 us -> 162 us (1.012)
  blocking collectives: 58 us -> 18.3 us
  starting transfers between devices: 37.6 us -> 74.8 us
  waiting for transfers between devices: 28.3 us -> 38.1 us
  local copies, waits for them, and re-layouts: 14.6 us -> 5.05 us
  Pallas kernels: 12.9 us -> 16.7 us
  other arithmetic: 5.09 us -> 6.98 us
    all_to_all x1 -> x0, blocking collectives: 37.3 us -> none  [copies(): lax.all_to_all(jnp.broadcast_to(array[None], (n, *array.shape)), axes, 0,...]
    ppermute x4 -> x12, starting transfers between devices: 15.2 us -> 49.1 us  [shifted(): return lax.ppermute(array, axis, [(i, (i + k) % n) for i in range(n)])]
    all_to_all x2, waiting for transfers between devices: 0.01 us -> 7.11 us  [copies(): lax.all_to_all(jnp.broadcast_to(array[None], (n, *array.shape)), axes, 0,...]
    all_to_all x1 -> x2, starting transfers between devices: 3.49 us -> 8.82 us  [exchanged(): return lax.all_to_all(array, axes, 0, 0, tiled=True)]
    slice x6 -> x1, local copies, waits for them, and re-layouts: 5.04 us -> 0.85 us  [step(): gate = vectors[:, 4].reshape(width)]
    pallas_call x2 -> x3, Pallas kernels: 12.9 us -> 16.7 us  [the longest x1 8.11 us: step(): pl.pallas_call(functools.partial(attend_kernel, factor=factor, tok=tok, n...]
    concatenate x2 -> x0, local copies, waits for them, and re-layouts: 3.22 us -> none  [the longest x1 2.25 us: body(): jnp.concatenate([w_qn, split_pairs(w_qr), split_pairs(w_rope_key)], axis=1)]
    ppermute x4 -> x12, waiting for transfers between devices: 11.4 us -> 14 us  [shifted(): return lax.ppermute(array, axis, [(i, (i + k) % n) for i in range(n)])]
  transfers between devices with their start and end apart: 7 -> 16, of which waited for: 3 -> 4; matrix products, arithmetic and copies ran while one was open for 7% -> 5% of each run, Pallas kernels for 0% -> 0%
where the time goes in v3:
time: 162 us; the launch traced here: 161 us
  starting transfers between devices  74.8 us (46%)
  waiting for transfers between devices  38.1 us (24%)
  blocking collectives  18.3 us (11%)
  Pallas kernels  16.7 us (10%)
  other arithmetic  6.98 us (4%)
  local copies, waits for them, and re-layouts  5.05 us (3%)
    ppermute x12, starting transfers between devices, shifted(): return lax.ppermute(array, axis, [(i, (i + k) % n) for i in range(n)])  49.1 us
    all_to_all x1, blocking collectives, exchanged(): return lax.all_to_all(array, axes, 0, 0, tiled=True)  18.3 us
    all_to_all x2, waiting for transfers between devices, exchanged(): return lax.all_to_all(array, axes, 0, 0, tiled=True)  17 us
    all_to_all x2, starting transfers between devices, copies(): lax.all_to_all(jnp.broadcast_to(array[None], (n, *array.shape)), axes, 0,...  16.8 us
    ppermute x12, waiting for transfers between devices, shifted(): return lax.ppermute(array, axis, [(i, (i + k) % n) for i in range(n)])  14 us
    all_to_all x2, starting transfers between devices, exchanged(): return lax.all_to_all(array, axes, 0, 0, tiled=True)  8.82 us
    pallas_call x1, Pallas kernels, step(): pl.pallas_call(functools.partial(attend_kernel, factor=factor, tok=tok, n...  8.11 us
    all_to_all x2, waiting for transfers between devices, copies(): lax.all_to_all(jnp.broadcast_to(array[None], (n, *array.shape)), axes, 0,...  7.11 us
  transfers between devices with their start and end apart: 16, of which 4 were waited for; matrix products, arithmetic and copies ran while one was open for 5% of the time, Pallas kernels for 0%

profile of v3, /device:TPU:1, one launch (start us, length us, event | category | flops | bytes accessed | tf_op | source)
XLA Modules:
  0.0 160.9 jit_solution(17751561667879410448)
XLA Ops:
  0.0 0.0 copy-start.6
  0.0 0.8 reduce
  0.8 0.8 pad_maximum_fusion.1
  1.6 4.0 %collective-permute-start = (bf16[16,2176]{1,0:T(8,128)(2,1)S(1)}, bf16[16,2176]{1,0:T(8,128)(2,1)S(1)}, u32[]{:S(2)}, u32[]{:S(2)}) collective-permute-start(bf16[16,2176]{1,0:T(8,128)(2,1)S(1)} %pad_maximum_fusion.1), channel_id=1, source_target_pairs={{0,2},{2,4},{4,6},{6,8},{8,10},{10,12},{12,14},{14,0},{1,3},{3,5},... | collective-permute-start | bytes 208904 | tf_op jit(solution)/shard_map/ppermute | solution.py:48
  5.7 4.2 %collective-permute-start.1 = (bf16[16,2176]{1,0:T(8,128)(2,1)S(1)}, bf16[16,2176]{1,0:T(8,128)(2,1)S(1)}, u32[]{:S(2)}, u32[]{:S(2)}) collective-permute-start(bf16[16,2176]{1,0:T(8,128)(2,1)S(1)} %pad_maximum_fusion.1), channel_id=1, source_target_pairs={{0,4},{2,6},{4,8},{6,10},{8,12},{10,14},{12,0},{14,2},{1,5},{3,7},... | collective-permute-start | bytes 208904 | tf_op jit(solution)/shard_map/ppermute | solution.py:48
  9.9 4.6 %collective-permute-start.2 = (bf16[16,2176]{1,0:T(8,128)(2,1)S(1)}, bf16[16,2176]{1,0:T(8,128)(2,1)S(1)}, u32[]{:S(2)}, u32[]{:S(2)}) collective-permute-start(bf16[16,2176]{1,0:T(8,128)(2,1)S(1)} %pad_maximum_fusion.1), channel_id=1, source_target_pairs={{0,6},{2,8},{4,10},{6,12},{8,14},{10,0},{12,2},{14,4},{1,7},{3,9},... | collective-permute-start | bytes 208904 | tf_op jit(solution)/shard_map/ppermute | solution.py:48
  14.5 3.5 %collective-permute-start.3 = (bf16[16,2176]{1,0:T(8,128)(2,1)S(1)}, bf16[16,2176]{1,0:T(8,128)(2,1)S(1)}, u32[]{:S(2)}, u32[]{:S(2)}) collective-permute-start(bf16[16,2176]{1,0:T(8,128)(2,1)S(1)} %pad_maximum_fusion.1), channel_id=1, source_target_pairs={{0,8},{2,10},{4,12},{6,14},{8,0},{10,2},{12,4},{14,6},{1,9},{3,11}... | collective-permute-start | bytes 208904 | tf_op jit(solution)/shard_map/ppermute | solution.py:48
  18.1 4.9 %collective-permute-start.4 = (bf16[16,2176]{1,0:T(8,128)(2,1)S(1)}, bf16[16,2176]{1,0:T(8,128)(2,1)S(1)}, u32[]{:S(2)}, u32[]{:S(2)}) collective-permute-start(bf16[16,2176]{1,0:T(8,128)(2,1)S(1)} %pad_maximum_fusion.1), channel_id=1, source_target_pairs={{0,10},{2,12},{4,14},{6,0},{8,2},{10,4},{12,6},{14,8},{1,11},{3,13... | collective-permute-start | bytes 208904 | tf_op jit(solution)/shard_map/ppermute | solution.py:48
  23.0 0.8 dynamic-slice_bitcast_fusion
  23.8 0.9 multiply_reduce_fusion.3
  24.7 0.7 broadcast_in_dim.16
  25.4 12.9 %all-to-all-start = ((f32[32,5,128]{2,1,0:T(8,128)}), f32[32,5,128]{2,1,0:T(8,128)S(1)}, u32[]{:S(2)}, u32[]{:S(2)}) async-start(f32[32,5,128]{2,1,0:T(8,128)} %broadcast_in_dim.16), calls=%async_computation | async-start | bytes 262144 | tf_op jit(solution)/shard_map/all_to_all | solution.py:26
  38.3 0.8 bitcast_dynamic-update-slice_fusion.7
  39.2 0.0 collective-permute-done
  39.2 5.0 %collective-permute-start.5 = (bf16[16,2176]{1,0:T(8,128)(2,1)S(1)}, bf16[16,2176]{1,0:T(8,128)(2,1)S(1)}, u32[]{:S(2)}, u32[]{:S(2)}) collective-permute-start(bf16[16,2176]{1,0:T(8,128)(2,1)S(1)} %pad_maximum_fusion.1), channel_id=1, source_target_pairs={{0,12},{2,14},{4,0},{6,2},{8,4},{10,6},{12,8},{14,10},{1,13},{3,15... | collective-permute-start | bytes 208904 | tf_op jit(solution)/shard_map/ppermute | solution.py:48
  44.2 0.0 collective-permute-done.1
  44.2 3.0 %collective-permute-start.6 = (bf16[16,2176]{1,0:T(8,128)(2,1)S(1)}, bf16[16,2176]{1,0:T(8,128)(2,1)S(1)}, u32[]{:S(2)}, u32[]{:S(2)}) collective-permute-start(bf16[16,2176]{1,0:T(8,128)(2,1)S(1)} %pad_maximum_fusion.1), channel_id=1, source_target_pairs={{0,14},{2,0},{4,2},{6,4},{8,6},{10,8},{12,10},{14,12},{1,15},{3,1}... | collective-permute-start | bytes 208904 | tf_op jit(solution)/shard_map/ppermute | solution.py:48
  47.2 0.0 collective-permute-done.2
  47.2 4.8 %collective-permute-start.8 = (bf16[128,2048]{1,0:T(8,128)(2,1)}, bf16[128,2048]{1,0:T(8,128)(2,1)S(1)}, u32[]{:S(2)}, u32[]{:S(2)}) collective-permute-start(bf16[128,2048]{1,0:T(8,128)(2,1)} %w_own_ref.1), channel_id=1, source_target_pairs={{0,1},{1,0},{2,3},{3,2},{4,5},{5,4},{6,7},{7,6},{8,9},{9,8},{10,11... | collective-permute-start | bytes 1572872 | tf_op jit(solution)/shard_map/ppermute | solution.py:48
  52.0 0.0 collective-permute-done.3
  52.1 0.0 collective-permute-done.4
  52.1 0.0 collective-permute-done.5
  52.1 0.0 collective-permute-done.6
  52.2 0.0 copy-start.1
  52.2 2.8 %collective-permute-start.7 = (bf16[8,16,2176]{2,1,0:T(8,128)(2,1)S(1)}, bf16[8,16,2176]{2,1,0:T(8,128)(2,1)S(1)}, u32[]{:S(2)}, u32[]{:S(2)}) collective-permute-start(bf16[8,16,2176]{2,1,0:T(8,128)(2,1)S(1)} %bitcast_dynamic-update-slice_fusion.own_ref), channel_id=1, source_target_pairs={{0,1},{1,0},{2,3},{3,2},{4,5},{5,4},{6,7},{7,6},{8,9},{9,8},{10,11... | collective-permute-start | bytes 1671176 | tf_op jit(solution)/shard_map/ppermute | solution.py:48
  55.0 0.0 copy-done.7
  55.0 0.0 copy-done.6
  55.0 0.8 pad_maximum_fusion.w_turn_ref
  55.8 1.3 sine_multiply_fusion
  57.1 0.0 all-to-all-done
  57.1 0.6 broadcast_in_dim.17
  57.8 4.0 %all-to-all-start.1 = ((f32[16,5,128]{2,1,0:T(8,128)}), f32[16,5,128]{2,1,0:T(8,128)S(1)}, u32[]{:S(2)}, u32[]{:S(2)}) async-start(f32[16,5,128]{2,1,0:T(8,128)} %broadcast_in_dim.17), calls=%async_computation.1 | async-start | bytes 131072 | tf_op jit(solution)/shard_map/all_to_all | solution.py:26
  61.7 0.7 add_bitcast_fusion.at_ref
  62.4 7.1 %all-to-all-done.1.vec_ref = f32[16,5,128]{2,1,0:T(8,128)S(1)} async-done(((f32[16,5,128]{2,1,0:T(8,128)}), f32[16,5,128]{2,1,0:T(8,128)S(1)}, u32[]{:S(2)}, u32[]{:S(2)}) %all-to-all-start.1) | async-done | bytes 40992 | tf_op jit(solution)/shard_map/all_to_all | solution.py:26
  69.5 0.0 collective-permute-done.8.w_other_ref
  69.5 0.0 collective-permute-done.7.other_ref
  69.5 0.0 copy-start.3
  69.5 0.0 copy-done.1
  69.5 0.8 copy-done.5
  70.3 0.1 copy-done.3
  70.4 5.9 %project.1 = (bf16[384,128]{1,0:T(8,128)(2,1)}, bf16[8,688,128]{2,1,0:T(8,128)(2,1)}) custom-call(s32[1,2]{1,0:T(1,128)} %add_bitcast_fusion.at_ref, bf16[8,16,2176]{2,1,0:T(8,128)(2,1)} %copy-done.1, bf16[8,16,2176]{2,1,0:T(8,128)(2,1)} %copy-done.3, f32[16,5,128]{2,1,0:T(8,128)} %copy-done.5, f32[1,2048]{1,0:T(1,128)} %bitcast.52, f32[1,512]{1,0:T(1,128)} %bitcast.53, ...), custom_call_target="tpu_custom_call" | custom-call | tf_op jit(solution)/shard_map/project/pallas_call | solution.py:206
  76.3 5.3 %all-to-all-start.2 = ((bf16[8,688,128]{2,1,0:T(8,128)(2,1)}), bf16[8,688,128]{2,1,0:T(8,128)(2,1)S(1)}, u32[]{:S(2)}, u32[]{:S(2)}) async-start(bf16[8,688,128]{2,1,0:T(8,128)(2,1)} %get-tuple-element.17), calls=%async_computation.2 | async-start | bytes 2818048 | tf_op jit(solution)/shard_map/all_to_all | solution.py:30
  81.6 0.0 copy-done.8
  81.6 6.1 %collective-permute-start.10 = (bf16[384,128]{1,0:T(8,128)(2,1)S(1)}, bf16[384,128]{1,0:T(8,128)(2,1)S(1)}, u32[]{:S(2)}, u32[]{:S(2)}) collective-permute-start(bf16[384,128]{1,0:T(8,128)(2,1)S(1)} %copy-done.8), channel_id=1, source_target_pairs={{0,256},{128,384},{256,0},{384,128},{1,257},{129,385},{257,1},{385... | collective-permute-start | bytes 294920 | tf_op jit(solution)/shard_map/ppermute | solution.py:48
  87.8 3.1 %collective-permute-start.11 = (bf16[384,128]{1,0:T(8,128)(2,1)S(1)}, bf16[384,128]{1,0:T(8,128)(2,1)S(1)}, u32[]{:S(2)}, u32[]{:S(2)}) collective-permute-start(bf16[384,128]{1,0:T(8,128)(2,1)S(1)} %copy-done.8), channel_id=1, source_target_pairs={{0,384},{128,0},{256,128},{384,256},{1,385},{129,1},{257,129},{385... | collective-permute-start | bytes 294920 | tf_op jit(solution)/shard_map/ppermute | solution.py:48
  90.8 3.1 %collective-permute-start.9 = (bf16[384,128]{1,0:T(8,128)(2,1)S(1)}, bf16[384,128]{1,0:T(8,128)(2,1)S(1)}, u32[]{:S(2)}, u32[]{:S(2)}) collective-permute-start(bf16[384,128]{1,0:T(8,128)(2,1)S(1)} %copy-done.8), channel_id=1, source_target_pairs={{0,128},{128,256},{256,384},{384,0},{1,129},{129,257},{257,385},{3... | collective-permute-start | bytes 294920 | tf_op jit(solution)/shard_map/ppermute | solution.py:48
  94.6 11.8 %collective-permute-done.10.q2 = bf16[384,128]{1,0:T(8,128)(2,1)S(1)} collective-permute-done((bf16[384,128]{1,0:T(8,128)(2,1)S(1)}, bf16[384,128]{1,0:T(8,128)(2,1)S(1)}, u32[]{:S(2)}, u32[]{:S(2)}) %collective-permute-start.10) | collective-permute-done | bytes 98336 | tf_op jit(solution)/shard_map/ppermute | solution.py:48
  106.5 0.0 collective-permute-done.11.q3
  106.5 2.1 %collective-permute-done.9.q1 = bf16[384,128]{1,0:T(8,128)(2,1)S(1)} collective-permute-done((bf16[384,128]{1,0:T(8,128)(2,1)S(1)}, bf16[384,128]{1,0:T(8,128)(2,1)S(1)}, u32[]{:S(2)}, u32[]{:S(2)}) %collective-permute-start.9) | collective-permute-done | bytes 98336 | tf_op jit(solution)/shard_map/ppermute | solution.py:48
  108.6 0.0 all-to-all-done.2.kv_ref
  108.6 0.0 copy-done.9
  108.6 0.0 copy-done.10
  108.6 0.6 copy-done.11
  109.2 0.5 copy-done
  109.7 8.1 %attend.1 = bf16[4,2,144,128]{3,2,1,0:T(8,128)(2,1)} custom-call(s32[1,1]{1,0:T(1,128)} %bitcast.11.place_ref, f32[1,1]{1,0:T(1,128)} %bitcast.44.bias_ref, bf16[384,128]{1,0:T(8,128)(2,1)} %get-tuple-element.16.q0, bf16[384,128]{1,0:T(8,128)(2,1)} %copy-done.11, bf16[384,128]{1,0:T(8,128)(2,1)} %copy-done.9, bf16[384,128]{1,0:T(8,128)(2,1)} %copy-done.10, ...), custom_call_target="tpu_custom_call" | custom-call | tf_op jit(solution)/shard_map/attend/pallas_call | solution.py:224
  117.8 0.0 copy-done.4
  117.8 18.3 %all_to_all.25 = bf16[8,144,128]{2,1,0:T(8,128)(2,1)} all-to-all(bf16[8,144,128]{2,1,0:T(8,128)(2,1)} %bitcast.45), channel_id=1, replica_groups=mesh['za'=4,'zb'=2,'x'=4,'y'=8,'c'=2] {'za','c'}, dimensions={0} | all-to-all | bytes 589824 | tf_op jit(solution)/shard_map/all_to_all | solution.py:30
  136.1 2.7 %merge.1 = bf16[8,16,2048]{2,1,0:T(8,128)(2,1)} custom-call(s32[1,1]{1,0:T(1,128)} %bitcast.10.at_ref, bf16[4,2,144,128]{3,2,1,0:T(8,128)(2,1)} %bitcast.46, bf16[128,2048]{1,0:T(8,128)(2,1)} %w_own_ref.1, bf16[128,2048]{1,0:T(8,128)(2,1)} %copy-done.4), custom_call_target="tpu_custom_call" | custom-call | tf_op jit(solution)/shard_map/merge/pallas_call | solution.py:238
  138.8 3.5 %all-to-all-start.4 = ((bf16[8,16,2048]{2,1,0:T(8,128)(2,1)}), bf16[8,16,2048]{2,1,0:T(8,128)(2,1)S(1)}, u32[]{:S(2)}, u32[]{:S(2)}) async-start(bf16[8,16,2048]{2,1,0:T(8,128)(2,1)} %merge.1), calls=%async_computation.4 | async-start | bytes 1048576 | tf_op jit(solution)/shard_map/all_to_all | solution.py:30
  142.3 0.9 slice.15
  143.2 17.0 %all-to-all-done.4 = bf16[8,16,2048]{2,1,0:T(8,128)(2,1)S(1)} async-done(((bf16[8,16,2048]{2,1,0:T(8,128)(2,1)}), bf16[8,16,2048]{2,1,0:T(8,128)(2,1)S(1)}, u32[]{:S(2)}, u32[]{:S(2)}) %all-to-all-start.4) | async-done | bytes 524320 | tf_op jit(solution)/shard_map/all_to_all | solution.py:30
  160.2 0.1 convert_reduce_fusion
  160.2 0.0 copy-done.2
  160.2 0.7 add_convert_fusion
  (23 shorter events, 0.2 us)
Async XLA Ops:
  0.0 55.0 %copy-start.7 = (bf16[2048,64]{0,1:T(8,128)(2,1)S(1)}, bf16[2048,64]{0,1:T(8,128)(2,1)}, u32[]{:S(2)}) copy-start(bf16[2048,64]{0,1:T(8,128)(2,1)} %param.26) | copy-start | bytes 786436
  0.0 55.0 %copy-start.6 = (bf16[2048,64]{0,1:T(8,128)(2,1)S(1)}, bf16[2048,64]{0,1:T(8,128)(2,1)}, u32[]{:S(2)}) copy-start(bf16[2048,64]{0,1:T(8,128)(2,1)} %param.28) | copy-start | bytes 786436
  1.6 37.5 %collective-permute-start = (bf16[16,2176]{1,0:T(8,128)(2,1)S(1)}, bf16[16,2176]{1,0:T(8,128)(2,1)S(1)}, u32[]{:S(2)}, u32[]{:S(2)}) collective-permute-start(bf16[16,2176]{1,0:T(8,128)(2,1)S(1)} %pad_maximum_fusion.1), channel_id=1, source_target_pairs={{0,2},{2,4},{4,6},{6,8},{8,10},{10,12},{12,14},{14,0},{1,3},{3,5},... | collective-permute-start | bytes 208904 | tf_op jit(solution)/shard_map/ppermute | solution.py:48
  5.7 38.5 %collective-permute-start.1 = (bf16[16,2176]{1,0:T(8,128)(2,1)S(1)}, bf16[16,2176]{1,0:T(8,128)(2,1)S(1)}, u32[]{:S(2)}, u32[]{:S(2)}) collective-permute-start(bf16[16,2176]{1,0:T(8,128)(2,1)S(1)} %pad_maximum_fusion.1), channel_id=1, source_target_pairs={{0,4},{2,6},{4,8},{6,10},{8,12},{10,14},{12,0},{14,2},{1,5},{3,7},... | collective-permute-start | bytes 208904 | tf_op jit(solution)/shard_map/ppermute | solution.py:48
  9.9 37.3 %collective-permute-start.2 = (bf16[16,2176]{1,0:T(8,128)(2,1)S(1)}, bf16[16,2176]{1,0:T(8,128)(2,1)S(1)}, u32[]{:S(2)}, u32[]{:S(2)}) collective-permute-start(bf16[16,2176]{1,0:T(8,128)(2,1)S(1)} %pad_maximum_fusion.1), channel_id=1, source_target_pairs={{0,6},{2,8},{4,10},{6,12},{8,14},{10,0},{12,2},{14,4},{1,7},{3,9},... | collective-permute-start | bytes 208904 | tf_op jit(solution)/shard_map/ppermute | solution.py:48
  14.5 37.5 %collective-permute-start.3 = (bf16[16,2176]{1,0:T(8,128)(2,1)S(1)}, bf16[16,2176]{1,0:T(8,128)(2,1)S(1)}, u32[]{:S(2)}, u32[]{:S(2)}) collective-permute-start(bf16[16,2176]{1,0:T(8,128)(2,1)S(1)} %pad_maximum_fusion.1), channel_id=1, source_target_pairs={{0,8},{2,10},{4,12},{6,14},{8,0},{10,2},{12,4},{14,6},{1,9},{3,11}... | collective-permute-start | bytes 208904 | tf_op jit(solution)/shard_map/ppermute | solution.py:48
  18.1 34.0 %collective-permute-start.4 = (bf16[16,2176]{1,0:T(8,128)(2,1)S(1)}, bf16[16,2176]{1,0:T(8,128)(2,1)S(1)}, u32[]{:S(2)}, u32[]{:S(2)}) collective-permute-start(bf16[16,2176]{1,0:T(8,128)(2,1)S(1)} %pad_maximum_fusion.1), channel_id=1, source_target_pairs={{0,10},{2,12},{4,14},{6,0},{8,2},{10,4},{12,6},{14,8},{1,11},{3,13... | collective-permute-start | bytes 208904 | tf_op jit(solution)/shard_map/ppermute | solution.py:48
  25.4 31.7 %all-to-all-start = ((f32[32,5,128]{2,1,0:T(8,128)}), f32[32,5,128]{2,1,0:T(8,128)S(1)}, u32[]{:S(2)}, u32[]{:S(2)}) async-start(f32[32,5,128]{2,1,0:T(8,128)} %broadcast_in_dim.16), calls=%async_computation | async-start | bytes 262144 | tf_op jit(solution)/shard_map/all_to_all | solution.py:26
  39.2 12.9 %collective-permute-start.5 = (bf16[16,2176]{1,0:T(8,128)(2,1)S(1)}, bf16[16,2176]{1,0:T(8,128)(2,1)S(1)}, u32[]{:S(2)}, u32[]{:S(2)}) collective-permute-start(bf16[16,2176]{1,0:T(8,128)(2,1)S(1)} %pad_maximum_fusion.1), channel_id=1, source_target_pairs={{0,12},{2,14},{4,0},{6,2},{8,4},{10,6},{12,8},{14,10},{1,13},{3,15... | collective-permute-start | bytes 208904 | tf_op jit(solution)/shard_map/ppermute | solution.py:48
  44.2 7.9 %collective-permute-start.6 = (bf16[16,2176]{1,0:T(8,128)(2,1)S(1)}, bf16[16,2176]{1,0:T(8,128)(2,1)S(1)}, u32[]{:S(2)}, u32[]{:S(2)}) collective-permute-start(bf16[16,2176]{1,0:T(8,128)(2,1)S(1)} %pad_maximum_fusion.1), channel_id=1, source_target_pairs={{0,14},{2,0},{4,2},{6,4},{8,6},{10,8},{12,10},{14,12},{1,15},{3,1}... | collective-permute-start | bytes 208904 | tf_op jit(solution)/shard_map/ppermute | solution.py:48
  47.2 22.3 %collective-permute-start.8 = (bf16[128,2048]{1,0:T(8,128)(2,1)}, bf16[128,2048]{1,0:T(8,128)(2,1)S(1)}, u32[]{:S(2)}, u32[]{:S(2)}) collective-permute-start(bf16[128,2048]{1,0:T(8,128)(2,1)} %w_own_ref.1), channel_id=1, source_target_pairs={{0,1},{1,0},{2,3},{3,2},{4,5},{5,4},{6,7},{7,6},{8,9},{9,8},{10,11... | collective-permute-start | bytes 1572872 | tf_op jit(solution)/shard_map/ppermute | solution.py:48
  52.2 17.4 %copy-start.1 = (bf16[8,16,2176]{2,1,0:T(8,128)(2,1)}, bf16[8,16,2176]{2,1,0:T(8,128)(2,1)S(1)}, u32[]{:S(2)}) copy-start(bf16[8,16,2176]{2,1,0:T(8,128)(2,1)S(1)} %bitcast_dynamic-update-slice_fusion.own_ref) | copy-start | bytes 1671172
  52.2 17.3 %collective-permute-start.7 = (bf16[8,16,2176]{2,1,0:T(8,128)(2,1)S(1)}, bf16[8,16,2176]{2,1,0:T(8,128)(2,1)S(1)}, u32[]{:S(2)}, u32[]{:S(2)}) collective-permute-start(bf16[8,16,2176]{2,1,0:T(8,128)(2,1)S(1)} %bitcast_dynamic-update-slice_fusion.own_ref), channel_id=1, source_target_pairs={{0,1},{1,0},{2,3},{3,2},{4,5},{5,4},{6,7},{7,6},{8,9},{9,8},{10,11... | collective-permute-start | bytes 1671176 | tf_op jit(solution)/shard_map/ppermute | solution.py:48
  57.8 11.7 %all-to-all-start.1 = ((f32[16,5,128]{2,1,0:T(8,128)}), f32[16,5,128]{2,1,0:T(8,128)S(1)}, u32[]{:S(2)}, u32[]{:S(2)}) async-start(f32[16,5,128]{2,1,0:T(8,128)} %broadcast_in_dim.17), calls=%async_computation.1 | async-start | bytes 131072 | tf_op jit(solution)/shard_map/all_to_all | solution.py:26
  69.5 0.8 copy-start.5
  69.5 48.3 %copy-start.4 = (bf16[128,2048]{1,0:T(8,128)(2,1)}, bf16[128,2048]{1,0:T(8,128)(2,1)S(1)}, u32[]{:S(2)}) copy-start(bf16[128,2048]{1,0:T(8,128)(2,1)S(1)} %collective-permute-done.8.w_other_ref) | copy-start | bytes 1572868
  69.5 0.9 copy-start.3
  76.3 5.3 %copy-start.8 = (bf16[384,128]{1,0:T(8,128)(2,1)S(1)}, bf16[384,128]{1,0:T(8,128)(2,1)}, u32[]{:S(2)}) copy-start(bf16[384,128]{1,0:T(8,128)(2,1)} %get-tuple-element.16.q0) | copy-start | bytes 294916
  76.3 32.3 %all-to-all-start.2 = ((bf16[8,688,128]{2,1,0:T(8,128)(2,1)}), bf16[8,688,128]{2,1,0:T(8,128)(2,1)S(1)}, u32[]{:S(2)}, u32[]{:S(2)}) async-start(bf16[8,688,128]{2,1,0:T(8,128)(2,1)} %get-tuple-element.17), calls=%async_computation.2 | async-start | bytes 2818048 | tf_op jit(solution)/shard_map/all_to_all | solution.py:30
  81.6 24.8 %collective-permute-start.10 = (bf16[384,128]{1,0:T(8,128)(2,1)S(1)}, bf16[384,128]{1,0:T(8,128)(2,1)S(1)}, u32[]{:S(2)}, u32[]{:S(2)}) collective-permute-start(bf16[384,128]{1,0:T(8,128)(2,1)S(1)} %copy-done.8), channel_id=1, source_target_pairs={{0,256},{128,384},{256,0},{384,128},{1,257},{129,385},{257,1},{385... | collective-permute-start | bytes 294920 | tf_op jit(solution)/shard_map/ppermute | solution.py:48
  87.8 18.7 %collective-permute-start.11 = (bf16[384,128]{1,0:T(8,128)(2,1)S(1)}, bf16[384,128]{1,0:T(8,128)(2,1)S(1)}, u32[]{:S(2)}, u32[]{:S(2)}) collective-permute-start(bf16[384,128]{1,0:T(8,128)(2,1)S(1)} %copy-done.8), channel_id=1, source_target_pairs={{0,384},{128,0},{256,128},{384,256},{1,385},{129,1},{257,129},{385... | collective-permute-start | bytes 294920 | tf_op jit(solution)/shard_map/ppermute | solution.py:48
  90.8 17.7 %collective-permute-start.9 = (bf16[384,128]{1,0:T(8,128)(2,1)S(1)}, bf16[384,128]{1,0:T(8,128)(2,1)S(1)}, u32[]{:S(2)}, u32[]{:S(2)}) collective-permute-start(bf16[384,128]{1,0:T(8,128)(2,1)S(1)} %copy-done.8), channel_id=1, source_target_pairs={{0,128},{128,256},{256,384},{384,0},{1,129},{129,257},{257,385},{3... | collective-permute-start | bytes 294920 | tf_op jit(solution)/shard_map/ppermute | solution.py:48
  106.5 2.1 %copy-start.9 = (bf16[384,128]{1,0:T(8,128)(2,1)}, bf16[384,128]{1,0:T(8,128)(2,1)S(1)}, u32[]{:S(2)}) copy-start(bf16[384,128]{1,0:T(8,128)(2,1)S(1)} %collective-permute-done.10.q2) | copy-start | bytes 294916
  106.5 2.1 %copy-start.10 = (bf16[384,128]{1,0:T(8,128)(2,1)}, bf16[384,128]{1,0:T(8,128)(2,1)S(1)}, u32[]{:S(2)}) copy-start(bf16[384,128]{1,0:T(8,128)(2,1)S(1)} %collective-permute-done.11.q3) | copy-start | bytes 294916
  108.6 0.6 copy-start.11
  108.6 1.1 copy-start
  136.1 24.1 %copy-start.2 = (bf16[16,2048]{1,0:T(8,128)(2,1)S(1)}, bf16[16,2048]{1,0:T(8,128)(2,1)}, u32[]{:S(2)}) copy-start(bf16[16,2048]{1,0:T(8,128)(2,1)} %param.17) | copy-start | bytes 196612
  138.8 21.4 %all-to-all-start.4 = ((bf16[8,16,2048]{2,1,0:T(8,128)(2,1)}), bf16[8,16,2048]{2,1,0:T(8,128)(2,1)S(1)}, u32[]{:S(2)}, u32[]{:S(2)}) async-start(bf16[8,16,2048]{2,1,0:T(8,128)(2,1)} %merge.1), calls=%async_computation.4 | async-start | bytes 1048576 | tf_op jit(solution)/shard_map/all_to_all | solution.py:30

commit v4 on v3

--- a/solution.py
+++ b/solution.py
@@ -15,10 +15,9 @@
 LOG2E = 1.4426950408889634
 F32 = jnp.float32
 BF16 = jnp.bfloat16
-SP = ("za", "zb", "x")
+SP = ("z", "x")
 TP = ("y", "c")
-KV_AXES = ("zb", "x")
-Q_AXIS = "za"
+Q_AXIS = "x"
 
 
 def copies(array, axes):
@@ -46,6 +45,10 @@
 def shifted(array, axis, k):
     n = lax.axis_size(axis)
     return lax.ppermute(array, axis, [(i, (i + k) % n) for i in range(n)])
+
+
+def ring_step(up, down, axis):
+    return shifted(up, axis, 1), shifted(down, axis, lax.axis_size(axis) - 1)
 
 
 def project_kernel(
@@ -75,7 +78,7 @@
     context = jnp.concatenate([ctx_ref[pl.ds(i, n_ctx, stride=rows), :] for i in range(rows)], axis=1)
     h_ref[tok:, :] = modulated(context, shift_ctx, scale_ctx)
     h = h_ref[...]
-    q_ref[:tok, :] = jnp.dot(h[:tok], w_qn_ref[...], preferred_element_type=F32).astype(BF16)
+    query = jnp.dot(h[:tok], w_qn_ref[...], preferred_element_type=F32).astype(BF16)
     pair = lax.dot_general(h, w_turn_ref[...], (((1,), (1,)), ((), ())), preferred_element_type=F32)
     own = pair[:tok]
     lane = lax.broadcasted_iota(jnp.int32, own.shape, 1)
@@ -84,7 +87,10 @@
     half = tok // 2
     swapped = pltpu.roll(turned, lanes // 2, 1)
     low = lax.broadcasted_iota(jnp.int32, (half, lanes), 1) < lanes // 2
-    q_ref[tok:, :] = jnp.where(low, turned[:half], swapped[half:]).astype(BF16)
+    query_turned = jnp.where(low, turned[:half], swapped[half:]).astype(BF16)
+    for i in range(q_ref.shape[0]):
+        q_ref[i, :tok, :] = query
+        q_ref[i, tok:, :] = query_turned
     inner = jnp.dot(h, w_down_ref[...], preferred_element_type=F32)
     inner = (inner * lax.rsqrt(jnp.mean(inner * inner, axis=1, keepdims=True) + EPS) * kv_gain_ref[...]).astype(BF16)
     keys = jnp.dot(inner, w_key_ref[...], preferred_element_type=F32).astype(BF16)
@@ -92,52 +98,93 @@
     turned = jnp.where(low, swapped[:half], turned[half:]).astype(BF16)
     still = pltpu.roll(pair[tok:], lanes // 2, 1).astype(BF16)
     count = tok + n_ctx
-    for i in range(kv_ref.shape[0]):
-        kv_ref[i, :count, :] = keys
-        kv_ref[i, count : 2 * count, :] = values
-        kv_ref[i, 2 * count : 2 * count + half, :] = turned
-        kv_ref[i, 2 * count + half :, :] = still
-
-
-def attend_kernel(place_ref, bias_ref, q0, q1, q2, q3, kv_ref, o_ref, k_ref, kc_ref, vc_ref, *, factor, tok, n_ctx):
-    n_blocks, _, lanes = kv_ref.shape
+    kv_ref[:count, :] = keys
+    kv_ref[count : 2 * count, :] = values
+    kv_ref[2 * count : 2 * count + half, :] = turned
+    kv_ref[2 * count + half :, :] = still
+
+
+def attend_kernel(bias_ref, q_ref, *refs, n_blocks, first, last, factor, tok, n_ctx):
+    kv_refs, refs = refs[:n_blocks], refs[n_blocks:]
+    if not first:
+        old_acc_ref, old_stat_ref, refs = refs[0], refs[1], refs[2:]
+    if last:
+        o_ref, refs = refs[0], refs[1:]
+    else:
+        acc_ref, stat_ref, refs = refs[0], refs[1], refs[2:]
+    k_ref, kc_ref, vc_ref = refs
+    lanes = q_ref.shape[2]
     count = tok + n_ctx
     half = tok // 2
     rope = lanes // 2
-    for i in range(n_blocks):
-        k_ref[i, :, :lanes] = kv_ref[i, :tok]
-        k_ref[i, :half, lanes:] = kv_ref[i, 2 * count : 2 * count + half, :rope]
-        k_ref[i, half:, lanes:] = kv_ref[i, 2 * count : 2 * count + half, rope:]
+    for i, kv_ref in enumerate(kv_refs):
+        k_ref[i, :, :lanes] = kv_ref[:tok]
+        k_ref[i, :half, lanes:] = kv_ref[2 * count : 2 * count + half, :rope]
+        k_ref[i, half:, lanes:] = kv_ref[2 * count : 2 * count + half, rope:]
         at = slice(i * n_ctx, (i + 1) * n_ctx)
-        kc_ref[at, :lanes] = kv_ref[i, tok:count]
-        kc_ref[at, lanes:] = kv_ref[i, 2 * count + half :, :rope]
-        vc_ref[at, :] = kv_ref[i, count + tok : 2 * count]
+        kc_ref[at, :lanes] = kv_ref[tok:count]
+        kc_ref[at, lanes:] = kv_ref[2 * count + half :, :rope]
+        vc_ref[at, :] = kv_ref[count + tok : 2 * count]
     dims = (((1,), (1,)), ((), ()))
     step = factor * LOG2E
     bias = bias_ref[0, 0] * LOG2E
-    blocks = (q0, q1, q2, q3)
-    for k, block in enumerate(blocks):
-        to = (place_ref[0, 0] + (len(blocks) - k)) % len(blocks)
+    for k in range(q_ref.shape[0]):
         for part in range(2):
             rows = slice(part * half, (part + 1) * half)
-            q = jnp.concatenate([block[rows, :], block[tok:, part * rope : (part + 1) * rope]], axis=1)
+            flat = slice(k * tok + part * half, k * tok + (part + 1) * half)
+            q = jnp.concatenate([q_ref[k, rows, :], q_ref[k, tok:, part * rope : (part + 1) * rope]], axis=1)
             scores = [lax.dot_general(q, k_ref[i], dims, preferred_element_type=F32) * step for i in range(n_blocks)]
             scores.append(lax.dot_general(q, kc_ref[...], dims, preferred_element_type=F32) * step + bias)
             tops = [jnp.max(s, axis=1, keepdims=True) for s in scores]
+            if not first:
+                tops.append(old_stat_ref[flat, 0:1])
             top = functools.reduce(jnp.maximum, tops)
             weights = [jnp.exp2(s - top) for s in scores]
             total = functools.reduce(jnp.add, [jnp.sum(w, axis=1, keepdims=True) for w in weights])
-            values = [kv_ref[i, count : count + tok] for i in range(n_blocks)] + [vc_ref[...]]
+            values = [kv_ref[count : count + tok] for kv_ref in kv_refs] + [vc_ref[...]]
             out = functools.reduce(
                 jnp.add, [jnp.dot(w.astype(BF16), v, preferred_element_type=F32) for w, v in zip(weights, values, strict=True)]
             )
-            o_ref[to, part, :half, :] = (out / total).astype(BF16)
+            if not first:
+                kept = jnp.exp2(tops[-1] - top)
+                total = total + old_stat_ref[flat, 1:2] * kept
+                out = out + old_acc_ref[flat, :] * kept
+            if not last:
+                acc_ref[flat, :] = out
+                lane = lax.broadcasted_iota(jnp.int32, (half, lanes), 1)
+                stat_ref[flat, :] = jnp.where(lane == 0, top, total)
+                continue
+            o_ref[k, part, :half, :] = (out / total).astype(BF16)
             lse = jnp.transpose(jnp.broadcast_to(top + jnp.log2(total), (half, lanes)))[:16]
             high = lse.astype(BF16).astype(F32)
             middle = (lse - high).astype(BF16).astype(F32)
             row = lax.broadcasted_iota(jnp.int32, lse.shape, 0)
             stats = jnp.where(row == 0, high, jnp.where(row == 1, middle, jnp.where(row == 2, lse - high - middle, 0.0)))
-            o_ref[to, part, half:, :] = stats.astype(BF16)
+            o_ref[k, part, half:, :] = stats.astype(BF16)
+
+
+def attend(queries, blocks, state, bias, last, factor, tok, n_ctx):
+    n_q, _, lanes = queries.shape
+    n = len(blocks)
+    vmem = pl.BlockSpec(memory_space=pltpu.VMEM)
+    if last:
+        out_shape = jax.ShapeDtypeStruct((n_q, 2, tok // 2 + 16, lanes), BF16)
+        out_specs = vmem
+    else:
+        out_shape = [jax.ShapeDtypeStruct((n_q * tok, lanes), F32)] * 2
+        out_specs = [vmem, vmem]
+    return pl.pallas_call(
+        functools.partial(attend_kernel, n_blocks=n, first=not state, last=last, factor=factor, tok=tok, n_ctx=n_ctx),
+        in_specs=[pl.BlockSpec(memory_space=pltpu.SMEM)] + [vmem] * (1 + n + len(state)),
+        out_specs=out_specs,
+        out_shape=out_shape,
+        scratch_shapes=[
+            pltpu.VMEM((n, tok, lanes + lanes // 2), BF16),
+            pltpu.VMEM((n * n_ctx, lanes + lanes // 2), BF16),
+            pltpu.VMEM((n * n_ctx, lanes), BF16),
+        ],
+        name="attend",
+    )(bias, queries, *blocks, *state)
 
 
 def merge_kernel(at_ref, got_ref, w_own_ref, w_other_ref, o_ref):
@@ -180,8 +227,11 @@
     factor = (nope + rope) ** (-0.5)
 
     block = jnp.concatenate([latent, context.reshape(rows, lanes)], axis=1)
-    moved = [shifted(block, "y", k) for k in range(1, n_y)]
-    mine = jnp.stack([block] + moved)
+    up1, down1 = ring_step(block, block, "y")
+    up2, down2 = ring_step(up1, down1, "y")
+    up3, down3 = ring_step(up2, down2, "y")
+    up4 = shifted(up3, "y", 1)
+    mine = jnp.stack([block, up1, up2, up3, up4, down3, down2, down1])
     other = shifted(mine, "c", 1)
 
     feat = shift_w.shape[0]
@@ -203,13 +253,13 @@
     at = jnp.stack([lax.axis_index("y"), lax.axis_index("c")]).astype(jnp.int32).reshape(1, 2)
     smem = pl.BlockSpec(memory_space=pltpu.SMEM)
     vmem = pl.BlockSpec(memory_space=pltpu.VMEM)
-    q_own, kv_copies = pl.pallas_call(
+    q_copies, kv_own = pl.pallas_call(
         project_kernel,
         in_specs=[smem] + [vmem] * 12,
         out_specs=[vmem, vmem],
         out_shape=[
-            jax.ShapeDtypeStruct((tok + tok // 2, lanes), BF16),
-            jax.ShapeDtypeStruct((lax.axis_size(KV_AXES), 2 * (tok + n_tp) + tok // 2 + n_tp, lanes), BF16),
+            jax.ShapeDtypeStruct((n_q, tok + tok // 2, lanes), BF16),
+            jax.ShapeDtypeStruct((2 * (tok + n_tp) + tok // 2 + n_tp, lanes), BF16),
         ],
         scratch_shapes=[pltpu.VMEM((tok, lanes), F32), pltpu.VMEM((tok + n_tp, width), BF16)],
         name="project",
@@ -218,21 +268,17 @@
         w_value_up,
     )
 
-    queries = [q_own] + [shifted(q_own, Q_AXIS, k) for k in range(1, n_q)]
-    kv = exchanged(kv_copies, KV_AXES)
-    n_kv = kv.shape[0]
-    out = pl.pallas_call(
-        functools.partial(attend_kernel, factor=factor, tok=tok, n_ctx=n_tp),
-        in_specs=[smem, smem] + [vmem] * 5,
-        out_specs=vmem,
-        out_shape=jax.ShapeDtypeStruct((n_q, n_c, half + 16, vsize), BF16),
-        scratch_shapes=[
-            pltpu.VMEM((n_kv, tok, nope + rope), BF16),
-            pltpu.VMEM((n_kv * n_tp, nope + rope), BF16),
-            pltpu.VMEM((n_kv * n_tp, vsize), BF16),
-        ],
-        name="attend",
-    )(lax.axis_index(Q_AXIS).astype(jnp.int32).reshape(1, 1), ctx_bias.reshape(1, 1), *queries, kv)
+    up1, down1 = ring_step(kv_own, kv_own, "z")
+    queries = exchanged(q_copies, Q_AXIS)
+    up2, down2 = ring_step(up1, down1, "z")
+    up3, down3 = ring_step(up2, down2, "z")
+    up4 = shifted(up3, "z", 1)
+    bias = ctx_bias.reshape(1, 1)
+    rest = (factor, tok, n_tp)
+    state = attend(queries, [kv_own, up1, down1], [], bias, False, *rest)
+    state = attend(queries, [up2, down2], state, bias, False, *rest)
+    state = attend(queries, [up3, down3], state, bias, False, *rest)
+    out = attend(queries, [up4], state, bias, True, *rest)
 
     got = exchanged(out.reshape(n_q * n_c, half + 16, vsize), (Q_AXIS, "c")).reshape(n_q, n_c, half + 16, vsize)
     term = pl.pallas_call(
@@ -247,7 +293,7 @@
 
 
 def solution(mesh):
-    fine = Mesh(mesh.devices.reshape(4, 2, 4, 8, 2), ("za", "zb", "x", "y", "c"))
+    fine = Mesh(mesh.devices.reshape(8, 4, 8, 2), ("z", "x", "y", "c"))
     row = P((*SP, *TP), None)
     placed = (
         row, P(), P(), row, P(SP, TP), P(SP, TP), P(SP, TP), P(), P(None, TP), P(None, TP), P(), P(), P(), P(None, TP),

time: 162 us -> 177 us (1.093)
  Pallas kernels: 16.7 us -> 32.6 us
  starting transfers between devices: 74.8 us -> 79.5 us
  waiting for transfers between devices: 38.1 us -> 33.4 us
  blocking collectives: 18.3 us -> 15 us
    pallas_call x1 -> x4, Pallas kernels: 8.11 us -> 24.5 us  [attend(): pl.pallas_call(functools.partial(attend_kernel, n_blocks=n, first=not sta...]
    ppermute x12 -> x16, waiting for transfers between devices: 14 us -> 9.26 us  [shifted(): return lax.ppermute(array, axis, [(i, (i + k) % n) for i in range(n)])]
    all_to_all x1, blocking collectives: 18.3 us -> 15 us  [exchanged(): return lax.all_to_all(array, axes, 0, 0, tiled=True)]
    ppermute x12 -> x16, starting transfers between devices: 49.1 us -> 52.3 us  [shifted(): return lax.ppermute(array, axis, [(i, (i + k) % n) for i in range(n)])]
    all_to_all x2, starting transfers between devices: 16.8 us -> 19.9 us  [copies(): lax.all_to_all(jnp.broadcast_to(array[None], (n, *array.shape)), axes, 0,...]
  transfers between devices with their start and end apart: 16 -> 20, of which waited for: 4 -> 6; matrix products, arithmetic and copies ran while one was open for 5% -> 5% of each run, Pallas kernels for 0% -> 10%
where the time goes in v4:
time: 177 us; the launch traced here: 176 us
  starting transfers between devices  79.5 us (45%)
  waiting for transfers between devices  33.4 us (19%)
  Pallas kernels  32.6 us (18%)
  blocking collectives  15 us (8%)
  other arithmetic  7.98 us (5%)
  local copies, waits for them, and re-layouts  6.01 us (3%)
    ppermute x16, starting transfers between devices, shifted(): return lax.ppermute(array, axis, [(i, (i + k) % n) for i in range(n)])  52.3 us
    pallas_call x4, Pallas kernels, attend(): pl.pallas_call(functools.partial(attend_kernel, n_blocks=n, first=not sta...  24.5 us
    all_to_all x2, starting transfers between devices, copies(): lax.all_to_all(jnp.broadcast_to(array[None], (n, *array.shape)), axes, 0,...  19.9 us
    all_to_all x2, waiting for transfers between devices, exchanged(): return lax.all_to_all(array, axes, 0, 0, tiled=True)  17 us
    all_to_all x1, blocking collectives, exchanged(): return lax.all_to_all(array, axes, 0, 0, tiled=True)  15 us
    ppermute x16, waiting for transfers between devices, shifted(): return lax.ppermute(array, axis, [(i, (i + k) % n) for i in range(n)])  9.26 us
    all_to_all x2, starting transfers between devices, exchanged(): return lax.all_to_all(array, axes, 0, 0, tiled=True)  7.34 us
    all_to_all x2, waiting for transfers between devices, copies(): lax.all_to_all(jnp.broadcast_to(array[None], (n, *array.shape)), axes, 0,...  7.13 us
  transfers between devices with their start and end apart: 20, of which 6 were waited for; matrix products, arithmetic and copies ran while one was open for 5% of the time, Pallas kernels for 10%

profile of v4, /device:TPU:1, one launch (start us, length us, event | category | flops | bytes accessed | tf_op | source)
XLA Modules:
  0.0 175.6 jit_solution(7791350781933517778)
XLA Ops:
  0.0 0.7 reduce
  0.7 0.8 pad_maximum_fusion.1
  1.6 4.0 %collective-permute-start = (bf16[16,2176]{1,0:T(8,128)(2,1)S(1)}, bf16[16,2176]{1,0:T(8,128)(2,1)S(1)}, u32[]{:S(2)}, u32[]{:S(2)}) collective-permute-start(bf16[16,2176]{1,0:T(8,128)(2,1)S(1)} %pad_maximum_fusion.1), channel_id=1, source_target_pairs={{0,2},{2,4},{4,6},{6,8},{8,10},{10,12},{12,14},{14,0},{1,3},{3,5},... | collective-permute-start | bytes 208904 | tf_op jit(solution)/shard_map/ppermute | solution.py:47
  5.6 3.8 %collective-permute-start.4 = (bf16[16,2176]{1,0:T(8,128)(2,1)S(1)}, bf16[16,2176]{1,0:T(8,128)(2,1)S(1)}, u32[]{:S(2)}, u32[]{:S(2)}) collective-permute-start(bf16[16,2176]{1,0:T(8,128)(2,1)S(1)} %pad_maximum_fusion.1), channel_id=1, source_target_pairs={{0,14},{2,0},{4,2},{6,4},{8,6},{10,8},{12,10},{14,12},{1,15},{3,1}... | collective-permute-start | bytes 208904 | tf_op jit(solution)/shard_map/ppermute | solution.py:47
  9.4 0.8 dynamic-slice_bitcast_fusion
  10.2 0.9 multiply_reduce_fusion.3
  11.2 0.7 broadcast_in_dim.16
  11.8 12.9 %all-to-all-start = ((f32[32,5,128]{2,1,0:T(8,128)}), f32[32,5,128]{2,1,0:T(8,128)S(1)}, u32[]{:S(2)}, u32[]{:S(2)}) async-start(f32[32,5,128]{2,1,0:T(8,128)} %broadcast_in_dim.16), calls=%async_computation | async-start | bytes 262144 | tf_op jit(solution)/shard_map/all_to_all | solution.py:25
  24.7 3.1 %collective-permute-start.8 = (bf16[128,2048]{1,0:T(8,128)(2,1)}, bf16[128,2048]{1,0:T(8,128)(2,1)S(1)}, u32[]{:S(2)}, u32[]{:S(2)}) collective-permute-start(bf16[128,2048]{1,0:T(8,128)(2,1)} %w_own_ref.1), channel_id=1, source_target_pairs={{0,1},{1,0},{2,3},{3,2},{4,5},{5,4},{6,7},{7,6},{8,9},{9,8},{10,11... | collective-permute-start | bytes 1572872 | tf_op jit(solution)/shard_map/ppermute | solution.py:47
  27.9 0.8 bitcast_dynamic-update-slice_fusion.7
  28.8 0.0 collective-permute-done
  28.8 1.9 %collective-permute-start.1 = (bf16[16,2176]{1,0:T(8,128)(2,1)S(1)}, bf16[16,2176]{1,0:T(8,128)(2,1)S(1)}, u32[]{:S(2)}, u32[]{:S(2)}) collective-permute-start(bf16[16,2176]{1,0:T(8,128)(2,1)S(1)} %collective-permute-done), channel_id=1, source_target_pairs={{0,2},{2,4},{4,6},{6,8},{8,10},{10,12},{12,14},{14,0},{1,3},{3,5},... | collective-permute-start | bytes 208904 | tf_op jit(solution)/shard_map/ppermute | solution.py:47
  30.7 0.0 collective-permute-done.4
  30.7 4.6 %collective-permute-start.5 = (bf16[16,2176]{1,0:T(8,128)(2,1)S(1)}, bf16[16,2176]{1,0:T(8,128)(2,1)S(1)}, u32[]{:S(2)}, u32[]{:S(2)}) collective-permute-start(bf16[16,2176]{1,0:T(8,128)(2,1)S(1)} %collective-permute-done.4), channel_id=1, source_target_pairs={{0,14},{2,0},{4,2},{6,4},{8,6},{10,8},{12,10},{14,12},{1,15},{3,1}... | collective-permute-start | bytes 208904 | tf_op jit(solution)/shard_map/ppermute | solution.py:47
  35.3 0.3 collective-permute-done.1
  35.6 1.9 %collective-permute-start.2 = (bf16[16,2176]{1,0:T(8,128)(2,1)S(1)}, bf16[16,2176]{1,0:T(8,128)(2,1)S(1)}, u32[]{:S(2)}, u32[]{:S(2)}) collective-permute-start(bf16[16,2176]{1,0:T(8,128)(2,1)S(1)} %collective-permute-done.1), channel_id=1, source_target_pairs={{0,2},{2,4},{4,6},{6,8},{8,10},{10,12},{12,14},{14,0},{1,3},{3,5},... | collective-permute-start | bytes 208904 | tf_op jit(solution)/shard_map/ppermute | solution.py:47
  37.6 0.0 collective-permute-done.5
  37.6 4.6 %collective-permute-start.6 = (bf16[16,2176]{1,0:T(8,128)(2,1)S(1)}, bf16[16,2176]{1,0:T(8,128)(2,1)S(1)}, u32[]{:S(2)}, u32[]{:S(2)}) collective-permute-start(bf16[16,2176]{1,0:T(8,128)(2,1)S(1)} %collective-permute-done.5), channel_id=1, source_target_pairs={{0,14},{2,0},{4,2},{6,4},{8,6},{10,8},{12,10},{14,12},{1,15},{3,1}... | collective-permute-start | bytes 208904 | tf_op jit(solution)/shard_map/ppermute | solution.py:47
  42.1 0.0 collective-permute-done.2
  42.2 1.9 %collective-permute-start.3 = (bf16[16,2176]{1,0:T(8,128)(2,1)S(1)}, bf16[16,2176]{1,0:T(8,128)(2,1)S(1)}, u32[]{:S(2)}, u32[]{:S(2)}) collective-permute-start(bf16[16,2176]{1,0:T(8,128)(2,1)S(1)} %collective-permute-done.2), channel_id=1, source_target_pairs={{0,2},{2,4},{4,6},{6,8},{8,10},{10,12},{12,14},{14,0},{1,3},{3,5},... | collective-permute-start | bytes 208904 | tf_op jit(solution)/shard_map/ppermute | solution.py:47
  44.1 4.3 %collective-permute-done.3 = bf16[16,2176]{1,0:T(8,128)(2,1)S(1)} collective-permute-done((bf16[16,2176]{1,0:T(8,128)(2,1)S(1)}, bf16[16,2176]{1,0:T(8,128)(2,1)S(1)}, u32[]{:S(2)}, u32[]{:S(2)}) %collective-permute-start.3) | collective-permute-done | bytes 69664 | tf_op jit(solution)/shard_map/ppermute | solution.py:47
  48.4 0.0 collective-permute-done.6
  48.5 4.8 %collective-permute-start.7 = (bf16[8,16,2176]{2,1,0:T(8,128)(2,1)S(1)}, bf16[8,16,2176]{2,1,0:T(8,128)(2,1)S(1)}, u32[]{:S(2)}, u32[]{:S(2)}) collective-permute-start(bf16[8,16,2176]{2,1,0:T(8,128)(2,1)S(1)} %bitcast_dynamic-update-slice_fusion.own_ref), channel_id=1, source_target_pairs={{0,1},{1,0},{2,3},{3,2},{4,5},{5,4},{6,7},{7,6},{8,9},{9,8},{10,11... | collective-permute-start | bytes 1671176 | tf_op jit(solution)/shard_map/ppermute | solution.py:47
  53.3 1.9 %pad_maximum_fusion.w_turn_ref = bf16[128,2048]{1,0:T(8,128)(2,1)} fusion(bf16[64,2048]{1,0:T(8,128)(2,1)} %bitcast.49, bf16[64,2048]{1,0:T(8,128)(2,1)} %bitcast.50), kind=kLoop, calls=%fused_computation.1 | loop fusion | flops 1048576 | bytes 1048576 | tf_op jit(solution)/shard_map/concatenate | solution.py:247
  55.2 1.3 sine_multiply_fusion
  56.5 0.0 all-to-all-done
  56.5 0.6 broadcast_in_dim.17
  57.1 7.0 %all-to-all-start.1 = ((f32[16,5,128]{2,1,0:T(8,128)}), f32[16,5,128]{2,1,0:T(8,128)S(1)}, u32[]{:S(2)}, u32[]{:S(2)}) async-start(f32[16,5,128]{2,1,0:T(8,128)} %broadcast_in_dim.17), calls=%async_computation.1 | async-start | bytes 131072 | tf_op jit(solution)/shard_map/all_to_all | solution.py:25
  64.1 0.6 add_bitcast_fusion.at_ref
  64.8 7.1 %all-to-all-done.1.vec_ref = f32[16,5,128]{2,1,0:T(8,128)S(1)} async-done(((f32[16,5,128]{2,1,0:T(8,128)}), f32[16,5,128]{2,1,0:T(8,128)S(1)}, u32[]{:S(2)}, u32[]{:S(2)}) %all-to-all-start.1) | async-done | bytes 40992 | tf_op jit(solution)/shard_map/all_to_all | solution.py:25
  71.9 0.0 collective-permute-done.8.w_other_ref
  71.9 0.0 collective-permute-done.7.other_ref
  71.9 0.8 copy-done.5
  72.7 0.1 copy-done.3
  72.8 5.5 %project.1 = (bf16[4,384,128]{2,1,0:T(8,128)(2,1)}, bf16[688,128]{1,0:T(8,128)(2,1)}) custom-call(s32[1,2]{1,0:T(1,128)} %add_bitcast_fusion.at_ref, bf16[8,16,2176]{2,1,0:T(8,128)(2,1)} %copy-done.1, bf16[8,16,2176]{2,1,0:T(8,128)(2,1)} %copy-done.3, f32[16,5,128]{2,1,0:T(8,128)} %copy-done.5, f32[1,2048]{1,0:T(1,128)} %bitcast.54, f32[1,512]{1,0:T(1,128)} %bitcast.55, ...), custom_call_target="tpu_custom_call" | custom-call | tf_op jit(solution)/shard_map/project/pallas_call | solution.py:256
  78.3 3.4 %collective-permute-start.9 = (bf16[688,128]{1,0:T(8,128)(2,1)}, bf16[688,128]{1,0:T(8,128)(2,1)S(1)}, u32[]{:S(2)}, u32[]{:S(2)}) collective-permute-start(bf16[688,128]{1,0:T(8,128)(2,1)} %get-tuple-element.23.refs_0_), channel_id=1, source_target_pairs={{0,64},{64,128},{128,192},{192,256},{256,320},{320,384},{384,448},... | collective-permute-start | bytes 528392 | tf_op jit(solution)/shard_map/ppermute | solution.py:47
  81.7 3.2 %collective-permute-start.13 = (bf16[688,128]{1,0:T(8,128)(2,1)}, bf16[688,128]{1,0:T(8,128)(2,1)S(1)}, u32[]{:S(2)}, u32[]{:S(2)}) collective-permute-start(bf16[688,128]{1,0:T(8,128)(2,1)} %get-tuple-element.23.refs_0_), channel_id=1, source_target_pairs={{0,448},{64,0},{128,64},{192,128},{256,192},{320,256},{384,320},{4... | collective-permute-start | bytes 528392 | tf_op jit(solution)/shard_map/ppermute | solution.py:47
  84.9 2.9 %collective-permute-done.9.refs_1_ = bf16[688,128]{1,0:T(8,128)(2,1)S(1)} collective-permute-done((bf16[688,128]{1,0:T(8,128)(2,1)}, bf16[688,128]{1,0:T(8,128)(2,1)S(1)}, u32[]{:S(2)}, u32[]{:S(2)}) %collective-permute-start.9) | collective-permute-done | bytes 176160 | tf_op jit(solution)/shard_map/ppermute | solution.py:47
  87.7 1.9 %collective-permute-start.10 = (bf16[688,128]{1,0:T(8,128)(2,1)S(1)}, bf16[688,128]{1,0:T(8,128)(2,1)S(1)}, u32[]{:S(2)}, u32[]{:S(2)}) collective-permute-start(bf16[688,128]{1,0:T(8,128)(2,1)S(1)} %collective-permute-done.9.refs_1_), channel_id=1, source_target_pairs={{0,64},{64,128},{128,192},{192,256},{256,320},{320,384},{384,448},... | collective-permute-start | bytes 528392 | tf_op jit(solution)/shard_map/ppermute | solution.py:47
  89.7 0.0 collective-permute-done.13.refs_2_
  89.7 4.6 %collective-permute-start.14 = (bf16[688,128]{1,0:T(8,128)(2,1)S(1)}, bf16[688,128]{1,0:T(8,128)(2,1)S(1)}, u32[]{:S(2)}, u32[]{:S(2)}) collective-permute-start(bf16[688,128]{1,0:T(8,128)(2,1)S(1)} %collective-permute-done.13.refs_2_), channel_id=1, source_target_pairs={{0,448},{64,0},{128,64},{192,128},{256,192},{320,256},{384,320},{4... | collective-permute-start | bytes 528392 | tf_op jit(solution)/shard_map/ppermute | solution.py:47
  94.3 1.8 %collective-permute-done.10.refs_0_ = bf16[688,128]{1,0:T(8,128)(2,1)S(1)} collective-permute-done((bf16[688,128]{1,0:T(8,128)(2,1)S(1)}, bf16[688,128]{1,0:T(8,128)(2,1)S(1)}, u32[]{:S(2)}, u32[]{:S(2)}) %collective-permute-start.10) | collective-permute-done | bytes 176160 | tf_op jit(solution)/shard_map/ppermute | solution.py:47
  96.0 1.9 %collective-permute-start.11 = (bf16[688,128]{1,0:T(8,128)(2,1)S(1)}, bf16[688,128]{1,0:T(8,128)(2,1)S(1)}, u32[]{:S(2)}, u32[]{:S(2)}) collective-permute-start(bf16[688,128]{1,0:T(8,128)(2,1)S(1)} %collective-permute-done.10.refs_0_), channel_id=1, source_target_pairs={{0,64},{64,128},{128,192},{192,256},{256,320},{320,384},{384,448},... | collective-permute-start | bytes 528392 | tf_op jit(solution)/shard_map/ppermute | solution.py:47
  97.9 3.8 %all-to-all-start.2 = ((bf16[4,384,128]{2,1,0:T(8,128)(2,1)}), bf16[4,384,128]{2,1,0:T(8,128)(2,1)S(1)}, u32[]{:S(2)}, u32[]{:S(2)}) async-start(bf16[4,384,128]{2,1,0:T(8,128)(2,1)} %get-tuple-element.22), calls=%async_computation.2 | async-start | bytes 786432 | tf_op jit(solution)/shard_map/all_to_all | solution.py:29
  101.8 0.0 collective-permute-done.14.refs_1_
  101.8 4.6 %collective-permute-start.15 = (bf16[688,128]{1,0:T(8,128)(2,1)S(1)}, bf16[688,128]{1,0:T(8,128)(2,1)S(1)}, u32[]{:S(2)}, u32[]{:S(2)}) collective-permute-start(bf16[688,128]{1,0:T(8,128)(2,1)S(1)} %collective-permute-done.14.refs_1_), channel_id=1, source_target_pairs={{0,448},{64,0},{128,64},{192,128},{256,192},{320,256},{384,320},{4... | collective-permute-start | bytes 528392 | tf_op jit(solution)/shard_map/ppermute | solution.py:47
  106.4 0.0 collective-permute-done.11.refs_0_
  106.4 2.1 %collective-permute-start.12 = (bf16[688,128]{1,0:T(8,128)(2,1)S(1)}, bf16[688,128]{1,0:T(8,128)(2,1)S(1)}, u32[]{:S(2)}, u32[]{:S(2)}) collective-permute-start(bf16[688,128]{1,0:T(8,128)(2,1)S(1)} %collective-permute-done.11.refs_0_), channel_id=1, source_target_pairs={{0,64},{64,128},{128,192},{192,256},{256,320},{320,384},{384,448},... | collective-permute-start | bytes 528392 | tf_op jit(solution)/shard_map/ppermute | solution.py:47
  109.2 0.0 all-to-all-done.2.q_ref
  109.2 0.7 copy-done
  109.9 5.6 %attend.4 = (f32[1024,128]{1,0:T(8,128)}, f32[1024,128]{1,0:T(8,128)}) custom-call(f32[1,1]{1,0:T(1,128)} %bitcast.43.bias_ref, bf16[4,384,128]{2,1,0:T(8,128)(2,1)} %copy-done, bf16[688,128]{1,0:T(8,128)(2,1)} %get-tuple-element.23.refs_0_, bf16[688,128]{1,0:T(8,128)(2,1)} %copy-done.6, bf16[688,128]{1,0:T(8,128)(2,1)} %copy-done.7), custom_call_target="tpu_custom_call" | custom-call | tf_op jit(solution)/shard_map/attend/pallas_call | solution.py:176
  115.6 6.0 %attend.5 = (f32[1024,128]{1,0:T(8,128)}, f32[1024,128]{1,0:T(8,128)}) custom-call(f32[1,1]{1,0:T(1,128)} %bitcast.44.bias_ref, bf16[4,384,128]{2,1,0:T(8,128)(2,1)} %copy-done, bf16[688,128]{1,0:T(8,128)(2,1)} %copy-done.8, bf16[688,128]{1,0:T(8,128)(2,1)} %copy-done.10, f32[1024,128]{1,0:T(8,128)} %get-tuple-element.24.refs_2_, ...), custom_call_target="tpu_custom_call" | custom-call | tf_op jit(solution)/shard_map/attend/pallas_call | solution.py:176
  121.6 0.7 copy-done.12
  122.2 6.0 %attend.6 = (f32[1024,128]{1,0:T(8,128)}, f32[1024,128]{1,0:T(8,128)}) custom-call(f32[1,1]{1,0:T(1,128)} %bitcast.45.bias_ref, bf16[4,384,128]{2,1,0:T(8,128)(2,1)} %copy-done, bf16[688,128]{1,0:T(8,128)(2,1)} %copy-done.9, bf16[688,128]{1,0:T(8,128)(2,1)} %copy-done.12, f32[1024,128]{1,0:T(8,128)} %get-tuple-element.26.refs_2_, ...), custom_call_target="tpu_custom_call" | custom-call | tf_op jit(solution)/shard_map/attend/pallas_call | solution.py:176
  128.2 0.0 collective-permute-done.12.refs_0_
  128.2 0.7 copy-done.11
  128.9 6.8 %attend.7 = bf16[4,2,144,128]{3,2,1,0:T(8,128)(2,1)} custom-call(f32[1,1]{1,0:T(1,128)} %bitcast.46.bias_ref, bf16[4,384,128]{2,1,0:T(8,128)(2,1)} %copy-done, bf16[688,128]{1,0:T(8,128)(2,1)} %copy-done.11, f32[1024,128]{1,0:T(8,128)} %get-tuple-element.28.refs_1_, f32[1024,128]{1,0:T(8,128)} %get-tuple-element.29.refs_2_), custom_call_target="tpu_custom_call" | custom-call | tf_op jit(solution)/shard_map/attend/pallas_call | solution.py:176
  135.8 15.0 %all_to_all.25 = bf16[8,144,128]{2,1,0:T(8,128)(2,1)} all-to-all(bf16[8,144,128]{2,1,0:T(8,128)(2,1)} %bitcast.47), channel_id=1, replica_groups=mesh['z'=8,'x'=4,'y'=8,'c'=2] {'x','c'}, dimensions={0} | all-to-all | bytes 589824 | tf_op jit(solution)/shard_map/all_to_all | solution.py:29
  150.8 2.7 %merge.1 = bf16[8,16,2048]{2,1,0:T(8,128)(2,1)} custom-call(s32[1,1]{1,0:T(1,128)} %bitcast.10.at_ref, bf16[4,2,144,128]{3,2,1,0:T(8,128)(2,1)} %bitcast.48, bf16[128,2048]{1,0:T(8,128)(2,1)} %w_own_ref.1, bf16[128,2048]{1,0:T(8,128)(2,1)} %copy-done.4), custom_call_target="tpu_custom_call" | custom-call | tf_op jit(solution)/shard_map/merge/pallas_call | solution.py:284
  153.4 3.5 %all-to-all-start.4 = ((bf16[8,16,2048]{2,1,0:T(8,128)(2,1)}), bf16[8,16,2048]{2,1,0:T(8,128)(2,1)S(1)}, u32[]{:S(2)}, u32[]{:S(2)}) async-start(bf16[8,16,2048]{2,1,0:T(8,128)(2,1)} %merge.1), calls=%async_computation.4 | async-start | bytes 1048576 | tf_op jit(solution)/shard_map/all_to_all | solution.py:29
  156.9 0.9 slice.15
  157.8 17.0 %all-to-all-done.4 = bf16[8,16,2048]{2,1,0:T(8,128)(2,1)S(1)} async-done(((bf16[8,16,2048]{2,1,0:T(8,128)(2,1)}), bf16[8,16,2048]{2,1,0:T(8,128)(2,1)S(1)}, u32[]{:S(2)}, u32[]{:S(2)}) %all-to-all-start.4) | async-done | bytes 524320 | tf_op jit(solution)/shard_map/all_to_all | solution.py:29
  174.8 0.1 convert_reduce_fusion
  174.9 0.7 add_convert_fusion
  (36 shorter events, 0.3 us)
Async XLA Ops:
  1.6 27.2 %collective-permute-start = (bf16[16,2176]{1,0:T(8,128)(2,1)S(1)}, bf16[16,2176]{1,0:T(8,128)(2,1)S(1)}, u32[]{:S(2)}, u32[]{:S(2)}) collective-permute-start(bf16[16,2176]{1,0:T(8,128)(2,1)S(1)} %pad_maximum_fusion.1), channel_id=1, source_target_pairs={{0,2},{2,4},{4,6},{6,8},{8,10},{10,12},{12,14},{14,0},{1,3},{3,5},... | collective-permute-start | bytes 208904 | tf_op jit(solution)/shard_map/ppermute | solution.py:47
  5.6 25.1 %collective-permute-start.4 = (bf16[16,2176]{1,0:T(8,128)(2,1)S(1)}, bf16[16,2176]{1,0:T(8,128)(2,1)S(1)}, u32[]{:S(2)}, u32[]{:S(2)}) collective-permute-start(bf16[16,2176]{1,0:T(8,128)(2,1)S(1)} %pad_maximum_fusion.1), channel_id=1, source_target_pairs={{0,14},{2,0},{4,2},{6,4},{8,6},{10,8},{12,10},{14,12},{1,15},{3,1}... | collective-permute-start | bytes 208904 | tf_op jit(solution)/shard_map/ppermute | solution.py:47
  11.8 44.7 %all-to-all-start = ((f32[32,5,128]{2,1,0:T(8,128)}), f32[32,5,128]{2,1,0:T(8,128)S(1)}, u32[]{:S(2)}, u32[]{:S(2)}) async-start(f32[32,5,128]{2,1,0:T(8,128)} %broadcast_in_dim.16), calls=%async_computation | async-start | bytes 262144 | tf_op jit(solution)/shard_map/all_to_all | solution.py:25
  24.7 47.2 %collective-permute-start.8 = (bf16[128,2048]{1,0:T(8,128)(2,1)}, bf16[128,2048]{1,0:T(8,128)(2,1)S(1)}, u32[]{:S(2)}, u32[]{:S(2)}) collective-permute-start(bf16[128,2048]{1,0:T(8,128)(2,1)} %w_own_ref.1), channel_id=1, source_target_pairs={{0,1},{1,0},{2,3},{3,2},{4,5},{5,4},{6,7},{7,6},{8,9},{9,8},{10,11... | collective-permute-start | bytes 1572872 | tf_op jit(solution)/shard_map/ppermute | solution.py:47
  28.8 6.8 %collective-permute-start.1 = (bf16[16,2176]{1,0:T(8,128)(2,1)S(1)}, bf16[16,2176]{1,0:T(8,128)(2,1)S(1)}, u32[]{:S(2)}, u32[]{:S(2)}) collective-permute-start(bf16[16,2176]{1,0:T(8,128)(2,1)S(1)} %collective-permute-done), channel_id=1, source_target_pairs={{0,2},{2,4},{4,6},{6,8},{8,10},{10,12},{12,14},{14,0},{1,3},{3,5},... | collective-permute-start | bytes 208904 | tf_op jit(solution)/shard_map/ppermute | solution.py:47
  30.7 6.8 %collective-permute-start.5 = (bf16[16,2176]{1,0:T(8,128)(2,1)S(1)}, bf16[16,2176]{1,0:T(8,128)(2,1)S(1)}, u32[]{:S(2)}, u32[]{:S(2)}) collective-permute-start(bf16[16,2176]{1,0:T(8,128)(2,1)S(1)} %collective-permute-done.4), channel_id=1, source_target_pairs={{0,14},{2,0},{4,2},{6,4},{8,6},{10,8},{12,10},{14,12},{1,15},{3,1}... | collective-permute-start | bytes 208904 | tf_op jit(solution)/shard_map/ppermute | solution.py:47
  35.6 6.5 %collective-permute-start.2 = (bf16[16,2176]{1,0:T(8,128)(2,1)S(1)}, bf16[16,2176]{1,0:T(8,128)(2,1)S(1)}, u32[]{:S(2)}, u32[]{:S(2)}) collective-permute-start(bf16[16,2176]{1,0:T(8,128)(2,1)S(1)} %collective-permute-done.1), channel_id=1, source_target_pairs={{0,2},{2,4},{4,6},{6,8},{8,10},{10,12},{12,14},{14,0},{1,3},{3,5},... | collective-permute-start | bytes 208904 | tf_op jit(solution)/shard_map/ppermute | solution.py:47
  37.6 10.9 %collective-permute-start.6 = (bf16[16,2176]{1,0:T(8,128)(2,1)S(1)}, bf16[16,2176]{1,0:T(8,128)(2,1)S(1)}, u32[]{:S(2)}, u32[]{:S(2)}) collective-permute-start(bf16[16,2176]{1,0:T(8,128)(2,1)S(1)} %collective-permute-done.5), channel_id=1, source_target_pairs={{0,14},{2,0},{4,2},{6,4},{8,6},{10,8},{12,10},{14,12},{1,15},{3,1}... | collective-permute-start | bytes 208904 | tf_op jit(solution)/shard_map/ppermute | solution.py:47
  42.2 6.3 %collective-permute-start.3 = (bf16[16,2176]{1,0:T(8,128)(2,1)S(1)}, bf16[16,2176]{1,0:T(8,128)(2,1)S(1)}, u32[]{:S(2)}, u32[]{:S(2)}) collective-permute-start(bf16[16,2176]{1,0:T(8,128)(2,1)S(1)} %collective-permute-done.2), channel_id=1, source_target_pairs={{0,2},{2,4},{4,6},{6,8},{8,10},{10,12},{12,14},{14,0},{1,3},{3,5},... | collective-permute-start | bytes 208904 | tf_op jit(solution)/shard_map/ppermute | solution.py:47
  48.5 23.4 %copy-start.1 = (bf16[8,16,2176]{2,1,0:T(8,128)(2,1)}, bf16[8,16,2176]{2,1,0:T(8,128)(2,1)S(1)}, u32[]{:S(2)}) copy-start(bf16[8,16,2176]{2,1,0:T(8,128)(2,1)S(1)} %bitcast_dynamic-update-slice_fusion.own_ref) | copy-start | bytes 1671172
  48.5 23.4 %collective-permute-start.7 = (bf16[8,16,2176]{2,1,0:T(8,128)(2,1)S(1)}, bf16[8,16,2176]{2,1,0:T(8,128)(2,1)S(1)}, u32[]{:S(2)}, u32[]{:S(2)}) collective-permute-start(bf16[8,16,2176]{2,1,0:T(8,128)(2,1)S(1)} %bitcast_dynamic-update-slice_fusion.own_ref), channel_id=1, source_target_pairs={{0,1},{1,0},{2,3},{3,2},{4,5},{5,4},{6,7},{7,6},{8,9},{9,8},{10,11... | collective-permute-start | bytes 1671176 | tf_op jit(solution)/shard_map/ppermute | solution.py:47
  57.1 14.8 %all-to-all-start.1 = ((f32[16,5,128]{2,1,0:T(8,128)}), f32[16,5,128]{2,1,0:T(8,128)S(1)}, u32[]{:S(2)}, u32[]{:S(2)}) async-start(f32[16,5,128]{2,1,0:T(8,128)} %broadcast_in_dim.17), calls=%async_computation.1 | async-start | bytes 131072 | tf_op jit(solution)/shard_map/all_to_all | solution.py:25
  71.9 0.8 copy-start.5
  71.9 78.9 %copy-start.4 = (bf16[128,2048]{1,0:T(8,128)(2,1)}, bf16[128,2048]{1,0:T(8,128)(2,1)S(1)}, u32[]{:S(2)}) copy-start(bf16[128,2048]{1,0:T(8,128)(2,1)S(1)} %collective-permute-done.8.w_other_ref) | copy-start | bytes 1572868
  71.9 0.9 copy-start.3
  78.3 9.5 %collective-permute-start.9 = (bf16[688,128]{1,0:T(8,128)(2,1)}, bf16[688,128]{1,0:T(8,128)(2,1)S(1)}, u32[]{:S(2)}, u32[]{:S(2)}) collective-permute-start(bf16[688,128]{1,0:T(8,128)(2,1)} %get-tuple-element.23.refs_0_), channel_id=1, source_target_pairs={{0,64},{64,128},{128,192},{192,256},{256,320},{320,384},{384,448},... | collective-permute-start | bytes 528392 | tf_op jit(solution)/shard_map/ppermute | solution.py:47
  81.7 8.0 %collective-permute-start.13 = (bf16[688,128]{1,0:T(8,128)(2,1)}, bf16[688,128]{1,0:T(8,128)(2,1)S(1)}, u32[]{:S(2)}, u32[]{:S(2)}) collective-permute-start(bf16[688,128]{1,0:T(8,128)(2,1)} %get-tuple-element.23.refs_0_), channel_id=1, source_target_pairs={{0,448},{64,0},{128,64},{192,128},{256,192},{320,256},{384,320},{4... | collective-permute-start | bytes 528392 | tf_op jit(solution)/shard_map/ppermute | solution.py:47
  87.7 21.4 %copy-start.6 = (bf16[688,128]{1,0:T(8,128)(2,1)}, bf16[688,128]{1,0:T(8,128)(2,1)S(1)}, u32[]{:S(2)}) copy-start(bf16[688,128]{1,0:T(8,128)(2,1)S(1)} %collective-permute-done.9.refs_1_) | copy-start | bytes 528388
  87.7 8.3 %collective-permute-start.10 = (bf16[688,128]{1,0:T(8,128)(2,1)S(1)}, bf16[688,128]{1,0:T(8,128)(2,1)S(1)}, u32[]{:S(2)}, u32[]{:S(2)}) collective-permute-start(bf16[688,128]{1,0:T(8,128)(2,1)S(1)} %collective-permute-done.9.refs_1_), channel_id=1, source_target_pairs={{0,64},{64,128},{128,192},{192,256},{256,320},{320,384},{384,448},... | collective-permute-start | bytes 528392 | tf_op jit(solution)/shard_map/ppermute | solution.py:47
  89.7 19.5 %copy-start.7 = (bf16[688,128]{1,0:T(8,128)(2,1)}, bf16[688,128]{1,0:T(8,128)(2,1)S(1)}, u32[]{:S(2)}) copy-start(bf16[688,128]{1,0:T(8,128)(2,1)S(1)} %collective-permute-done.13.refs_2_) | copy-start | bytes 528388
  89.7 12.1 %collective-permute-start.14 = (bf16[688,128]{1,0:T(8,128)(2,1)S(1)}, bf16[688,128]{1,0:T(8,128)(2,1)S(1)}, u32[]{:S(2)}, u32[]{:S(2)}) collective-permute-start(bf16[688,128]{1,0:T(8,128)(2,1)S(1)} %collective-permute-done.13.refs_2_), channel_id=1, source_target_pairs={{0,448},{64,0},{128,64},{192,128},{256,192},{320,256},{384,320},{4... | collective-permute-start | bytes 528392 | tf_op jit(solution)/shard_map/ppermute | solution.py:47
  96.0 19.5 %copy-start.8 = (bf16[688,128]{1,0:T(8,128)(2,1)}, bf16[688,128]{1,0:T(8,128)(2,1)S(1)}, u32[]{:S(2)}) copy-start(bf16[688,128]{1,0:T(8,128)(2,1)S(1)} %collective-permute-done.10.refs_0_) | copy-start | bytes 528388
  96.0 10.3 %collective-permute-start.11 = (bf16[688,128]{1,0:T(8,128)(2,1)S(1)}, bf16[688,128]{1,0:T(8,128)(2,1)S(1)}, u32[]{:S(2)}, u32[]{:S(2)}) collective-permute-start(bf16[688,128]{1,0:T(8,128)(2,1)S(1)} %collective-permute-done.10.refs_0_), channel_id=1, source_target_pairs={{0,64},{64,128},{128,192},{192,256},{256,320},{320,384},{384,448},... | collective-permute-start | bytes 528392 | tf_op jit(solution)/shard_map/ppermute | solution.py:47
  97.9 11.2 %all-to-all-start.2 = ((bf16[4,384,128]{2,1,0:T(8,128)(2,1)}), bf16[4,384,128]{2,1,0:T(8,128)(2,1)S(1)}, u32[]{:S(2)}, u32[]{:S(2)}) async-start(bf16[4,384,128]{2,1,0:T(8,128)(2,1)} %get-tuple-element.22), calls=%async_computation.2 | async-start | bytes 786432 | tf_op jit(solution)/shard_map/all_to_all | solution.py:29
  101.8 13.8 %copy-start.10 = (bf16[688,128]{1,0:T(8,128)(2,1)}, bf16[688,128]{1,0:T(8,128)(2,1)S(1)}, u32[]{:S(2)}) copy-start(bf16[688,128]{1,0:T(8,128)(2,1)S(1)} %collective-permute-done.14.refs_1_) | copy-start | bytes 528388
  101.8 19.8 %collective-permute-start.15 = (bf16[688,128]{1,0:T(8,128)(2,1)S(1)}, bf16[688,128]{1,0:T(8,128)(2,1)S(1)}, u32[]{:S(2)}, u32[]{:S(2)}) collective-permute-start(bf16[688,128]{1,0:T(8,128)(2,1)S(1)} %collective-permute-done.14.refs_1_), channel_id=1, source_target_pairs={{0,448},{64,0},{128,64},{192,128},{256,192},{320,256},{384,320},{4... | collective-permute-start | bytes 528392 | tf_op jit(solution)/shard_map/ppermute | solution.py:47
  106.4 15.2 %copy-start.9 = (bf16[688,128]{1,0:T(8,128)(2,1)}, bf16[688,128]{1,0:T(8,128)(2,1)S(1)}, u32[]{:S(2)}) copy-start(bf16[688,128]{1,0:T(8,128)(2,1)S(1)} %collective-permute-done.11.refs_0_) | copy-start | bytes 528388
  106.4 21.8 %collective-permute-start.12 = (bf16[688,128]{1,0:T(8,128)(2,1)S(1)}, bf16[688,128]{1,0:T(8,128)(2,1)S(1)}, u32[]{:S(2)}, u32[]{:S(2)}) collective-permute-start(bf16[688,128]{1,0:T(8,128)(2,1)S(1)} %collective-permute-done.11.refs_0_), channel_id=1, source_target_pairs={{0,64},{64,128},{128,192},{192,256},{256,320},{320,384},{384,448},... | collective-permute-start | bytes 528392 | tf_op jit(solution)/shard_map/ppermute | solution.py:47
  109.2 0.8 copy-start
  121.6 0.7 copy-start.12
  128.2 0.7 copy-start.11
  135.8 39.1 %copy-start.2 = (bf16[16,2048]{1,0:T(8,128)(2,1)S(1)}, bf16[16,2048]{1,0:T(8,128)(2,1)}, u32[]{:S(2)}) copy-start(bf16[16,2048]{1,0:T(8,128)(2,1)} %param.17) | copy-start | bytes 196612
  153.4 21.4 %all-to-all-start.4 = ((bf16[8,16,2048]{2,1,0:T(8,128)(2,1)}), bf16[8,16,2048]{2,1,0:T(8,128)(2,1)S(1)}, u32[]{:S(2)}, u32[]{:S(2)}) async-start(bf16[8,16,2048]{2,1,0:T(8,128)(2,1)} %merge.1), calls=%async_computation.4 | async-start | bytes 1048576 | tf_op jit(solution)/shard_map/all_to_all | solution.py:29

commit v5 on v3

--- a/solution.py
+++ b/solution.py
@@ -48,17 +48,42 @@
     return lax.ppermute(array, axis, [(i, (i + k) % n) for i in range(n)])
 
 
+def pack_kernel(sums_ref, block_ref, o_ref):
+    n_sp = sums_ref.shape[0]
+    rows, width = block_ref.shape
+    total = functools.reduce(jnp.add, [sums_ref[i] for i in range(n_sp)])
+    high = total.astype(BF16).astype(F32)
+    middle = (total - high).astype(BF16).astype(F32)
+    low = total - high - middle
+    spare = jnp.zeros((rows - 3 * total.shape[0], total.shape[1]), F32)
+    parts = jnp.concatenate([high, middle, low, spare], axis=0).astype(BF16)
+    block = block_ref[...]
+    for i in range(o_ref.shape[0]):
+        o_ref[i, :, :width] = block
+        o_ref[i, :, width:] = parts
+
+
 def project_kernel(
-    at_ref, own_ref, other_ref, vec_ref, gain_ref, kv_gain_ref, cos_ref, sin_ref, w_qn_ref, w_turn_ref, w_down_ref, w_key_ref, w_value_ref,
-    q_ref, kv_ref, ctx_ref, h_ref,
+    at_ref, own_ref, other_ref, gain_ref, kv_gain_ref, cos_ref, sin_ref, w_qn_ref, w_turn_ref, w_down_ref, w_key_ref, w_value_ref,
+    q_ref, kv_ref, gate_ref, ctx_ref, h_ref,
 ):
     n_y, rows, _ = own_ref.shape
-    tok = 2 * n_y * rows
+    side_rows = n_y * rows
+    tok = 2 * side_rows
     width = gain_ref.shape[1]
     lanes = width // rows
     n_ctx = 2 * n_y
-    columns = jnp.concatenate([vec_ref[t] for t in range(vec_ref.shape[0])], axis=1)
+    core = at_ref[0, 0]
+    columns = []
+    for y in range(n_y):
+        pair = []
+        for ref in (own_ref, other_ref):
+            part = ref[y, :, width + lanes :].astype(F32)
+            pair.append(part[0:5] + part[5:10] + part[10:15])
+        columns += [jnp.where(core == 0, pair[0], pair[1]), jnp.where(core == 0, pair[1], pair[0])]
+    columns = jnp.concatenate(columns, axis=1)
     shift, shift_ctx, scale, scale_ctx = (columns[j : j + 1] for j in range(4))
+    gate_ref[...] = columns[4:5]
     gain = gain_ref[...]
 
     def modulated(values, shift, scale):
@@ -66,12 +91,11 @@
         return (normed * (gain * (1.0 + scale)) + shift).astype(BF16)
 
     for side, ref in enumerate((own_ref, other_ref)):
-        core = (at_ref[0, 1] + side) % 2
-        for k in range(n_y):
-            block = core * n_y + (at_ref[0, 0] + (n_y - k)) % n_y
-            h_ref[pl.ds(pl.multiple_of(block * rows, rows), rows), :] = modulated(ref[k, :, :width].astype(F32), shift, scale)
-            t = side * n_y + k
-            ctx_ref[t * rows : (t + 1) * rows, :] = ref[k, :, width:].astype(F32)
+        at = pl.multiple_of((core + side) % 2 * side_rows, side_rows)
+        h_ref[pl.ds(at, side_rows), :] = modulated(ref[:, :, :width].reshape(side_rows, width).astype(F32), shift, scale)
+        ctx_ref[side * side_rows : (side + 1) * side_rows, :] = (
+            ref[:, :, width : width + lanes].reshape(side_rows, lanes).astype(F32)
+        )
     context = jnp.concatenate([ctx_ref[pl.ds(i, n_ctx, stride=rows), :] for i in range(rows)], axis=1)
     h_ref[tok:, :] = modulated(context, shift_ctx, scale_ctx)
     h = h_ref[...]
@@ -116,48 +140,56 @@
     step = factor * LOG2E
     bias = bias_ref[0, 0] * LOG2E
     blocks = (q0, q1, q2, q3)
-    for k, block in enumerate(blocks):
-        to = (place_ref[0, 0] + (len(blocks) - k)) % len(blocks)
-        for part in range(2):
-            rows = slice(part * half, (part + 1) * half)
-            q = jnp.concatenate([block[rows, :], block[tok:, part * rope : (part + 1) * rope]], axis=1)
-            scores = [lax.dot_general(q, k_ref[i], dims, preferred_element_type=F32) * step for i in range(n_blocks)]
-            scores.append(lax.dot_general(q, kc_ref[...], dims, preferred_element_type=F32) * step + bias)
-            tops = [jnp.max(s, axis=1, keepdims=True) for s in scores]
-            top = functools.reduce(jnp.maximum, tops)
-            weights = [jnp.exp2(s - top) for s in scores]
-            total = functools.reduce(jnp.add, [jnp.sum(w, axis=1, keepdims=True) for w in weights])
-            values = [kv_ref[i, count : count + tok] for i in range(n_blocks)] + [vc_ref[...]]
-            out = functools.reduce(
-                jnp.add, [jnp.dot(w.astype(BF16), v, preferred_element_type=F32) for w, v in zip(weights, values, strict=True)]
-            )
-            o_ref[to, part, :half, :] = (out / total).astype(BF16)
-            lse = jnp.transpose(jnp.broadcast_to(top + jnp.log2(total), (half, lanes)))[:16]
-            high = lse.astype(BF16).astype(F32)
-            middle = (lse - high).astype(BF16).astype(F32)
-            row = lax.broadcasted_iota(jnp.int32, lse.shape, 0)
-            stats = jnp.where(row == 0, high, jnp.where(row == 1, middle, jnp.where(row == 2, lse - high - middle, 0.0)))
-            o_ref[to, part, half:, :] = stats.astype(BF16)
+    size = len(blocks)
+    values = [kv_ref[i, count : count + tok] for i in range(n_blocks)] + [vc_ref[...]]
+    for first in range(0, size, 2):
+        pieces = []
+        for block in blocks[first : first + 2]:
+            turned = jnp.concatenate([block[tok:, :rope], block[tok:, rope:]], axis=0)
+            pieces.append(jnp.concatenate([block[:tok, :], turned], axis=1))
+        q = jnp.concatenate(pieces, axis=0)
+        scores = [lax.dot_general(q, k_ref[i], dims, preferred_element_type=F32) * step for i in range(n_blocks)]
+        scores.append(lax.dot_general(q, kc_ref[...], dims, preferred_element_type=F32) * step + bias)
+        widest = functools.reduce(jnp.maximum, scores[:-1])
+        top = jnp.maximum(jnp.max(widest, axis=1, keepdims=True), jnp.max(scores[-1], axis=1, keepdims=True))
+        weights = [jnp.exp2(s - top) for s in scores]
+        total = jnp.sum(functools.reduce(jnp.add, weights[:-1]), axis=1, keepdims=True) + jnp.sum(weights[-1], axis=1, keepdims=True)
+        out = functools.reduce(
+            jnp.add, [jnp.dot(w.astype(BF16), v, preferred_element_type=F32) for w, v in zip(weights, values, strict=True)]
+        )
+        out = (out / total).astype(BF16)
+        lse = jnp.transpose(jnp.broadcast_to(top + jnp.log2(total), (2 * tok, lanes)))[:16]
+        high = lse.astype(BF16).astype(F32)
+        middle = (lse - high).astype(BF16).astype(F32)
+        row = lax.broadcasted_iota(jnp.int32, lse.shape, 0)
+        stats = jnp.where(row == 0, high, jnp.where(row == 1, middle, jnp.where(row == 2, lse - high - middle, 0.0))).astype(BF16)
+        for k in range(2):
+            to = (place_ref[0, 0] + (size - first - k)) % size
+            for part in range(2):
+                rows = slice(k * tok + part * half, k * tok + (part + 1) * half)
+                o_ref[to, part, :half, :] = out[rows]
+                o_ref[to, part, half:, :] = stats[:, rows]
 
 
 def merge_kernel(at_ref, got_ref, w_own_ref, w_other_ref, o_ref):
     n_q, _, height, lanes = got_ref.shape
     half = height - 16
     n_y, rows, width = o_ref.shape
-    term = None
-    for side, w_ref in enumerate((w_own_ref, w_other_ref)):
-        core = (at_ref[0, 0] + side) % 2
+    cores = [(at_ref[0, 0] + side) % 2 for side in range(2)]
+    shares = []
+    for core in cores:
         lse = [jnp.sum(got_ref[i, core, half:, :].astype(F32), axis=0, keepdims=True) for i in range(n_q)]
         top = functools.reduce(jnp.maximum, lse)
-        shares = [jnp.exp2(v - top) for v in lse]
-        total = functools.reduce(jnp.add, shares)
-        mixed = None
-        for i in range(n_q):
-            share = jnp.transpose(jnp.broadcast_to(shares[i] / total, (lanes, half)))
-            piece = got_ref[i, core, :half, :].astype(F32) * share
-            mixed = piece if mixed is None else mixed + piece
-        out = jnp.dot(mixed.astype(BF16), w_ref[...], preferred_element_type=F32)
-        term = out if term is None else term + out
+        raised = [jnp.exp2(v - top) for v in lse]
+        total = functools.reduce(jnp.add, raised)
+        shares += [v / total for v in raised]
+    shares = jnp.transpose(jnp.concatenate(shares + [jnp.zeros((lanes - len(shares), half), F32)], axis=0))
+    mixed = []
+    for side, core in enumerate(cores):
+        pieces = [got_ref[i, core, :half, :].astype(F32) * shares[:, side * n_q + i : side * n_q + i + 1] for i in range(n_q)]
+        mixed.append(functools.reduce(jnp.add, pieces).astype(BF16))
+    term = jnp.dot(mixed[0], w_own_ref[...], preferred_element_type=F32)
+    term = term + jnp.dot(mixed[1], w_other_ref[...], preferred_element_type=F32)
     o_ref[...] = term.astype(BF16).reshape(n_y, rows, width)
 
 
@@ -179,42 +211,47 @@
     rope = w_rope_key.shape[1]
     factor = (nope + rope) ** (-0.5)
 
-    block = jnp.concatenate([latent, context.reshape(rows, lanes)], axis=1)
-    moved = [shifted(block, "y", k) for k in range(1, n_y)]
-    mine = jnp.stack([block] + moved)
-    other = shifted(mine, "c", 1)
-
     feat = shift_w.shape[0]
     own = jnp.stack([lax.dynamic_slice_in_dim(v, sp_index * feat, feat) for v in (cond, ctx_mod)])
     own = jax.nn.silu(own)
     parts = [jnp.sum(own[i][:, None] * w, axis=0) for w, i in ((shift_w, 0), (shift_w, 1), (scale_w, 0), (scale_w, 1), (gate_w, 0))]
     summed = copies(jnp.stack(parts), SP)
-    summed = jnp.sum(summed, axis=0)
-    vectors = copies(summed, TP)
-    gate = vectors[:, 4].reshape(width)
+    smem = pl.BlockSpec(memory_space=pltpu.SMEM)
+    vmem = pl.BlockSpec(memory_space=pltpu.VMEM)
+    block = jnp.concatenate([latent, context.reshape(rows, lanes)], axis=1)
+    message = pl.pallas_call(
+        pack_kernel,
+        in_specs=[vmem, vmem],
+        out_specs=vmem,
+        out_shape=jax.ShapeDtypeStruct((n_y, rows, width + 2 * lanes), BF16),
+        name="pack",
+    )(summed, block)
+
+    mine = exchanged(message, "y")
+    other = shifted(mine, "c", 1)
 
     w_other = shifted(w_out, "c", 1)
     w_turn = jnp.concatenate([w_qr.T, w_rope_key.T], axis=0)
     place = jnp.arange(tok, dtype=jnp.int32)
     place = (place // rows % n_y * n_c + place // (rows * n_y)) * rows + place % rows
     cosine, sine = turn_table(sp_index * tok + place, rope, lanes)
-    vectors, w_turn, cosine, sine, w_other = lax.optimization_barrier((vectors, w_turn, cosine, sine, w_other))
-
-    at = jnp.stack([lax.axis_index("y"), lax.axis_index("c")]).astype(jnp.int32).reshape(1, 2)
-    smem = pl.BlockSpec(memory_space=pltpu.SMEM)
-    vmem = pl.BlockSpec(memory_space=pltpu.VMEM)
-    q_own, kv_copies = pl.pallas_call(
+    at = lax.axis_index("c").astype(jnp.int32).reshape(1, 1)
+    to = lax.axis_index(Q_AXIS).astype(jnp.int32).reshape(1, 1)
+    mine, w_turn, cosine, sine, w_other, at, to = lax.optimization_barrier((mine, w_turn, cosine, sine, w_other, at, to))
+
+    q_own, kv_copies, gate = pl.pallas_call(
         project_kernel,
-        in_specs=[smem] + [vmem] * 12,
-        out_specs=[vmem, vmem],
+        in_specs=[smem] + [vmem] * 11,
+        out_specs=[vmem, vmem, vmem],
         out_shape=[
             jax.ShapeDtypeStruct((tok + tok // 2, lanes), BF16),
             jax.ShapeDtypeStruct((lax.axis_size(KV_AXES), 2 * (tok + n_tp) + tok // 2 + n_tp, lanes), BF16),
+            jax.ShapeDtypeStruct((1, width), F32),
         ],
         scratch_shapes=[pltpu.VMEM((tok, lanes), F32), pltpu.VMEM((tok + n_tp, width), BF16)],
         name="project",
     )(
-        at, mine, other, vectors, norm_gain.reshape(1, width), kv_gain.reshape(1, -1), cosine, sine, w_qn, w_turn, w_kv_down, w_key_up,
+        at, mine, other, norm_gain.reshape(1, width), kv_gain.reshape(1, -1), cosine, sine, w_qn, w_turn, w_kv_down, w_key_up,
         w_value_up,
     )
 
@@ -232,7 +269,7 @@
             pltpu.VMEM((n_kv * n_tp, vsize), BF16),
         ],
         name="attend",
-    )(lax.axis_index(Q_AXIS).astype(jnp.int32).reshape(1, 1), ctx_bias.reshape(1, 1), *queries, kv)
+    )(to, ctx_bias.reshape(1, 1), *queries, kv)
 
     got = exchanged(out.reshape(n_q * n_c, half + 16, vsize), (Q_AXIS, "c")).reshape(n_q, n_c, half + 16, vsize)
     term = pl.pallas_call(
@@ -241,7 +278,7 @@
         out_specs=vmem,
         out_shape=jax.ShapeDtypeStruct((n_y, rows, width), BF16),
         name="merge",
-    )(lax.axis_index("c").astype(jnp.int32).reshape(1, 1), got, w_out, w_other)
+    )(at, got, w_out, w_other)
     branch = jnp.sum(exchanged(term, ("y",)).astype(F32), axis=0)
     return (latent.astype(F32) + gate * branch).astype(BF16)
 

time: 162 us -> 146 us (0.901)
  starting transfers between devices: 74.8 us -> 43.7 us
  blocking collectives: 18.3 us -> 39.7 us
  waiting for transfers between devices: 38.1 us -> 32.6 us
    ppermute x12 -> x5, starting transfers between devices: 49.1 us -> 19.5 us  [shifted(): return lax.ppermute(array, axis, [(i, (i + k) % n) for i in range(n)])]
    all_to_all x1 -> x2, blocking collectives: 18.3 us -> 39.7 us  [exchanged(): return lax.all_to_all(array, axes, 0, 0, tiled=True)]
    all_to_all x2, waiting for transfers between devices: 17 us -> 12.7 us  [exchanged(): return lax.all_to_all(array, axes, 0, 0, tiled=True)]
    all_to_all x2 -> x1, starting transfers between devices: 16.8 us -> 13.7 us  [copies(): lax.all_to_all(jnp.broadcast_to(array[None], (n, *array.shape)), axes, 0,...]
    pallas_call x1 -> x2, Pallas kernels: 5.93 us -> 7.81 us  [the longest x1 6.01 us: step(): pl.pallas_call(project_kernel, in_specs=[smem] + [vmem] * 11, out_specs=[...]
    all_to_all x2, starting transfers between devices: 8.82 us -> 10.5 us  [exchanged(): return lax.all_to_all(array, axes, 0, 0, tiled=True)]
    ppermute x12 -> x5, waiting for transfers between devices: 14 us -> 12.8 us  [shifted(): return lax.ppermute(array, axis, [(i, (i + k) % n) for i in range(n)])]
    all_to_all x2 -> x1, waiting for transfers between devices: 7.11 us -> 7.14 us  [copies(): lax.all_to_all(jnp.broadcast_to(array[None], (n, *array.shape)), axes, 0,...]
  transfers between devices with their start and end apart: 16 -> 8, of which waited for: 4 -> 4; matrix products, arithmetic and copies ran while one was open for 5% -> 3% of each run, Pallas kernels for 0% -> 0%
where the time goes in v5:
time: 146 us; the launch traced here: 144 us
  starting transfers between devices  43.7 us (30%)
  blocking collectives  39.7 us (27%)
  waiting for transfers between devices  32.6 us (22%)
  Pallas kernels  17.3 us (12%)
  other arithmetic  6.02 us (4%)
  local copies, waits for them, and re-layouts  4.19 us (3%)
    all_to_all x2, blocking collectives, exchanged(): return lax.all_to_all(array, axes, 0, 0, tiled=True)  39.7 us
    ppermute x5, starting transfers between devices, shifted(): return lax.ppermute(array, axis, [(i, (i + k) % n) for i in range(n)])  19.5 us
    all_to_all x1, starting transfers between devices, copies(): lax.all_to_all(jnp.broadcast_to(array[None], (n, *array.shape)), axes, 0,...  13.7 us
    ppermute x5, waiting for transfers between devices, shifted(): return lax.ppermute(array, axis, [(i, (i + k) % n) for i in range(n)])  12.8 us
    all_to_all x2, waiting for transfers between devices, exchanged(): return lax.all_to_all(array, axes, 0, 0, tiled=True)  12.7 us
    all_to_all x2, starting transfers between devices, exchanged(): return lax.all_to_all(array, axes, 0, 0, tiled=True)  10.5 us
    all_to_all x1, waiting for transfers between devices, copies(): lax.all_to_all(jnp.broadcast_to(array[None], (n, *array.shape)), axes, 0,...  7.14 us
    pallas_call x1, Pallas kernels, step(): pl.pallas_call(functools.partial(attend_kernel, factor=factor, tok=tok, n...  6.69 us
  transfers between devices with their start and end apart: 8, of which 4 were waited for; matrix products, arithmetic and copies ran while one was open for 3% of the time, Pallas kernels for 0%

profile of v5, /device:TPU:1, one launch (start us, length us, event | category | flops | bytes accessed | tf_op | source)
XLA Modules:
  0.0 144.3 jit_solution(7705233317151845095)
XLA Ops:
  0.0 0.0 copy-start.4
  0.0 0.8 dynamic-slice_bitcast_fusion
  0.9 0.9 multiply_reduce_fusion.3
  1.8 0.0 copy-start.7
  1.8 0.0 copy-start.8
  1.8 0.6 broadcast_in_dim.16
  2.5 13.7 %all-to-all-start = ((f32[32,5,128]{2,1,0:T(8,128)}), f32[32,5,128]{2,1,0:T(8,128)S(1)}, u32[]{:S(2)}, u32[]{:S(2)}) async-start(f32[32,5,128]{2,1,0:T(8,128)} %broadcast_in_dim.16), calls=%async_computation | async-start | bytes 262144 | tf_op jit(solution)/shard_map/all_to_all | solution.py:26
  16.2 0.7 reduce
  16.9 1.5 %pad_maximum_fusion.1.block_ref = bf16[16,2176]{1,0:T(8,128)(2,1)} fusion(bf16[16,128]{1,0:T(8,128)(2,1)S(1)} %bitcast.29, bf16[16,2048]{1,0:T(8,128)(2,1)} %param.17), kind=kLoop, calls=%fused_computation.6 | loop fusion | flops 139264 | bytes 139264 | tf_op jit(solution)/shard_map/concatenate | solution.py:221
  18.4 7.1 %all-to-all-done.sums_ref = f32[32,5,128]{2,1,0:T(8,128)S(1)} async-done(((f32[32,5,128]{2,1,0:T(8,128)}), f32[32,5,128]{2,1,0:T(8,128)S(1)}, u32[]{:S(2)}, u32[]{:S(2)}) %all-to-all-start) | async-done | bytes 81952 | tf_op jit(solution)/shard_map/all_to_all | solution.py:26
  25.5 0.0 copy-start.3
  25.5 0.6 copy-done.3
  26.2 1.8 %pack.1 = bf16[8,16,2304]{2,1,0:T(8,128)(2,1)} custom-call(f32[32,5,128]{2,1,0:T(8,128)} %copy-done.3, bf16[16,2176]{1,0:T(8,128)(2,1)} %pad_maximum_fusion.1.block_ref), custom_call_target="tpu_custom_call" | custom-call | tf_op jit(solution)/shard_map/pack/pallas_call | solution.py:222
  28.0 6.8 %all-to-all-start.1 = ((bf16[8,16,2304]{2,1,0:T(8,128)(2,1)}), bf16[8,16,2304]{2,1,0:T(8,128)(2,1)S(1)}, u32[]{:S(2)}, u32[]{:S(2)}) async-start(bf16[8,16,2304]{2,1,0:T(8,128)(2,1)} %pack.1), calls=%async_computation.1 | async-start | bytes 1179648 | tf_op jit(solution)/shard_map/all_to_all | solution.py:30
  34.8 0.0 copy-done.4
  34.8 4.2 %collective-permute-start = (bf16[128,2048]{1,0:T(8,128)(2,1)S(1)}, bf16[128,2048]{1,0:T(8,128)(2,1)S(1)}, u32[]{:S(2)}, u32[]{:S(2)}) collective-permute-start(bf16[128,2048]{1,0:T(8,128)(2,1)S(1)} %copy-done.4), channel_id=1, source_target_pairs={{0,1},{1,0},{2,3},{3,2},{4,5},{5,4},{6,7},{7,6},{8,9},{9,8},{10,11... | collective-permute-start | bytes 1572872 | tf_op jit(solution)/shard_map/ppermute | solution.py:48
  39.1 12.7 %all-to-all-done.1.own_ref = bf16[8,16,2304]{2,1,0:T(8,128)(2,1)S(1)} async-done(((bf16[8,16,2304]{2,1,0:T(8,128)(2,1)}), bf16[8,16,2304]{2,1,0:T(8,128)(2,1)S(1)}, u32[]{:S(2)}, u32[]{:S(2)}) %all-to-all-start.1) | async-done | bytes 589856 | tf_op jit(solution)/shard_map/all_to_all | solution.py:30
  51.8 0.0 copy-start.1
  51.8 4.8 %collective-permute-start.1 = (bf16[8,16,2304]{2,1,0:T(8,128)(2,1)S(1)}, bf16[8,16,2304]{2,1,0:T(8,128)(2,1)S(1)}, u32[]{:S(2)}, u32[]{:S(2)}) collective-permute-start(bf16[8,16,2304]{2,1,0:T(8,128)(2,1)S(1)} %all-to-all-done.1.own_ref), channel_id=1, source_target_pairs={{0,1},{1,0},{2,3},{3,2},{4,5},{5,4},{6,7},{7,6},{8,9},{9,8},{10,11... | collective-permute-start | bytes 1769480 | tf_op jit(solution)/shard_map/ppermute | solution.py:48
  56.6 1.3 sine_multiply_fusion
  57.9 0.0 copy-done.7
  57.9 0.0 copy-done.8
  57.9 0.8 pad_maximum_fusion.w_turn_ref
  58.7 0.0 collective-permute-done.w_other_ref
  58.7 0.0 copy-start.5
  58.7 0.0 collective-permute-done.1.other_ref
  58.7 0.0 copy-start.2
  58.7 0.0 copy-done.1
  58.8 0.8 copy-done.2
  59.6 6.0 %project.1 = (bf16[384,128]{1,0:T(8,128)(2,1)}, bf16[8,688,128]{2,1,0:T(8,128)(2,1)}, f32[1,2048]{1,0:T(1,128)}) custom-call(s32[1,1]{1,0:T(1,128)} %bitcast.11.at_ref, bf16[8,16,2304]{2,1,0:T(8,128)(2,1)} %copy-done.1, bf16[8,16,2304]{2,1,0:T(8,128)(2,1)} %copy-done.2, f32[1,2048]{1,0:T(1,128)} %bitcast.30, f32[1,512]{1,0:T(1,128)} %bitcast.32, ...), custom_call_target="tpu_custom_call" | custom-call | tf_op jit(solution)/shard_map/project/pallas_call | solution.py:242
  65.6 0.0 copy-start.9
  65.6 3.7 %all-to-all-start.2 = ((bf16[8,688,128]{2,1,0:T(8,128)(2,1)}), bf16[8,688,128]{2,1,0:T(8,128)(2,1)S(1)}, u32[]{:S(2)}, u32[]{:S(2)}) async-start(bf16[8,688,128]{2,1,0:T(8,128)(2,1)} %get-tuple-element.23), calls=%async_computation.2 | async-start | bytes 2818048 | tf_op jit(solution)/shard_map/all_to_all | solution.py:30
  69.3 0.0 copy-done.9
  69.3 2.9 %collective-permute-start.2 = (bf16[384,128]{1,0:T(8,128)(2,1)S(1)}, bf16[384,128]{1,0:T(8,128)(2,1)S(1)}, u32[]{:S(2)}, u32[]{:S(2)}) collective-permute-start(bf16[384,128]{1,0:T(8,128)(2,1)S(1)} %copy-done.9), channel_id=1, source_target_pairs={{0,128},{128,256},{256,384},{384,0},{1,129},{129,257},{257,385},{3... | collective-permute-start | bytes 294920 | tf_op jit(solution)/shard_map/ppermute | solution.py:48
  72.3 3.5 %collective-permute-start.3 = (bf16[384,128]{1,0:T(8,128)(2,1)S(1)}, bf16[384,128]{1,0:T(8,128)(2,1)S(1)}, u32[]{:S(2)}, u32[]{:S(2)}) collective-permute-start(bf16[384,128]{1,0:T(8,128)(2,1)S(1)} %copy-done.9), channel_id=1, source_target_pairs={{0,256},{128,384},{256,0},{384,128},{1,257},{129,385},{257,1},{385... | collective-permute-start | bytes 294920 | tf_op jit(solution)/shard_map/ppermute | solution.py:48
  75.8 4.0 %collective-permute-start.4 = (bf16[384,128]{1,0:T(8,128)(2,1)S(1)}, bf16[384,128]{1,0:T(8,128)(2,1)S(1)}, u32[]{:S(2)}, u32[]{:S(2)}) collective-permute-start(bf16[384,128]{1,0:T(8,128)(2,1)S(1)} %copy-done.9), channel_id=1, source_target_pairs={{0,384},{128,0},{256,128},{384,256},{1,385},{129,1},{257,129},{385... | collective-permute-start | bytes 294920 | tf_op jit(solution)/shard_map/ppermute | solution.py:48
  80.4 10.0 %collective-permute-done.2.q1 = bf16[384,128]{1,0:T(8,128)(2,1)S(1)} collective-permute-done((bf16[384,128]{1,0:T(8,128)(2,1)S(1)}, bf16[384,128]{1,0:T(8,128)(2,1)S(1)}, u32[]{:S(2)}, u32[]{:S(2)}) %collective-permute-start.2) | collective-permute-done | bytes 98336 | tf_op jit(solution)/shard_map/ppermute | solution.py:48
  90.5 0.0 copy-start.10
  90.5 2.8 %collective-permute-done.3.q2 = bf16[384,128]{1,0:T(8,128)(2,1)S(1)} collective-permute-done((bf16[384,128]{1,0:T(8,128)(2,1)S(1)}, bf16[384,128]{1,0:T(8,128)(2,1)S(1)}, u32[]{:S(2)}, u32[]{:S(2)}) %collective-permute-start.3) | collective-permute-done | bytes 98336 | tf_op jit(solution)/shard_map/ppermute | solution.py:48
  93.2 0.0 copy-start.11
  93.2 0.0 collective-permute-done.4.q3
  93.2 0.0 copy-start.12
  93.2 0.0 all-to-all-done.2.kv_ref
  93.2 0.0 copy-start
  93.2 0.0 copy-done.10
  93.2 0.6 copy-done.11
  93.9 0.1 copy-done.12
  93.9 0.5 copy-done
  94.4 6.7 %attend.1 = bf16[4,2,144,128]{3,2,1,0:T(8,128)(2,1)} custom-call(s32[1,1]{1,0:T(1,128)} %bitcast.12.place_ref, f32[1,1]{1,0:T(1,128)} %bitcast.24.bias_ref, bf16[384,128]{1,0:T(8,128)(2,1)} %get-tuple-element.22.q0, bf16[384,128]{1,0:T(8,128)(2,1)} %copy-done.10, bf16[384,128]{1,0:T(8,128)(2,1)} %copy-done.11, bf16[384,128]{1,0:T(8,128)(2,1)} %copy-done.12, ...), custom_call_target="tpu_custom_call" | custom-call | tf_op jit(solution)/shard_map/attend/pallas_call | solution.py:261
  101.1 0.0 copy-done.5
  101.1 19.8 %all_to_all.25 = bf16[8,144,128]{2,1,0:T(8,128)(2,1)} all-to-all(bf16[8,144,128]{2,1,0:T(8,128)(2,1)} %bitcast.25), channel_id=1, replica_groups=mesh['za'=4,'zb'=2,'x'=4,'y'=8,'c'=2] {'za','c'}, dimensions={0} | all-to-all | bytes 589824 | tf_op jit(solution)/shard_map/all_to_all | solution.py:30
  120.9 0.0 copy-start.6
  120.9 0.0 copy-start.13
  120.9 2.8 %merge.1 = bf16[8,16,2048]{2,1,0:T(8,128)(2,1)} custom-call(s32[1,1]{1,0:T(1,128)} %bitcast.11.at_ref, bf16[4,2,144,128]{3,2,1,0:T(8,128)(2,1)} %bitcast.26, bf16[128,2048]{1,0:T(8,128)(2,1)} %w_own_ref.1, bf16[128,2048]{1,0:T(8,128)(2,1)} %copy-done.5), custom_call_target="tpu_custom_call" | custom-call | tf_op jit(solution)/shard_map/merge/pallas_call | solution.py:275
  123.7 19.8 %all_to_all.26 = bf16[8,16,2048]{2,1,0:T(8,128)(2,1)S(1)} all-to-all(bf16[8,16,2048]{2,1,0:T(8,128)(2,1)} %merge.1), channel_id=1, replica_groups=mesh['za'=4,'zb'=2,'x'=4,'y'=8,'c'=2] {'y'}, dimensions={0} | all-to-all | bytes 1048576 | tf_op jit(solution)/shard_map/all_to_all | solution.py:30
  143.5 0.1 convert_reduce_fusion
  143.6 0.0 copy-done.6
  143.6 0.0 copy-done.13
  143.6 0.7 add_convert_fusion
  (6 shorter events, 0.1 us)
Async XLA Ops:
  0.0 34.8 %copy-start.4 = (bf16[128,2048]{1,0:T(8,128)(2,1)S(1)}, bf16[128,2048]{1,0:T(8,128)(2,1)}, u32[]{:S(2)}) copy-start(bf16[128,2048]{1,0:T(8,128)(2,1)} %w_own_ref.1) | copy-start | bytes 1572868
  1.8 56.1 %copy-start.7 = (bf16[2048,64]{0,1:T(8,128)(2,1)S(1)}, bf16[2048,64]{0,1:T(8,128)(2,1)}, u32[]{:S(2)}) copy-start(bf16[2048,64]{0,1:T(8,128)(2,1)} %param.28) | copy-start | bytes 786436
  1.8 56.1 %copy-start.8 = (bf16[2048,64]{0,1:T(8,128)(2,1)S(1)}, bf16[2048,64]{0,1:T(8,128)(2,1)}, u32[]{:S(2)}) copy-start(bf16[2048,64]{0,1:T(8,128)(2,1)} %param.26) | copy-start | bytes 786436
  2.5 23.1 %all-to-all-start = ((f32[32,5,128]{2,1,0:T(8,128)}), f32[32,5,128]{2,1,0:T(8,128)S(1)}, u32[]{:S(2)}, u32[]{:S(2)}) async-start(f32[32,5,128]{2,1,0:T(8,128)} %broadcast_in_dim.16), calls=%async_computation | async-start | bytes 262144 | tf_op jit(solution)/shard_map/all_to_all | solution.py:26
  25.5 0.6 copy-start.3
  28.0 23.8 %all-to-all-start.1 = ((bf16[8,16,2304]{2,1,0:T(8,128)(2,1)}), bf16[8,16,2304]{2,1,0:T(8,128)(2,1)S(1)}, u32[]{:S(2)}, u32[]{:S(2)}) async-start(bf16[8,16,2304]{2,1,0:T(8,128)(2,1)} %pack.1), calls=%async_computation.1 | async-start | bytes 1179648 | tf_op jit(solution)/shard_map/all_to_all | solution.py:30
  34.8 23.9 %collective-permute-start = (bf16[128,2048]{1,0:T(8,128)(2,1)S(1)}, bf16[128,2048]{1,0:T(8,128)(2,1)S(1)}, u32[]{:S(2)}, u32[]{:S(2)}) collective-permute-start(bf16[128,2048]{1,0:T(8,128)(2,1)S(1)} %copy-done.4), channel_id=1, source_target_pairs={{0,1},{1,0},{2,3},{3,2},{4,5},{5,4},{6,7},{7,6},{8,9},{9,8},{10,11... | collective-permute-start | bytes 1572872 | tf_op jit(solution)/shard_map/ppermute | solution.py:48
  51.8 7.0 %copy-start.1 = (bf16[8,16,2304]{2,1,0:T(8,128)(2,1)}, bf16[8,16,2304]{2,1,0:T(8,128)(2,1)S(1)}, u32[]{:S(2)}) copy-start(bf16[8,16,2304]{2,1,0:T(8,128)(2,1)S(1)} %all-to-all-done.1.own_ref) | copy-start | bytes 1769476
  51.8 7.0 %collective-permute-start.1 = (bf16[8,16,2304]{2,1,0:T(8,128)(2,1)S(1)}, bf16[8,16,2304]{2,1,0:T(8,128)(2,1)S(1)}, u32[]{:S(2)}, u32[]{:S(2)}) collective-permute-start(bf16[8,16,2304]{2,1,0:T(8,128)(2,1)S(1)} %all-to-all-done.1.own_ref), channel_id=1, source_target_pairs={{0,1},{1,0},{2,3},{3,2},{4,5},{5,4},{6,7},{7,6},{8,9},{9,8},{10,11... | collective-permute-start | bytes 1769480 | tf_op jit(solution)/shard_map/ppermute | solution.py:48
  58.7 42.4 %copy-start.5 = (bf16[128,2048]{1,0:T(8,128)(2,1)}, bf16[128,2048]{1,0:T(8,128)(2,1)S(1)}, u32[]{:S(2)}) copy-start(bf16[128,2048]{1,0:T(8,128)(2,1)S(1)} %collective-permute-done.w_other_ref) | copy-start | bytes 1572868
  58.7 0.9 copy-start.2
  65.6 3.7 %copy-start.9 = (bf16[384,128]{1,0:T(8,128)(2,1)S(1)}, bf16[384,128]{1,0:T(8,128)(2,1)}, u32[]{:S(2)}) copy-start(bf16[384,128]{1,0:T(8,128)(2,1)} %get-tuple-element.22.q0) | copy-start | bytes 294916
  65.6 27.6 %all-to-all-start.2 = ((bf16[8,688,128]{2,1,0:T(8,128)(2,1)}), bf16[8,688,128]{2,1,0:T(8,128)(2,1)S(1)}, u32[]{:S(2)}, u32[]{:S(2)}) async-start(bf16[8,688,128]{2,1,0:T(8,128)(2,1)} %get-tuple-element.23), calls=%async_computation.2 | async-start | bytes 2818048 | tf_op jit(solution)/shard_map/all_to_all | solution.py:30
  69.3 21.1 %collective-permute-start.2 = (bf16[384,128]{1,0:T(8,128)(2,1)S(1)}, bf16[384,128]{1,0:T(8,128)(2,1)S(1)}, u32[]{:S(2)}, u32[]{:S(2)}) collective-permute-start(bf16[384,128]{1,0:T(8,128)(2,1)S(1)} %copy-done.9), channel_id=1, source_target_pairs={{0,128},{128,256},{256,384},{384,0},{1,129},{129,257},{257,385},{3... | collective-permute-start | bytes 294920 | tf_op jit(solution)/shard_map/ppermute | solution.py:48
  72.3 20.9 %collective-permute-start.3 = (bf16[384,128]{1,0:T(8,128)(2,1)S(1)}, bf16[384,128]{1,0:T(8,128)(2,1)S(1)}, u32[]{:S(2)}, u32[]{:S(2)}) collective-permute-start(bf16[384,128]{1,0:T(8,128)(2,1)S(1)} %copy-done.9), channel_id=1, source_target_pairs={{0,256},{128,384},{256,0},{384,128},{1,257},{129,385},{257,1},{385... | collective-permute-start | bytes 294920 | tf_op jit(solution)/shard_map/ppermute | solution.py:48
  75.8 17.5 %collective-permute-start.4 = (bf16[384,128]{1,0:T(8,128)(2,1)S(1)}, bf16[384,128]{1,0:T(8,128)(2,1)S(1)}, u32[]{:S(2)}, u32[]{:S(2)}) collective-permute-start(bf16[384,128]{1,0:T(8,128)(2,1)S(1)} %copy-done.9), channel_id=1, source_target_pairs={{0,384},{128,0},{256,128},{384,256},{1,385},{129,1},{257,129},{385... | collective-permute-start | bytes 294920 | tf_op jit(solution)/shard_map/ppermute | solution.py:48
  90.5 2.8 %copy-start.10 = (bf16[384,128]{1,0:T(8,128)(2,1)}, bf16[384,128]{1,0:T(8,128)(2,1)S(1)}, u32[]{:S(2)}) copy-start(bf16[384,128]{1,0:T(8,128)(2,1)S(1)} %collective-permute-done.2.q1) | copy-start | bytes 294916
  93.2 0.6 copy-start.11
  93.2 0.7 copy-start.12
  93.2 1.2 copy-start
  120.9 22.7 %copy-start.6 = (bf16[16,2048]{1,0:T(8,128)(2,1)S(1)}, bf16[16,2048]{1,0:T(8,128)(2,1)}, u32[]{:S(2)}) copy-start(bf16[16,2048]{1,0:T(8,128)(2,1)} %param.17) | copy-start | bytes 196612
  120.9 22.7 %copy-start.13 = (f32[1,2048]{1,0:T(1,128)S(1)}, f32[1,2048]{1,0:T(1,128)}, u32[]{:S(2)}) copy-start(f32[1,2048]{1,0:T(1,128)} %get-tuple-element.20) | copy-start | bytes 24580

commit v6 on v5

--- a/solution.py
+++ b/solution.py
@@ -16,7 +16,8 @@
 F32 = jnp.float32
 BF16 = jnp.bfloat16
 SP = ("za", "zb", "x")
-TP = ("y", "c")
+Y = ("ya", "yb")
+TP = ("ya", "yb", "c")
 KV_AXES = ("zb", "x")
 Q_AXIS = "za"
 
@@ -64,12 +65,19 @@
 
 
 def project_kernel(
-    at_ref, own_ref, other_ref, gain_ref, kv_gain_ref, cos_ref, sin_ref, w_qn_ref, w_turn_ref, w_down_ref, w_key_ref, w_value_ref,
-    q_ref, kv_ref, gate_ref, ctx_ref, h_ref,
+    at_ref, own_ref, other_ref, gain_ref, kv_gain_ref, cos_ref, sin_ref, w_side_hbm, w_down_hbm, w_up_hbm,
+    q_ref, kv_ref, gate_ref, ctx_ref, h_ref, w_side_ref, w_down_ref, w_up_ref, side_sem, down_sem, up_sem,
 ):
+    loads = [
+        pltpu.make_async_copy(w_side_hbm, w_side_ref, side_sem), pltpu.make_async_copy(w_down_hbm, w_down_ref, down_sem),
+        pltpu.make_async_copy(w_up_hbm, w_up_ref, up_sem),
+    ]
+    for load in loads:
+        load.start()
     n_y, rows, _ = own_ref.shape
     side_rows = n_y * rows
     tok = 2 * side_rows
+    half = tok // 2
     width = gain_ref.shape[1]
     lanes = width // rows
     n_ctx = 2 * n_y
@@ -90,35 +98,40 @@
         normed = values * lax.rsqrt(jnp.mean(values * values, axis=1, keepdims=True) + EPS)
         return (normed * (gain * (1.0 + scale)) + shift).astype(BF16)
 
+    quarter = side_rows // 2
     for side, ref in enumerate((own_ref, other_ref)):
-        at = pl.multiple_of((core + side) % 2 * side_rows, side_rows)
-        h_ref[pl.ds(at, side_rows), :] = modulated(ref[:, :, :width].reshape(side_rows, width).astype(F32), shift, scale)
         ctx_ref[side * side_rows : (side + 1) * side_rows, :] = (
             ref[:, :, width : width + lanes].reshape(side_rows, lanes).astype(F32)
         )
+        for yb in range(2):
+            at = pl.multiple_of((yb * 2 + (core + side) % 2) * quarter, quarter)
+            some = jnp.concatenate([ref[y, :, :width] for y in range(yb, n_y, 2)], axis=0)
+            h_ref[pl.ds(at, quarter), :] = modulated(some.astype(F32), shift, scale)
     context = jnp.concatenate([ctx_ref[pl.ds(i, n_ctx, stride=rows), :] for i in range(rows)], axis=1)
     h_ref[tok:, :] = modulated(context, shift_ctx, scale_ctx)
     h = h_ref[...]
-    q_ref[:tok, :] = jnp.dot(h[:tok], w_qn_ref[...], preferred_element_type=F32).astype(BF16)
-    pair = lax.dot_general(h, w_turn_ref[...], (((1,), (1,)), ((), ())), preferred_element_type=F32)
+    loads[0].wait()
+    mixed = jnp.dot(h, w_side_ref[...], preferred_element_type=F32)
+    loads[1].wait()
+    inner = jnp.dot(h, w_down_ref[...], preferred_element_type=F32)
+    inner = (inner * lax.rsqrt(jnp.mean(inner * inner, axis=1, keepdims=True) + EPS) * kv_gain_ref[...]).astype(BF16)
+    loads[2].wait()
+    both = jnp.dot(inner, w_up_ref[...], preferred_element_type=F32).astype(BF16)
+    q_ref[:tok, :] = mixed[:tok, :lanes].astype(BF16)
+    pair = mixed[:, lanes:]
     own = pair[:tok]
     lane = lax.broadcasted_iota(jnp.int32, own.shape, 1)
     other = jnp.where(lane % 2 == 0, pltpu.roll(own, lanes - 1, 1), pltpu.roll(own, 1, 1))
     turned = own * cos_ref[...] + other * sin_ref[...]
-    half = tok // 2
     swapped = pltpu.roll(turned, lanes // 2, 1)
     low = lax.broadcasted_iota(jnp.int32, (half, lanes), 1) < lanes // 2
     q_ref[tok:, :] = jnp.where(low, turned[:half], swapped[half:]).astype(BF16)
-    inner = jnp.dot(h, w_down_ref[...], preferred_element_type=F32)
-    inner = (inner * lax.rsqrt(jnp.mean(inner * inner, axis=1, keepdims=True) + EPS) * kv_gain_ref[...]).astype(BF16)
-    keys = jnp.dot(inner, w_key_ref[...], preferred_element_type=F32).astype(BF16)
-    values = jnp.dot(inner, w_value_ref[...], preferred_element_type=F32).astype(BF16)
     turned = jnp.where(low, swapped[:half], turned[half:]).astype(BF16)
     still = pltpu.roll(pair[tok:], lanes // 2, 1).astype(BF16)
     count = tok + n_ctx
     for i in range(kv_ref.shape[0]):
-        kv_ref[i, :count, :] = keys
-        kv_ref[i, count : 2 * count, :] = values
+        kv_ref[i, :count, :] = both[:, :lanes]
+        kv_ref[i, count : 2 * count, :] = both[:, lanes:]
         kv_ref[i, 2 * count : 2 * count + half, :] = turned
         kv_ref[i, 2 * count + half :, :] = still
 
@@ -163,34 +176,42 @@
         middle = (lse - high).astype(BF16).astype(F32)
         row = lax.broadcasted_iota(jnp.int32, lse.shape, 0)
         stats = jnp.where(row == 0, high, jnp.where(row == 1, middle, jnp.where(row == 2, lse - high - middle, 0.0))).astype(BF16)
+        quarter = tok // 4
         for k in range(2):
             to = (place_ref[0, 0] + (size - first - k)) % size
-            for part in range(2):
-                rows = slice(k * tok + part * half, k * tok + (part + 1) * half)
-                o_ref[to, part, :half, :] = out[rows]
-                o_ref[to, part, half:, :] = stats[:, rows]
-
-
-def merge_kernel(at_ref, got_ref, w_own_ref, w_other_ref, o_ref):
+            for part in range(4):
+                at = k * tok + part * quarter
+                o_ref[to, part, :quarter, :] = out[at : at + quarter]
+                o_ref[to, part, quarter:, :quarter] = stats[:, at : at + quarter]
+                o_ref[to, part, quarter:, quarter:] = jnp.zeros((16, lanes - quarter), BF16)
+
+
+def merge_kernel(at_ref, got_ref, *refs):
+    hbm, o_ref, w_refs, sems = refs[:4], refs[4], refs[5:9], refs[9:]
+    loads = [pltpu.make_async_copy(src, dst, sem) for src, dst, sem in zip(hbm, w_refs, sems, strict=True)]
+    for load in loads:
+        load.start()
     n_q, _, height, lanes = got_ref.shape
-    half = height - 16
-    n_y, rows, width = o_ref.shape
-    cores = [(at_ref[0, 0] + side) % 2 for side in range(2)]
+    quarter = height - 16
+    n_ya, rows, width = o_ref.shape
+    core, yb = at_ref[0, 0], at_ref[0, 1]
+    sources = [(yb + i) % 2 * 2 + (core + j) % 2 for i in range(2) for j in range(2)]
     shares = []
-    for core in cores:
-        lse = [jnp.sum(got_ref[i, core, half:, :].astype(F32), axis=0, keepdims=True) for i in range(n_q)]
+    for source in sources:
+        lse = [jnp.sum(got_ref[i, source, quarter:, :].astype(F32), axis=0, keepdims=True) for i in range(n_q)]
         top = functools.reduce(jnp.maximum, lse)
         raised = [jnp.exp2(v - top) for v in lse]
         total = functools.reduce(jnp.add, raised)
         shares += [v / total for v in raised]
-    shares = jnp.transpose(jnp.concatenate(shares + [jnp.zeros((lanes - len(shares), half), F32)], axis=0))
-    mixed = []
-    for side, core in enumerate(cores):
-        pieces = [got_ref[i, core, :half, :].astype(F32) * shares[:, side * n_q + i : side * n_q + i + 1] for i in range(n_q)]
-        mixed.append(functools.reduce(jnp.add, pieces).astype(BF16))
-    term = jnp.dot(mixed[0], w_own_ref[...], preferred_element_type=F32)
-    term = term + jnp.dot(mixed[1], w_other_ref[...], preferred_element_type=F32)
-    o_ref[...] = term.astype(BF16).reshape(n_y, rows, width)
+    shares = jnp.transpose(jnp.concatenate(shares + [jnp.zeros((lanes - len(shares), lanes), F32)], axis=0))[:quarter]
+    term = None
+    for s, source in enumerate(sources):
+        pieces = [got_ref[i, source, :quarter, :].astype(F32) * shares[:, s * n_q + i : s * n_q + i + 1] for i in range(n_q)]
+        mixed = functools.reduce(jnp.add, pieces).astype(BF16)
+        loads[s].wait()
+        out = jnp.dot(mixed, w_refs[s][...], preferred_element_type=F32)
+        term = out if term is None else term + out
+    o_ref[...] = term.astype(BF16).reshape(n_ya, rows, width)
 
 
 def step(
@@ -199,13 +220,14 @@
 ):
     n_tp = lax.axis_size(TP)
     n_c = lax.axis_size("c")
-    n_y = lax.axis_size("y")
+    n_y = lax.axis_size(Y)
+    n_ya = lax.axis_size("ya")
     n_q = lax.axis_size(Q_AXIS)
     sp_index = lax.axis_index(SP)
     rows, width = latent.shape
     lanes = width // rows
     tok = rows * n_tp
-    half = tok // n_c
+    quarter = tok // (2 * n_c)
     nope = w_key_up.shape[1]
     vsize = w_value_up.shape[1]
     rope = w_rope_key.shape[1]
@@ -216,75 +238,86 @@
     own = jax.nn.silu(own)
     parts = [jnp.sum(own[i][:, None] * w, axis=0) for w, i in ((shift_w, 0), (shift_w, 1), (scale_w, 0), (scale_w, 1), (gate_w, 0))]
     summed = copies(jnp.stack(parts), SP)
+    w_other = shifted(w_out, "c", 1)
+    w_side = jnp.concatenate([w_qn, w_qr, w_rope_key], axis=1)
+    w_up = jnp.concatenate([w_key_up, w_value_up], axis=1)
+    place = jnp.arange(tok, dtype=jnp.int32)
+    place = (place // rows % n_ya * 2 + place // (tok // 2)) * (n_c * rows) + place // quarter % n_c * rows + place % rows
+    cosine, sine = turn_table(sp_index * tok + place, rope, lanes)
+    at = jnp.stack([lax.axis_index("c"), lax.axis_index("yb")]).astype(jnp.int32).reshape(1, 2)
+    to = lax.axis_index(Q_AXIS).astype(jnp.int32).reshape(1, 1)
+    block = jnp.concatenate([latent, context.reshape(rows, lanes)], axis=1)
+    block, w_side, w_up, cosine, sine, at, to = lax.optimization_barrier((block, w_side, w_up, cosine, sine, at, to))
     smem = pl.BlockSpec(memory_space=pltpu.SMEM)
     vmem = pl.BlockSpec(memory_space=pltpu.VMEM)
-    block = jnp.concatenate([latent, context.reshape(rows, lanes)], axis=1)
-    message = pl.pallas_call(
+    any_space = pl.BlockSpec(memory_space=pl.ANY)
+    pack = pl.pallas_call(
         pack_kernel,
         in_specs=[vmem, vmem],
         out_specs=vmem,
         out_shape=jax.ShapeDtypeStruct((n_y, rows, width + 2 * lanes), BF16),
         name="pack",
-    )(summed, block)
-
-    mine = exchanged(message, "y")
+    )
+    message = pack(summed, block)
+
+    mine = exchanged(message, Y)
     other = shifted(mine, "c", 1)
-
-    w_other = shifted(w_out, "c", 1)
-    w_turn = jnp.concatenate([w_qr.T, w_rope_key.T], axis=0)
-    place = jnp.arange(tok, dtype=jnp.int32)
-    place = (place // rows % n_y * n_c + place // (rows * n_y)) * rows + place % rows
-    cosine, sine = turn_table(sp_index * tok + place, rope, lanes)
-    at = lax.axis_index("c").astype(jnp.int32).reshape(1, 1)
-    to = lax.axis_index(Q_AXIS).astype(jnp.int32).reshape(1, 1)
-    mine, w_turn, cosine, sine, w_other, at, to = lax.optimization_barrier((mine, w_turn, cosine, sine, w_other, at, to))
 
     q_own, kv_copies, gate = pl.pallas_call(
         project_kernel,
-        in_specs=[smem] + [vmem] * 11,
+        in_specs=[smem] + [vmem] * 6 + [any_space] * 3,
         out_specs=[vmem, vmem, vmem],
         out_shape=[
             jax.ShapeDtypeStruct((tok + tok // 2, lanes), BF16),
             jax.ShapeDtypeStruct((lax.axis_size(KV_AXES), 2 * (tok + n_tp) + tok // 2 + n_tp, lanes), BF16),
             jax.ShapeDtypeStruct((1, width), F32),
         ],
-        scratch_shapes=[pltpu.VMEM((tok, lanes), F32), pltpu.VMEM((tok + n_tp, width), BF16)],
+        scratch_shapes=[
+            pltpu.VMEM((tok, lanes), F32),
+            pltpu.VMEM((tok + n_tp, width), BF16),
+            pltpu.VMEM(w_side.shape, BF16),
+            pltpu.VMEM(w_kv_down.shape, BF16),
+            pltpu.VMEM(w_up.shape, BF16),
+            pltpu.SemaphoreType.DMA,
+            pltpu.SemaphoreType.DMA,
+            pltpu.SemaphoreType.DMA,
+        ],
         name="project",
-    )(
-        at, mine, other, norm_gain.reshape(1, width), kv_gain.reshape(1, -1), cosine, sine, w_qn, w_turn, w_kv_down, w_key_up,
-        w_value_up,
-    )
+    )(at, mine, other, norm_gain.reshape(1, width), kv_gain.reshape(1, -1), cosine, sine, w_side, w_kv_down, w_up)
 
     queries = [q_own] + [shifted(q_own, Q_AXIS, k) for k in range(1, n_q)]
     kv = exchanged(kv_copies, KV_AXES)
+    w_near = [shifted(w, "yb", 1) for w in (w_out, w_other)]
     n_kv = kv.shape[0]
-    out = pl.pallas_call(
+    attend = pl.pallas_call(
         functools.partial(attend_kernel, factor=factor, tok=tok, n_ctx=n_tp),
         in_specs=[smem, smem] + [vmem] * 5,
         out_specs=vmem,
-        out_shape=jax.ShapeDtypeStruct((n_q, n_c, half + 16, vsize), BF16),
+        out_shape=jax.ShapeDtypeStruct((n_q, 2 * n_c, quarter + 16, vsize), BF16),
         scratch_shapes=[
             pltpu.VMEM((n_kv, tok, nope + rope), BF16),
             pltpu.VMEM((n_kv * n_tp, nope + rope), BF16),
             pltpu.VMEM((n_kv * n_tp, vsize), BF16),
         ],
         name="attend",
-    )(to, ctx_bias.reshape(1, 1), *queries, kv)
-
-    got = exchanged(out.reshape(n_q * n_c, half + 16, vsize), (Q_AXIS, "c")).reshape(n_q, n_c, half + 16, vsize)
+    )
+    out = attend(to, ctx_bias.reshape(1, 1), *queries, kv)
+
+    got = exchanged(out.reshape(n_q * 2 * n_c, quarter + 16, vsize), (Q_AXIS, "yb", "c"))
     term = pl.pallas_call(
         merge_kernel,
-        in_specs=[smem] + [vmem] * 3,
+        in_specs=[smem, vmem] + [any_space] * 4,
         out_specs=vmem,
-        out_shape=jax.ShapeDtypeStruct((n_y, rows, width), BF16),
+        out_shape=jax.ShapeDtypeStruct((n_ya, rows, width), BF16),
+        scratch_shapes=[pltpu.VMEM(w_out.shape, BF16)] * 4 + [pltpu.SemaphoreType.DMA] * 4,
         name="merge",
-    )(at, got, w_out, w_other)
-    branch = jnp.sum(exchanged(term, ("y",)).astype(F32), axis=0)
+    )(at, got.reshape(n_q, 2 * n_c, quarter + 16, vsize), w_out, w_other, *w_near)
+    branch = jnp.sum(exchanged(term, ("ya",)).astype(F32), axis=0)
     return (latent.astype(F32) + gate * branch).astype(BF16)
 
 
 def solution(mesh):
-    fine = Mesh(mesh.devices.reshape(4, 2, 4, 8, 2), ("za", "zb", "x", "y", "c"))
+    fine = Mesh(mesh.devices.reshape(4, 2, 4, 4, 2, 2), ("za", "zb", "x", "ya", "yb", "c"))
     row = P((*SP, *TP), None)
     placed = (
         row, P(), P(), row, P(SP, TP), P(SP, TP), P(SP, TP), P(), P(None, TP), P(None, TP), P(), P(), P(), P(None, TP),

time: 146 us -> 156 us (1.068)
  starting transfers between devices: 43.7 us -> 49.9 us
  blocking collectives: 39.7 us -> 35 us
  waiting for transfers between devices: 32.6 us -> 36.9 us
  local copies, waits for them, and re-layouts: 4.19 us -> 7.61 us
    ppermute x5 -> x7, waiting for transfers between devices: 12.8 us -> 34.8 us  [shifted(): return lax.ppermute(array, axis, [(i, (i + k) % n) for i in range(n)])]
    all_to_all x2, waiting for transfers between devices: 12.7 us -> 0.01 us  [exchanged(): return lax.all_to_all(array, axes, 0, 0, tiled=True)]
    ppermute x5 -> x7, starting transfers between devices: 19.5 us -> 26.6 us  [shifted(): return lax.ppermute(array, axis, [(i, (i + k) % n) for i in range(n)])]
    all_to_all x1, waiting for transfers between devices: 7.14 us -> 2.07 us  [copies(): lax.all_to_all(jnp.broadcast_to(array[None], (n, *array.shape)), axes, 0,...]
    all_to_all x2, blocking collectives: 39.7 us -> 35 us  [exchanged(): return lax.all_to_all(array, axes, 0, 0, tiled=True)]
    unnamed x28 -> x40, local copies, waits for them, and re-layouts: 2.67 us -> 6.07 us
  transfers between devices with their start and end apart: 8 -> 10, of which waited for: 4 -> 6; matrix products, arithmetic and copies ran while one was open for 3% -> 5% of each run, Pallas kernels for 0% -> 4%
where the time goes in v6:
time: 156 us; the launch traced here: 154 us
  starting transfers between devices  49.9 us (32%)
  waiting for transfers between devices  36.9 us (24%)
  blocking collectives  35 us (22%)
  Pallas kernels  17.5 us (11%)
  local copies, waits for them, and re-layouts  7.61 us (5%)
  other arithmetic  6.3 us (4%)
    all_to_all x2, blocking collectives, exchanged(): return lax.all_to_all(array, axes, 0, 0, tiled=True)  35 us
    ppermute x7, waiting for transfers between devices, shifted(): return lax.ppermute(array, axis, [(i, (i + k) % n) for i in range(n)])  34.8 us
    ppermute x7, starting transfers between devices, shifted(): return lax.ppermute(array, axis, [(i, (i + k) % n) for i in range(n)])  26.6 us
    all_to_all x1, starting transfers between devices, copies(): lax.all_to_all(jnp.broadcast_to(array[None], (n, *array.shape)), axes, 0,...  13.7 us
    all_to_all x2, starting transfers between devices, exchanged(): return lax.all_to_all(array, axes, 0, 0, tiled=True)  9.6 us
    pallas_call x1, Pallas kernels, step(): out = attend(to, ctx_bias.reshape(1, 1), *queries, kv)  6.69 us
    unnamed x40, local copies, waits for them, and re-layouts  6.07 us
    pallas_call x1, Pallas kernels, step(): pl.pallas_call(project_kernel, in_specs=[smem] + [vmem] * 6 + [any_space]...  5.55 us
  transfers between devices with their start and end apart: 10, of which 6 were waited for; matrix products, arithmetic and copies ran while one was open for 5% of the time, Pallas kernels for 4%

profile of v6, /device:TPU:1, one launch (start us, length us, event | category | flops | bytes accessed | tf_op | source)
XLA Modules:
  0.0 154.2 jit_solution(3909164221670330459)
XLA Ops:
  0.0 0.0 copy-start.10
  0.0 0.0 copy-start.4
  0.0 0.8 dynamic-slice_bitcast_fusion
  0.9 0.9 multiply_reduce_fusion.3
  1.8 0.7 broadcast_in_dim.28
  2.5 13.7 %all-to-all-start = ((f32[32,5,128]{2,1,0:T(8,128)}), f32[32,5,128]{2,1,0:T(8,128)S(1)}, u32[]{:S(2)}, u32[]{:S(2)}) async-start(f32[32,5,128]{2,1,0:T(8,128)} %broadcast_in_dim.28), calls=%async_computation | async-start | bytes 262144 | tf_op jit(solution)/shard_map/all_to_all | solution.py:27
  16.3 1.2 copy.18
  17.5 0.0 copy-start.11
  17.5 0.0 copy-start.12
  17.5 1.3 copy.19
  18.8 0.0 copy-done.18
  18.8 0.0 copy-done.10
  18.8 0.6 pad_maximum_fusion.2.block_ref
  19.5 0.0 copy-done.4
  19.5 1.3 pad_maximum_fusion.w_side_hbm
  20.8 1.3 sine_multiply_fusion
  22.0 0.7 add_bitcast_fusion.at_ref
  22.7 0.0 copy-done.11
  22.7 0.0 copy-done.12
  22.7 0.7 pad_maximum_fusion.1.w_up_hbm
  23.5 2.1 %all-to-all-done.sums_ref = f32[32,5,128]{2,1,0:T(8,128)S(1)} async-done(((f32[32,5,128]{2,1,0:T(8,128)}), f32[32,5,128]{2,1,0:T(8,128)S(1)}, u32[]{:S(2)}, u32[]{:S(2)}) %all-to-all-start) | async-done | bytes 81952 | tf_op jit(solution)/shard_map/all_to_all | solution.py:27
  25.5 0.7 copy-done.5
  26.2 1.8 %pack.1 = bf16[8,16,2304]{2,1,0:T(8,128)(2,1)} custom-call(f32[32,5,128]{2,1,0:T(8,128)} %copy-done.5, bf16[16,2176]{1,0:T(8,128)(2,1)} %pad_maximum_fusion.2.block_ref), custom_call_target="tpu_custom_call" | custom-call | tf_op jit(solution)/shard_map/pack/pallas_call | solution.py:261
  28.0 22.5 %all_to_all.25.own_ref = bf16[8,16,2304]{2,1,0:T(8,128)(2,1)S(1)} all-to-all(bf16[8,16,2304]{2,1,0:T(8,128)(2,1)} %pack.1), channel_id=1, replica_groups=mesh['za'=4,'zb'=2,'x'=4,'ya'=4,'yb'=2,'c'=2] {'ya','yb'}, dimensions={0} | all-to-all | bytes 1179648 | tf_op jit(solution)/shard_map/all_to_all | solution.py:31
  50.5 6.0 %collective-permute-start = (bf16[8,16,2304]{2,1,0:T(8,128)(2,1)S(1)}, bf16[8,16,2304]{2,1,0:T(8,128)(2,1)S(1)}, u32[]{:S(2)}, u32[]{:S(2)}) collective-permute-start(bf16[8,16,2304]{2,1,0:T(8,128)(2,1)S(1)} %all_to_all.25.own_ref), channel_id=1, source_target_pairs={{0,1},{1,0},{2,3},{3,2},{4,5},{5,4},{6,7},{7,6},{8,9},{9,8},{10,11... | collective-permute-start | bytes 1769480 | tf_op jit(solution)/shard_map/ppermute | solution.py:49
  56.6 1.6 %collective-permute-done.other_ref = bf16[8,16,2304]{2,1,0:T(8,128)(2,1)S(1)} collective-permute-done((bf16[8,16,2304]{2,1,0:T(8,128)(2,1)S(1)}, bf16[8,16,2304]{2,1,0:T(8,128)(2,1)S(1)}, u32[]{:S(2)}, u32[]{:S(2)}) %collective-permute-start) | collective-permute-done | bytes 589856 | tf_op jit(solution)/shard_map/ppermute | solution.py:49
  58.2 0.0 copy-done.1
  58.2 0.8 copy-done.3
  59.0 5.6 %project.1 = (bf16[384,128]{1,0:T(8,128)(2,1)}, bf16[8,688,128]{2,1,0:T(8,128)(2,1)}, f32[1,2048]{1,0:T(1,128)}) custom-call(s32[1,2]{1,0:T(1,128)} %add_bitcast_fusion.at_ref, bf16[8,16,2304]{2,1,0:T(8,128)(2,1)} %copy-done.1, bf16[8,16,2304]{2,1,0:T(8,128)(2,1)} %copy-done.3, f32[1,2048]{1,0:T(1,128)} %bitcast.29, f32[1,512]{1,0:T(1,128)} %bitcast.31, ...), custom_call_target="tpu_custom_call" | custom-call | tf_op jit(solution)/shard_map/project/pallas_call | solution.py:266
  64.6 0.0 copy-start.6
  64.6 0.0 copy-start.13
  64.6 3.7 %all-to-all-start.2 = ((bf16[8,688,128]{2,1,0:T(8,128)(2,1)}), bf16[8,688,128]{2,1,0:T(8,128)(2,1)S(1)}, u32[]{:S(2)}, u32[]{:S(2)}) async-start(bf16[8,688,128]{2,1,0:T(8,128)(2,1)} %get-tuple-element.24), calls=%async_computation.2 | async-start | bytes 2818048 | tf_op jit(solution)/shard_map/all_to_all | solution.py:31
  68.3 0.0 copy-done.6
  68.3 2.3 %collective-permute-start.4 = (bf16[128,2048]{1,0:T(8,128)(2,1)S(1)}, bf16[128,2048]{1,0:T(8,128)(2,1)S(1)}, u32[]{:S(2)}, u32[]{:S(2)}) collective-permute-start(bf16[128,2048]{1,0:T(8,128)(2,1)S(1)} %copy-done.6), channel_id=1, source_target_pairs={{0,1},{1,0},{2,3},{3,2},{4,5},{5,4},{6,7},{7,6},{8,9},{9,8},{10,11... | collective-permute-start | bytes 1572872 | tf_op jit(solution)/shard_map/ppermute | solution.py:49
  70.6 0.0 copy-done.13
  70.6 3.5 %collective-permute-start.1 = (bf16[384,128]{1,0:T(8,128)(2,1)S(1)}, bf16[384,128]{1,0:T(8,128)(2,1)S(1)}, u32[]{:S(2)}, u32[]{:S(2)}) collective-permute-start(bf16[384,128]{1,0:T(8,128)(2,1)S(1)} %copy-done.13), channel_id=1, source_target_pairs={{0,128},{128,256},{256,384},{384,0},{1,129},{129,257},{257,385},{3... | collective-permute-start | bytes 294920 | tf_op jit(solution)/shard_map/ppermute | solution.py:49
  74.2 4.4 %collective-permute-start.2 = (bf16[384,128]{1,0:T(8,128)(2,1)S(1)}, bf16[384,128]{1,0:T(8,128)(2,1)S(1)}, u32[]{:S(2)}, u32[]{:S(2)}) collective-permute-start(bf16[384,128]{1,0:T(8,128)(2,1)S(1)} %copy-done.13), channel_id=1, source_target_pairs={{0,256},{128,384},{256,0},{384,128},{1,257},{129,385},{257,1},{385... | collective-permute-start | bytes 294920 | tf_op jit(solution)/shard_map/ppermute | solution.py:49
  78.6 5.1 %collective-permute-start.3 = (bf16[384,128]{1,0:T(8,128)(2,1)S(1)}, bf16[384,128]{1,0:T(8,128)(2,1)S(1)}, u32[]{:S(2)}, u32[]{:S(2)}) collective-permute-start(bf16[384,128]{1,0:T(8,128)(2,1)S(1)} %copy-done.13), channel_id=1, source_target_pairs={{0,384},{128,0},{256,128},{384,256},{1,385},{129,1},{257,129},{385... | collective-permute-start | bytes 294920 | tf_op jit(solution)/shard_map/ppermute | solution.py:49
  84.4 5.8 %collective-permute-done.1.q1 = bf16[384,128]{1,0:T(8,128)(2,1)S(1)} collective-permute-done((bf16[384,128]{1,0:T(8,128)(2,1)S(1)}, bf16[384,128]{1,0:T(8,128)(2,1)S(1)}, u32[]{:S(2)}, u32[]{:S(2)}) %collective-permute-start.1) | collective-permute-done | bytes 98336 | tf_op jit(solution)/shard_map/ppermute | solution.py:49
  90.1 4.6 %collective-permute-done.2.q2 = bf16[384,128]{1,0:T(8,128)(2,1)S(1)} collective-permute-done((bf16[384,128]{1,0:T(8,128)(2,1)S(1)}, bf16[384,128]{1,0:T(8,128)(2,1)S(1)}, u32[]{:S(2)}, u32[]{:S(2)}) %collective-permute-start.2) | collective-permute-done | bytes 98336 | tf_op jit(solution)/shard_map/ppermute | solution.py:49
  94.7 0.0 collective-permute-done.3.q3
  94.7 0.0 all-to-all-done.2.kv_ref
  94.7 0.0 copy-start
  94.7 0.0 copy-done.14
  94.7 0.6 copy-done.15
  95.3 0.0 copy-done.16
  95.4 0.5 copy-done
  95.8 6.7 %attend.1 = bf16[4,4,80,128]{3,2,1,0:T(8,128)(2,1)} custom-call(s32[1,1]{1,0:T(1,128)} %bitcast.3.place_ref, f32[1,1]{1,0:T(1,128)} %bitcast.25.bias_ref, bf16[384,128]{1,0:T(8,128)(2,1)} %get-tuple-element.23.q0, bf16[384,128]{1,0:T(8,128)(2,1)} %copy-done.14, bf16[384,128]{1,0:T(8,128)(2,1)} %copy-done.15, bf16[384,128]{1,0:T(8,128)(2,1)} %copy-done.16, ...), custom_call_target="tpu_custom_call" | custom-call | tf_op jit(solution)/shard_map/attend/pallas_call | solution.py:304
  102.5 5.9 %all-to-all-start.3 = ((bf16[16,80,128]{2,1,0:T(8,128)(2,1)}), bf16[16,80,128]{2,1,0:T(8,128)(2,1)S(1)}, u32[]{:S(2)}, u32[]{:S(2)}) async-start(bf16[16,80,128]{2,1,0:T(8,128)(2,1)} %bitcast.26), calls=%async_computation.3 | async-start | bytes 655360 | tf_op jit(solution)/shard_map/all_to_all | solution.py:31
  108.4 3.2 %collective-permute-start.5 = (bf16[128,2048]{1,0:T(8,128)(2,1)S(1)}, bf16[128,2048]{1,0:T(8,128)(2,1)S(1)}, u32[]{:S(2)}, u32[]{:S(2)}) collective-permute-start(bf16[128,2048]{1,0:T(8,128)(2,1)S(1)} %copy-done.6), channel_id=1, source_target_pairs={{0,2},{2,0},{1,3},{3,1},{4,6},{6,4},{5,7},{7,5},{8,10},{10,8},{9,1... | collective-permute-start | bytes 1572872 | tf_op jit(solution)/shard_map/ppermute | solution.py:49
  111.7 0.0 collective-permute-done.4.refs_1_
  111.7 0.0 copy-start.7
  111.7 2.0 %collective-permute-start.6 = (bf16[128,2048]{1,0:T(8,128)(2,1)S(1)}, bf16[128,2048]{1,0:T(8,128)(2,1)S(1)}, u32[]{:S(2)}, u32[]{:S(2)}) collective-permute-start(bf16[128,2048]{1,0:T(8,128)(2,1)S(1)} %collective-permute-done.4.refs_1_), channel_id=1, source_target_pairs={{0,2},{2,0},{1,3},{3,1},{4,6},{6,4},{5,7},{7,5},{8,10},{10,8},{9,1... | collective-permute-start | bytes 1572872 | tf_op jit(solution)/shard_map/ppermute | solution.py:49
  113.7 11.7 %collective-permute-done.5.refs_2_ = bf16[128,2048]{1,0:T(8,128)(2,1)S(1)} collective-permute-done((bf16[128,2048]{1,0:T(8,128)(2,1)S(1)}, bf16[128,2048]{1,0:T(8,128)(2,1)S(1)}, u32[]{:S(2)}, u32[]{:S(2)}) %collective-permute-start.5) | collective-permute-done | bytes 524320 | tf_op jit(solution)/shard_map/ppermute | solution.py:49
  125.4 11.2 %collective-permute-done.6.refs_3_ = bf16[128,2048]{1,0:T(8,128)(2,1)S(1)} collective-permute-done((bf16[128,2048]{1,0:T(8,128)(2,1)S(1)}, bf16[128,2048]{1,0:T(8,128)(2,1)S(1)}, u32[]{:S(2)}, u32[]{:S(2)}) %collective-permute-start.6) | collective-permute-done | bytes 524320 | tf_op jit(solution)/shard_map/ppermute | solution.py:49
  136.6 0.0 all-to-all-done.3
  136.6 0.0 copy-done.7
  136.6 0.0 copy-done.8
  136.6 0.8 copy-done.9
  137.4 0.1 copy-done.2
  137.6 3.5 %merge.1 = bf16[4,16,2048]{2,1,0:T(8,128)(2,1)} custom-call(s32[1,2]{1,0:T(1,128)} %add_bitcast_fusion.at_ref, bf16[4,4,80,128]{3,2,1,0:T(8,128)(2,1)} %bitcast.27, bf16[128,2048]{1,0:T(8,128)(2,1)} %refs_0_.1, bf16[128,2048]{1,0:T(8,128)(2,1)} %copy-done.7, bf16[128,2048]{1,0:T(8,128)(2,1)} %copy-done.8, bf16[128,2048]{1,0:T(8,128)(2,1)} %copy-done.9), custom_call_target="tpu_custom_call" | custom-call | tf_op jit(solution)/shard_map/merge/pallas_call | solution.py:307
  141.1 12.4 %all_to_all.26 = bf16[4,16,2048]{2,1,0:T(8,128)(2,1)S(1)} all-to-all(bf16[4,16,2048]{2,1,0:T(8,128)(2,1)} %merge.1), channel_id=1, replica_groups=mesh['za'=4,'zb'=2,'x'=4,'ya'=4,'yb'=2,'c'=2] {'ya'}, dimensions={0} | all-to-all | bytes 524288 | tf_op jit(solution)/shard_map/all_to_all | solution.py:31
  153.5 0.0 copy-done.17
  153.5 0.7 add_convert_fusion
  (19 shorter events, 0.2 us)
Async XLA Ops:
  0.0 18.8 %copy-start.18 = (bf16[1,2048]{1,0:T(2,128)(2,1)S(1)}, bf16[1,2048]{1,0:T(2,128)(2,1)}, u32[]{:S(2)}) copy-start(bf16[1,2048]{1,0:T(2,128)(2,1)} %param.20) | copy-start | bytes 12292
  0.0 18.8 %copy-start.10 = (bf16[16,2048]{1,0:T(8,128)(2,1)S(1)}, bf16[16,2048]{1,0:T(8,128)(2,1)}, u32[]{:S(2)}) copy-start(bf16[16,2048]{1,0:T(8,128)(2,1)} %param.17) | copy-start | bytes 196612
  0.0 19.5 %copy-start.4 = (bf16[2048,128]{1,0:T(8,128)(2,1)S(1)}, bf16[2048,128]{1,0:T(8,128)(2,1)}, u32[]{:S(2)}) copy-start(bf16[2048,128]{1,0:T(8,128)(2,1)} %param.25) | copy-start | bytes 1572868
  2.5 23.1 %all-to-all-start = ((f32[32,5,128]{2,1,0:T(8,128)}), f32[32,5,128]{2,1,0:T(8,128)S(1)}, u32[]{:S(2)}, u32[]{:S(2)}) async-start(f32[32,5,128]{2,1,0:T(8,128)} %broadcast_in_dim.28), calls=%async_computation | async-start | bytes 262144 | tf_op jit(solution)/shard_map/all_to_all | solution.py:27
  17.5 5.2 %copy-start.11 = (bf16[512,128]{1,0:T(8,128)(2,1)S(1)}, bf16[512,128]{1,0:T(8,128)(2,1)}, u32[]{:S(2)}) copy-start(bf16[512,128]{1,0:T(8,128)(2,1)} %param.31) | copy-start | bytes 393220
  17.5 5.2 %copy-start.12 = (bf16[512,128]{1,0:T(8,128)(2,1)S(1)}, bf16[512,128]{1,0:T(8,128)(2,1)}, u32[]{:S(2)}) copy-start(bf16[512,128]{1,0:T(8,128)(2,1)} %param.30) | copy-start | bytes 393220
  25.5 0.7 copy-start.5
  50.5 7.7 %copy-start.1 = (bf16[8,16,2304]{2,1,0:T(8,128)(2,1)}, bf16[8,16,2304]{2,1,0:T(8,128)(2,1)S(1)}, u32[]{:S(2)}) copy-start(bf16[8,16,2304]{2,1,0:T(8,128)(2,1)S(1)} %all_to_all.25.own_ref) | copy-start | bytes 1769476
  50.5 7.7 %collective-permute-start = (bf16[8,16,2304]{2,1,0:T(8,128)(2,1)S(1)}, bf16[8,16,2304]{2,1,0:T(8,128)(2,1)S(1)}, u32[]{:S(2)}, u32[]{:S(2)}) collective-permute-start(bf16[8,16,2304]{2,1,0:T(8,128)(2,1)S(1)} %all_to_all.25.own_ref), channel_id=1, source_target_pairs={{0,1},{1,0},{2,3},{3,2},{4,5},{5,4},{6,7},{7,6},{8,9},{9,8},{10,11... | collective-permute-start | bytes 1769480 | tf_op jit(solution)/shard_map/ppermute | solution.py:49
  58.2 0.8 copy-start.3
  64.6 3.7 %copy-start.6 = (bf16[128,2048]{1,0:T(8,128)(2,1)S(1)}, bf16[128,2048]{1,0:T(8,128)(2,1)}, u32[]{:S(2)}) copy-start(bf16[128,2048]{1,0:T(8,128)(2,1)} %refs_0_.1) | copy-start | bytes 1572868
  64.6 6.0 %copy-start.13 = (bf16[384,128]{1,0:T(8,128)(2,1)S(1)}, bf16[384,128]{1,0:T(8,128)(2,1)}, u32[]{:S(2)}) copy-start(bf16[384,128]{1,0:T(8,128)(2,1)} %get-tuple-element.23.q0) | copy-start | bytes 294916
  64.6 30.1 %all-to-all-start.2 = ((bf16[8,688,128]{2,1,0:T(8,128)(2,1)}), bf16[8,688,128]{2,1,0:T(8,128)(2,1)S(1)}, u32[]{:S(2)}, u32[]{:S(2)}) async-start(bf16[8,688,128]{2,1,0:T(8,128)(2,1)} %get-tuple-element.24), calls=%async_computation.2 | async-start | bytes 2818048 | tf_op jit(solution)/shard_map/all_to_all | solution.py:31
  68.3 43.3 %collective-permute-start.4 = (bf16[128,2048]{1,0:T(8,128)(2,1)S(1)}, bf16[128,2048]{1,0:T(8,128)(2,1)S(1)}, u32[]{:S(2)}, u32[]{:S(2)}) collective-permute-start(bf16[128,2048]{1,0:T(8,128)(2,1)S(1)} %copy-done.6), channel_id=1, source_target_pairs={{0,1},{1,0},{2,3},{3,2},{4,5},{5,4},{6,7},{7,6},{8,9},{9,8},{10,11... | collective-permute-start | bytes 1572872 | tf_op jit(solution)/shard_map/ppermute | solution.py:49
  70.6 19.5 %collective-permute-start.1 = (bf16[384,128]{1,0:T(8,128)(2,1)S(1)}, bf16[384,128]{1,0:T(8,128)(2,1)S(1)}, u32[]{:S(2)}, u32[]{:S(2)}) collective-permute-start(bf16[384,128]{1,0:T(8,128)(2,1)S(1)} %copy-done.13), channel_id=1, source_target_pairs={{0,128},{128,256},{256,384},{384,0},{1,129},{129,257},{257,385},{3... | collective-permute-start | bytes 294920 | tf_op jit(solution)/shard_map/ppermute | solution.py:49
  74.2 20.5 %collective-permute-start.2 = (bf16[384,128]{1,0:T(8,128)(2,1)S(1)}, bf16[384,128]{1,0:T(8,128)(2,1)S(1)}, u32[]{:S(2)}, u32[]{:S(2)}) collective-permute-start(bf16[384,128]{1,0:T(8,128)(2,1)S(1)} %copy-done.13), channel_id=1, source_target_pairs={{0,256},{128,384},{256,0},{384,128},{1,257},{129,385},{257,1},{385... | collective-permute-start | bytes 294920 | tf_op jit(solution)/shard_map/ppermute | solution.py:49
  78.6 16.1 %collective-permute-start.3 = (bf16[384,128]{1,0:T(8,128)(2,1)S(1)}, bf16[384,128]{1,0:T(8,128)(2,1)S(1)}, u32[]{:S(2)}, u32[]{:S(2)}) collective-permute-start(bf16[384,128]{1,0:T(8,128)(2,1)S(1)} %copy-done.13), channel_id=1, source_target_pairs={{0,384},{128,0},{256,128},{384,256},{1,385},{129,1},{257,129},{385... | collective-permute-start | bytes 294920 | tf_op jit(solution)/shard_map/ppermute | solution.py:49
  90.1 4.6 %copy-start.14 = (bf16[384,128]{1,0:T(8,128)(2,1)}, bf16[384,128]{1,0:T(8,128)(2,1)S(1)}, u32[]{:S(2)}) copy-start(bf16[384,128]{1,0:T(8,128)(2,1)S(1)} %collective-permute-done.1.q1) | copy-start | bytes 294916
  94.7 0.6 copy-start.15
  94.7 0.7 copy-start.16
  94.7 1.1 copy-start
  102.5 51.0 %copy-start.17 = (f32[1,2048]{1,0:T(1,128)S(1)}, f32[1,2048]{1,0:T(1,128)}, u32[]{:S(2)}) copy-start(f32[1,2048]{1,0:T(1,128)} %get-tuple-element.21) | copy-start | bytes 24580
  102.5 34.1 %all-to-all-start.3 = ((bf16[16,80,128]{2,1,0:T(8,128)(2,1)}), bf16[16,80,128]{2,1,0:T(8,128)(2,1)S(1)}, u32[]{:S(2)}, u32[]{:S(2)}) async-start(bf16[16,80,128]{2,1,0:T(8,128)(2,1)} %bitcast.26), calls=%async_computation.3 | async-start | bytes 655360 | tf_op jit(solution)/shard_map/all_to_all | solution.py:31
  108.4 17.0 %collective-permute-start.5 = (bf16[128,2048]{1,0:T(8,128)(2,1)S(1)}, bf16[128,2048]{1,0:T(8,128)(2,1)S(1)}, u32[]{:S(2)}, u32[]{:S(2)}) collective-permute-start(bf16[128,2048]{1,0:T(8,128)(2,1)S(1)} %copy-done.6), channel_id=1, source_target_pairs={{0,2},{2,0},{1,3},{3,1},{4,6},{6,4},{5,7},{7,5},{8,10},{10,8},{9,1... | collective-permute-start | bytes 1572872 | tf_op jit(solution)/shard_map/ppermute | solution.py:49
  111.7 24.9 %copy-start.7 = (bf16[128,2048]{1,0:T(8,128)(2,1)}, bf16[128,2048]{1,0:T(8,128)(2,1)S(1)}, u32[]{:S(2)}) copy-start(bf16[128,2048]{1,0:T(8,128)(2,1)S(1)} %collective-permute-done.4.refs_1_) | copy-start | bytes 1572868
  111.7 24.9 %collective-permute-start.6 = (bf16[128,2048]{1,0:T(8,128)(2,1)S(1)}, bf16[128,2048]{1,0:T(8,128)(2,1)S(1)}, u32[]{:S(2)}, u32[]{:S(2)}) collective-permute-start(bf16[128,2048]{1,0:T(8,128)(2,1)S(1)} %collective-permute-done.4.refs_1_), channel_id=1, source_target_pairs={{0,2},{2,0},{1,3},{3,1},{4,6},{6,4},{5,7},{7,5},{8,10},{10,8},{9,1... | collective-permute-start | bytes 1572872 | tf_op jit(solution)/shard_map/ppermute | solution.py:49
  125.4 11.3 %copy-start.8 = (bf16[128,2048]{1,0:T(8,128)(2,1)}, bf16[128,2048]{1,0:T(8,128)(2,1)S(1)}, u32[]{:S(2)}) copy-start(bf16[128,2048]{1,0:T(8,128)(2,1)S(1)} %collective-permute-done.5.refs_2_) | copy-start | bytes 1572868
  136.6 0.8 copy-start.9
  136.6 1.0 copy-start.2

commit v7 on v6

--- a/solution.py
+++ b/solution.py
@@ -187,8 +187,11 @@
 
 
 def merge_kernel(at_ref, got_ref, *refs):
-    hbm, o_ref, w_refs, sems = refs[:4], refs[4], refs[5:9], refs[9:]
-    loads = [pltpu.make_async_copy(src, dst, sem) for src, dst, sem in zip(hbm, w_refs, sems, strict=True)]
+    hbm, o_ref, w_ref, sems = refs[:4], refs[4], refs[5], refs[6:]
+    deep = hbm[0].shape[0]
+    loads = [
+        pltpu.make_async_copy(src, w_ref.at[pl.ds(i * deep, deep)], sem) for i, (src, sem) in enumerate(zip(hbm, sems, strict=True))
+    ]
     for load in loads:
         load.start()
     n_q, _, height, lanes = got_ref.shape
@@ -204,13 +207,13 @@
         total = functools.reduce(jnp.add, raised)
         shares += [v / total for v in raised]
     shares = jnp.transpose(jnp.concatenate(shares + [jnp.zeros((lanes - len(shares), lanes), F32)], axis=0))[:quarter]
-    term = None
+    mixed = []
     for s, source in enumerate(sources):
         pieces = [got_ref[i, source, :quarter, :].astype(F32) * shares[:, s * n_q + i : s * n_q + i + 1] for i in range(n_q)]
-        mixed = functools.reduce(jnp.add, pieces).astype(BF16)
-        loads[s].wait()
-        out = jnp.dot(mixed, w_refs[s][...], preferred_element_type=F32)
-        term = out if term is None else term + out
+        mixed.append(functools.reduce(jnp.add, pieces).astype(BF16))
+    for load in loads:
+        load.wait()
+    term = jnp.dot(jnp.concatenate(mixed, axis=1), w_ref[...], preferred_element_type=F32)
     o_ref[...] = term.astype(BF16).reshape(n_ya, rows, width)
 
 
@@ -238,16 +241,8 @@
     own = jax.nn.silu(own)
     parts = [jnp.sum(own[i][:, None] * w, axis=0) for w, i in ((shift_w, 0), (shift_w, 1), (scale_w, 0), (scale_w, 1), (gate_w, 0))]
     summed = copies(jnp.stack(parts), SP)
-    w_other = shifted(w_out, "c", 1)
-    w_side = jnp.concatenate([w_qn, w_qr, w_rope_key], axis=1)
-    w_up = jnp.concatenate([w_key_up, w_value_up], axis=1)
-    place = jnp.arange(tok, dtype=jnp.int32)
-    place = (place // rows % n_ya * 2 + place // (tok // 2)) * (n_c * rows) + place // quarter % n_c * rows + place % rows
-    cosine, sine = turn_table(sp_index * tok + place, rope, lanes)
-    at = jnp.stack([lax.axis_index("c"), lax.axis_index("yb")]).astype(jnp.int32).reshape(1, 2)
-    to = lax.axis_index(Q_AXIS).astype(jnp.int32).reshape(1, 1)
+    w_near = shifted(w_out, "yb", 1)
     block = jnp.concatenate([latent, context.reshape(rows, lanes)], axis=1)
-    block, w_side, w_up, cosine, sine, at, to = lax.optimization_barrier((block, w_side, w_up, cosine, sine, at, to))
     smem = pl.BlockSpec(memory_space=pltpu.SMEM)
     vmem = pl.BlockSpec(memory_space=pltpu.VMEM)
     any_space = pl.BlockSpec(memory_space=pl.ANY)
@@ -261,9 +256,18 @@
     message = pack(summed, block)
 
     mine = exchanged(message, Y)
+    w_other = shifted(w_out, "c", 1)
+    w_far = shifted(w_near, "c", 1)
+    w_side = jnp.concatenate([w_qn, w_qr, w_rope_key], axis=1)
+    w_up = jnp.concatenate([w_key_up, w_value_up], axis=1)
+    place = jnp.arange(tok, dtype=jnp.int32)
+    place = (place // rows % n_ya * 2 + place // (tok // 2)) * (n_c * rows) + place // quarter % n_c * rows + place % rows
+    cosine, sine = turn_table(sp_index * tok + place, rope, lanes)
+    at = jnp.stack([lax.axis_index("c"), lax.axis_index("yb")]).astype(jnp.int32).reshape(1, 2)
+    to = lax.axis_index(Q_AXIS).astype(jnp.int32).reshape(1, 1)
     other = shifted(mine, "c", 1)
 
-    q_own, kv_copies, gate = pl.pallas_call(
+    project = pl.pallas_call(
         project_kernel,
         in_specs=[smem] + [vmem] * 6 + [any_space] * 3,
         out_specs=[vmem, vmem, vmem],
@@ -283,11 +287,13 @@
             pltpu.SemaphoreType.DMA,
         ],
         name="project",
-    )(at, mine, other, norm_gain.reshape(1, width), kv_gain.reshape(1, -1), cosine, sine, w_side, w_kv_down, w_up)
+    )
+    q_own, kv_copies, gate = project(
+        at, mine, other, norm_gain.reshape(1, width), kv_gain.reshape(1, -1), cosine, sine, w_side, w_kv_down, w_up
+    )
 
     queries = [q_own] + [shifted(q_own, Q_AXIS, k) for k in range(1, n_q)]
     kv = exchanged(kv_copies, KV_AXES)
-    w_near = [shifted(w, "yb", 1) for w in (w_out, w_other)]
     n_kv = kv.shape[0]
     attend = pl.pallas_call(
         functools.partial(attend_kernel, factor=factor, tok=tok, n_ctx=n_tp),
@@ -309,9 +315,9 @@
         in_specs=[smem, vmem] + [any_space] * 4,
         out_specs=vmem,
         out_shape=jax.ShapeDtypeStruct((n_ya, rows, width), BF16),
-        scratch_shapes=[pltpu.VMEM(w_out.shape, BF16)] * 4 + [pltpu.SemaphoreType.DMA] * 4,
+        scratch_shapes=[pltpu.VMEM((4 * w_out.shape[0], width), BF16)] + [pltpu.SemaphoreType.DMA] * 4,
         name="merge",
-    )(at, got.reshape(n_q, 2 * n_c, quarter + 16, vsize), w_out, w_other, *w_near)
+    )(at, got.reshape(n_q, 2 * n_c, quarter + 16, vsize), w_out, w_other, w_near, w_far)
     branch = jnp.sum(exchanged(term, ("ya",)).astype(F32), axis=0)
     return (latent.astype(F32) + gate * branch).astype(BF16)
 

time: 156 us -> 143 us (0.917)
  blocking collectives: 35 us -> 14.9 us
  waiting for transfers between devices: 36.9 us -> 41.5 us
  starting transfers between devices: 49.9 us -> 53.5 us
  local copies, waits for them, and re-layouts: 7.61 us -> 5.45 us
    ppermute x7, waiting for transfers between devices: 34.8 us -> 12.1 us  [shifted(): return lax.ppermute(array, axis, [(i, (i + k) % n) for i in range(n)])]
    all_to_all x2 -> x3, waiting for transfers between devices: 0.01 us -> 22.3 us  [exchanged(): return lax.all_to_all(array, axes, 0, 0, tiled=True)]
    all_to_all x2 -> x1, blocking collectives: 35 us -> 14.9 us  [exchanged(): return lax.all_to_all(array, axes, 0, 0, tiled=True)]
    all_to_all x2 -> x3, starting transfers between devices: 9.6 us -> 18.1 us  [exchanged(): return lax.all_to_all(array, axes, 0, 0, tiled=True)]
    all_to_all x1, waiting for transfers between devices: 2.07 us -> 7.14 us  [copies(): lax.all_to_all(jnp.broadcast_to(array[None], (n, *array.shape)), axes, 0,...]
    ppermute x7, starting transfers between devices: 26.6 us -> 21.7 us  [shifted(): return lax.ppermute(array, axis, [(i, (i + k) % n) for i in range(n)])]
    unnamed x40 -> x42, local copies, waits for them, and re-layouts: 6.07 us -> 3.93 us
  transfers between devices with their start and end apart: 10 -> 11, of which waited for: 6 -> 6; matrix products, arithmetic and copies ran while one was open for 5% -> 5% of each run, Pallas kernels for 4% -> 5%
where the time goes in v7:
time: 143 us; the launch traced here: 142 us
  starting transfers between devices  53.5 us (37%)
  waiting for transfers between devices  41.5 us (29%)
  Pallas kernels  17.8 us (12%)
  blocking collectives  14.9 us (10%)
  other arithmetic  7.81 us (5%)
  local copies, waits for them, and re-layouts  5.45 us (4%)
    all_to_all x3, waiting for transfers between devices, exchanged(): return lax.all_to_all(array, axes, 0, 0, tiled=True)  22.3 us
    ppermute x7, starting transfers between devices, shifted(): return lax.ppermute(array, axis, [(i, (i + k) % n) for i in range(n)])  21.7 us
    all_to_all x3, starting transfers between devices, exchanged(): return lax.all_to_all(array, axes, 0, 0, tiled=True)  18.1 us
    all_to_all x1, blocking collectives, exchanged(): return lax.all_to_all(array, axes, 0, 0, tiled=True)  14.9 us
    all_to_all x1, starting transfers between devices, copies(): lax.all_to_all(jnp.broadcast_to(array[None], (n, *array.shape)), axes, 0,...  13.7 us
    ppermute x7, waiting for transfers between devices, shifted(): return lax.ppermute(array, axis, [(i, (i + k) % n) for i in range(n)])  12.1 us
    all_to_all x1, waiting for transfers between devices, copies(): lax.all_to_all(jnp.broadcast_to(array[None], (n, *array.shape)), axes, 0,...  7.14 us
    pallas_call x1, Pallas kernels, step(): out = attend(to, ctx_bias.reshape(1, 1), *queries, kv)  6.69 us
  transfers between devices with their start and end apart: 11, of which 6 were waited for; matrix products, arithmetic and copies ran while one was open for 5% of the time, Pallas kernels for 5%

profile of v7, /device:TPU:1, one launch (start us, length us, event | category | flops | bytes accessed | tf_op | source)
XLA Modules:
  0.0 141.9 jit_solution(13540329278909616748)
XLA Ops:
  0.0 0.8 dynamic-slice_bitcast_fusion
  0.9 0.0 copy-start.13
  0.9 0.0 copy-start.14
  0.9 0.9 multiply_reduce_fusion.3
  1.9 0.7 broadcast_in_dim.16
  2.5 13.7 %all-to-all-start = ((f32[32,5,128]{2,1,0:T(8,128)}), f32[32,5,128]{2,1,0:T(8,128)S(1)}, u32[]{:S(2)}, u32[]{:S(2)}) async-start(f32[32,5,128]{2,1,0:T(8,128)} %broadcast_in_dim.16), calls=%async_computation | async-start | bytes 262144 | tf_op jit(solution)/shard_map/all_to_all | solution.py:27
  16.2 0.7 reduce
  16.9 1.5 %pad_maximum_fusion.2.block_ref = bf16[16,2176]{1,0:T(8,128)(2,1)} fusion(bf16[16,128]{1,0:T(8,128)(2,1)S(1)} %bitcast.28, bf16[16,2048]{1,0:T(8,128)(2,1)} %param.17), kind=kLoop, calls=%fused_computation.7 | loop fusion | flops 139264 | bytes 139264 | tf_op jit(solution)/shard_map/concatenate | solution.py:245
  18.4 7.1 %all-to-all-done.sums_ref = f32[32,5,128]{2,1,0:T(8,128)S(1)} async-done(((f32[32,5,128]{2,1,0:T(8,128)}), f32[32,5,128]{2,1,0:T(8,128)S(1)}, u32[]{:S(2)}, u32[]{:S(2)}) %all-to-all-start) | async-done | bytes 81952 | tf_op jit(solution)/shard_map/all_to_all | solution.py:27
  25.6 0.7 copy-done.5
  26.2 1.8 %pack.1 = bf16[8,16,2304]{2,1,0:T(8,128)(2,1)} custom-call(f32[32,5,128]{2,1,0:T(8,128)} %copy-done.5, bf16[16,2176]{1,0:T(8,128)(2,1)} %pad_maximum_fusion.2.block_ref), custom_call_target="tpu_custom_call" | custom-call | tf_op jit(solution)/shard_map/pack/pallas_call | solution.py:256
  28.0 6.8 %all-to-all-start.1 = ((bf16[8,16,2304]{2,1,0:T(8,128)(2,1)}), bf16[8,16,2304]{2,1,0:T(8,128)(2,1)S(1)}, u32[]{:S(2)}, u32[]{:S(2)}) async-start(bf16[8,16,2304]{2,1,0:T(8,128)(2,1)} %pack.1), calls=%async_computation.1 | async-start | bytes 1179648 | tf_op jit(solution)/shard_map/all_to_all | solution.py:31
  34.9 0.0 copy-done.10
  34.9 0.3 copy.18
  35.1 0.0 copy-done.11
  35.2 0.3 copy.19
  35.5 0.0 copy-done.13
  35.5 0.0 copy-done.14
  35.5 0.7 pad_maximum_fusion.1.w_up_hbm
  36.3 15.6 %all-to-all-done.1.own_ref = bf16[8,16,2304]{2,1,0:T(8,128)(2,1)S(1)} async-done(((bf16[8,16,2304]{2,1,0:T(8,128)(2,1)}), bf16[8,16,2304]{2,1,0:T(8,128)(2,1)S(1)}, u32[]{:S(2)}, u32[]{:S(2)}) %all-to-all-start.1) | async-done | bytes 589856 | tf_op jit(solution)/shard_map/all_to_all | solution.py:31
  51.8 4.8 %collective-permute-start = (bf16[8,16,2304]{2,1,0:T(8,128)(2,1)S(1)}, bf16[8,16,2304]{2,1,0:T(8,128)(2,1)S(1)}, u32[]{:S(2)}, u32[]{:S(2)}) collective-permute-start(bf16[8,16,2304]{2,1,0:T(8,128)(2,1)S(1)} %all-to-all-done.1.own_ref), channel_id=1, source_target_pairs={{0,1},{1,0},{2,3},{3,2},{4,5},{5,4},{6,7},{7,6},{8,9},{9,8},{10,11... | collective-permute-start | bytes 1769480 | tf_op jit(solution)/shard_map/ppermute | solution.py:49
  56.6 0.6 add_bitcast_fusion.at_ref
  57.2 1.3 sine_multiply_fusion
  58.5 0.0 copy-done.4
  58.5 1.3 pad_maximum_fusion.w_side_hbm
  59.8 0.0 collective-permute-done.other_ref
  59.8 0.0 copy-done.1
  59.8 0.8 copy-done.3
  60.6 5.6 %project.1 = (bf16[384,128]{1,0:T(8,128)(2,1)}, bf16[8,688,128]{2,1,0:T(8,128)(2,1)}, f32[1,2048]{1,0:T(1,128)}) custom-call(s32[1,2]{1,0:T(1,128)} %add_bitcast_fusion.at_ref, bf16[8,16,2304]{2,1,0:T(8,128)(2,1)} %copy-done.1, bf16[8,16,2304]{2,1,0:T(8,128)(2,1)} %copy-done.3, f32[1,2048]{1,0:T(1,128)} %bitcast.29, f32[1,512]{1,0:T(1,128)} %bitcast.31, ...), custom_call_target="tpu_custom_call" | custom-call | tf_op jit(solution)/shard_map/project/pallas_call | solution.py:291
  66.2 0.0 copy-start.6
  66.2 0.0 copy-start.15
  66.2 3.7 %all-to-all-start.2 = ((bf16[8,688,128]{2,1,0:T(8,128)(2,1)}), bf16[8,688,128]{2,1,0:T(8,128)(2,1)S(1)}, u32[]{:S(2)}, u32[]{:S(2)}) async-start(bf16[8,688,128]{2,1,0:T(8,128)(2,1)} %get-tuple-element.10), calls=%async_computation.2 | async-start | bytes 2818048 | tf_op jit(solution)/shard_map/all_to_all | solution.py:31
  69.9 0.0 copy-done.6
  69.9 2.2 %collective-permute-start.5 = (bf16[128,2048]{1,0:T(8,128)(2,1)S(1)}, bf16[128,2048]{1,0:T(8,128)(2,1)S(1)}, u32[]{:S(2)}, u32[]{:S(2)}) collective-permute-start(bf16[128,2048]{1,0:T(8,128)(2,1)S(1)} %copy-done.6), channel_id=1, source_target_pairs={{0,2},{2,0},{1,3},{3,1},{4,6},{6,4},{5,7},{7,5},{8,10},{10,8},{9,1... | collective-permute-start | bytes 1572872 | tf_op jit(solution)/shard_map/ppermute | solution.py:49
  72.1 0.0 copy-done.15
  72.1 2.9 %collective-permute-start.1 = (bf16[384,128]{1,0:T(8,128)(2,1)S(1)}, bf16[384,128]{1,0:T(8,128)(2,1)S(1)}, u32[]{:S(2)}, u32[]{:S(2)}) collective-permute-start(bf16[384,128]{1,0:T(8,128)(2,1)S(1)} %copy-done.15), channel_id=1, source_target_pairs={{0,128},{128,256},{256,384},{384,0},{1,129},{129,257},{257,385},{3... | collective-permute-start | bytes 294920 | tf_op jit(solution)/shard_map/ppermute | solution.py:49
  75.1 3.5 %collective-permute-start.2 = (bf16[384,128]{1,0:T(8,128)(2,1)S(1)}, bf16[384,128]{1,0:T(8,128)(2,1)S(1)}, u32[]{:S(2)}, u32[]{:S(2)}) collective-permute-start(bf16[384,128]{1,0:T(8,128)(2,1)S(1)} %copy-done.15), channel_id=1, source_target_pairs={{0,256},{128,384},{256,0},{384,128},{1,257},{129,385},{257,1},{385... | collective-permute-start | bytes 294920 | tf_op jit(solution)/shard_map/ppermute | solution.py:49
  78.6 4.0 %collective-permute-start.3 = (bf16[384,128]{1,0:T(8,128)(2,1)S(1)}, bf16[384,128]{1,0:T(8,128)(2,1)S(1)}, u32[]{:S(2)}, u32[]{:S(2)}) collective-permute-start(bf16[384,128]{1,0:T(8,128)(2,1)S(1)} %copy-done.15), channel_id=1, source_target_pairs={{0,384},{128,0},{256,128},{384,256},{1,385},{129,1},{257,129},{385... | collective-permute-start | bytes 294920 | tf_op jit(solution)/shard_map/ppermute | solution.py:49
  83.2 7.8 %collective-permute-done.1.q1 = bf16[384,128]{1,0:T(8,128)(2,1)S(1)} collective-permute-done((bf16[384,128]{1,0:T(8,128)(2,1)S(1)}, bf16[384,128]{1,0:T(8,128)(2,1)S(1)}, u32[]{:S(2)}, u32[]{:S(2)}) %collective-permute-start.1) | collective-permute-done | bytes 98336 | tf_op jit(solution)/shard_map/ppermute | solution.py:49
  91.1 2.7 %collective-permute-done.2.q2 = bf16[384,128]{1,0:T(8,128)(2,1)S(1)} collective-permute-done((bf16[384,128]{1,0:T(8,128)(2,1)S(1)}, bf16[384,128]{1,0:T(8,128)(2,1)S(1)}, u32[]{:S(2)}, u32[]{:S(2)}) %collective-permute-start.2) | collective-permute-done | bytes 98336 | tf_op jit(solution)/shard_map/ppermute | solution.py:49
  93.8 0.0 collective-permute-done.3.q3
  93.8 0.0 all-to-all-done.2.kv_ref
  93.8 0.0 copy-start
  93.8 0.0 copy-done.16
  93.8 0.6 copy-done.17
  94.4 0.0 copy-done.18
  94.5 0.5 copy-done
  95.0 6.7 %attend.1 = bf16[4,4,80,128]{3,2,1,0:T(8,128)(2,1)} custom-call(s32[1,1]{1,0:T(1,128)} %bitcast.15.place_ref, f32[1,1]{1,0:T(1,128)} %bitcast.25.bias_ref, bf16[384,128]{1,0:T(8,128)(2,1)} %get-tuple-element.9.q0, bf16[384,128]{1,0:T(8,128)(2,1)} %copy-done.16, bf16[384,128]{1,0:T(8,128)(2,1)} %copy-done.17, bf16[384,128]{1,0:T(8,128)(2,1)} %copy-done.18, ...), custom_call_target="tpu_custom_call" | custom-call | tf_op jit(solution)/shard_map/attend/pallas_call | solution.py:310
  101.7 7.6 %all-to-all-start.3 = ((bf16[16,80,128]{2,1,0:T(8,128)(2,1)}), bf16[16,80,128]{2,1,0:T(8,128)(2,1)S(1)}, u32[]{:S(2)}, u32[]{:S(2)}) async-start(bf16[16,80,128]{2,1,0:T(8,128)(2,1)} %bitcast.26), calls=%async_computation.3 | async-start | bytes 655360 | tf_op jit(solution)/shard_map/all_to_all | solution.py:31
  109.2 2.0 %collective-permute-start.4 = (bf16[128,2048]{1,0:T(8,128)(2,1)S(1)}, bf16[128,2048]{1,0:T(8,128)(2,1)S(1)}, u32[]{:S(2)}, u32[]{:S(2)}) collective-permute-start(bf16[128,2048]{1,0:T(8,128)(2,1)S(1)} %copy-done.6), channel_id=1, source_target_pairs={{0,1},{1,0},{2,3},{3,2},{4,5},{5,4},{6,7},{7,6},{8,9},{9,8},{10,11... | collective-permute-start | bytes 1572872 | tf_op jit(solution)/shard_map/ppermute | solution.py:49
  111.3 0.0 collective-permute-done.5.refs_2_
  111.3 0.0 copy-start.7
  111.3 2.3 %collective-permute-start.6 = (bf16[128,2048]{1,0:T(8,128)(2,1)S(1)}, bf16[128,2048]{1,0:T(8,128)(2,1)S(1)}, u32[]{:S(2)}, u32[]{:S(2)}) collective-permute-start(bf16[128,2048]{1,0:T(8,128)(2,1)S(1)} %collective-permute-done.5.refs_2_), channel_id=1, source_target_pairs={{0,1},{1,0},{2,3},{3,2},{4,5},{5,4},{6,7},{7,6},{8,9},{9,8},{10,11... | collective-permute-start | bytes 1572872 | tf_op jit(solution)/shard_map/ppermute | solution.py:49
  113.6 0.0 collective-permute-done.4.refs_1_
  113.6 0.0 copy-start.8
  113.6 1.5 %collective-permute-done.6.refs_3_ = bf16[128,2048]{1,0:T(8,128)(2,1)S(1)} collective-permute-done((bf16[128,2048]{1,0:T(8,128)(2,1)S(1)}, bf16[128,2048]{1,0:T(8,128)(2,1)S(1)}, u32[]{:S(2)}, u32[]{:S(2)}) %collective-permute-start.6) | collective-permute-done | bytes 524320 | tf_op jit(solution)/shard_map/ppermute | solution.py:49
  115.1 6.7 %all-to-all-done.3 = bf16[16,80,128]{2,1,0:T(8,128)(2,1)S(1)} async-done(((bf16[16,80,128]{2,1,0:T(8,128)(2,1)}), bf16[16,80,128]{2,1,0:T(8,128)(2,1)S(1)}, u32[]{:S(2)}, u32[]{:S(2)}) %all-to-all-start.3) | async-done | bytes 327712 | tf_op jit(solution)/shard_map/all_to_all | solution.py:31
  121.9 0.0 copy-done.7
  121.9 0.0 copy-done.8
  121.9 0.0 copy-done.9
  121.9 0.7 copy-done.2
  122.6 3.7 %merge.1 = bf16[4,16,2048]{2,1,0:T(8,128)(2,1)} custom-call(s32[1,2]{1,0:T(1,128)} %add_bitcast_fusion.at_ref, bf16[4,4,80,128]{3,2,1,0:T(8,128)(2,1)} %bitcast.27, bf16[128,2048]{1,0:T(8,128)(2,1)} %refs_0_.1, bf16[128,2048]{1,0:T(8,128)(2,1)} %copy-done.8, bf16[128,2048]{1,0:T(8,128)(2,1)} %copy-done.7, bf16[128,2048]{1,0:T(8,128)(2,1)} %copy-done.9), custom_call_target="tpu_custom_call" | custom-call | tf_op jit(solution)/shard_map/merge/pallas_call | solution.py:313
  126.3 14.9 %all_to_all.25 = bf16[4,16,2048]{2,1,0:T(8,128)(2,1)S(1)} all-to-all(bf16[4,16,2048]{2,1,0:T(8,128)(2,1)} %merge.1), channel_id=1, replica_groups=mesh['za'=4,'zb'=2,'x'=4,'ya'=4,'yb'=2,'c'=2] {'ya'}, dimensions={0} | all-to-all | bytes 524288 | tf_op jit(solution)/shard_map/all_to_all | solution.py:31
  141.3 0.7 add_convert_fusion
  (22 shorter events, 0.2 us)
Async XLA Ops:
  0.0 34.9 %copy-start.10 = (bf16[2048,64]{0,1:T(8,128)(2,1)S(1)}, bf16[2048,64]{0,1:T(8,128)(2,1)}, u32[]{:S(2)}) copy-start(bf16[2048,64]{0,1:T(8,128)(2,1)} %param.26) | copy-start | bytes 786436
  0.0 35.1 %copy-start.11 = (bf16[2048,64]{0,1:T(8,128)(2,1)S(1)}, bf16[2048,64]{0,1:T(8,128)(2,1)}, u32[]{:S(2)}) copy-start(bf16[2048,64]{0,1:T(8,128)(2,1)} %param.28) | copy-start | bytes 786436
  0.9 34.6 %copy-start.13 = (bf16[512,128]{1,0:T(8,128)(2,1)S(1)}, bf16[512,128]{1,0:T(8,128)(2,1)}, u32[]{:S(2)}) copy-start(bf16[512,128]{1,0:T(8,128)(2,1)} %param.31) | copy-start | bytes 393220
  0.9 34.6 %copy-start.14 = (bf16[512,128]{1,0:T(8,128)(2,1)S(1)}, bf16[512,128]{1,0:T(8,128)(2,1)}, u32[]{:S(2)}) copy-start(bf16[512,128]{1,0:T(8,128)(2,1)} %param.30) | copy-start | bytes 393220
  2.5 23.1 %all-to-all-start = ((f32[32,5,128]{2,1,0:T(8,128)}), f32[32,5,128]{2,1,0:T(8,128)S(1)}, u32[]{:S(2)}, u32[]{:S(2)}) async-start(f32[32,5,128]{2,1,0:T(8,128)} %broadcast_in_dim.16), calls=%async_computation | async-start | bytes 262144 | tf_op jit(solution)/shard_map/all_to_all | solution.py:27
  18.4 40.1 %copy-start.4 = (bf16[2048,128]{1,0:T(8,128)(2,1)S(1)}, bf16[2048,128]{1,0:T(8,128)(2,1)}, u32[]{:S(2)}) copy-start(bf16[2048,128]{1,0:T(8,128)(2,1)} %param.25) | copy-start | bytes 1572868
  25.6 0.7 copy-start.5
  28.0 23.8 %all-to-all-start.1 = ((bf16[8,16,2304]{2,1,0:T(8,128)(2,1)}), bf16[8,16,2304]{2,1,0:T(8,128)(2,1)S(1)}, u32[]{:S(2)}, u32[]{:S(2)}) async-start(bf16[8,16,2304]{2,1,0:T(8,128)(2,1)} %pack.1), calls=%async_computation.1 | async-start | bytes 1179648 | tf_op jit(solution)/shard_map/all_to_all | solution.py:31
  51.8 8.0 %copy-start.1 = (bf16[8,16,2304]{2,1,0:T(8,128)(2,1)}, bf16[8,16,2304]{2,1,0:T(8,128)(2,1)S(1)}, u32[]{:S(2)}) copy-start(bf16[8,16,2304]{2,1,0:T(8,128)(2,1)S(1)} %all-to-all-done.1.own_ref) | copy-start | bytes 1769476
  51.8 8.0 %collective-permute-start = (bf16[8,16,2304]{2,1,0:T(8,128)(2,1)S(1)}, bf16[8,16,2304]{2,1,0:T(8,128)(2,1)S(1)}, u32[]{:S(2)}, u32[]{:S(2)}) collective-permute-start(bf16[8,16,2304]{2,1,0:T(8,128)(2,1)S(1)} %all-to-all-done.1.own_ref), channel_id=1, source_target_pairs={{0,1},{1,0},{2,3},{3,2},{4,5},{5,4},{6,7},{7,6},{8,9},{9,8},{10,11... | collective-permute-start | bytes 1769480 | tf_op jit(solution)/shard_map/ppermute | solution.py:49
  59.8 0.8 copy-start.3
  66.2 3.7 %copy-start.6 = (bf16[128,2048]{1,0:T(8,128)(2,1)S(1)}, bf16[128,2048]{1,0:T(8,128)(2,1)}, u32[]{:S(2)}) copy-start(bf16[128,2048]{1,0:T(8,128)(2,1)} %refs_0_.1) | copy-start | bytes 1572868
  66.2 5.9 %copy-start.15 = (bf16[384,128]{1,0:T(8,128)(2,1)S(1)}, bf16[384,128]{1,0:T(8,128)(2,1)}, u32[]{:S(2)}) copy-start(bf16[384,128]{1,0:T(8,128)(2,1)} %get-tuple-element.9.q0) | copy-start | bytes 294916
  66.2 27.6 %all-to-all-start.2 = ((bf16[8,688,128]{2,1,0:T(8,128)(2,1)}), bf16[8,688,128]{2,1,0:T(8,128)(2,1)S(1)}, u32[]{:S(2)}, u32[]{:S(2)}) async-start(bf16[8,688,128]{2,1,0:T(8,128)(2,1)} %get-tuple-element.10), calls=%async_computation.2 | async-start | bytes 2818048 | tf_op jit(solution)/shard_map/all_to_all | solution.py:31
  69.9 41.3 %collective-permute-start.5 = (bf16[128,2048]{1,0:T(8,128)(2,1)S(1)}, bf16[128,2048]{1,0:T(8,128)(2,1)S(1)}, u32[]{:S(2)}, u32[]{:S(2)}) collective-permute-start(bf16[128,2048]{1,0:T(8,128)(2,1)S(1)} %copy-done.6), channel_id=1, source_target_pairs={{0,2},{2,0},{1,3},{3,1},{4,6},{6,4},{5,7},{7,5},{8,10},{10,8},{9,1... | collective-permute-start | bytes 1572872 | tf_op jit(solution)/shard_map/ppermute | solution.py:49
  72.1 18.9 %collective-permute-start.1 = (bf16[384,128]{1,0:T(8,128)(2,1)S(1)}, bf16[384,128]{1,0:T(8,128)(2,1)S(1)}, u32[]{:S(2)}, u32[]{:S(2)}) collective-permute-start(bf16[384,128]{1,0:T(8,128)(2,1)S(1)} %copy-done.15), channel_id=1, source_target_pairs={{0,128},{128,256},{256,384},{384,0},{1,129},{129,257},{257,385},{3... | collective-permute-start | bytes 294920 | tf_op jit(solution)/shard_map/ppermute | solution.py:49
  75.1 18.7 %collective-permute-start.2 = (bf16[384,128]{1,0:T(8,128)(2,1)S(1)}, bf16[384,128]{1,0:T(8,128)(2,1)S(1)}, u32[]{:S(2)}, u32[]{:S(2)}) collective-permute-start(bf16[384,128]{1,0:T(8,128)(2,1)S(1)} %copy-done.15), channel_id=1, source_target_pairs={{0,256},{128,384},{256,0},{384,128},{1,257},{129,385},{257,1},{385... | collective-permute-start | bytes 294920 | tf_op jit(solution)/shard_map/ppermute | solution.py:49
  78.6 15.2 %collective-permute-start.3 = (bf16[384,128]{1,0:T(8,128)(2,1)S(1)}, bf16[384,128]{1,0:T(8,128)(2,1)S(1)}, u32[]{:S(2)}, u32[]{:S(2)}) collective-permute-start(bf16[384,128]{1,0:T(8,128)(2,1)S(1)} %copy-done.15), channel_id=1, source_target_pairs={{0,384},{128,0},{256,128},{384,256},{1,385},{129,1},{257,129},{385... | collective-permute-start | bytes 294920 | tf_op jit(solution)/shard_map/ppermute | solution.py:49
  91.1 2.7 %copy-start.16 = (bf16[384,128]{1,0:T(8,128)(2,1)}, bf16[384,128]{1,0:T(8,128)(2,1)S(1)}, u32[]{:S(2)}) copy-start(bf16[384,128]{1,0:T(8,128)(2,1)S(1)} %collective-permute-done.1.q1) | copy-start | bytes 294916
  93.8 0.6 copy-start.17
  93.8 0.7 copy-start.18
  93.8 1.2 copy-start
  101.7 39.6 %copy-start.12 = (bf16[16,2048]{1,0:T(8,128)(2,1)S(1)}, bf16[16,2048]{1,0:T(8,128)(2,1)}, u32[]{:S(2)}) copy-start(bf16[16,2048]{1,0:T(8,128)(2,1)} %param.17) | copy-start | bytes 196612
  101.7 39.6 %copy-start.19 = (f32[1,2048]{1,0:T(1,128)S(1)}, f32[1,2048]{1,0:T(1,128)}, u32[]{:S(2)}) copy-start(f32[1,2048]{1,0:T(1,128)} %get-tuple-element.8) | copy-start | bytes 24580
  101.7 20.2 %all-to-all-start.3 = ((bf16[16,80,128]{2,1,0:T(8,128)(2,1)}), bf16[16,80,128]{2,1,0:T(8,128)(2,1)S(1)}, u32[]{:S(2)}, u32[]{:S(2)}) async-start(bf16[16,80,128]{2,1,0:T(8,128)(2,1)} %bitcast.26), calls=%async_computation.3 | async-start | bytes 655360 | tf_op jit(solution)/shard_map/all_to_all | solution.py:31
  109.2 4.4 %collective-permute-start.4 = (bf16[128,2048]{1,0:T(8,128)(2,1)S(1)}, bf16[128,2048]{1,0:T(8,128)(2,1)S(1)}, u32[]{:S(2)}, u32[]{:S(2)}) collective-permute-start(bf16[128,2048]{1,0:T(8,128)(2,1)S(1)} %copy-done.6), channel_id=1, source_target_pairs={{0,1},{1,0},{2,3},{3,2},{4,5},{5,4},{6,7},{7,6},{8,9},{9,8},{10,11... | collective-permute-start | bytes 1572872 | tf_op jit(solution)/shard_map/ppermute | solution.py:49
  111.3 10.6 %copy-start.7 = (bf16[128,2048]{1,0:T(8,128)(2,1)}, bf16[128,2048]{1,0:T(8,128)(2,1)S(1)}, u32[]{:S(2)}) copy-start(bf16[128,2048]{1,0:T(8,128)(2,1)S(1)} %collective-permute-done.5.refs_2_) | copy-start | bytes 1572868
  111.3 3.8 %collective-permute-start.6 = (bf16[128,2048]{1,0:T(8,128)(2,1)S(1)}, bf16[128,2048]{1,0:T(8,128)(2,1)S(1)}, u32[]{:S(2)}, u32[]{:S(2)}) collective-permute-start(bf16[128,2048]{1,0:T(8,128)(2,1)S(1)} %collective-permute-done.5.refs_2_), channel_id=1, source_target_pairs={{0,1},{1,0},{2,3},{3,2},{4,5},{5,4},{6,7},{7,6},{8,9},{9,8},{10,11... | collective-permute-start | bytes 1572872 | tf_op jit(solution)/shard_map/ppermute | solution.py:49
  113.6 8.3 %copy-start.8 = (bf16[128,2048]{1,0:T(8,128)(2,1)}, bf16[128,2048]{1,0:T(8,128)(2,1)S(1)}, u32[]{:S(2)}) copy-start(bf16[128,2048]{1,0:T(8,128)(2,1)S(1)} %collective-permute-done.4.refs_1_) | copy-start | bytes 1572868
  115.1 6.8 %copy-start.9 = (bf16[128,2048]{1,0:T(8,128)(2,1)}, bf16[128,2048]{1,0:T(8,128)(2,1)S(1)}, u32[]{:S(2)}) copy-start(bf16[128,2048]{1,0:T(8,128)(2,1)S(1)} %collective-permute-done.6.refs_3_) | copy-start | bytes 1572868
  121.9 0.7 copy-start.2

commit v8 on v7

--- a/solution.py
+++ b/solution.py
@@ -49,24 +49,9 @@
     return lax.ppermute(array, axis, [(i, (i + k) % n) for i in range(n)])
 
 
-def pack_kernel(sums_ref, block_ref, o_ref):
-    n_sp = sums_ref.shape[0]
-    rows, width = block_ref.shape
-    total = functools.reduce(jnp.add, [sums_ref[i] for i in range(n_sp)])
-    high = total.astype(BF16).astype(F32)
-    middle = (total - high).astype(BF16).astype(F32)
-    low = total - high - middle
-    spare = jnp.zeros((rows - 3 * total.shape[0], total.shape[1]), F32)
-    parts = jnp.concatenate([high, middle, low, spare], axis=0).astype(BF16)
-    block = block_ref[...]
-    for i in range(o_ref.shape[0]):
-        o_ref[i, :, :width] = block
-        o_ref[i, :, width:] = parts
-
-
 def project_kernel(
-    at_ref, own_ref, other_ref, gain_ref, kv_gain_ref, cos_ref, sin_ref, w_side_hbm, w_down_hbm, w_up_hbm,
-    q_ref, kv_ref, gate_ref, ctx_ref, h_ref, w_side_ref, w_down_ref, w_up_ref, side_sem, down_sem, up_sem,
+    at_ref, own_ref, other_ref, vec_ref, gain_ref, kv_gain_ref, cos_ref, sin_ref, w_side_hbm, w_down_hbm, w_up_hbm,
+    q_ref, kv_ref, ctx_ref, h_ref, w_side_ref, w_down_ref, w_up_ref, side_sem, down_sem, up_sem,
 ):
     loads = [
         pltpu.make_async_copy(w_side_hbm, w_side_ref, side_sem), pltpu.make_async_copy(w_down_hbm, w_down_ref, down_sem),
@@ -82,31 +67,21 @@
     lanes = width // rows
     n_ctx = 2 * n_y
     core = at_ref[0, 0]
-    columns = []
-    for y in range(n_y):
-        pair = []
-        for ref in (own_ref, other_ref):
-            part = ref[y, :, width + lanes :].astype(F32)
-            pair.append(part[0:5] + part[5:10] + part[10:15])
-        columns += [jnp.where(core == 0, pair[0], pair[1]), jnp.where(core == 0, pair[1], pair[0])]
-    columns = jnp.concatenate(columns, axis=1)
+    columns = jnp.concatenate([vec_ref[t] for t in range(vec_ref.shape[0])], axis=1)
     shift, shift_ctx, scale, scale_ctx = (columns[j : j + 1] for j in range(4))
-    gate_ref[...] = columns[4:5]
     gain = gain_ref[...]
 
     def modulated(values, shift, scale):
         normed = values * lax.rsqrt(jnp.mean(values * values, axis=1, keepdims=True) + EPS)
         return (normed * (gain * (1.0 + scale)) + shift).astype(BF16)
 
-    quarter = side_rows // 2
     for side, ref in enumerate((own_ref, other_ref)):
-        ctx_ref[side * side_rows : (side + 1) * side_rows, :] = (
-            ref[:, :, width : width + lanes].reshape(side_rows, lanes).astype(F32)
-        )
-        for yb in range(2):
-            at = pl.multiple_of((yb * 2 + (core + side) % 2) * quarter, quarter)
-            some = jnp.concatenate([ref[y, :, :width] for y in range(yb, n_y, 2)], axis=0)
-            h_ref[pl.ds(at, quarter), :] = modulated(some.astype(F32), shift, scale)
+        ctx_ref[side * side_rows : (side + 1) * side_rows, :] = ref[:, :, width:].reshape(side_rows, lanes).astype(F32)
+        some = modulated(ref[:, :, :width].reshape(side_rows, width).astype(F32), shift, scale)
+        for k in range(n_y):
+            y = (at_ref[0, 2] + k) % n_y
+            block = (y % 2 * 2 + (core + side) % 2) * (n_y // 2) + y // 2
+            h_ref[pl.ds(pl.multiple_of(block * rows, rows), rows), :] = some[k * rows : (k + 1) * rows]
     context = jnp.concatenate([ctx_ref[pl.ds(i, n_ctx, stride=rows), :] for i in range(rows)], axis=1)
     h_ref[tok:, :] = modulated(context, shift_ctx, scale_ctx)
     h = h_ref[...]
@@ -236,26 +211,27 @@
     rope = w_rope_key.shape[1]
     factor = (nope + rope) ** (-0.5)
 
+    block = jnp.concatenate([latent, context.reshape(rows, lanes)], axis=1)
+    before = shifted(block, Y, 1)
+    after = shifted(block, Y, n_y - 1)
+    three = jnp.stack([before, block, after])
+    behind = shifted(three, Y, 3)
+    ahead = shifted(three[:2], Y, n_y - 3)
+    mine = jnp.concatenate([block[None], after[None], ahead, behind, before[None]], axis=0)
+    other = shifted(mine, "c", 1)
+
     feat = shift_w.shape[0]
     own = jnp.stack([lax.dynamic_slice_in_dim(v, sp_index * feat, feat) for v in (cond, ctx_mod)])
     own = jax.nn.silu(own)
     parts = [jnp.sum(own[i][:, None] * w, axis=0) for w, i in ((shift_w, 0), (shift_w, 1), (scale_w, 0), (scale_w, 1), (gate_w, 0))]
     summed = copies(jnp.stack(parts), SP)
+    summed = jnp.sum(summed, axis=0)
+    vectors = copies(summed, TP)
+    gate = vectors[:, 4].reshape(width)
     w_near = shifted(w_out, "yb", 1)
-    block = jnp.concatenate([latent, context.reshape(rows, lanes)], axis=1)
     smem = pl.BlockSpec(memory_space=pltpu.SMEM)
     vmem = pl.BlockSpec(memory_space=pltpu.VMEM)
     any_space = pl.BlockSpec(memory_space=pl.ANY)
-    pack = pl.pallas_call(
-        pack_kernel,
-        in_specs=[vmem, vmem],
-        out_specs=vmem,
-        out_shape=jax.ShapeDtypeStruct((n_y, rows, width + 2 * lanes), BF16),
-        name="pack",
-    )
-    message = pack(summed, block)
-
-    mine = exchanged(message, Y)
     w_other = shifted(w_out, "c", 1)
     w_far = shifted(w_near, "c", 1)
     w_side = jnp.concatenate([w_qn, w_qr, w_rope_key], axis=1)
@@ -263,18 +239,15 @@
     place = jnp.arange(tok, dtype=jnp.int32)
     place = (place // rows % n_ya * 2 + place // (tok // 2)) * (n_c * rows) + place // quarter % n_c * rows + place % rows
     cosine, sine = turn_table(sp_index * tok + place, rope, lanes)
-    at = jnp.stack([lax.axis_index("c"), lax.axis_index("yb")]).astype(jnp.int32).reshape(1, 2)
+    at = jnp.stack([lax.axis_index("c"), lax.axis_index("yb"), lax.axis_index(Y)]).astype(jnp.int32).reshape(1, 3)
     to = lax.axis_index(Q_AXIS).astype(jnp.int32).reshape(1, 1)
-    other = shifted(mine, "c", 1)
-
     project = pl.pallas_call(
         project_kernel,
-        in_specs=[smem] + [vmem] * 6 + [any_space] * 3,
-        out_specs=[vmem, vmem, vmem],
+        in_specs=[smem] + [vmem] * 7 + [any_space] * 3,
+        out_specs=[vmem, vmem],
         out_shape=[
             jax.ShapeDtypeStruct((tok + tok // 2, lanes), BF16),
             jax.ShapeDtypeStruct((lax.axis_size(KV_AXES), 2 * (tok + n_tp) + tok // 2 + n_tp, lanes), BF16),
-            jax.ShapeDtypeStruct((1, width), F32),
         ],
         scratch_shapes=[
             pltpu.VMEM((tok, lanes), F32),
@@ -288,8 +261,8 @@
         ],
         name="project",
     )
-    q_own, kv_copies, gate = project(
-        at, mine, other, norm_gain.reshape(1, width), kv_gain.reshape(1, -1), cosine, sine, w_side, w_kv_down, w_up
+    q_own, kv_copies = project(
+        at, mine, other, vectors, norm_gain.reshape(1, width), kv_gain.reshape(1, -1), cosine, sine, w_side, w_kv_down, w_up
     )
 
     queries = [q_own] + [shifted(q_own, Q_AXIS, k) for k in range(1, n_q)]

time: 143 us -> 157 us (1.098)
  starting transfers between devices: 53.5 us -> 69.9 us
  blocking collectives: 14.9 us -> 0 us
  waiting for transfers between devices: 41.5 us -> 52.7 us
  local copies, waits for them, and re-layouts: 5.45 us -> 8.22 us
  Pallas kernels: 17.8 us -> 16 us
    ppermute x7 -> x11, starting transfers between devices: 21.7 us -> 39.2 us  [shifted(): return lax.ppermute(array, axis, [(i, (i + k) % n) for i in range(n)])]
    ppermute x7 -> x11, waiting for transfers between devices: 12.1 us -> 28.5 us  [shifted(): return lax.ppermute(array, axis, [(i, (i + k) % n) for i in range(n)])]
    all_to_all x1 -> x0, blocking collectives: 14.9 us -> none  [exchanged(): return lax.all_to_all(array, axes, 0, 0, tiled=True)]
    all_to_all x3, waiting for transfers between devices: 22.3 us -> 17 us  [exchanged(): return lax.all_to_all(array, axes, 0, 0, tiled=True)]
    all_to_all x3, starting transfers between devices: 18.1 us -> 14.1 us  [exchanged(): return lax.all_to_all(array, axes, 0, 0, tiled=True)]
    all_to_all x1 -> x2, starting transfers between devices: 13.7 us -> 16.6 us  [copies(): lax.all_to_all(jnp.broadcast_to(array[None], (n, *array.shape)), axes, 0,...]
    pallas_call x2 -> x1, Pallas kernels: 7.37 us -> 5.52 us  [step(): project(at, mine, other, vectors, norm_gain.reshape(1, width), kv_gain.re...]
    unnamed x42 -> x39, local copies, waits for them, and re-layouts: 3.93 us -> 5.23 us
  transfers between devices with their start and end apart: 11 -> 16, of which waited for: 6 -> 8; matrix products, arithmetic and copies ran while one was open for 5% -> 7% of each run, Pallas kernels for 5% -> 4%
where the time goes in v8:
time: 157 us; the launch traced here: 156 us
  starting transfers between devices  69.9 us (45%)
  waiting for transfers between devices  52.7 us (34%)
  Pallas kernels  16 us (10%)
  other arithmetic  8.23 us (5%)
  local copies, waits for them, and re-layouts  8.22 us (5%)
    ppermute x11, starting transfers between devices, shifted(): return lax.ppermute(array, axis, [(i, (i + k) % n) for i in range(n)])  39.2 us
    ppermute x11, waiting for transfers between devices, shifted(): return lax.ppermute(array, axis, [(i, (i + k) % n) for i in range(n)])  28.5 us
    all_to_all x3, waiting for transfers between devices, exchanged(): return lax.all_to_all(array, axes, 0, 0, tiled=True)  17 us
    all_to_all x2, starting transfers between devices, copies(): lax.all_to_all(jnp.broadcast_to(array[None], (n, *array.shape)), axes, 0,...  16.6 us
    all_to_all x3, starting transfers between devices, exchanged(): return lax.all_to_all(array, axes, 0, 0, tiled=True)  14.1 us
    all_to_all x2, waiting for transfers between devices, copies(): lax.all_to_all(jnp.broadcast_to(array[None], (n, *array.shape)), axes, 0,...  7.11 us
    pallas_call x1, Pallas kernels, step(): out = attend(to, ctx_bias.reshape(1, 1), *queries, kv)  6.7 us
    pallas_call x1, Pallas kernels, step(): project(at, mine, other, vectors, norm_gain.reshape(1, width), kv_gain.re...  5.52 us
  transfers between devices with their start and end apart: 16, of which 8 were waited for; matrix products, arithmetic and copies ran while one was open for 7% of the time, Pallas kernels for 4%

profile of v8, /device:TPU:1, one launch (start us, length us, event | category | flops | bytes accessed | tf_op | source)
XLA Modules:
  0.0 155.9 jit_solution(7417709756953292547)
XLA Ops:
  0.0 0.8 reduce
  0.8 0.9 fusion.20
  1.6 4.0 %collective-permute-start.1 = (bf16[16,2176]{1,0:T(8,128)(2,1)S(1)}, bf16[16,2176]{1,0:T(8,128)(2,1)S(1)}, u32[]{:S(2)}, u32[]{:S(2)}) collective-permute-start(bf16[16,2176]{1,0:T(8,128)(2,1)S(1)} %get-tuple-element.17), channel_id=1, source_target_pairs={{0,2},{2,4},{4,6},{6,8},{8,10},{10,12},{12,14},{14,0},{1,3},{3,5},... | collective-permute-start | bytes 208904 | tf_op jit(solution)/shard_map/ppermute | solution.py:49
  5.7 3.8 %collective-permute-start = (bf16[16,2176]{1,0:T(8,128)(2,1)S(1)}, bf16[16,2176]{1,0:T(8,128)(2,1)S(1)}, u32[]{:S(2)}, u32[]{:S(2)}) collective-permute-start(bf16[16,2176]{1,0:T(8,128)(2,1)S(1)} %get-tuple-element.17), channel_id=1, source_target_pairs={{0,14},{2,0},{4,2},{6,4},{8,6},{10,8},{12,10},{14,12},{1,15},{3,1}... | collective-permute-start | bytes 208904 | tf_op jit(solution)/shard_map/ppermute | solution.py:49
  9.5 0.8 dynamic-slice_bitcast_fusion
  10.3 0.9 multiply_reduce_fusion.3
  11.2 0.7 broadcast_in_dim.20
  11.9 12.9 %all-to-all-start = ((f32[32,5,128]{2,1,0:T(8,128)}), f32[32,5,128]{2,1,0:T(8,128)S(1)}, u32[]{:S(2)}, u32[]{:S(2)}) async-start(f32[32,5,128]{2,1,0:T(8,128)} %broadcast_in_dim.20), calls=%async_computation | async-start | bytes 262144 | tf_op jit(solution)/shard_map/all_to_all | solution.py:27
  24.8 0.8 constant_dynamic-update-slice_fusion.4
  25.7 1.2 copy.23
  26.9 1.2 copy.24
  28.1 0.0 copy-done.5
  28.1 0.0 copy-start.11
  28.2 0.0 copy-start.12
  28.2 1.3 pad_maximum_fusion.w_side_hbm
  29.5 0.0 collective-permute-done.1
  29.5 4.9 %collective-permute-start.2 = (bf16[2,16,2176]{2,1,0:T(8,128)(2,1)S(1)}, bf16[2,16,2176]{2,1,0:T(8,128)(2,1)S(1)}, u32[]{:S(2)}, u32[]{:S(2)}) collective-permute-start(bf16[2,16,2176]{2,1,0:T(8,128)(2,1)S(1)} %pad_maximum_fusion.3), channel_id=1, source_target_pairs={{0,10},{2,12},{4,14},{6,0},{8,2},{10,4},{12,6},{14,8},{1,11},{3,13... | collective-permute-start | bytes 417800 | tf_op jit(solution)/shard_map/ppermute | solution.py:49
  34.5 0.0 collective-permute-done
  34.5 2.1 %collective-permute-start.3 = (bf16[3,16,2176]{2,1,0:T(8,128)(2,1)S(1)}, bf16[3,16,2176]{2,1,0:T(8,128)(2,1)S(1)}, u32[]{:S(2)}, u32[]{:S(2)}) collective-permute-start(bf16[3,16,2176]{2,1,0:T(8,128)(2,1)S(1)} %pad_maximum_fusion.2), channel_id=1, source_target_pairs={{0,6},{2,8},{4,10},{6,12},{8,14},{10,0},{12,2},{14,4},{1,7},{3,9},... | collective-permute-start | bytes 626696 | tf_op jit(solution)/shard_map/ppermute | solution.py:49
  36.7 0.6 collective-permute-done.2
  37.4 15.8 %collective-permute-done.3 = bf16[3,16,2176]{2,1,0:T(8,128)(2,1)S(1)} collective-permute-done((bf16[3,16,2176]{2,1,0:T(8,128)(2,1)S(1)}, bf16[3,16,2176]{2,1,0:T(8,128)(2,1)S(1)}, u32[]{:S(2)}, u32[]{:S(2)}) %collective-permute-start.3) | collective-permute-done | bytes 208928 | tf_op jit(solution)/shard_map/ppermute | solution.py:49
  53.2 4.4 %collective-permute-start.4 = (bf16[8,16,2176]{2,1,0:T(8,128)(2,1)S(1)}, bf16[8,16,2176]{2,1,0:T(8,128)(2,1)S(1)}, u32[]{:S(2)}, u32[]{:S(2)}) collective-permute-start(bf16[8,16,2176]{2,1,0:T(8,128)(2,1)S(1)} %constant_dynamic-update-slice_fusion.own_ref), channel_id=1, source_target_pairs={{0,1},{1,0},{2,3},{3,2},{4,5},{5,4},{6,7},{7,6},{8,9},{9,8},{10,11... | collective-permute-start | bytes 1671176 | tf_op jit(solution)/shard_map/ppermute | solution.py:49
  57.5 1.3 sine_multiply_fusion
  58.8 0.0 copy-done.12
  58.8 0.7 pad_maximum_fusion.1.w_up_hbm
  59.6 0.0 all-to-all-done
  59.6 0.6 broadcast_in_dim.23
  60.3 3.7 %all-to-all-start.1 = ((f32[16,5,128]{2,1,0:T(8,128)}), f32[16,5,128]{2,1,0:T(8,128)S(1)}, u32[]{:S(2)}, u32[]{:S(2)}) async-start(f32[16,5,128]{2,1,0:T(8,128)} %broadcast_in_dim.23), calls=%async_computation.1 | async-start | bytes 131072 | tf_op jit(solution)/shard_map/all_to_all | solution.py:27
  64.0 0.7 add_bitcast_fusion.at_ref
  64.6 7.1 %all-to-all-done.1.vec_ref = f32[16,5,128]{2,1,0:T(8,128)S(1)} async-done(((f32[16,5,128]{2,1,0:T(8,128)}), f32[16,5,128]{2,1,0:T(8,128)S(1)}, u32[]{:S(2)}, u32[]{:S(2)}) %all-to-all-start.1) | async-done | bytes 40992 | tf_op jit(solution)/shard_map/all_to_all | solution.py:27
  71.7 0.0 collective-permute-done.4.other_ref
  71.7 0.0 copy-done.2
  71.7 0.6 copy-done.10
  72.4 0.2 copy-done.4
  72.6 5.5 %project.1 = (bf16[384,128]{1,0:T(8,128)(2,1)}, bf16[8,688,128]{2,1,0:T(8,128)(2,1)}) custom-call(s32[1,3]{1,0:T(1,128)} %add_bitcast_fusion.at_ref, bf16[8,16,2176]{2,1,0:T(8,128)(2,1)} %copy-done.2, bf16[8,16,2176]{2,1,0:T(8,128)(2,1)} %copy-done.4, f32[16,5,128]{2,1,0:T(8,128)} %copy-done.10, f32[1,2048]{1,0:T(1,128)} %bitcast.42, f32[1,512]{1,0:T(1,128)} %bitcast.43, ...), custom_call_target="tpu_custom_call" | custom-call | tf_op jit(solution)/shard_map/project/pallas_call | solution.py:264
  78.1 0.0 copy-start.6
  78.1 0.0 copy-start.13
  78.1 5.1 %all-to-all-start.2 = ((bf16[8,688,128]{2,1,0:T(8,128)(2,1)}), bf16[8,688,128]{2,1,0:T(8,128)(2,1)S(1)}, u32[]{:S(2)}, u32[]{:S(2)}) async-start(bf16[8,688,128]{2,1,0:T(8,128)(2,1)} %get-tuple-element.8), calls=%async_computation.2 | async-start | bytes 2818048 | tf_op jit(solution)/shard_map/all_to_all | solution.py:31
  83.2 2.1 %collective-permute-start.9 = (bf16[128,2048]{1,0:T(8,128)(2,1)S(1)}, bf16[128,2048]{1,0:T(8,128)(2,1)S(1)}, u32[]{:S(2)}, u32[]{:S(2)}) collective-permute-start(bf16[128,2048]{1,0:T(8,128)(2,1)S(1)} %copy-done.6), channel_id=1, source_target_pairs={{0,2},{2,0},{1,3},{3,1},{4,6},{6,4},{5,7},{7,5},{8,10},{10,8},{9,1... | collective-permute-start | bytes 1572872 | tf_op jit(solution)/shard_map/ppermute | solution.py:49
  85.3 4.0 %collective-permute-start.5 = (bf16[384,128]{1,0:T(8,128)(2,1)S(1)}, bf16[384,128]{1,0:T(8,128)(2,1)S(1)}, u32[]{:S(2)}, u32[]{:S(2)}) collective-permute-start(bf16[384,128]{1,0:T(8,128)(2,1)S(1)} %copy-done.13), channel_id=1, source_target_pairs={{0,128},{128,256},{256,384},{384,0},{1,129},{129,257},{257,385},{3... | collective-permute-start | bytes 294920 | tf_op jit(solution)/shard_map/ppermute | solution.py:49
  89.3 4.4 %collective-permute-start.6 = (bf16[384,128]{1,0:T(8,128)(2,1)S(1)}, bf16[384,128]{1,0:T(8,128)(2,1)S(1)}, u32[]{:S(2)}, u32[]{:S(2)}) collective-permute-start(bf16[384,128]{1,0:T(8,128)(2,1)S(1)} %copy-done.13), channel_id=1, source_target_pairs={{0,256},{128,384},{256,0},{384,128},{1,257},{129,385},{257,1},{385... | collective-permute-start | bytes 294920 | tf_op jit(solution)/shard_map/ppermute | solution.py:49
  93.7 5.1 %collective-permute-start.7 = (bf16[384,128]{1,0:T(8,128)(2,1)S(1)}, bf16[384,128]{1,0:T(8,128)(2,1)S(1)}, u32[]{:S(2)}, u32[]{:S(2)}) collective-permute-start(bf16[384,128]{1,0:T(8,128)(2,1)S(1)} %copy-done.13), channel_id=1, source_target_pairs={{0,384},{128,0},{256,128},{384,256},{1,385},{129,1},{257,129},{385... | collective-permute-start | bytes 294920 | tf_op jit(solution)/shard_map/ppermute | solution.py:49
  99.5 6.5 %collective-permute-done.5.q1 = bf16[384,128]{1,0:T(8,128)(2,1)S(1)} collective-permute-done((bf16[384,128]{1,0:T(8,128)(2,1)S(1)}, bf16[384,128]{1,0:T(8,128)(2,1)S(1)}, u32[]{:S(2)}, u32[]{:S(2)}) %collective-permute-start.5) | collective-permute-done | bytes 98336 | tf_op jit(solution)/shard_map/ppermute | solution.py:49
  106.0 4.2 %collective-permute-done.6.q2 = bf16[384,128]{1,0:T(8,128)(2,1)S(1)} collective-permute-done((bf16[384,128]{1,0:T(8,128)(2,1)S(1)}, bf16[384,128]{1,0:T(8,128)(2,1)S(1)}, u32[]{:S(2)}, u32[]{:S(2)}) %collective-permute-start.6) | collective-permute-done | bytes 98336 | tf_op jit(solution)/shard_map/ppermute | solution.py:49
  110.1 0.0 collective-permute-done.7.q3
  110.1 0.0 all-to-all-done.2.kv_ref
  110.2 0.6 copy-done.15
  110.8 0.0 copy-done.16
  110.8 0.5 copy-done
  111.3 6.7 %attend.1 = bf16[4,4,80,128]{3,2,1,0:T(8,128)(2,1)} custom-call(s32[1,1]{1,0:T(1,128)} %bitcast.14.place_ref, f32[1,1]{1,0:T(1,128)} %bitcast.33.bias_ref, bf16[384,128]{1,0:T(8,128)(2,1)} %get-tuple-element.7.q0, bf16[384,128]{1,0:T(8,128)(2,1)} %copy-done.14, bf16[384,128]{1,0:T(8,128)(2,1)} %copy-done.15, bf16[384,128]{1,0:T(8,128)(2,1)} %copy-done.16, ...), custom_call_target="tpu_custom_call" | custom-call | tf_op jit(solution)/shard_map/attend/pallas_call | solution.py:283
  118.0 5.6 %all-to-all-start.3 = ((bf16[16,80,128]{2,1,0:T(8,128)(2,1)}), bf16[16,80,128]{2,1,0:T(8,128)(2,1)S(1)}, u32[]{:S(2)}, u32[]{:S(2)}) async-start(bf16[16,80,128]{2,1,0:T(8,128)(2,1)} %bitcast.34), calls=%async_computation.3 | async-start | bytes 655360 | tf_op jit(solution)/shard_map/all_to_all | solution.py:31
  123.6 2.0 %collective-permute-start.8 = (bf16[128,2048]{1,0:T(8,128)(2,1)S(1)}, bf16[128,2048]{1,0:T(8,128)(2,1)S(1)}, u32[]{:S(2)}, u32[]{:S(2)}) collective-permute-start(bf16[128,2048]{1,0:T(8,128)(2,1)S(1)} %copy-done.6), channel_id=1, source_target_pairs={{0,1},{1,0},{2,3},{3,2},{4,5},{5,4},{6,7},{7,6},{8,9},{9,8},{10,11... | collective-permute-start | bytes 1572872 | tf_op jit(solution)/shard_map/ppermute | solution.py:49
  125.6 0.0 collective-permute-done.9.refs_2_
  125.6 2.3 %collective-permute-start.10 = (bf16[128,2048]{1,0:T(8,128)(2,1)S(1)}, bf16[128,2048]{1,0:T(8,128)(2,1)S(1)}, u32[]{:S(2)}, u32[]{:S(2)}) collective-permute-start(bf16[128,2048]{1,0:T(8,128)(2,1)S(1)} %collective-permute-done.9.refs_2_), channel_id=1, source_target_pairs={{0,1},{1,0},{2,3},{3,2},{4,5},{5,4},{6,7},{7,6},{8,9},{9,8},{10,11... | collective-permute-start | bytes 1572872 | tf_op jit(solution)/shard_map/ppermute | solution.py:49
  128.0 0.0 collective-permute-done.8.refs_1_
  128.0 1.5 collective-permute-done.10.refs_3_
  129.5 6.9 %all-to-all-done.3 = bf16[16,80,128]{2,1,0:T(8,128)(2,1)S(1)} async-done(((bf16[16,80,128]{2,1,0:T(8,128)(2,1)}), bf16[16,80,128]{2,1,0:T(8,128)(2,1)S(1)}, u32[]{:S(2)}, u32[]{:S(2)}) %all-to-all-start.3) | async-done | bytes 327712 | tf_op jit(solution)/shard_map/all_to_all | solution.py:31
  136.4 0.0 copy-done.7
  136.4 0.7 copy-done.1
  137.1 3.7 %merge.1 = bf16[4,16,2048]{2,1,0:T(8,128)(2,1)} custom-call(s32[1,3]{1,0:T(1,128)} %add_bitcast_fusion.at_ref, bf16[4,4,80,128]{3,2,1,0:T(8,128)(2,1)} %bitcast.35, bf16[128,2048]{1,0:T(8,128)(2,1)} %refs_0_.1, bf16[128,2048]{1,0:T(8,128)(2,1)} %copy-done.8, bf16[128,2048]{1,0:T(8,128)(2,1)} %copy-done.7, bf16[128,2048]{1,0:T(8,128)(2,1)} %copy-done.9), custom_call_target="tpu_custom_call" | custom-call | tf_op jit(solution)/shard_map/merge/pallas_call | solution.py:286
  140.8 3.4 %all-to-all-start.4 = ((bf16[4,16,2048]{2,1,0:T(8,128)(2,1)}), bf16[4,16,2048]{2,1,0:T(8,128)(2,1)S(1)}, u32[]{:S(2)}, u32[]{:S(2)}) async-start(bf16[4,16,2048]{2,1,0:T(8,128)(2,1)} %merge.1), calls=%async_computation.4 | async-start | bytes 524288 | tf_op jit(solution)/shard_map/all_to_all | solution.py:31
  144.3 0.9 slice.17
  145.1 10.1 %all-to-all-done.4 = bf16[4,16,2048]{2,1,0:T(8,128)(2,1)S(1)} async-done(((bf16[4,16,2048]{2,1,0:T(8,128)(2,1)}), bf16[4,16,2048]{2,1,0:T(8,128)(2,1)S(1)}, u32[]{:S(2)}, u32[]{:S(2)}) %all-to-all-start.4) | async-done | bytes 262176 | tf_op jit(solution)/shard_map/all_to_all | solution.py:31
  155.3 0.7 add_convert_fusion
  (34 shorter events, 0.3 us)
Async XLA Ops:
  0.0 28.1 %copy-start.5 = (bf16[2048,128]{1,0:T(8,128)(2,1)S(1)}, bf16[2048,128]{1,0:T(8,128)(2,1)}, u32[]{:S(2)}) copy-start(bf16[2048,128]{1,0:T(8,128)(2,1)} %param.25) | copy-start | bytes 1572868
  1.6 27.9 %collective-permute-start.1 = (bf16[16,2176]{1,0:T(8,128)(2,1)S(1)}, bf16[16,2176]{1,0:T(8,128)(2,1)S(1)}, u32[]{:S(2)}, u32[]{:S(2)}) collective-permute-start(bf16[16,2176]{1,0:T(8,128)(2,1)S(1)} %get-tuple-element.17), channel_id=1, source_target_pairs={{0,2},{2,4},{4,6},{6,8},{8,10},{10,12},{12,14},{14,0},{1,3},{3,5},... | collective-permute-start | bytes 208904 | tf_op jit(solution)/shard_map/ppermute | solution.py:49
  5.7 28.8 %collective-permute-start = (bf16[16,2176]{1,0:T(8,128)(2,1)S(1)}, bf16[16,2176]{1,0:T(8,128)(2,1)S(1)}, u32[]{:S(2)}, u32[]{:S(2)}) collective-permute-start(bf16[16,2176]{1,0:T(8,128)(2,1)S(1)} %get-tuple-element.17), channel_id=1, source_target_pairs={{0,14},{2,0},{4,2},{6,4},{8,6},{10,8},{12,10},{14,12},{1,15},{3,1}... | collective-permute-start | bytes 208904 | tf_op jit(solution)/shard_map/ppermute | solution.py:49
  11.9 47.7 %all-to-all-start = ((f32[32,5,128]{2,1,0:T(8,128)}), f32[32,5,128]{2,1,0:T(8,128)S(1)}, u32[]{:S(2)}, u32[]{:S(2)}) async-start(f32[32,5,128]{2,1,0:T(8,128)} %broadcast_in_dim.20), calls=%async_computation | async-start | bytes 262144 | tf_op jit(solution)/shard_map/all_to_all | solution.py:27
  28.1 30.7 %copy-start.11 = (bf16[512,128]{1,0:T(8,128)(2,1)S(1)}, bf16[512,128]{1,0:T(8,128)(2,1)}, u32[]{:S(2)}) copy-start(bf16[512,128]{1,0:T(8,128)(2,1)} %param.31) | copy-start | bytes 393220
  28.2 30.7 %copy-start.12 = (bf16[512,128]{1,0:T(8,128)(2,1)S(1)}, bf16[512,128]{1,0:T(8,128)(2,1)}, u32[]{:S(2)}) copy-start(bf16[512,128]{1,0:T(8,128)(2,1)} %param.30) | copy-start | bytes 393220
  29.5 7.8 %collective-permute-start.2 = (bf16[2,16,2176]{2,1,0:T(8,128)(2,1)S(1)}, bf16[2,16,2176]{2,1,0:T(8,128)(2,1)S(1)}, u32[]{:S(2)}, u32[]{:S(2)}) collective-permute-start(bf16[2,16,2176]{2,1,0:T(8,128)(2,1)S(1)} %pad_maximum_fusion.3), channel_id=1, source_target_pairs={{0,10},{2,12},{4,14},{6,0},{8,2},{10,4},{12,6},{14,8},{1,11},{3,13... | collective-permute-start | bytes 417800 | tf_op jit(solution)/shard_map/ppermute | solution.py:49
  34.5 18.6 %collective-permute-start.3 = (bf16[3,16,2176]{2,1,0:T(8,128)(2,1)S(1)}, bf16[3,16,2176]{2,1,0:T(8,128)(2,1)S(1)}, u32[]{:S(2)}, u32[]{:S(2)}) collective-permute-start(bf16[3,16,2176]{2,1,0:T(8,128)(2,1)S(1)} %pad_maximum_fusion.2), channel_id=1, source_target_pairs={{0,6},{2,8},{4,10},{6,12},{8,14},{10,0},{12,2},{14,4},{1,7},{3,9},... | collective-permute-start | bytes 626696 | tf_op jit(solution)/shard_map/ppermute | solution.py:49
  53.1 18.6 %copy-start.2 = (bf16[8,16,2176]{2,1,0:T(8,128)(2,1)}, bf16[8,16,2176]{2,1,0:T(8,128)(2,1)S(1)}, u32[]{:S(2)}) copy-start(bf16[8,16,2176]{2,1,0:T(8,128)(2,1)S(1)} %constant_dynamic-update-slice_fusion.own_ref) | copy-start | bytes 1671172
  53.2 18.6 %collective-permute-start.4 = (bf16[8,16,2176]{2,1,0:T(8,128)(2,1)S(1)}, bf16[8,16,2176]{2,1,0:T(8,128)(2,1)S(1)}, u32[]{:S(2)}, u32[]{:S(2)}) collective-permute-start(bf16[8,16,2176]{2,1,0:T(8,128)(2,1)S(1)} %constant_dynamic-update-slice_fusion.own_ref), channel_id=1, source_target_pairs={{0,1},{1,0},{2,3},{3,2},{4,5},{5,4},{6,7},{7,6},{8,9},{9,8},{10,11... | collective-permute-start | bytes 1671176 | tf_op jit(solution)/shard_map/ppermute | solution.py:49
  60.3 11.5 %all-to-all-start.1 = ((f32[16,5,128]{2,1,0:T(8,128)}), f32[16,5,128]{2,1,0:T(8,128)S(1)}, u32[]{:S(2)}, u32[]{:S(2)}) async-start(f32[16,5,128]{2,1,0:T(8,128)} %broadcast_in_dim.23), calls=%async_computation.1 | async-start | bytes 131072 | tf_op jit(solution)/shard_map/all_to_all | solution.py:27
  71.7 0.6 copy-start.10
  71.7 0.8 copy-start.4
  78.1 5.1 %copy-start.6 = (bf16[128,2048]{1,0:T(8,128)(2,1)S(1)}, bf16[128,2048]{1,0:T(8,128)(2,1)}, u32[]{:S(2)}) copy-start(bf16[128,2048]{1,0:T(8,128)(2,1)} %refs_0_.1) | copy-start | bytes 1572868
  78.1 7.2 %copy-start.13 = (bf16[384,128]{1,0:T(8,128)(2,1)S(1)}, bf16[384,128]{1,0:T(8,128)(2,1)}, u32[]{:S(2)}) copy-start(bf16[384,128]{1,0:T(8,128)(2,1)} %get-tuple-element.7.q0) | copy-start | bytes 294916
  78.1 32.0 %all-to-all-start.2 = ((bf16[8,688,128]{2,1,0:T(8,128)(2,1)}), bf16[8,688,128]{2,1,0:T(8,128)(2,1)S(1)}, u32[]{:S(2)}, u32[]{:S(2)}) async-start(bf16[8,688,128]{2,1,0:T(8,128)(2,1)} %get-tuple-element.8), calls=%async_computation.2 | async-start | bytes 2818048 | tf_op jit(solution)/shard_map/all_to_all | solution.py:31
  83.2 42.5 %collective-permute-start.9 = (bf16[128,2048]{1,0:T(8,128)(2,1)S(1)}, bf16[128,2048]{1,0:T(8,128)(2,1)S(1)}, u32[]{:S(2)}, u32[]{:S(2)}) collective-permute-start(bf16[128,2048]{1,0:T(8,128)(2,1)S(1)} %copy-done.6), channel_id=1, source_target_pairs={{0,2},{2,0},{1,3},{3,1},{4,6},{6,4},{5,7},{7,5},{8,10},{10,8},{9,1... | collective-permute-start | bytes 1572872 | tf_op jit(solution)/shard_map/ppermute | solution.py:49
  85.3 20.7 %collective-permute-start.5 = (bf16[384,128]{1,0:T(8,128)(2,1)S(1)}, bf16[384,128]{1,0:T(8,128)(2,1)S(1)}, u32[]{:S(2)}, u32[]{:S(2)}) collective-permute-start(bf16[384,128]{1,0:T(8,128)(2,1)S(1)} %copy-done.13), channel_id=1, source_target_pairs={{0,128},{128,256},{256,384},{384,0},{1,129},{129,257},{257,385},{3... | collective-permute-start | bytes 294920 | tf_op jit(solution)/shard_map/ppermute | solution.py:49
  89.3 20.8 %collective-permute-start.6 = (bf16[384,128]{1,0:T(8,128)(2,1)S(1)}, bf16[384,128]{1,0:T(8,128)(2,1)S(1)}, u32[]{:S(2)}, u32[]{:S(2)}) collective-permute-start(bf16[384,128]{1,0:T(8,128)(2,1)S(1)} %copy-done.13), channel_id=1, source_target_pairs={{0,256},{128,384},{256,0},{384,128},{1,257},{129,385},{257,1},{385... | collective-permute-start | bytes 294920 | tf_op jit(solution)/shard_map/ppermute | solution.py:49
  93.7 16.5 %collective-permute-start.7 = (bf16[384,128]{1,0:T(8,128)(2,1)S(1)}, bf16[384,128]{1,0:T(8,128)(2,1)S(1)}, u32[]{:S(2)}, u32[]{:S(2)}) collective-permute-start(bf16[384,128]{1,0:T(8,128)(2,1)S(1)} %copy-done.13), channel_id=1, source_target_pairs={{0,384},{128,0},{256,128},{384,256},{1,385},{129,1},{257,129},{385... | collective-permute-start | bytes 294920 | tf_op jit(solution)/shard_map/ppermute | solution.py:49
  106.0 4.2 %copy-start.14 = (bf16[384,128]{1,0:T(8,128)(2,1)}, bf16[384,128]{1,0:T(8,128)(2,1)S(1)}, u32[]{:S(2)}) copy-start(bf16[384,128]{1,0:T(8,128)(2,1)S(1)} %collective-permute-done.5.q1) | copy-start | bytes 294916
  110.1 0.6 copy-start.15
  110.1 0.7 copy-start.16
  110.2 1.1 copy-start
  118.0 37.3 %copy-start.3 = (bf16[16,2048]{1,0:T(8,128)(2,1)S(1)}, bf16[16,2048]{1,0:T(8,128)(2,1)}, u32[]{:S(2)}) copy-start(bf16[16,2048]{1,0:T(8,128)(2,1)} %param.17) | copy-start | bytes 196612
  118.0 18.3 %all-to-all-start.3 = ((bf16[16,80,128]{2,1,0:T(8,128)(2,1)}), bf16[16,80,128]{2,1,0:T(8,128)(2,1)S(1)}, u32[]{:S(2)}, u32[]{:S(2)}) async-start(bf16[16,80,128]{2,1,0:T(8,128)(2,1)} %bitcast.34), calls=%async_computation.3 | async-start | bytes 655360 | tf_op jit(solution)/shard_map/all_to_all | solution.py:31
  123.6 4.4 %collective-permute-start.8 = (bf16[128,2048]{1,0:T(8,128)(2,1)S(1)}, bf16[128,2048]{1,0:T(8,128)(2,1)S(1)}, u32[]{:S(2)}, u32[]{:S(2)}) collective-permute-start(bf16[128,2048]{1,0:T(8,128)(2,1)S(1)} %copy-done.6), channel_id=1, source_target_pairs={{0,1},{1,0},{2,3},{3,2},{4,5},{5,4},{6,7},{7,6},{8,9},{9,8},{10,11... | collective-permute-start | bytes 1572872 | tf_op jit(solution)/shard_map/ppermute | solution.py:49
  125.6 10.7 %copy-start.7 = (bf16[128,2048]{1,0:T(8,128)(2,1)}, bf16[128,2048]{1,0:T(8,128)(2,1)S(1)}, u32[]{:S(2)}) copy-start(bf16[128,2048]{1,0:T(8,128)(2,1)S(1)} %collective-permute-done.9.refs_2_) | copy-start | bytes 1572868
  125.6 3.8 %collective-permute-start.10 = (bf16[128,2048]{1,0:T(8,128)(2,1)S(1)}, bf16[128,2048]{1,0:T(8,128)(2,1)S(1)}, u32[]{:S(2)}, u32[]{:S(2)}) collective-permute-start(bf16[128,2048]{1,0:T(8,128)(2,1)S(1)} %collective-permute-done.9.refs_2_), channel_id=1, source_target_pairs={{0,1},{1,0},{2,3},{3,2},{4,5},{5,4},{6,7},{7,6},{8,9},{9,8},{10,11... | collective-permute-start | bytes 1572872 | tf_op jit(solution)/shard_map/ppermute | solution.py:49
  128.0 8.4 %copy-start.8 = (bf16[128,2048]{1,0:T(8,128)(2,1)}, bf16[128,2048]{1,0:T(8,128)(2,1)S(1)}, u32[]{:S(2)}) copy-start(bf16[128,2048]{1,0:T(8,128)(2,1)S(1)} %collective-permute-done.8.refs_1_) | copy-start | bytes 1572868
  129.5 6.9 %copy-start.9 = (bf16[128,2048]{1,0:T(8,128)(2,1)}, bf16[128,2048]{1,0:T(8,128)(2,1)S(1)}, u32[]{:S(2)}) copy-start(bf16[128,2048]{1,0:T(8,128)(2,1)S(1)} %collective-permute-done.10.refs_3_) | copy-start | bytes 1572868
  136.4 0.7 copy-start.1
  140.8 14.4 %all-to-all-start.4 = ((bf16[4,16,2048]{2,1,0:T(8,128)(2,1)}), bf16[4,16,2048]{2,1,0:T(8,128)(2,1)S(1)}, u32[]{:S(2)}, u32[]{:S(2)}) async-start(bf16[4,16,2048]{2,1,0:T(8,128)(2,1)} %merge.1), calls=%async_computation.4 | async-start | bytes 524288 | tf_op jit(solution)/shard_map/all_to_all | solution.py:31

commit v9 on v7

--- a/solution.py
+++ b/solution.py
@@ -22,11 +22,6 @@
 Q_AXIS = "za"
 
 
-def copies(array, axes):
-    n = lax.axis_size(axes)
-    return lax.all_to_all(jnp.broadcast_to(array[None], (n, *array.shape)), axes, 0, 0, tiled=True)
-
-
 def exchanged(array, axes):
     return lax.all_to_all(array, axes, 0, 0, tiled=True)
 
@@ -47,6 +42,24 @@
 def shifted(array, axis, k):
     n = lax.axis_size(axis)
     return lax.ppermute(array, axis, [(i, (i + k) % n) for i in range(n)])
+
+
+def front_kernel(at_ref, cond_ref, mod_ref, shift_ref, scale_ref, gate_ref, o_ref):
+    feat = shift_ref.shape[0]
+    lanes = cond_ref.shape[1]
+    per = lanes // feat
+    rows = []
+    for ref in (cond_ref, mod_ref):
+        row = ref[pl.ds(at_ref[0, 0] // per, 1), :]
+        row = jnp.where(at_ref[0, 0] % per == 0, row, pltpu.roll(row, lanes - feat, 1))
+        rows.append(row / (1.0 + jnp.exp(-row)))
+    pair = jnp.concatenate(rows + [jnp.zeros((6, lanes), F32)], axis=0)[:, :feat]
+    shift, scale, gate = (
+        jnp.dot(pair, ref[...], precision=lax.Precision.HIGHEST, preferred_element_type=F32) for ref in (shift_ref, scale_ref, gate_ref)
+    )
+    parts = jnp.concatenate([shift[:2], scale[:2], gate[:1]], axis=0)
+    for i in range(o_ref.shape[0]):
+        o_ref[i] = parts
 
 
 def pack_kernel(sums_ref, block_ref, o_ref):
@@ -155,14 +168,19 @@
     blocks = (q0, q1, q2, q3)
     size = len(blocks)
     values = [kv_ref[i, count : count + tok] for i in range(n_blocks)] + [vc_ref[...]]
-    for first in range(0, size, 2):
-        pieces = []
-        for block in blocks[first : first + 2]:
-            turned = jnp.concatenate([block[tok:, :rope], block[tok:, rope:]], axis=0)
-            pieces.append(jnp.concatenate([block[:tok, :], turned], axis=1))
-        q = jnp.concatenate(pieces, axis=0)
+    quarter = tok // 4
+
+    def scored(block):
+        turned = jnp.concatenate([block[tok:, :rope], block[tok:, rope:]], axis=0)
+        q = jnp.concatenate([block[:tok, :], turned], axis=1)
         scores = [lax.dot_general(q, k_ref[i], dims, preferred_element_type=F32) * step for i in range(n_blocks)]
-        scores.append(lax.dot_general(q, kc_ref[...], dims, preferred_element_type=F32) * step + bias)
+        return scores + [lax.dot_general(q, kc_ref[...], dims, preferred_element_type=F32) * step + bias]
+
+    ready = scored(blocks[0])
+    for k in range(size):
+        scores = ready
+        if k + 1 < size:
+            ready = scored(blocks[k + 1])
         widest = functools.reduce(jnp.maximum, scores[:-1])
         top = jnp.maximum(jnp.max(widest, axis=1, keepdims=True), jnp.max(scores[-1], axis=1, keepdims=True))
         weights = [jnp.exp2(s - top) for s in scores]
@@ -171,19 +189,17 @@
             jnp.add, [jnp.dot(w.astype(BF16), v, preferred_element_type=F32) for w, v in zip(weights, values, strict=True)]
         )
         out = (out / total).astype(BF16)
-        lse = jnp.transpose(jnp.broadcast_to(top + jnp.log2(total), (2 * tok, lanes)))[:16]
+        lse = jnp.transpose(jnp.broadcast_to(top + jnp.log2(total), (tok, lanes)))[:8]
         high = lse.astype(BF16).astype(F32)
         middle = (lse - high).astype(BF16).astype(F32)
         row = lax.broadcasted_iota(jnp.int32, lse.shape, 0)
         stats = jnp.where(row == 0, high, jnp.where(row == 1, middle, jnp.where(row == 2, lse - high - middle, 0.0))).astype(BF16)
-        quarter = tok // 4
-        for k in range(2):
-            to = (place_ref[0, 0] + (size - first - k)) % size
-            for part in range(4):
-                at = k * tok + part * quarter
-                o_ref[to, part, :quarter, :] = out[at : at + quarter]
-                o_ref[to, part, quarter:, :quarter] = stats[:, at : at + quarter]
-                o_ref[to, part, quarter:, quarter:] = jnp.zeros((16, lanes - quarter), BF16)
+        to = (place_ref[0, 0] + (size - k)) % size
+        for part in range(4):
+            at = part * quarter
+            o_ref[to, part, :quarter, :] = out[at : at + quarter]
+            o_ref[to, part, quarter:, :quarter] = stats[:, at : at + quarter]
+            o_ref[to, part, quarter:, quarter:] = jnp.zeros((8, lanes - quarter), BF16)
 
 
 def merge_kernel(at_ref, got_ref, *refs):
@@ -195,7 +211,7 @@
     for load in loads:
         load.start()
     n_q, _, height, lanes = got_ref.shape
-    quarter = height - 16
+    quarter = height - 8
     n_ya, rows, width = o_ref.shape
     core, yb = at_ref[0, 0], at_ref[0, 1]
     sources = [(yb + i) % 2 * 2 + (core + j) % 2 for i in range(2) for j in range(2)]
@@ -236,11 +252,16 @@
     rope = w_rope_key.shape[1]
     factor = (nope + rope) ** (-0.5)
 
-    feat = shift_w.shape[0]
-    own = jnp.stack([lax.dynamic_slice_in_dim(v, sp_index * feat, feat) for v in (cond, ctx_mod)])
-    own = jax.nn.silu(own)
-    parts = [jnp.sum(own[i][:, None] * w, axis=0) for w, i in ((shift_w, 0), (shift_w, 1), (scale_w, 0), (scale_w, 1), (gate_w, 0))]
-    summed = copies(jnp.stack(parts), SP)
+    smem = pl.BlockSpec(memory_space=pltpu.SMEM)
+    vmem = pl.BlockSpec(memory_space=pltpu.VMEM)
+    parts = pl.pallas_call(
+        front_kernel,
+        in_specs=[smem] + [vmem] * 5,
+        out_specs=vmem,
+        out_shape=jax.ShapeDtypeStruct((lax.axis_size(SP), 5, lanes), F32),
+        name="front",
+    )(sp_index.astype(jnp.int32).reshape(1, 1), cond.reshape(-1, lanes), ctx_mod.reshape(-1, lanes), shift_w, scale_w, gate_w)
+    summed = exchanged(parts, SP)
     w_near = shifted(w_out, "yb", 1)
     block = jnp.concatenate([latent, context.reshape(rows, lanes)], axis=1)
     smem = pl.BlockSpec(memory_space=pltpu.SMEM)
@@ -299,7 +320,7 @@
         functools.partial(attend_kernel, factor=factor, tok=tok, n_ctx=n_tp),
         in_specs=[smem, smem] + [vmem] * 5,
         out_specs=vmem,
-        out_shape=jax.ShapeDtypeStruct((n_q, 2 * n_c, quarter + 16, vsize), BF16),
+        out_shape=jax.ShapeDtypeStruct((n_q, 2 * n_c, quarter + 8, vsize), BF16),
         scratch_shapes=[
             pltpu.VMEM((n_kv, tok, nope + rope), BF16),
             pltpu.VMEM((n_kv * n_tp, nope + rope), BF16),
@@ -309,7 +330,7 @@
     )
     out = attend(to, ctx_bias.reshape(1, 1), *queries, kv)
 
-    got = exchanged(out.reshape(n_q * 2 * n_c, quarter + 16, vsize), (Q_AXIS, "yb", "c"))
+    got = exchanged(out.reshape(n_q * 2 * n_c, quarter + 8, vsize), (Q_AXIS, "yb", "c"))
     term = pl.pallas_call(
         merge_kernel,
         in_specs=[smem, vmem] + [any_space] * 4,
@@ -317,7 +338,7 @@
         out_shape=jax.ShapeDtypeStruct((n_ya, rows, width), BF16),
         scratch_shapes=[pltpu.VMEM((4 * w_out.shape[0], width), BF16)] + [pltpu.SemaphoreType.DMA] * 4,
         name="merge",
-    )(at, got.reshape(n_q, 2 * n_c, quarter + 16, vsize), w_out, w_other, w_near, w_far)
+    )(at, got.reshape(n_q, 2 * n_c, quarter + 8, vsize), w_out, w_other, w_near, w_far)
     branch = jnp.sum(exchanged(term, ("ya",)).astype(F32), axis=0)
     return (latent.astype(F32) + gate * branch).astype(BF16)
 

time: 143 us -> 141 us (0.986)
  local copies, waits for them, and re-layouts: 5.45 us -> 3.96 us
    all_to_all x1 -> x0, starting transfers between devices: 13.7 us -> none  [copies(): lax.all_to_all(jnp.broadcast_to(array[None], (n, *array.shape)), axes, 0,...]
    all_to_all x3 -> x4, starting transfers between devices: 18.1 us -> 31.8 us  [exchanged(): return lax.all_to_all(array, axes, 0, 0, tiled=True)]
    all_to_all x1 -> x0, waiting for transfers between devices: 7.14 us -> none  [copies(): lax.all_to_all(jnp.broadcast_to(array[None], (n, *array.shape)), axes, 0,...]
    all_to_all x3 -> x4, waiting for transfers between devices: 22.3 us -> 28.8 us  [exchanged(): return lax.all_to_all(array, axes, 0, 0, tiled=True)]
    pallas_call x0 -> x1, Pallas kernels: none -> 1.84 us  [step(): pl.pallas_call(front_kernel, in_specs=[smem] + [vmem] * 5, out_specs=vmem...]
  transfers between devices with their start and end apart: 11 -> 11, of which waited for: 6 -> 6; matrix products, arithmetic and copies ran while one was open for 5% -> 5% of each run, Pallas kernels for 5% -> 4%
where the time goes in v9:
time: 141 us; the launch traced here: 140 us
  starting transfers between devices  53.5 us (38%)
  waiting for transfers between devices  40.8 us (29%)
  Pallas kernels  19.1 us (14%)
  blocking collectives  14.8 us (10%)
  other arithmetic  6.85 us (5%)
  local copies, waits for them, and re-layouts  3.96 us (3%)
    all_to_all x4, starting transfers between devices, exchanged(): return lax.all_to_all(array, axes, 0, 0, tiled=True)  31.8 us
    all_to_all x4, waiting for transfers between devices, exchanged(): return lax.all_to_all(array, axes, 0, 0, tiled=True)  28.8 us
    ppermute x7, starting transfers between devices, shifted(): return lax.ppermute(array, axis, [(i, (i + k) % n) for i in range(n)])  21.7 us
    all_to_all x1, blocking collectives, exchanged(): return lax.all_to_all(array, axes, 0, 0, tiled=True)  14.8 us
    ppermute x7, waiting for transfers between devices, shifted(): return lax.ppermute(array, axis, [(i, (i + k) % n) for i in range(n)])  12.1 us
    pallas_call x1, Pallas kernels, step(): out = attend(to, ctx_bias.reshape(1, 1), *queries, kv)  6.2 us
    pallas_call x1, Pallas kernels, step(): project(at, mine, other, norm_gain.reshape(1, width), kv_gain.reshape(1,...  5.57 us
    unnamed x42, local copies, waits for them, and re-layouts  3.96 us
  transfers between devices with their start and end apart: 11, of which 6 were waited for; matrix products, arithmetic and copies ran while one was open for 5% of the time, Pallas kernels for 4%

profile of v9, /device:TPU:1, one launch (start us, length us, event | category | flops | bytes accessed | tf_op | source)
XLA Modules:
  0.0 140.0 jit_solution(5226181301502027124)
XLA Ops:
  0.0 0.0 copy-start.11
  0.0 0.0 copy-start.14
  0.0 1.8 %front.1 = f32[32,5,128]{2,1,0:T(8,128)} custom-call(s32[1,1]{1,0:T(1,128)} %bitcast.3.at_ref, f32[16,128]{1,0:T(8,128)} %bitcast.20, f32[16,128]{1,0:T(8,128)} %bitcast.21, f32[64,128]{1,0:T(8,128)} %shift_ref.1, f32[64,128]{1,0:T(8,128)} %scale_ref.1, f32[64,128]{1,0:T(8,128)} %gate_ref.1), custom_call_target="tpu_custom_call" | custom-call | tf_op jit(solution)/shard_map/front/pallas_call | solution.py:257
  1.9 13.7 %all-to-all-start = ((f32[32,5,128]{2,1,0:T(8,128)}), f32[32,5,128]{2,1,0:T(8,128)S(1)}, u32[]{:S(2)}, u32[]{:S(2)}) async-start(f32[32,5,128]{2,1,0:T(8,128)} %front.1), calls=%async_computation | async-start | bytes 262144 | tf_op jit(solution)/shard_map/all_to_all | solution.py:26
  15.6 0.7 reduce
  16.3 1.5 %pad_maximum_fusion.2.block_ref = bf16[16,2176]{1,0:T(8,128)(2,1)} fusion(bf16[16,128]{1,0:T(8,128)(2,1)S(1)} %bitcast.18, bf16[16,2048]{1,0:T(8,128)(2,1)} %param.17), kind=kLoop, calls=%fused_computation.7 | loop fusion | flops 139264 | bytes 139264 | tf_op jit(solution)/shard_map/concatenate | solution.py:266
  17.8 7.1 %all-to-all-done.sums_ref = f32[32,5,128]{2,1,0:T(8,128)S(1)} async-done(((f32[32,5,128]{2,1,0:T(8,128)}), f32[32,5,128]{2,1,0:T(8,128)S(1)}, u32[]{:S(2)}, u32[]{:S(2)}) %all-to-all-start) | async-done | bytes 81952 | tf_op jit(solution)/shard_map/all_to_all | solution.py:26
  24.9 0.6 copy-done.5
  25.6 1.8 %pack.1 = bf16[8,16,2304]{2,1,0:T(8,128)(2,1)} custom-call(f32[32,5,128]{2,1,0:T(8,128)} %copy-done.5, bf16[16,2176]{1,0:T(8,128)(2,1)} %pad_maximum_fusion.2.block_ref), custom_call_target="tpu_custom_call" | custom-call | tf_op jit(solution)/shard_map/pack/pallas_call | solution.py:277
  27.4 6.8 %all-to-all-start.1 = ((bf16[8,16,2304]{2,1,0:T(8,128)(2,1)}), bf16[8,16,2304]{2,1,0:T(8,128)(2,1)S(1)}, u32[]{:S(2)}, u32[]{:S(2)}) async-start(bf16[8,16,2304]{2,1,0:T(8,128)(2,1)} %pack.1), calls=%async_computation.1 | async-start | bytes 1179648 | tf_op jit(solution)/shard_map/all_to_all | solution.py:26
  34.2 0.0 copy-done.10
  34.2 0.3 copy.18
  34.5 0.0 copy-done.11
  34.5 0.3 copy.19
  34.8 0.0 copy-done.13
  34.8 0.0 copy-done.14
  34.9 0.7 pad_maximum_fusion.1.w_up_hbm
  35.6 15.6 %all-to-all-done.1.own_ref = bf16[8,16,2304]{2,1,0:T(8,128)(2,1)S(1)} async-done(((bf16[8,16,2304]{2,1,0:T(8,128)(2,1)}), bf16[8,16,2304]{2,1,0:T(8,128)(2,1)S(1)}, u32[]{:S(2)}, u32[]{:S(2)}) %all-to-all-start.1) | async-done | bytes 589856 | tf_op jit(solution)/shard_map/all_to_all | solution.py:26
  51.2 4.8 %collective-permute-start = (bf16[8,16,2304]{2,1,0:T(8,128)(2,1)S(1)}, bf16[8,16,2304]{2,1,0:T(8,128)(2,1)S(1)}, u32[]{:S(2)}, u32[]{:S(2)}) collective-permute-start(bf16[8,16,2304]{2,1,0:T(8,128)(2,1)S(1)} %all-to-all-done.1.own_ref), channel_id=1, source_target_pairs={{0,1},{1,0},{2,3},{3,2},{4,5},{5,4},{6,7},{7,6},{8,9},{9,8},{10,11... | collective-permute-start | bytes 1769480 | tf_op jit(solution)/shard_map/ppermute | solution.py:44
  56.0 0.6 add_bitcast_fusion.at_ref
  56.6 1.3 sine_multiply_fusion
  57.8 0.0 copy-done.4
  57.8 1.3 pad_maximum_fusion.w_side_hbm
  59.1 0.0 collective-permute-done.other_ref
  59.1 0.0 copy-done.1
  59.1 0.8 copy-done.3
  60.0 5.6 %project.1 = (bf16[384,128]{1,0:T(8,128)(2,1)}, bf16[8,688,128]{2,1,0:T(8,128)(2,1)}, f32[1,2048]{1,0:T(1,128)}) custom-call(s32[1,2]{1,0:T(1,128)} %add_bitcast_fusion.at_ref, bf16[8,16,2304]{2,1,0:T(8,128)(2,1)} %copy-done.1, bf16[8,16,2304]{2,1,0:T(8,128)(2,1)} %copy-done.3, f32[1,2048]{1,0:T(1,128)} %bitcast.19, f32[1,512]{1,0:T(1,128)} %bitcast.23, ...), custom_call_target="tpu_custom_call" | custom-call | tf_op jit(solution)/shard_map/project/pallas_call | solution.py:312
  65.5 0.0 copy-start.6
  65.6 0.0 copy-start.15
  65.6 3.7 %all-to-all-start.2 = ((bf16[8,688,128]{2,1,0:T(8,128)(2,1)}), bf16[8,688,128]{2,1,0:T(8,128)(2,1)S(1)}, u32[]{:S(2)}, u32[]{:S(2)}) async-start(bf16[8,688,128]{2,1,0:T(8,128)(2,1)} %get-tuple-element.10), calls=%async_computation.2 | async-start | bytes 2818048 | tf_op jit(solution)/shard_map/all_to_all | solution.py:26
  69.3 0.0 copy-done.6
  69.3 2.2 %collective-permute-start.5 = (bf16[128,2048]{1,0:T(8,128)(2,1)S(1)}, bf16[128,2048]{1,0:T(8,128)(2,1)S(1)}, u32[]{:S(2)}, u32[]{:S(2)}) collective-permute-start(bf16[128,2048]{1,0:T(8,128)(2,1)S(1)} %copy-done.6), channel_id=1, source_target_pairs={{0,2},{2,0},{1,3},{3,1},{4,6},{6,4},{5,7},{7,5},{8,10},{10,8},{9,1... | collective-permute-start | bytes 1572872 | tf_op jit(solution)/shard_map/ppermute | solution.py:44
  71.5 0.0 copy-done.15
  71.5 2.9 %collective-permute-start.1 = (bf16[384,128]{1,0:T(8,128)(2,1)S(1)}, bf16[384,128]{1,0:T(8,128)(2,1)S(1)}, u32[]{:S(2)}, u32[]{:S(2)}) collective-permute-start(bf16[384,128]{1,0:T(8,128)(2,1)S(1)} %copy-done.15), channel_id=1, source_target_pairs={{0,128},{128,256},{256,384},{384,0},{1,129},{129,257},{257,385},{3... | collective-permute-start | bytes 294920 | tf_op jit(solution)/shard_map/ppermute | solution.py:44
  74.4 3.5 %collective-permute-start.2 = (bf16[384,128]{1,0:T(8,128)(2,1)S(1)}, bf16[384,128]{1,0:T(8,128)(2,1)S(1)}, u32[]{:S(2)}, u32[]{:S(2)}) collective-permute-start(bf16[384,128]{1,0:T(8,128)(2,1)S(1)} %copy-done.15), channel_id=1, source_target_pairs={{0,256},{128,384},{256,0},{384,128},{1,257},{129,385},{257,1},{385... | collective-permute-start | bytes 294920 | tf_op jit(solution)/shard_map/ppermute | solution.py:44
  77.9 4.0 %collective-permute-start.3 = (bf16[384,128]{1,0:T(8,128)(2,1)S(1)}, bf16[384,128]{1,0:T(8,128)(2,1)S(1)}, u32[]{:S(2)}, u32[]{:S(2)}) collective-permute-start(bf16[384,128]{1,0:T(8,128)(2,1)S(1)} %copy-done.15), channel_id=1, source_target_pairs={{0,384},{128,0},{256,128},{384,256},{1,385},{129,1},{257,129},{385... | collective-permute-start | bytes 294920 | tf_op jit(solution)/shard_map/ppermute | solution.py:44
  82.6 7.9 %collective-permute-done.1.q1 = bf16[384,128]{1,0:T(8,128)(2,1)S(1)} collective-permute-done((bf16[384,128]{1,0:T(8,128)(2,1)S(1)}, bf16[384,128]{1,0:T(8,128)(2,1)S(1)}, u32[]{:S(2)}, u32[]{:S(2)}) %collective-permute-start.1) | collective-permute-done | bytes 98336 | tf_op jit(solution)/shard_map/ppermute | solution.py:44
  90.5 2.7 %collective-permute-done.2.q2 = bf16[384,128]{1,0:T(8,128)(2,1)S(1)} collective-permute-done((bf16[384,128]{1,0:T(8,128)(2,1)S(1)}, bf16[384,128]{1,0:T(8,128)(2,1)S(1)}, u32[]{:S(2)}, u32[]{:S(2)}) %collective-permute-start.2) | collective-permute-done | bytes 98336 | tf_op jit(solution)/shard_map/ppermute | solution.py:44
  93.2 0.0 collective-permute-done.3.q3
  93.2 0.0 all-to-all-done.2.kv_ref
  93.2 0.0 copy-start
  93.2 0.0 copy-done.16
  93.2 0.6 copy-done.17
  93.8 0.0 copy-done.18
  93.8 0.5 copy-done
  94.3 6.2 %attend.1 = bf16[4,4,72,128]{3,2,1,0:T(8,128)(2,1)} custom-call(s32[1,1]{1,0:T(1,128)} %bitcast.9.place_ref, f32[1,1]{1,0:T(1,128)} %bitcast.15.bias_ref, bf16[384,128]{1,0:T(8,128)(2,1)} %get-tuple-element.9.q0, bf16[384,128]{1,0:T(8,128)(2,1)} %copy-done.16, bf16[384,128]{1,0:T(8,128)(2,1)} %copy-done.17, bf16[384,128]{1,0:T(8,128)(2,1)} %copy-done.18, ...), custom_call_target="tpu_custom_call" | custom-call | tf_op jit(solution)/shard_map/attend/pallas_call | solution.py:331
  100.5 7.6 %all-to-all-start.3 = ((bf16[16,72,128]{2,1,0:T(8,128)(2,1)}), bf16[16,72,128]{2,1,0:T(8,128)(2,1)S(1)}, u32[]{:S(2)}, u32[]{:S(2)}) async-start(bf16[16,72,128]{2,1,0:T(8,128)(2,1)} %bitcast.16), calls=%async_computation.3 | async-start | bytes 589824 | tf_op jit(solution)/shard_map/all_to_all | solution.py:26
  108.1 2.0 %collective-permute-start.4 = (bf16[128,2048]{1,0:T(8,128)(2,1)S(1)}, bf16[128,2048]{1,0:T(8,128)(2,1)S(1)}, u32[]{:S(2)}, u32[]{:S(2)}) collective-permute-start(bf16[128,2048]{1,0:T(8,128)(2,1)S(1)} %copy-done.6), channel_id=1, source_target_pairs={{0,1},{1,0},{2,3},{3,2},{4,5},{5,4},{6,7},{7,6},{8,9},{9,8},{10,11... | collective-permute-start | bytes 1572872 | tf_op jit(solution)/shard_map/ppermute | solution.py:44
  110.1 0.0 collective-permute-done.5.refs_2_
  110.2 0.0 copy-start.7
  110.2 2.3 %collective-permute-start.6 = (bf16[128,2048]{1,0:T(8,128)(2,1)S(1)}, bf16[128,2048]{1,0:T(8,128)(2,1)S(1)}, u32[]{:S(2)}, u32[]{:S(2)}) collective-permute-start(bf16[128,2048]{1,0:T(8,128)(2,1)S(1)} %collective-permute-done.5.refs_2_), channel_id=1, source_target_pairs={{0,1},{1,0},{2,3},{3,2},{4,5},{5,4},{6,7},{7,6},{8,9},{9,8},{10,11... | collective-permute-start | bytes 1572872 | tf_op jit(solution)/shard_map/ppermute | solution.py:44
  112.5 0.0 collective-permute-done.4.refs_1_
  112.5 0.0 copy-start.8
  112.5 1.5 %collective-permute-done.6.refs_3_ = bf16[128,2048]{1,0:T(8,128)(2,1)S(1)} collective-permute-done((bf16[128,2048]{1,0:T(8,128)(2,1)S(1)}, bf16[128,2048]{1,0:T(8,128)(2,1)S(1)}, u32[]{:S(2)}, u32[]{:S(2)}) %collective-permute-start.6) | collective-permute-done | bytes 524320 | tf_op jit(solution)/shard_map/ppermute | solution.py:44
  114.0 6.1 %all-to-all-done.3 = bf16[16,72,128]{2,1,0:T(8,128)(2,1)S(1)} async-done(((bf16[16,72,128]{2,1,0:T(8,128)(2,1)}), bf16[16,72,128]{2,1,0:T(8,128)(2,1)S(1)}, u32[]{:S(2)}, u32[]{:S(2)}) %all-to-all-start.3) | async-done | bytes 294944 | tf_op jit(solution)/shard_map/all_to_all | solution.py:26
  120.1 0.0 copy-done.7
  120.1 0.0 copy-done.8
  120.1 0.0 copy-done.9
  120.1 0.7 copy-done.2
  120.8 3.7 %merge.1 = bf16[4,16,2048]{2,1,0:T(8,128)(2,1)} custom-call(s32[1,2]{1,0:T(1,128)} %add_bitcast_fusion.at_ref, bf16[4,4,72,128]{3,2,1,0:T(8,128)(2,1)} %bitcast.17, bf16[128,2048]{1,0:T(8,128)(2,1)} %refs_0_.1, bf16[128,2048]{1,0:T(8,128)(2,1)} %copy-done.8, bf16[128,2048]{1,0:T(8,128)(2,1)} %copy-done.7, bf16[128,2048]{1,0:T(8,128)(2,1)} %copy-done.9), custom_call_target="tpu_custom_call" | custom-call | tf_op jit(solution)/shard_map/merge/pallas_call | solution.py:334
  124.5 14.8 %all_to_all.25 = bf16[4,16,2048]{2,1,0:T(8,128)(2,1)S(1)} all-to-all(bf16[4,16,2048]{2,1,0:T(8,128)(2,1)} %merge.1), channel_id=1, replica_groups=mesh['za'=4,'zb'=2,'x'=4,'ya'=4,'yb'=2,'c'=2] {'ya'}, dimensions={0} | all-to-all | bytes 524288 | tf_op jit(solution)/shard_map/all_to_all | solution.py:26
  139.4 0.0 copy-done.12
  139.4 0.0 copy-done.19
  139.4 0.7 add_convert_fusion
  (17 shorter events, 0.1 us)
Async XLA Ops:
  0.0 34.2 %copy-start.10 = (bf16[2048,64]{0,1:T(8,128)(2,1)S(1)}, bf16[2048,64]{0,1:T(8,128)(2,1)}, u32[]{:S(2)}) copy-start(bf16[2048,64]{0,1:T(8,128)(2,1)} %param.26) | copy-start | bytes 786436
  0.0 34.5 %copy-start.11 = (bf16[2048,64]{0,1:T(8,128)(2,1)S(1)}, bf16[2048,64]{0,1:T(8,128)(2,1)}, u32[]{:S(2)}) copy-start(bf16[2048,64]{0,1:T(8,128)(2,1)} %param.28) | copy-start | bytes 786436
  0.0 34.8 %copy-start.13 = (bf16[512,128]{1,0:T(8,128)(2,1)S(1)}, bf16[512,128]{1,0:T(8,128)(2,1)}, u32[]{:S(2)}) copy-start(bf16[512,128]{1,0:T(8,128)(2,1)} %param.31) | copy-start | bytes 393220
  0.0 34.8 %copy-start.14 = (bf16[512,128]{1,0:T(8,128)(2,1)S(1)}, bf16[512,128]{1,0:T(8,128)(2,1)}, u32[]{:S(2)}) copy-start(bf16[512,128]{1,0:T(8,128)(2,1)} %param.30) | copy-start | bytes 393220
  1.9 23.1 %all-to-all-start = ((f32[32,5,128]{2,1,0:T(8,128)}), f32[32,5,128]{2,1,0:T(8,128)S(1)}, u32[]{:S(2)}, u32[]{:S(2)}) async-start(f32[32,5,128]{2,1,0:T(8,128)} %front.1), calls=%async_computation | async-start | bytes 262144 | tf_op jit(solution)/shard_map/all_to_all | solution.py:26
  17.8 40.1 %copy-start.4 = (bf16[2048,128]{1,0:T(8,128)(2,1)S(1)}, bf16[2048,128]{1,0:T(8,128)(2,1)}, u32[]{:S(2)}) copy-start(bf16[2048,128]{1,0:T(8,128)(2,1)} %param.25) | copy-start | bytes 1572868
  24.9 0.6 copy-start.5
  27.4 23.8 %all-to-all-start.1 = ((bf16[8,16,2304]{2,1,0:T(8,128)(2,1)}), bf16[8,16,2304]{2,1,0:T(8,128)(2,1)S(1)}, u32[]{:S(2)}, u32[]{:S(2)}) async-start(bf16[8,16,2304]{2,1,0:T(8,128)(2,1)} %pack.1), calls=%async_computation.1 | async-start | bytes 1179648 | tf_op jit(solution)/shard_map/all_to_all | solution.py:26
  51.2 8.0 %copy-start.1 = (bf16[8,16,2304]{2,1,0:T(8,128)(2,1)}, bf16[8,16,2304]{2,1,0:T(8,128)(2,1)S(1)}, u32[]{:S(2)}) copy-start(bf16[8,16,2304]{2,1,0:T(8,128)(2,1)S(1)} %all-to-all-done.1.own_ref) | copy-start | bytes 1769476
  51.2 8.0 %collective-permute-start = (bf16[8,16,2304]{2,1,0:T(8,128)(2,1)S(1)}, bf16[8,16,2304]{2,1,0:T(8,128)(2,1)S(1)}, u32[]{:S(2)}, u32[]{:S(2)}) collective-permute-start(bf16[8,16,2304]{2,1,0:T(8,128)(2,1)S(1)} %all-to-all-done.1.own_ref), channel_id=1, source_target_pairs={{0,1},{1,0},{2,3},{3,2},{4,5},{5,4},{6,7},{7,6},{8,9},{9,8},{10,11... | collective-permute-start | bytes 1769480 | tf_op jit(solution)/shard_map/ppermute | solution.py:44
  59.1 0.8 copy-start.3
  65.5 3.7 %copy-start.6 = (bf16[128,2048]{1,0:T(8,128)(2,1)S(1)}, bf16[128,2048]{1,0:T(8,128)(2,1)}, u32[]{:S(2)}) copy-start(bf16[128,2048]{1,0:T(8,128)(2,1)} %refs_0_.1) | copy-start | bytes 1572868
  65.6 5.9 %copy-start.15 = (bf16[384,128]{1,0:T(8,128)(2,1)S(1)}, bf16[384,128]{1,0:T(8,128)(2,1)}, u32[]{:S(2)}) copy-start(bf16[384,128]{1,0:T(8,128)(2,1)} %get-tuple-element.9.q0) | copy-start | bytes 294916
  65.6 27.6 %all-to-all-start.2 = ((bf16[8,688,128]{2,1,0:T(8,128)(2,1)}), bf16[8,688,128]{2,1,0:T(8,128)(2,1)S(1)}, u32[]{:S(2)}, u32[]{:S(2)}) async-start(bf16[8,688,128]{2,1,0:T(8,128)(2,1)} %get-tuple-element.10), calls=%async_computation.2 | async-start | bytes 2818048 | tf_op jit(solution)/shard_map/all_to_all | solution.py:26
  69.3 40.9 %collective-permute-start.5 = (bf16[128,2048]{1,0:T(8,128)(2,1)S(1)}, bf16[128,2048]{1,0:T(8,128)(2,1)S(1)}, u32[]{:S(2)}, u32[]{:S(2)}) collective-permute-start(bf16[128,2048]{1,0:T(8,128)(2,1)S(1)} %copy-done.6), channel_id=1, source_target_pairs={{0,2},{2,0},{1,3},{3,1},{4,6},{6,4},{5,7},{7,5},{8,10},{10,8},{9,1... | collective-permute-start | bytes 1572872 | tf_op jit(solution)/shard_map/ppermute | solution.py:44
  71.5 18.9 %collective-permute-start.1 = (bf16[384,128]{1,0:T(8,128)(2,1)S(1)}, bf16[384,128]{1,0:T(8,128)(2,1)S(1)}, u32[]{:S(2)}, u32[]{:S(2)}) collective-permute-start(bf16[384,128]{1,0:T(8,128)(2,1)S(1)} %copy-done.15), channel_id=1, source_target_pairs={{0,128},{128,256},{256,384},{384,0},{1,129},{129,257},{257,385},{3... | collective-permute-start | bytes 294920 | tf_op jit(solution)/shard_map/ppermute | solution.py:44
  74.4 18.7 %collective-permute-start.2 = (bf16[384,128]{1,0:T(8,128)(2,1)S(1)}, bf16[384,128]{1,0:T(8,128)(2,1)S(1)}, u32[]{:S(2)}, u32[]{:S(2)}) collective-permute-start(bf16[384,128]{1,0:T(8,128)(2,1)S(1)} %copy-done.15), channel_id=1, source_target_pairs={{0,256},{128,384},{256,0},{384,128},{1,257},{129,385},{257,1},{385... | collective-permute-start | bytes 294920 | tf_op jit(solution)/shard_map/ppermute | solution.py:44
  77.9 15.2 %collective-permute-start.3 = (bf16[384,128]{1,0:T(8,128)(2,1)S(1)}, bf16[384,128]{1,0:T(8,128)(2,1)S(1)}, u32[]{:S(2)}, u32[]{:S(2)}) collective-permute-start(bf16[384,128]{1,0:T(8,128)(2,1)S(1)} %copy-done.15), channel_id=1, source_target_pairs={{0,384},{128,0},{256,128},{384,256},{1,385},{129,1},{257,129},{385... | collective-permute-start | bytes 294920 | tf_op jit(solution)/shard_map/ppermute | solution.py:44
  90.5 2.7 %copy-start.16 = (bf16[384,128]{1,0:T(8,128)(2,1)}, bf16[384,128]{1,0:T(8,128)(2,1)S(1)}, u32[]{:S(2)}) copy-start(bf16[384,128]{1,0:T(8,128)(2,1)S(1)} %collective-permute-done.1.q1) | copy-start | bytes 294916
  93.2 0.6 copy-start.17
  93.2 0.7 copy-start.18
  93.2 1.2 copy-start
  100.5 38.8 %copy-start.12 = (bf16[16,2048]{1,0:T(8,128)(2,1)S(1)}, bf16[16,2048]{1,0:T(8,128)(2,1)}, u32[]{:S(2)}) copy-start(bf16[16,2048]{1,0:T(8,128)(2,1)} %param.17) | copy-start | bytes 196612
  100.5 38.8 %copy-start.19 = (f32[1,2048]{1,0:T(1,128)S(1)}, f32[1,2048]{1,0:T(1,128)}, u32[]{:S(2)}) copy-start(f32[1,2048]{1,0:T(1,128)} %get-tuple-element.8) | copy-start | bytes 24580
  100.5 19.5 %all-to-all-start.3 = ((bf16[16,72,128]{2,1,0:T(8,128)(2,1)}), bf16[16,72,128]{2,1,0:T(8,128)(2,1)S(1)}, u32[]{:S(2)}, u32[]{:S(2)}) async-start(bf16[16,72,128]{2,1,0:T(8,128)(2,1)} %bitcast.16), calls=%async_computation.3 | async-start | bytes 589824 | tf_op jit(solution)/shard_map/all_to_all | solution.py:26
  108.1 4.4 %collective-permute-start.4 = (bf16[128,2048]{1,0:T(8,128)(2,1)S(1)}, bf16[128,2048]{1,0:T(8,128)(2,1)S(1)}, u32[]{:S(2)}, u32[]{:S(2)}) collective-permute-start(bf16[128,2048]{1,0:T(8,128)(2,1)S(1)} %copy-done.6), channel_id=1, source_target_pairs={{0,1},{1,0},{2,3},{3,2},{4,5},{5,4},{6,7},{7,6},{8,9},{9,8},{10,11... | collective-permute-start | bytes 1572872 | tf_op jit(solution)/shard_map/ppermute | solution.py:44
  110.2 9.9 %copy-start.7 = (bf16[128,2048]{1,0:T(8,128)(2,1)}, bf16[128,2048]{1,0:T(8,128)(2,1)S(1)}, u32[]{:S(2)}) copy-start(bf16[128,2048]{1,0:T(8,128)(2,1)S(1)} %collective-permute-done.5.refs_2_) | copy-start | bytes 1572868
  110.2 3.8 %collective-permute-start.6 = (bf16[128,2048]{1,0:T(8,128)(2,1)S(1)}, bf16[128,2048]{1,0:T(8,128)(2,1)S(1)}, u32[]{:S(2)}, u32[]{:S(2)}) collective-permute-start(bf16[128,2048]{1,0:T(8,128)(2,1)S(1)} %collective-permute-done.5.refs_2_), channel_id=1, source_target_pairs={{0,1},{1,0},{2,3},{3,2},{4,5},{5,4},{6,7},{7,6},{8,9},{9,8},{10,11... | collective-permute-start | bytes 1572872 | tf_op jit(solution)/shard_map/ppermute | solution.py:44
  112.5 7.6 %copy-start.8 = (bf16[128,2048]{1,0:T(8,128)(2,1)}, bf16[128,2048]{1,0:T(8,128)(2,1)S(1)}, u32[]{:S(2)}) copy-start(bf16[128,2048]{1,0:T(8,128)(2,1)S(1)} %collective-permute-done.4.refs_1_) | copy-start | bytes 1572868
  114.0 6.1 %copy-start.9 = (bf16[128,2048]{1,0:T(8,128)(2,1)}, bf16[128,2048]{1,0:T(8,128)(2,1)S(1)}, u32[]{:S(2)}) copy-start(bf16[128,2048]{1,0:T(8,128)(2,1)S(1)} %collective-permute-done.6.refs_3_) | copy-start | bytes 1572868
  120.1 0.8 copy-start.2

commit v10 on v9

--- a/solution.py
+++ b/solution.py
@@ -164,46 +164,52 @@
         vc_ref[at, :] = kv_ref[i, count + tok : 2 * count]
     dims = (((1,), (1,)), ((), ()))
     step = factor * LOG2E
-    bias = bias_ref[0, 0] * LOG2E
+    bias = bias_ref[0, 0] * (1.0 / factor)
     blocks = (q0, q1, q2, q3)
     size = len(blocks)
     values = [kv_ref[i, count : count + tok] for i in range(n_blocks)] + [vc_ref[...]]
     quarter = tok // 4
 
-    def scored(block):
-        turned = jnp.concatenate([block[tok:, :rope], block[tok:, rope:]], axis=0)
-        q = jnp.concatenate([block[:tok, :], turned], axis=1)
-        scores = [lax.dot_general(q, k_ref[i], dims, preferred_element_type=F32) * step for i in range(n_blocks)]
-        return scores + [lax.dot_general(q, kc_ref[...], dims, preferred_element_type=F32) * step + bias]
-
-    ready = scored(blocks[0])
-    for k in range(size):
+    def scored(pair):
+        pieces = []
+        for block in pair:
+            turned = jnp.concatenate([block[tok:, :rope], block[tok:, rope:]], axis=0)
+            pieces.append(jnp.concatenate([block[:tok, :], turned], axis=1))
+        q = jnp.concatenate(pieces, axis=0)
+        scores = [lax.dot_general(q, k_ref[i], dims, preferred_element_type=F32) for i in range(n_blocks)]
+        return scores + [lax.dot_general(q, kc_ref[...], dims, preferred_element_type=F32) + bias]
+
+    ready = scored(blocks[:2])
+    for first in range(0, size, 2):
         scores = ready
-        if k + 1 < size:
-            ready = scored(blocks[k + 1])
+        if first + 2 < size:
+            ready = scored(blocks[first + 2 : first + 4])
         widest = functools.reduce(jnp.maximum, scores[:-1])
         top = jnp.maximum(jnp.max(widest, axis=1, keepdims=True), jnp.max(scores[-1], axis=1, keepdims=True))
-        weights = [jnp.exp2(s - top) for s in scores]
+        weights = [jnp.exp2((s - top) * step) for s in scores]
         total = jnp.sum(functools.reduce(jnp.add, weights[:-1]), axis=1, keepdims=True) + jnp.sum(weights[-1], axis=1, keepdims=True)
         out = functools.reduce(
             jnp.add, [jnp.dot(w.astype(BF16), v, preferred_element_type=F32) for w, v in zip(weights, values, strict=True)]
         )
         out = (out / total).astype(BF16)
-        lse = jnp.transpose(jnp.broadcast_to(top + jnp.log2(total), (tok, lanes)))[:8]
+        lse = jnp.transpose(jnp.broadcast_to(top * step + jnp.log2(total), (2 * tok, lanes)))[:8]
         high = lse.astype(BF16).astype(F32)
         middle = (lse - high).astype(BF16).astype(F32)
         row = lax.broadcasted_iota(jnp.int32, lse.shape, 0)
         stats = jnp.where(row == 0, high, jnp.where(row == 1, middle, jnp.where(row == 2, lse - high - middle, 0.0))).astype(BF16)
-        to = (place_ref[0, 0] + (size - k)) % size
-        for part in range(4):
-            at = part * quarter
-            o_ref[to, part, :quarter, :] = out[at : at + quarter]
-            o_ref[to, part, quarter:, :quarter] = stats[:, at : at + quarter]
-            o_ref[to, part, quarter:, quarter:] = jnp.zeros((8, lanes - quarter), BF16)
-
-
-def merge_kernel(at_ref, got_ref, *refs):
-    hbm, o_ref, w_ref, sems = refs[:4], refs[4], refs[5], refs[6:]
+        for k in range(2):
+            to = (place_ref[0, 0] + (size - first - k)) % size
+            for part in range(4):
+                at = k * tok + part * quarter
+                o_ref[to, part, :quarter, :] = out[at : at + quarter]
+                o_ref[to, part, quarter:, :quarter] = stats[:, at : at + quarter]
+                o_ref[to, part, quarter:, quarter:] = jnp.zeros((8, lanes - quarter), BF16)
+
+
+def merge_kernel(at_ref, got_hbm, *refs):
+    hbm, o_ref, w_ref, got_ref, sems, got_sem = refs[:4], refs[4], refs[5], refs[6], refs[7:11], refs[11]
+    got_load = pltpu.make_async_copy(got_hbm, got_ref, got_sem)
+    got_load.start()
     deep = hbm[0].shape[0]
     loads = [
         pltpu.make_async_copy(src, w_ref.at[pl.ds(i * deep, deep)], sem) for i, (src, sem) in enumerate(zip(hbm, sems, strict=True))
@@ -215,6 +221,7 @@
     n_ya, rows, width = o_ref.shape
     core, yb = at_ref[0, 0], at_ref[0, 1]
     sources = [(yb + i) % 2 * 2 + (core + j) % 2 for i in range(2) for j in range(2)]
+    got_load.wait()
     shares = []
     for source in sources:
         lse = [jnp.sum(got_ref[i, source, quarter:, :].astype(F32), axis=0, keepdims=True) for i in range(n_q)]
@@ -333,10 +340,14 @@
     got = exchanged(out.reshape(n_q * 2 * n_c, quarter + 8, vsize), (Q_AXIS, "yb", "c"))
     term = pl.pallas_call(
         merge_kernel,
-        in_specs=[smem, vmem] + [any_space] * 4,
+        in_specs=[smem] + [any_space] * 5,
         out_specs=vmem,
         out_shape=jax.ShapeDtypeStruct((n_ya, rows, width), BF16),
-        scratch_shapes=[pltpu.VMEM((4 * w_out.shape[0], width), BF16)] + [pltpu.SemaphoreType.DMA] * 4,
+        scratch_shapes=[
+            pltpu.VMEM((4 * w_out.shape[0], width), BF16),
+            pltpu.VMEM((n_q, 2 * n_c, quarter + 8, vsize), BF16),
+        ]
+        + [pltpu.SemaphoreType.DMA] * 5,
         name="merge",
     )(at, got.reshape(n_q, 2 * n_c, quarter + 8, vsize), w_out, w_other, w_near, w_far)
     branch = jnp.sum(exchanged(term, ("ya",)).astype(F32), axis=0)

time: 141 us -> 140 us (level)
  no operation moved by 1% of the time
where the time goes in v10:
time: 140 us; the launch traced here: 139 us
  starting transfers between devices  53.5 us (38%)
  waiting for transfers between devices  40.8 us (29%)
  Pallas kernels  18.5 us (13%)
  blocking collectives  14.8 us (11%)
  other arithmetic  6.85 us (5%)
  local copies, waits for them, and re-layouts  3.96 us (3%)
    all_to_all x4, starting transfers between devices, exchanged(): return lax.all_to_all(array, axes, 0, 0, tiled=True)  31.8 us
    all_to_all x4, waiting for transfers between devices, exchanged(): return lax.all_to_all(array, axes, 0, 0, tiled=True)  28.8 us
    ppermute x7, starting transfers between devices, shifted(): return lax.ppermute(array, axis, [(i, (i + k) % n) for i in range(n)])  21.7 us
    all_to_all x1, blocking collectives, exchanged(): return lax.all_to_all(array, axes, 0, 0, tiled=True)  14.8 us
    ppermute x7, waiting for transfers between devices, shifted(): return lax.ppermute(array, axis, [(i, (i + k) % n) for i in range(n)])  12.1 us
    pallas_call x1, Pallas kernels, step(): out = attend(to, ctx_bias.reshape(1, 1), *queries, kv)  5.62 us
    pallas_call x1, Pallas kernels, step(): project(at, mine, other, norm_gain.reshape(1, width), kv_gain.reshape(1,...  5.57 us
    unnamed x42, local copies, waits for them, and re-layouts  3.96 us
  transfers between devices with their start and end apart: 11, of which 6 were waited for; matrix products, arithmetic and copies ran while one was open for 5% of the time, Pallas kernels for 4%

profile of v10, /device:TPU:1, one launch (start us, length us, event | category | flops | bytes accessed | tf_op | source)
XLA Modules:
  0.0 139.4 jit_solution(5973716638799891517)
XLA Ops:
  0.0 0.0 copy-start.11
  0.0 0.0 copy-start.14
  0.0 1.8 %front.1 = f32[32,5,128]{2,1,0:T(8,128)} custom-call(s32[1,1]{1,0:T(1,128)} %bitcast.3.at_ref, f32[16,128]{1,0:T(8,128)} %bitcast.20, f32[16,128]{1,0:T(8,128)} %bitcast.21, f32[64,128]{1,0:T(8,128)} %shift_ref.1, f32[64,128]{1,0:T(8,128)} %scale_ref.1, f32[64,128]{1,0:T(8,128)} %gate_ref.1), custom_call_target="tpu_custom_call" | custom-call | tf_op jit(solution)/shard_map/front/pallas_call | solution.py:264
  1.9 13.7 %all-to-all-start = ((f32[32,5,128]{2,1,0:T(8,128)}), f32[32,5,128]{2,1,0:T(8,128)S(1)}, u32[]{:S(2)}, u32[]{:S(2)}) async-start(f32[32,5,128]{2,1,0:T(8,128)} %front.1), calls=%async_computation | async-start | bytes 262144 | tf_op jit(solution)/shard_map/all_to_all | solution.py:26
  15.6 0.7 reduce
  16.3 1.5 %pad_maximum_fusion.2.block_ref = bf16[16,2176]{1,0:T(8,128)(2,1)} fusion(bf16[16,128]{1,0:T(8,128)(2,1)S(1)} %bitcast.18, bf16[16,2048]{1,0:T(8,128)(2,1)} %param.17), kind=kLoop, calls=%fused_computation.7 | loop fusion | flops 139264 | bytes 139264 | tf_op jit(solution)/shard_map/concatenate | solution.py:273
  17.8 7.1 %all-to-all-done.sums_ref = f32[32,5,128]{2,1,0:T(8,128)S(1)} async-done(((f32[32,5,128]{2,1,0:T(8,128)}), f32[32,5,128]{2,1,0:T(8,128)S(1)}, u32[]{:S(2)}, u32[]{:S(2)}) %all-to-all-start) | async-done | bytes 81952 | tf_op jit(solution)/shard_map/all_to_all | solution.py:26
  24.9 0.6 copy-done.5
  25.6 1.8 %pack.1 = bf16[8,16,2304]{2,1,0:T(8,128)(2,1)} custom-call(f32[32,5,128]{2,1,0:T(8,128)} %copy-done.5, bf16[16,2176]{1,0:T(8,128)(2,1)} %pad_maximum_fusion.2.block_ref), custom_call_target="tpu_custom_call" | custom-call | tf_op jit(solution)/shard_map/pack/pallas_call | solution.py:284
  27.4 6.8 %all-to-all-start.1 = ((bf16[8,16,2304]{2,1,0:T(8,128)(2,1)}), bf16[8,16,2304]{2,1,0:T(8,128)(2,1)S(1)}, u32[]{:S(2)}, u32[]{:S(2)}) async-start(bf16[8,16,2304]{2,1,0:T(8,128)(2,1)} %pack.1), calls=%async_computation.1 | async-start | bytes 1179648 | tf_op jit(solution)/shard_map/all_to_all | solution.py:26
  34.2 0.0 copy-done.10
  34.2 0.3 copy.18
  34.5 0.0 copy-done.11
  34.5 0.3 copy.19
  34.8 0.0 copy-done.13
  34.8 0.0 copy-done.14
  34.9 0.7 pad_maximum_fusion.1.w_up_hbm
  35.6 15.6 %all-to-all-done.1.own_ref = bf16[8,16,2304]{2,1,0:T(8,128)(2,1)S(1)} async-done(((bf16[8,16,2304]{2,1,0:T(8,128)(2,1)}), bf16[8,16,2304]{2,1,0:T(8,128)(2,1)S(1)}, u32[]{:S(2)}, u32[]{:S(2)}) %all-to-all-start.1) | async-done | bytes 589856 | tf_op jit(solution)/shard_map/all_to_all | solution.py:26
  51.2 4.8 %collective-permute-start = (bf16[8,16,2304]{2,1,0:T(8,128)(2,1)S(1)}, bf16[8,16,2304]{2,1,0:T(8,128)(2,1)S(1)}, u32[]{:S(2)}, u32[]{:S(2)}) collective-permute-start(bf16[8,16,2304]{2,1,0:T(8,128)(2,1)S(1)} %all-to-all-done.1.own_ref), channel_id=1, source_target_pairs={{0,1},{1,0},{2,3},{3,2},{4,5},{5,4},{6,7},{7,6},{8,9},{9,8},{10,11... | collective-permute-start | bytes 1769480 | tf_op jit(solution)/shard_map/ppermute | solution.py:44
  56.0 0.6 add_bitcast_fusion.at_ref
  56.6 1.3 sine_multiply_fusion
  57.8 0.0 copy-done.4
  57.8 1.3 pad_maximum_fusion.w_side_hbm
  59.1 0.0 collective-permute-done.other_ref
  59.1 0.0 copy-done.1
  59.1 0.8 copy-done.3
  60.0 5.6 %project.1 = (bf16[384,128]{1,0:T(8,128)(2,1)}, bf16[8,688,128]{2,1,0:T(8,128)(2,1)}, f32[1,2048]{1,0:T(1,128)}) custom-call(s32[1,2]{1,0:T(1,128)} %add_bitcast_fusion.at_ref, bf16[8,16,2304]{2,1,0:T(8,128)(2,1)} %copy-done.1, bf16[8,16,2304]{2,1,0:T(8,128)(2,1)} %copy-done.3, f32[1,2048]{1,0:T(1,128)} %bitcast.19, f32[1,512]{1,0:T(1,128)} %bitcast.23, ...), custom_call_target="tpu_custom_call" | custom-call | tf_op jit(solution)/shard_map/project/pallas_call | solution.py:319
  65.5 0.0 copy-start.6
  65.6 0.0 copy-start.15
  65.6 3.7 %all-to-all-start.2 = ((bf16[8,688,128]{2,1,0:T(8,128)(2,1)}), bf16[8,688,128]{2,1,0:T(8,128)(2,1)S(1)}, u32[]{:S(2)}, u32[]{:S(2)}) async-start(bf16[8,688,128]{2,1,0:T(8,128)(2,1)} %get-tuple-element.10), calls=%async_computation.2 | async-start | bytes 2818048 | tf_op jit(solution)/shard_map/all_to_all | solution.py:26
  69.3 0.0 copy-done.6
  69.3 2.2 %collective-permute-start.5 = (bf16[128,2048]{1,0:T(8,128)(2,1)S(1)}, bf16[128,2048]{1,0:T(8,128)(2,1)S(1)}, u32[]{:S(2)}, u32[]{:S(2)}) collective-permute-start(bf16[128,2048]{1,0:T(8,128)(2,1)S(1)} %copy-done.6), channel_id=1, source_target_pairs={{0,2},{2,0},{1,3},{3,1},{4,6},{6,4},{5,7},{7,5},{8,10},{10,8},{9,1... | collective-permute-start | bytes 1572872 | tf_op jit(solution)/shard_map/ppermute | solution.py:44
  71.5 0.0 copy-done.15
  71.5 2.9 %collective-permute-start.1 = (bf16[384,128]{1,0:T(8,128)(2,1)S(1)}, bf16[384,128]{1,0:T(8,128)(2,1)S(1)}, u32[]{:S(2)}, u32[]{:S(2)}) collective-permute-start(bf16[384,128]{1,0:T(8,128)(2,1)S(1)} %copy-done.15), channel_id=1, source_target_pairs={{0,128},{128,256},{256,384},{384,0},{1,129},{129,257},{257,385},{3... | collective-permute-start | bytes 294920 | tf_op jit(solution)/shard_map/ppermute | solution.py:44
  74.4 3.5 %collective-permute-start.2 = (bf16[384,128]{1,0:T(8,128)(2,1)S(1)}, bf16[384,128]{1,0:T(8,128)(2,1)S(1)}, u32[]{:S(2)}, u32[]{:S(2)}) collective-permute-start(bf16[384,128]{1,0:T(8,128)(2,1)S(1)} %copy-done.15), channel_id=1, source_target_pairs={{0,256},{128,384},{256,0},{384,128},{1,257},{129,385},{257,1},{385... | collective-permute-start | bytes 294920 | tf_op jit(solution)/shard_map/ppermute | solution.py:44
  77.9 4.0 %collective-permute-start.3 = (bf16[384,128]{1,0:T(8,128)(2,1)S(1)}, bf16[384,128]{1,0:T(8,128)(2,1)S(1)}, u32[]{:S(2)}, u32[]{:S(2)}) collective-permute-start(bf16[384,128]{1,0:T(8,128)(2,1)S(1)} %copy-done.15), channel_id=1, source_target_pairs={{0,384},{128,0},{256,128},{384,256},{1,385},{129,1},{257,129},{385... | collective-permute-start | bytes 294920 | tf_op jit(solution)/shard_map/ppermute | solution.py:44
  82.6 7.9 %collective-permute-done.1.q1 = bf16[384,128]{1,0:T(8,128)(2,1)S(1)} collective-permute-done((bf16[384,128]{1,0:T(8,128)(2,1)S(1)}, bf16[384,128]{1,0:T(8,128)(2,1)S(1)}, u32[]{:S(2)}, u32[]{:S(2)}) %collective-permute-start.1) | collective-permute-done | bytes 98336 | tf_op jit(solution)/shard_map/ppermute | solution.py:44
  90.5 2.7 %collective-permute-done.2.q2 = bf16[384,128]{1,0:T(8,128)(2,1)S(1)} collective-permute-done((bf16[384,128]{1,0:T(8,128)(2,1)S(1)}, bf16[384,128]{1,0:T(8,128)(2,1)S(1)}, u32[]{:S(2)}, u32[]{:S(2)}) %collective-permute-start.2) | collective-permute-done | bytes 98336 | tf_op jit(solution)/shard_map/ppermute | solution.py:44
  93.2 0.0 collective-permute-done.3.q3
  93.2 0.0 all-to-all-done.2.kv_ref
  93.2 0.0 copy-start
  93.2 0.0 copy-done.16
  93.2 0.6 copy-done.17
  93.8 0.0 copy-done.18
  93.8 0.5 copy-done
  94.3 5.6 %attend.1 = bf16[4,4,72,128]{3,2,1,0:T(8,128)(2,1)} custom-call(s32[1,1]{1,0:T(1,128)} %bitcast.9.place_ref, f32[1,1]{1,0:T(1,128)} %bitcast.15.bias_ref, bf16[384,128]{1,0:T(8,128)(2,1)} %get-tuple-element.9.q0, bf16[384,128]{1,0:T(8,128)(2,1)} %copy-done.16, bf16[384,128]{1,0:T(8,128)(2,1)} %copy-done.17, bf16[384,128]{1,0:T(8,128)(2,1)} %copy-done.18, ...), custom_call_target="tpu_custom_call" | custom-call | tf_op jit(solution)/shard_map/attend/pallas_call | solution.py:338
  100.0 7.6 %all-to-all-start.3 = ((bf16[16,72,128]{2,1,0:T(8,128)(2,1)}), bf16[16,72,128]{2,1,0:T(8,128)(2,1)S(1)}, u32[]{:S(2)}, u32[]{:S(2)}) async-start(bf16[16,72,128]{2,1,0:T(8,128)(2,1)} %bitcast.16), calls=%async_computation.3 | async-start | bytes 589824 | tf_op jit(solution)/shard_map/all_to_all | solution.py:26
  107.5 2.0 %collective-permute-start.4 = (bf16[128,2048]{1,0:T(8,128)(2,1)S(1)}, bf16[128,2048]{1,0:T(8,128)(2,1)S(1)}, u32[]{:S(2)}, u32[]{:S(2)}) collective-permute-start(bf16[128,2048]{1,0:T(8,128)(2,1)S(1)} %copy-done.6), channel_id=1, source_target_pairs={{0,1},{1,0},{2,3},{3,2},{4,5},{5,4},{6,7},{7,6},{8,9},{9,8},{10,11... | collective-permute-start | bytes 1572872 | tf_op jit(solution)/shard_map/ppermute | solution.py:44
  109.6 0.0 collective-permute-done.5.refs_2_
  109.6 0.0 copy-start.7
  109.6 2.3 %collective-permute-start.6 = (bf16[128,2048]{1,0:T(8,128)(2,1)S(1)}, bf16[128,2048]{1,0:T(8,128)(2,1)S(1)}, u32[]{:S(2)}, u32[]{:S(2)}) collective-permute-start(bf16[128,2048]{1,0:T(8,128)(2,1)S(1)} %collective-permute-done.5.refs_2_), channel_id=1, source_target_pairs={{0,1},{1,0},{2,3},{3,2},{4,5},{5,4},{6,7},{7,6},{8,9},{9,8},{10,11... | collective-permute-start | bytes 1572872 | tf_op jit(solution)/shard_map/ppermute | solution.py:44
  111.9 0.0 collective-permute-done.4.refs_1_
  111.9 0.0 copy-start.8
  111.9 1.5 %collective-permute-done.6.refs_3_ = bf16[128,2048]{1,0:T(8,128)(2,1)S(1)} collective-permute-done((bf16[128,2048]{1,0:T(8,128)(2,1)S(1)}, bf16[128,2048]{1,0:T(8,128)(2,1)S(1)}, u32[]{:S(2)}, u32[]{:S(2)}) %collective-permute-start.6) | collective-permute-done | bytes 524320 | tf_op jit(solution)/shard_map/ppermute | solution.py:44
  113.4 6.1 %all-to-all-done.3 = bf16[16,72,128]{2,1,0:T(8,128)(2,1)S(1)} async-done(((bf16[16,72,128]{2,1,0:T(8,128)(2,1)}), bf16[16,72,128]{2,1,0:T(8,128)(2,1)S(1)}, u32[]{:S(2)}, u32[]{:S(2)}) %all-to-all-start.3) | async-done | bytes 294944 | tf_op jit(solution)/shard_map/all_to_all | solution.py:26
  119.5 0.0 copy-done.7
  119.5 0.0 copy-done.8
  119.5 0.0 copy-done.9
  119.5 0.7 copy-done.2
  120.2 3.7 %merge.1 = bf16[4,16,2048]{2,1,0:T(8,128)(2,1)} custom-call(s32[1,2]{1,0:T(1,128)} %add_bitcast_fusion.at_ref, bf16[4,4,72,128]{3,2,1,0:T(8,128)(2,1)} %bitcast.17, bf16[128,2048]{1,0:T(8,128)(2,1)} %refs_0_.1, bf16[128,2048]{1,0:T(8,128)(2,1)} %copy-done.8, bf16[128,2048]{1,0:T(8,128)(2,1)} %copy-done.7, bf16[128,2048]{1,0:T(8,128)(2,1)} %copy-done.9), custom_call_target="tpu_custom_call" | custom-call | tf_op jit(solution)/shard_map/merge/pallas_call | solution.py:341
  123.9 14.8 %all_to_all.25 = bf16[4,16,2048]{2,1,0:T(8,128)(2,1)S(1)} all-to-all(bf16[4,16,2048]{2,1,0:T(8,128)(2,1)} %merge.1), channel_id=1, replica_groups=mesh['za'=4,'zb'=2,'x'=4,'ya'=4,'yb'=2,'c'=2] {'ya'}, dimensions={0} | all-to-all | bytes 524288 | tf_op jit(solution)/shard_map/all_to_all | solution.py:26
  138.8 0.0 copy-done.12
  138.8 0.0 copy-done.19
  138.8 0.7 add_convert_fusion
  (17 shorter events, 0.1 us)
Async XLA Ops:
  0.0 34.2 %copy-start.10 = (bf16[2048,64]{0,1:T(8,128)(2,1)S(1)}, bf16[2048,64]{0,1:T(8,128)(2,1)}, u32[]{:S(2)}) copy-start(bf16[2048,64]{0,1:T(8,128)(2,1)} %param.26) | copy-start | bytes 786436
  0.0 34.5 %copy-start.11 = (bf16[2048,64]{0,1:T(8,128)(2,1)S(1)}, bf16[2048,64]{0,1:T(8,128)(2,1)}, u32[]{:S(2)}) copy-start(bf16[2048,64]{0,1:T(8,128)(2,1)} %param.28) | copy-start | bytes 786436
  0.0 34.8 %copy-start.13 = (bf16[512,128]{1,0:T(8,128)(2,1)S(1)}, bf16[512,128]{1,0:T(8,128)(2,1)}, u32[]{:S(2)}) copy-start(bf16[512,128]{1,0:T(8,128)(2,1)} %param.31) | copy-start | bytes 393220
  0.0 34.8 %copy-start.14 = (bf16[512,128]{1,0:T(8,128)(2,1)S(1)}, bf16[512,128]{1,0:T(8,128)(2,1)}, u32[]{:S(2)}) copy-start(bf16[512,128]{1,0:T(8,128)(2,1)} %param.30) | copy-start | bytes 393220
  1.9 23.1 %all-to-all-start = ((f32[32,5,128]{2,1,0:T(8,128)}), f32[32,5,128]{2,1,0:T(8,128)S(1)}, u32[]{:S(2)}, u32[]{:S(2)}) async-start(f32[32,5,128]{2,1,0:T(8,128)} %front.1), calls=%async_computation | async-start | bytes 262144 | tf_op jit(solution)/shard_map/all_to_all | solution.py:26
  17.8 40.1 %copy-start.4 = (bf16[2048,128]{1,0:T(8,128)(2,1)S(1)}, bf16[2048,128]{1,0:T(8,128)(2,1)}, u32[]{:S(2)}) copy-start(bf16[2048,128]{1,0:T(8,128)(2,1)} %param.25) | copy-start | bytes 1572868
  24.9 0.6 copy-start.5
  27.4 23.8 %all-to-all-start.1 = ((bf16[8,16,2304]{2,1,0:T(8,128)(2,1)}), bf16[8,16,2304]{2,1,0:T(8,128)(2,1)S(1)}, u32[]{:S(2)}, u32[]{:S(2)}) async-start(bf16[8,16,2304]{2,1,0:T(8,128)(2,1)} %pack.1), calls=%async_computation.1 | async-start | bytes 1179648 | tf_op jit(solution)/shard_map/all_to_all | solution.py:26
  51.2 8.0 %copy-start.1 = (bf16[8,16,2304]{2,1,0:T(8,128)(2,1)}, bf16[8,16,2304]{2,1,0:T(8,128)(2,1)S(1)}, u32[]{:S(2)}) copy-start(bf16[8,16,2304]{2,1,0:T(8,128)(2,1)S(1)} %all-to-all-done.1.own_ref) | copy-start | bytes 1769476
  51.2 8.0 %collective-permute-start = (bf16[8,16,2304]{2,1,0:T(8,128)(2,1)S(1)}, bf16[8,16,2304]{2,1,0:T(8,128)(2,1)S(1)}, u32[]{:S(2)}, u32[]{:S(2)}) collective-permute-start(bf16[8,16,2304]{2,1,0:T(8,128)(2,1)S(1)} %all-to-all-done.1.own_ref), channel_id=1, source_target_pairs={{0,1},{1,0},{2,3},{3,2},{4,5},{5,4},{6,7},{7,6},{8,9},{9,8},{10,11... | collective-permute-start | bytes 1769480 | tf_op jit(solution)/shard_map/ppermute | solution.py:44
  59.1 0.8 copy-start.3
  65.5 3.7 %copy-start.6 = (bf16[128,2048]{1,0:T(8,128)(2,1)S(1)}, bf16[128,2048]{1,0:T(8,128)(2,1)}, u32[]{:S(2)}) copy-start(bf16[128,2048]{1,0:T(8,128)(2,1)} %refs_0_.1) | copy-start | bytes 1572868
  65.6 5.9 %copy-start.15 = (bf16[384,128]{1,0:T(8,128)(2,1)S(1)}, bf16[384,128]{1,0:T(8,128)(2,1)}, u32[]{:S(2)}) copy-start(bf16[384,128]{1,0:T(8,128)(2,1)} %get-tuple-element.9.q0) | copy-start | bytes 294916
  65.6 27.6 %all-to-all-start.2 = ((bf16[8,688,128]{2,1,0:T(8,128)(2,1)}), bf16[8,688,128]{2,1,0:T(8,128)(2,1)S(1)}, u32[]{:S(2)}, u32[]{:S(2)}) async-start(bf16[8,688,128]{2,1,0:T(8,128)(2,1)} %get-tuple-element.10), calls=%async_computation.2 | async-start | bytes 2818048 | tf_op jit(solution)/shard_map/all_to_all | solution.py:26
  69.3 40.3 %collective-permute-start.5 = (bf16[128,2048]{1,0:T(8,128)(2,1)S(1)}, bf16[128,2048]{1,0:T(8,128)(2,1)S(1)}, u32[]{:S(2)}, u32[]{:S(2)}) collective-permute-start(bf16[128,2048]{1,0:T(8,128)(2,1)S(1)} %copy-done.6), channel_id=1, source_target_pairs={{0,2},{2,0},{1,3},{3,1},{4,6},{6,4},{5,7},{7,5},{8,10},{10,8},{9,1... | collective-permute-start | bytes 1572872 | tf_op jit(solution)/shard_map/ppermute | solution.py:44
  71.5 18.9 %collective-permute-start.1 = (bf16[384,128]{1,0:T(8,128)(2,1)S(1)}, bf16[384,128]{1,0:T(8,128)(2,1)S(1)}, u32[]{:S(2)}, u32[]{:S(2)}) collective-permute-start(bf16[384,128]{1,0:T(8,128)(2,1)S(1)} %copy-done.15), channel_id=1, source_target_pairs={{0,128},{128,256},{256,384},{384,0},{1,129},{129,257},{257,385},{3... | collective-permute-start | bytes 294920 | tf_op jit(solution)/shard_map/ppermute | solution.py:44
  74.4 18.7 %collective-permute-start.2 = (bf16[384,128]{1,0:T(8,128)(2,1)S(1)}, bf16[384,128]{1,0:T(8,128)(2,1)S(1)}, u32[]{:S(2)}, u32[]{:S(2)}) collective-permute-start(bf16[384,128]{1,0:T(8,128)(2,1)S(1)} %copy-done.15), channel_id=1, source_target_pairs={{0,256},{128,384},{256,0},{384,128},{1,257},{129,385},{257,1},{385... | collective-permute-start | bytes 294920 | tf_op jit(solution)/shard_map/ppermute | solution.py:44
  77.9 15.2 %collective-permute-start.3 = (bf16[384,128]{1,0:T(8,128)(2,1)S(1)}, bf16[384,128]{1,0:T(8,128)(2,1)S(1)}, u32[]{:S(2)}, u32[]{:S(2)}) collective-permute-start(bf16[384,128]{1,0:T(8,128)(2,1)S(1)} %copy-done.15), channel_id=1, source_target_pairs={{0,384},{128,0},{256,128},{384,256},{1,385},{129,1},{257,129},{385... | collective-permute-start | bytes 294920 | tf_op jit(solution)/shard_map/ppermute | solution.py:44
  90.5 2.7 %copy-start.16 = (bf16[384,128]{1,0:T(8,128)(2,1)}, bf16[384,128]{1,0:T(8,128)(2,1)S(1)}, u32[]{:S(2)}) copy-start(bf16[384,128]{1,0:T(8,128)(2,1)S(1)} %collective-permute-done.1.q1) | copy-start | bytes 294916
  93.2 0.6 copy-start.17
  93.2 0.7 copy-start.18
  93.2 1.2 copy-start
  100.0 38.8 %copy-start.12 = (bf16[16,2048]{1,0:T(8,128)(2,1)S(1)}, bf16[16,2048]{1,0:T(8,128)(2,1)}, u32[]{:S(2)}) copy-start(bf16[16,2048]{1,0:T(8,128)(2,1)} %param.17) | copy-start | bytes 196612
  100.0 38.8 %copy-start.19 = (f32[1,2048]{1,0:T(1,128)S(1)}, f32[1,2048]{1,0:T(1,128)}, u32[]{:S(2)}) copy-start(f32[1,2048]{1,0:T(1,128)} %get-tuple-element.8) | copy-start | bytes 24580
  100.0 19.5 %all-to-all-start.3 = ((bf16[16,72,128]{2,1,0:T(8,128)(2,1)}), bf16[16,72,128]{2,1,0:T(8,128)(2,1)S(1)}, u32[]{:S(2)}, u32[]{:S(2)}) async-start(bf16[16,72,128]{2,1,0:T(8,128)(2,1)} %bitcast.16), calls=%async_computation.3 | async-start | bytes 589824 | tf_op jit(solution)/shard_map/all_to_all | solution.py:26
  107.5 4.4 %collective-permute-start.4 = (bf16[128,2048]{1,0:T(8,128)(2,1)S(1)}, bf16[128,2048]{1,0:T(8,128)(2,1)S(1)}, u32[]{:S(2)}, u32[]{:S(2)}) collective-permute-start(bf16[128,2048]{1,0:T(8,128)(2,1)S(1)} %copy-done.6), channel_id=1, source_target_pairs={{0,1},{1,0},{2,3},{3,2},{4,5},{5,4},{6,7},{7,6},{8,9},{9,8},{10,11... | collective-permute-start | bytes 1572872 | tf_op jit(solution)/shard_map/ppermute | solution.py:44
  109.6 9.9 %copy-start.7 = (bf16[128,2048]{1,0:T(8,128)(2,1)}, bf16[128,2048]{1,0:T(8,128)(2,1)S(1)}, u32[]{:S(2)}) copy-start(bf16[128,2048]{1,0:T(8,128)(2,1)S(1)} %collective-permute-done.5.refs_2_) | copy-start | bytes 1572868
  109.6 3.8 %collective-permute-start.6 = (bf16[128,2048]{1,0:T(8,128)(2,1)S(1)}, bf16[128,2048]{1,0:T(8,128)(2,1)S(1)}, u32[]{:S(2)}, u32[]{:S(2)}) collective-permute-start(bf16[128,2048]{1,0:T(8,128)(2,1)S(1)} %collective-permute-done.5.refs_2_), channel_id=1, source_target_pairs={{0,1},{1,0},{2,3},{3,2},{4,5},{5,4},{6,7},{7,6},{8,9},{9,8},{10,11... | collective-permute-start | bytes 1572872 | tf_op jit(solution)/shard_map/ppermute | solution.py:44
  111.9 7.6 %copy-start.8 = (bf16[128,2048]{1,0:T(8,128)(2,1)}, bf16[128,2048]{1,0:T(8,128)(2,1)S(1)}, u32[]{:S(2)}) copy-start(bf16[128,2048]{1,0:T(8,128)(2,1)S(1)} %collective-permute-done.4.refs_1_) | copy-start | bytes 1572868
  113.4 6.1 %copy-start.9 = (bf16[128,2048]{1,0:T(8,128)(2,1)}, bf16[128,2048]{1,0:T(8,128)(2,1)S(1)}, u32[]{:S(2)}) copy-start(bf16[128,2048]{1,0:T(8,128)(2,1)S(1)} %collective-permute-done.6.refs_3_) | copy-start | bytes 1572868
  119.5 0.8 copy-start.2

commit v11 on v10

--- a/solution.py
+++ b/solution.py
@@ -20,6 +20,10 @@
 TP = ("ya", "yb", "c")
 KV_AXES = ("zb", "x")
 Q_AXIS = "za"
+
+
+def near(array):
+    return pltpu.with_memory_space_constraint(array, pltpu.VMEM)
 
 
 def exchanged(array, axes):
@@ -206,10 +210,8 @@
                 o_ref[to, part, quarter:, quarter:] = jnp.zeros((8, lanes - quarter), BF16)
 
 
-def merge_kernel(at_ref, got_hbm, *refs):
-    hbm, o_ref, w_ref, got_ref, sems, got_sem = refs[:4], refs[4], refs[5], refs[6], refs[7:11], refs[11]
-    got_load = pltpu.make_async_copy(got_hbm, got_ref, got_sem)
-    got_load.start()
+def merge_kernel(at_ref, got_ref, *refs):
+    hbm, o_ref, w_ref, sems = refs[:4], refs[4], refs[5], refs[6:]
     deep = hbm[0].shape[0]
     loads = [
         pltpu.make_async_copy(src, w_ref.at[pl.ds(i * deep, deep)], sem) for i, (src, sem) in enumerate(zip(hbm, sems, strict=True))
@@ -221,7 +223,6 @@
     n_ya, rows, width = o_ref.shape
     core, yb = at_ref[0, 0], at_ref[0, 1]
     sources = [(yb + i) % 2 * 2 + (core + j) % 2 for i in range(2) for j in range(2)]
-    got_load.wait()
     shares = []
     for source in sources:
         lse = [jnp.sum(got_ref[i, source, quarter:, :].astype(F32), axis=0, keepdims=True) for i in range(n_q)]
@@ -281,7 +282,7 @@
         out_shape=jax.ShapeDtypeStruct((n_y, rows, width + 2 * lanes), BF16),
         name="pack",
     )
-    message = pack(summed, block)
+    message = pack(near(summed), near(block))
 
     mine = exchanged(message, Y)
     w_other = shifted(w_out, "c", 1)
@@ -300,7 +301,7 @@
         in_specs=[smem] + [vmem] * 6 + [any_space] * 3,
         out_specs=[vmem, vmem, vmem],
         out_shape=[
-            jax.ShapeDtypeStruct((tok + tok // 2, lanes), BF16),
+            pltpu.VMEM((tok + tok // 2, lanes), BF16),
             jax.ShapeDtypeStruct((lax.axis_size(KV_AXES), 2 * (tok + n_tp) + tok // 2 + n_tp, lanes), BF16),
             jax.ShapeDtypeStruct((1, width), F32),
         ],
@@ -317,7 +318,7 @@
         name="project",
     )
     q_own, kv_copies, gate = project(
-        at, mine, other, norm_gain.reshape(1, width), kv_gain.reshape(1, -1), cosine, sine, w_side, w_kv_down, w_up
+        at, near(mine), near(other), norm_gain.reshape(1, width), kv_gain.reshape(1, -1), cosine, sine, w_side, w_kv_down, w_up
     )
 
     queries = [q_own] + [shifted(q_own, Q_AXIS, k) for k in range(1, n_q)]
@@ -335,21 +336,20 @@
         ],
         name="attend",
     )
-    out = attend(to, ctx_bias.reshape(1, 1), *queries, kv)
+    out = attend(to, ctx_bias.reshape(1, 1), *(near(q) for q in queries), near(kv))
 
     got = exchanged(out.reshape(n_q * 2 * n_c, quarter + 8, vsize), (Q_AXIS, "yb", "c"))
     term = pl.pallas_call(
         merge_kernel,
-        in_specs=[smem] + [any_space] * 5,
+        in_specs=[smem, vmem] + [any_space] * 4,
         out_specs=vmem,
-        out_shape=jax.ShapeDtypeStruct((n_ya, rows, width), BF16),
+        out_shape=pltpu.VMEM((n_ya, rows, width), BF16),
         scratch_shapes=[
             pltpu.VMEM((4 * w_out.shape[0], width), BF16),
-            pltpu.VMEM((n_q, 2 * n_c, quarter + 8, vsize), BF16),
         ]
-        + [pltpu.SemaphoreType.DMA] * 5,
+        + [pltpu.SemaphoreType.DMA] * 4,
         name="merge",
-    )(at, got.reshape(n_q, 2 * n_c, quarter + 8, vsize), w_out, w_other, w_near, w_far)
+    )(at, near(got.reshape(n_q, 2 * n_c, quarter + 8, vsize)), w_out, w_other, w_near, w_far)
     branch = jnp.sum(exchanged(term, ("ya",)).astype(F32), axis=0)
     return (latent.astype(F32) + gate * branch).astype(BF16)
 

time: 140 us -> 132 us (0.943)
  Pallas kernels: 18.5 us -> 14.7 us
  local copies, waits for them, and re-layouts: 3.96 us -> 0.59 us
  blocking collectives: 14.8 us -> 13.2 us
    pallas_call x4, Pallas kernels: 16.7 us -> 12.9 us  [the longest x1 5.25 us: step(): project(at, near(mine), near(other), norm_gain.reshape(1, width), kv_gain...]
    unnamed x42 -> x24, local copies, waits for them, and re-layouts: 3.96 us -> 0.59 us
    all_to_all x1, blocking collectives: 14.8 us -> 13.2 us  [exchanged(): return lax.all_to_all(array, axes, 0, 0, tiled=True)]
  transfers between devices with their start and end apart: 11 -> 11, of which waited for: 6 -> 6; matrix products, arithmetic and copies ran while one was open for 5% -> 5% of each run, Pallas kernels for 4% -> 3%
where the time goes in v11:
time: 132 us; the launch traced here: 131 us
  starting transfers between devices  53.5 us (41%)
  waiting for transfers between devices  41.5 us (31%)
  Pallas kernels  14.7 us (11%)
  blocking collectives  13.2 us (10%)
  other arithmetic  6.25 us (5%)
    all_to_all x4, starting transfers between devices, exchanged(): return lax.all_to_all(array, axes, 0, 0, tiled=True)  31.8 us
    all_to_all x4, waiting for transfers between devices, exchanged(): return lax.all_to_all(array, axes, 0, 0, tiled=True)  29.4 us
    ppermute x7, starting transfers between devices, shifted(): return lax.ppermute(array, axis, [(i, (i + k) % n) for i in range(n)])  21.7 us
    all_to_all x1, blocking collectives, exchanged(): return lax.all_to_all(array, axes, 0, 0, tiled=True)  13.2 us
    ppermute x7, waiting for transfers between devices, shifted(): return lax.ppermute(array, axis, [(i, (i + k) % n) for i in range(n)])  12.1 us
    pallas_call x1, Pallas kernels, step(): project(at, near(mine), near(other), norm_gain.reshape(1, width), kv_gain...  5.25 us
    pallas_call x1, Pallas kernels, step(): attend(to, ctx_bias.reshape(1, 1), *(near(q) for q in queries), near(kv))  4.04 us
    pallas_call x1, Pallas kernels, step(): pl.pallas_call(merge_kernel, in_specs=[smem, vmem] + [any_space] * 4, out...  2.71 us
  transfers between devices with their start and end apart: 11, of which 6 were waited for; matrix products, arithmetic and copies ran while one was open for 5% of the time, Pallas kernels for 3%

profile of v11, /device:TPU:1, one launch (start us, length us, event | category | flops | bytes accessed | tf_op | source)
XLA Modules:
  0.0 130.7 jit_solution(16851659892730593526)
XLA Ops:
  0.0 0.0 copy-start.5
  0.0 0.0 copy-start.6
  0.0 0.0 copy-start.8
  0.0 0.0 copy-start.9
  0.0 1.8 %front.1 = f32[32,5,128]{2,1,0:T(8,128)} custom-call(s32[1,1]{1,0:T(1,128)} %bitcast.3.at_ref, f32[16,128]{1,0:T(8,128)} %bitcast.20, f32[16,128]{1,0:T(8,128)} %bitcast.21, f32[64,128]{1,0:T(8,128)} %shift_ref.1, f32[64,128]{1,0:T(8,128)} %scale_ref.1, f32[64,128]{1,0:T(8,128)} %gate_ref.1), custom_call_target="tpu_custom_call" | custom-call | tf_op jit(solution)/shard_map/front/pallas_call | solution.py:265
  1.8 13.7 %all-to-all-start = ((f32[32,5,128]{2,1,0:T(8,128)}), f32[32,5,128]{2,1,0:T(8,128)S(1)}, u32[]{:S(2)}, u32[]{:S(2)}) async-start(f32[32,5,128]{2,1,0:T(8,128)} %front.1), calls=%async_computation | async-start | bytes 262144 | tf_op jit(solution)/shard_map/all_to_all | solution.py:30
  15.6 0.7 reduce
  16.3 0.8 pad_maximum_fusion.2.block_ref
  17.1 0.0 copy-start
  17.1 7.8 %all-to-all-done.sums_ref = f32[32,5,128]{2,1,0:T(8,128)S(1)} async-done(((f32[32,5,128]{2,1,0:T(8,128)}), f32[32,5,128]{2,1,0:T(8,128)S(1)}, u32[]{:S(2)}, u32[]{:S(2)}) %all-to-all-start) | async-done | bytes 81952 | tf_op jit(solution)/shard_map/all_to_all | solution.py:30
  24.9 0.9 pack.1
  25.8 6.8 %all-to-all-start.1 = ((bf16[8,16,2304]{2,1,0:T(8,128)(2,1)}), bf16[8,16,2304]{2,1,0:T(8,128)(2,1)S(1)}, u32[]{:S(2)}, u32[]{:S(2)}) async-start(bf16[8,16,2304]{2,1,0:T(8,128)(2,1)} %pack.1), calls=%async_computation.1 | async-start | bytes 1179648 | tf_op jit(solution)/shard_map/all_to_all | solution.py:30
  32.6 0.0 copy-done.5
  32.6 0.3 copy.18
  32.9 0.0 copy-done.6
  32.9 0.3 copy.19
  33.3 0.0 copy-done.8
  33.3 0.0 copy-done.9
  33.3 0.7 pad_maximum_fusion.1.w_up_hbm
  34.0 15.6 %all-to-all-done.1.own_ref = bf16[8,16,2304]{2,1,0:T(8,128)(2,1)S(1)} async-done(((bf16[8,16,2304]{2,1,0:T(8,128)(2,1)}), bf16[8,16,2304]{2,1,0:T(8,128)(2,1)S(1)}, u32[]{:S(2)}, u32[]{:S(2)}) %all-to-all-start.1) | async-done | bytes 589856 | tf_op jit(solution)/shard_map/all_to_all | solution.py:30
  49.6 4.8 %collective-permute-start = (bf16[8,16,2304]{2,1,0:T(8,128)(2,1)S(1)}, bf16[8,16,2304]{2,1,0:T(8,128)(2,1)S(1)}, u32[]{:S(2)}, u32[]{:S(2)}) collective-permute-start(bf16[8,16,2304]{2,1,0:T(8,128)(2,1)S(1)} %all-to-all-done.1.own_ref), channel_id=1, source_target_pairs={{0,1},{1,0},{2,3},{3,2},{4,5},{5,4},{6,7},{7,6},{8,9},{9,8},{10,11... | collective-permute-start | bytes 1769480 | tf_op jit(solution)/shard_map/ppermute | solution.py:48
  54.4 0.6 add_bitcast_fusion.at_ref
  55.0 1.3 sine_multiply_fusion
  56.3 0.0 copy-done
  56.3 1.3 pad_maximum_fusion.w_side_hbm
  57.6 0.0 collective-permute-done.other_ref
  57.6 5.2 %project.1 = (bf16[384,128]{1,0:T(8,128)(2,1)S(1)}, bf16[8,688,128]{2,1,0:T(8,128)(2,1)}, f32[1,2048]{1,0:T(1,128)}) custom-call(s32[1,2]{1,0:T(1,128)} %add_bitcast_fusion.at_ref, bf16[8,16,2304]{2,1,0:T(8,128)(2,1)S(1)} %all-to-all-done.1.own_ref, bf16[8,16,2304]{2,1,0:T(8,128)(2,1)S(1)} %collective-permute-done.other_ref, f32[1,2048]{1,0:T(1,128)} %bitcast.19, ...), custom_call_target="tpu_custom_call" | custom-call | tf_op jit(solution)/shard_map/project/pallas_call | solution.py:320
  62.8 0.0 copy-start.1
  62.8 3.7 %all-to-all-start.2 = ((bf16[8,688,128]{2,1,0:T(8,128)(2,1)}), bf16[8,688,128]{2,1,0:T(8,128)(2,1)S(1)}, u32[]{:S(2)}, u32[]{:S(2)}) async-start(bf16[8,688,128]{2,1,0:T(8,128)(2,1)} %get-tuple-element.10), calls=%async_computation.2 | async-start | bytes 2818048 | tf_op jit(solution)/shard_map/all_to_all | solution.py:30
  66.6 0.0 copy-done.1
  66.6 2.2 %collective-permute-start.5 = (bf16[128,2048]{1,0:T(8,128)(2,1)S(1)}, bf16[128,2048]{1,0:T(8,128)(2,1)S(1)}, u32[]{:S(2)}, u32[]{:S(2)}) collective-permute-start(bf16[128,2048]{1,0:T(8,128)(2,1)S(1)} %copy-done.1), channel_id=1, source_target_pairs={{0,2},{2,0},{1,3},{3,1},{4,6},{6,4},{5,7},{7,5},{8,10},{10,8},{9,1... | collective-permute-start | bytes 1572872 | tf_op jit(solution)/shard_map/ppermute | solution.py:48
  68.8 2.9 %collective-permute-start.1 = (bf16[384,128]{1,0:T(8,128)(2,1)S(1)}, bf16[384,128]{1,0:T(8,128)(2,1)S(1)}, u32[]{:S(2)}, u32[]{:S(2)}) collective-permute-start(bf16[384,128]{1,0:T(8,128)(2,1)S(1)} %get-tuple-element.9.q0), channel_id=1, source_target_pairs={{0,128},{128,256},{256,384},{384,0},{1,129},{129,257},{257,385},{3... | collective-permute-start | bytes 294920 | tf_op jit(solution)/shard_map/ppermute | solution.py:48
  71.7 3.5 %collective-permute-start.2 = (bf16[384,128]{1,0:T(8,128)(2,1)S(1)}, bf16[384,128]{1,0:T(8,128)(2,1)S(1)}, u32[]{:S(2)}, u32[]{:S(2)}) collective-permute-start(bf16[384,128]{1,0:T(8,128)(2,1)S(1)} %get-tuple-element.9.q0), channel_id=1, source_target_pairs={{0,256},{128,384},{256,0},{384,128},{1,257},{129,385},{257,1},{385... | collective-permute-start | bytes 294920 | tf_op jit(solution)/shard_map/ppermute | solution.py:48
  75.2 4.0 %collective-permute-start.3 = (bf16[384,128]{1,0:T(8,128)(2,1)S(1)}, bf16[384,128]{1,0:T(8,128)(2,1)S(1)}, u32[]{:S(2)}, u32[]{:S(2)}) collective-permute-start(bf16[384,128]{1,0:T(8,128)(2,1)S(1)} %get-tuple-element.9.q0), channel_id=1, source_target_pairs={{0,384},{128,0},{256,128},{384,256},{1,385},{129,1},{257,129},{385... | collective-permute-start | bytes 294920 | tf_op jit(solution)/shard_map/ppermute | solution.py:48
  79.9 7.9 %collective-permute-done.1.q1 = bf16[384,128]{1,0:T(8,128)(2,1)S(1)} collective-permute-done((bf16[384,128]{1,0:T(8,128)(2,1)S(1)}, bf16[384,128]{1,0:T(8,128)(2,1)S(1)}, u32[]{:S(2)}, u32[]{:S(2)}) %collective-permute-start.1) | collective-permute-done | bytes 98336 | tf_op jit(solution)/shard_map/ppermute | solution.py:48
  87.7 2.7 %collective-permute-done.2.q2 = bf16[384,128]{1,0:T(8,128)(2,1)S(1)} collective-permute-done((bf16[384,128]{1,0:T(8,128)(2,1)S(1)}, bf16[384,128]{1,0:T(8,128)(2,1)S(1)}, u32[]{:S(2)}, u32[]{:S(2)}) %collective-permute-start.2) | collective-permute-done | bytes 98336 | tf_op jit(solution)/shard_map/ppermute | solution.py:48
  90.4 0.0 collective-permute-done.3.q3
  90.4 0.0 all-to-all-done.2.kv_ref
  90.5 4.0 %attend.1 = bf16[4,4,72,128]{3,2,1,0:T(8,128)(2,1)} custom-call(s32[1,1]{1,0:T(1,128)} %bitcast.9.place_ref, f32[1,1]{1,0:T(1,128)} %bitcast.15.bias_ref, bf16[384,128]{1,0:T(8,128)(2,1)S(1)} %get-tuple-element.9.q0, bf16[384,128]{1,0:T(8,128)(2,1)S(1)} %collective-permute-done.1.q1, bf16[384,128]{1,0:T(8,128)(2,1)S(1)} %collective-permute-done.2.q2, ...), custom_call_target="tpu_custom_call" | custom-call | tf_op jit(solution)/shard_map/attend/pallas_call | solution.py:339
  94.5 0.0 copy-start.7
  94.5 0.0 copy-start.10
  94.5 7.6 %all-to-all-start.3 = ((bf16[16,72,128]{2,1,0:T(8,128)(2,1)}), bf16[16,72,128]{2,1,0:T(8,128)(2,1)S(1)}, u32[]{:S(2)}, u32[]{:S(2)}) async-start(bf16[16,72,128]{2,1,0:T(8,128)(2,1)} %bitcast.17), calls=%async_computation.3 | async-start | bytes 589824 | tf_op jit(solution)/shard_map/all_to_all | solution.py:30
  102.1 2.0 %collective-permute-start.4 = (bf16[128,2048]{1,0:T(8,128)(2,1)S(1)}, bf16[128,2048]{1,0:T(8,128)(2,1)S(1)}, u32[]{:S(2)}, u32[]{:S(2)}) collective-permute-start(bf16[128,2048]{1,0:T(8,128)(2,1)S(1)} %copy-done.1), channel_id=1, source_target_pairs={{0,1},{1,0},{2,3},{3,2},{4,5},{5,4},{6,7},{7,6},{8,9},{9,8},{10,11... | collective-permute-start | bytes 1572872 | tf_op jit(solution)/shard_map/ppermute | solution.py:48
  104.1 0.0 collective-permute-done.5.refs_2_
  104.1 0.0 copy-start.2
  104.1 2.3 %collective-permute-start.6 = (bf16[128,2048]{1,0:T(8,128)(2,1)S(1)}, bf16[128,2048]{1,0:T(8,128)(2,1)S(1)}, u32[]{:S(2)}, u32[]{:S(2)}) collective-permute-start(bf16[128,2048]{1,0:T(8,128)(2,1)S(1)} %collective-permute-done.5.refs_2_), channel_id=1, source_target_pairs={{0,1},{1,0},{2,3},{3,2},{4,5},{5,4},{6,7},{7,6},{8,9},{9,8},{10,11... | collective-permute-start | bytes 1572872 | tf_op jit(solution)/shard_map/ppermute | solution.py:48
  106.4 0.0 collective-permute-done.4.refs_1_
  106.4 0.0 copy-start.3
  106.5 1.5 %collective-permute-done.6.refs_3_ = bf16[128,2048]{1,0:T(8,128)(2,1)S(1)} collective-permute-done((bf16[128,2048]{1,0:T(8,128)(2,1)S(1)}, bf16[128,2048]{1,0:T(8,128)(2,1)S(1)}, u32[]{:S(2)}, u32[]{:S(2)}) %collective-permute-start.6) | collective-permute-done | bytes 524320 | tf_op jit(solution)/shard_map/ppermute | solution.py:48
  108.0 0.0 copy-start.4
  108.0 6.1 %all-to-all-done.3 = bf16[16,72,128]{2,1,0:T(8,128)(2,1)S(1)} async-done(((bf16[16,72,128]{2,1,0:T(8,128)(2,1)}), bf16[16,72,128]{2,1,0:T(8,128)(2,1)S(1)}, u32[]{:S(2)}, u32[]{:S(2)}) %all-to-all-start.3) | async-done | bytes 294944 | tf_op jit(solution)/shard_map/all_to_all | solution.py:30
  114.0 0.0 copy-done.2
  114.0 0.0 copy-done.3
  114.0 0.0 copy-done.4
  114.0 2.7 %merge.1 = bf16[4,16,2048]{2,1,0:T(8,128)(2,1)S(1)} custom-call(s32[1,2]{1,0:T(1,128)} %add_bitcast_fusion.at_ref, bf16[4,4,72,128]{3,2,1,0:T(8,128)(2,1)S(1)} %bitcast.16, bf16[128,2048]{1,0:T(8,128)(2,1)} %refs_0_.1, bf16[128,2048]{1,0:T(8,128)(2,1)} %copy-done.3, bf16[128,2048]{1,0:T(8,128)(2,1)} %copy-done.2, bf16[128,2048]{1,0:T(8,128)(2,1)} %copy-done.4), custom_call_target="tpu_custom_call" | custom-call | tf_op jit(solution)/shard_map/merge/pallas_call | solution.py:342
  116.8 13.2 %all_to_all.25 = bf16[4,16,2048]{2,1,0:T(8,128)(2,1)S(1)} all-to-all(bf16[4,16,2048]{2,1,0:T(8,128)(2,1)S(1)} %merge.1), channel_id=1, replica_groups=mesh['za'=4,'zb'=2,'x'=4,'ya'=4,'yb'=2,'c'=2] {'ya'}, dimensions={0} | all-to-all | bytes 524288 | tf_op jit(solution)/shard_map/all_to_all | solution.py:30
  130.1 0.0 copy-done.7
  130.1 0.0 copy-done.10
  130.1 0.7 add_convert_fusion
  (4 shorter events, 0.1 us)
Async XLA Ops:
  0.0 32.6 %copy-start.5 = (bf16[2048,64]{0,1:T(8,128)(2,1)S(1)}, bf16[2048,64]{0,1:T(8,128)(2,1)}, u32[]{:S(2)}) copy-start(bf16[2048,64]{0,1:T(8,128)(2,1)} %param.26) | copy-start | bytes 786436
  0.0 32.9 %copy-start.6 = (bf16[2048,64]{0,1:T(8,128)(2,1)S(1)}, bf16[2048,64]{0,1:T(8,128)(2,1)}, u32[]{:S(2)}) copy-start(bf16[2048,64]{0,1:T(8,128)(2,1)} %param.28) | copy-start | bytes 786436
  0.0 33.3 %copy-start.8 = (bf16[512,128]{1,0:T(8,128)(2,1)S(1)}, bf16[512,128]{1,0:T(8,128)(2,1)}, u32[]{:S(2)}) copy-start(bf16[512,128]{1,0:T(8,128)(2,1)} %param.31) | copy-start | bytes 393220
  0.0 33.3 %copy-start.9 = (bf16[512,128]{1,0:T(8,128)(2,1)S(1)}, bf16[512,128]{1,0:T(8,128)(2,1)}, u32[]{:S(2)}) copy-start(bf16[512,128]{1,0:T(8,128)(2,1)} %param.30) | copy-start | bytes 393220
  1.8 23.1 %all-to-all-start = ((f32[32,5,128]{2,1,0:T(8,128)}), f32[32,5,128]{2,1,0:T(8,128)S(1)}, u32[]{:S(2)}, u32[]{:S(2)}) async-start(f32[32,5,128]{2,1,0:T(8,128)} %front.1), calls=%async_computation | async-start | bytes 262144 | tf_op jit(solution)/shard_map/all_to_all | solution.py:30
  17.1 39.1 %copy-start = (bf16[2048,128]{1,0:T(8,128)(2,1)S(1)}, bf16[2048,128]{1,0:T(8,128)(2,1)}, u32[]{:S(2)}) copy-start(bf16[2048,128]{1,0:T(8,128)(2,1)} %param.25) | copy-start | bytes 1572868
  25.8 23.8 %all-to-all-start.1 = ((bf16[8,16,2304]{2,1,0:T(8,128)(2,1)}), bf16[8,16,2304]{2,1,0:T(8,128)(2,1)S(1)}, u32[]{:S(2)}, u32[]{:S(2)}) async-start(bf16[8,16,2304]{2,1,0:T(8,128)(2,1)} %pack.1), calls=%async_computation.1 | async-start | bytes 1179648 | tf_op jit(solution)/shard_map/all_to_all | solution.py:30
  49.6 8.0 %collective-permute-start = (bf16[8,16,2304]{2,1,0:T(8,128)(2,1)S(1)}, bf16[8,16,2304]{2,1,0:T(8,128)(2,1)S(1)}, u32[]{:S(2)}, u32[]{:S(2)}) collective-permute-start(bf16[8,16,2304]{2,1,0:T(8,128)(2,1)S(1)} %all-to-all-done.1.own_ref), channel_id=1, source_target_pairs={{0,1},{1,0},{2,3},{3,2},{4,5},{5,4},{6,7},{7,6},{8,9},{9,8},{10,11... | collective-permute-start | bytes 1769480 | tf_op jit(solution)/shard_map/ppermute | solution.py:48
  62.8 3.7 %copy-start.1 = (bf16[128,2048]{1,0:T(8,128)(2,1)S(1)}, bf16[128,2048]{1,0:T(8,128)(2,1)}, u32[]{:S(2)}) copy-start(bf16[128,2048]{1,0:T(8,128)(2,1)} %refs_0_.1) | copy-start | bytes 1572868
  62.8 27.6 %all-to-all-start.2 = ((bf16[8,688,128]{2,1,0:T(8,128)(2,1)}), bf16[8,688,128]{2,1,0:T(8,128)(2,1)S(1)}, u32[]{:S(2)}, u32[]{:S(2)}) async-start(bf16[8,688,128]{2,1,0:T(8,128)(2,1)} %get-tuple-element.10), calls=%async_computation.2 | async-start | bytes 2818048 | tf_op jit(solution)/shard_map/all_to_all | solution.py:30
  66.6 37.5 %collective-permute-start.5 = (bf16[128,2048]{1,0:T(8,128)(2,1)S(1)}, bf16[128,2048]{1,0:T(8,128)(2,1)S(1)}, u32[]{:S(2)}, u32[]{:S(2)}) collective-permute-start(bf16[128,2048]{1,0:T(8,128)(2,1)S(1)} %copy-done.1), channel_id=1, source_target_pairs={{0,2},{2,0},{1,3},{3,1},{4,6},{6,4},{5,7},{7,5},{8,10},{10,8},{9,1... | collective-permute-start | bytes 1572872 | tf_op jit(solution)/shard_map/ppermute | solution.py:48
  68.8 19.0 %collective-permute-start.1 = (bf16[384,128]{1,0:T(8,128)(2,1)S(1)}, bf16[384,128]{1,0:T(8,128)(2,1)S(1)}, u32[]{:S(2)}, u32[]{:S(2)}) collective-permute-start(bf16[384,128]{1,0:T(8,128)(2,1)S(1)} %get-tuple-element.9.q0), channel_id=1, source_target_pairs={{0,128},{128,256},{256,384},{384,0},{1,129},{129,257},{257,385},{3... | collective-permute-start | bytes 294920 | tf_op jit(solution)/shard_map/ppermute | solution.py:48
  71.7 18.7 %collective-permute-start.2 = (bf16[384,128]{1,0:T(8,128)(2,1)S(1)}, bf16[384,128]{1,0:T(8,128)(2,1)S(1)}, u32[]{:S(2)}, u32[]{:S(2)}) collective-permute-start(bf16[384,128]{1,0:T(8,128)(2,1)S(1)} %get-tuple-element.9.q0), channel_id=1, source_target_pairs={{0,256},{128,384},{256,0},{384,128},{1,257},{129,385},{257,1},{385... | collective-permute-start | bytes 294920 | tf_op jit(solution)/shard_map/ppermute | solution.py:48
  75.2 15.2 %collective-permute-start.3 = (bf16[384,128]{1,0:T(8,128)(2,1)S(1)}, bf16[384,128]{1,0:T(8,128)(2,1)S(1)}, u32[]{:S(2)}, u32[]{:S(2)}) collective-permute-start(bf16[384,128]{1,0:T(8,128)(2,1)S(1)} %get-tuple-element.9.q0), channel_id=1, source_target_pairs={{0,384},{128,0},{256,128},{384,256},{1,385},{129,1},{257,129},{385... | collective-permute-start | bytes 294920 | tf_op jit(solution)/shard_map/ppermute | solution.py:48
  94.5 35.6 %copy-start.7 = (bf16[16,2048]{1,0:T(8,128)(2,1)S(1)}, bf16[16,2048]{1,0:T(8,128)(2,1)}, u32[]{:S(2)}) copy-start(bf16[16,2048]{1,0:T(8,128)(2,1)} %param.17) | copy-start | bytes 196612
  94.5 35.6 %copy-start.10 = (f32[1,2048]{1,0:T(1,128)S(1)}, f32[1,2048]{1,0:T(1,128)}, u32[]{:S(2)}) copy-start(f32[1,2048]{1,0:T(1,128)} %get-tuple-element.8) | copy-start | bytes 24580
  94.5 19.5 %all-to-all-start.3 = ((bf16[16,72,128]{2,1,0:T(8,128)(2,1)}), bf16[16,72,128]{2,1,0:T(8,128)(2,1)S(1)}, u32[]{:S(2)}, u32[]{:S(2)}) async-start(bf16[16,72,128]{2,1,0:T(8,128)(2,1)} %bitcast.17), calls=%async_computation.3 | async-start | bytes 589824 | tf_op jit(solution)/shard_map/all_to_all | solution.py:30
  102.1 4.4 %collective-permute-start.4 = (bf16[128,2048]{1,0:T(8,128)(2,1)S(1)}, bf16[128,2048]{1,0:T(8,128)(2,1)S(1)}, u32[]{:S(2)}, u32[]{:S(2)}) collective-permute-start(bf16[128,2048]{1,0:T(8,128)(2,1)S(1)} %copy-done.1), channel_id=1, source_target_pairs={{0,1},{1,0},{2,3},{3,2},{4,5},{5,4},{6,7},{7,6},{8,9},{9,8},{10,11... | collective-permute-start | bytes 1572872 | tf_op jit(solution)/shard_map/ppermute | solution.py:48
  104.1 9.9 %copy-start.2 = (bf16[128,2048]{1,0:T(8,128)(2,1)}, bf16[128,2048]{1,0:T(8,128)(2,1)S(1)}, u32[]{:S(2)}) copy-start(bf16[128,2048]{1,0:T(8,128)(2,1)S(1)} %collective-permute-done.5.refs_2_) | copy-start | bytes 1572868
  104.1 3.8 %collective-permute-start.6 = (bf16[128,2048]{1,0:T(8,128)(2,1)S(1)}, bf16[128,2048]{1,0:T(8,128)(2,1)S(1)}, u32[]{:S(2)}, u32[]{:S(2)}) collective-permute-start(bf16[128,2048]{1,0:T(8,128)(2,1)S(1)} %collective-permute-done.5.refs_2_), channel_id=1, source_target_pairs={{0,1},{1,0},{2,3},{3,2},{4,5},{5,4},{6,7},{7,6},{8,9},{9,8},{10,11... | collective-permute-start | bytes 1572872 | tf_op jit(solution)/shard_map/ppermute | solution.py:48
  106.4 7.6 %copy-start.3 = (bf16[128,2048]{1,0:T(8,128)(2,1)}, bf16[128,2048]{1,0:T(8,128)(2,1)S(1)}, u32[]{:S(2)}) copy-start(bf16[128,2048]{1,0:T(8,128)(2,1)S(1)} %collective-permute-done.4.refs_1_) | copy-start | bytes 1572868
  108.0 6.1 %copy-start.4 = (bf16[128,2048]{1,0:T(8,128)(2,1)}, bf16[128,2048]{1,0:T(8,128)(2,1)S(1)}, u32[]{:S(2)}) copy-start(bf16[128,2048]{1,0:T(8,128)(2,1)S(1)} %collective-permute-done.6.refs_3_) | copy-start | bytes 1572868

commit v12 on v11

--- a/solution.py
+++ b/solution.py
@@ -82,15 +82,11 @@
 
 
 def project_kernel(
-    at_ref, own_ref, other_ref, gain_ref, kv_gain_ref, cos_ref, sin_ref, w_side_hbm, w_down_hbm, w_up_hbm,
-    q_ref, kv_ref, gate_ref, ctx_ref, h_ref, w_side_ref, w_down_ref, w_up_ref, side_sem, down_sem, up_sem,
+    at_ref, own_ref, other_ref, gain_ref, kv_gain_ref, cos_ref, sin_ref, w_side_ref, w_up_ref, w_down_hbm,
+    q_ref, kv_ref, gate_ref, ctx_ref, h_ref, w_down_ref, down_sem,
 ):
-    loads = [
-        pltpu.make_async_copy(w_side_hbm, w_side_ref, side_sem), pltpu.make_async_copy(w_down_hbm, w_down_ref, down_sem),
-        pltpu.make_async_copy(w_up_hbm, w_up_ref, up_sem),
-    ]
-    for load in loads:
-        load.start()
+    load = pltpu.make_async_copy(w_down_hbm, w_down_ref, down_sem)
+    load.start()
     n_y, rows, _ = own_ref.shape
     side_rows = n_y * rows
     tok = 2 * side_rows
@@ -127,12 +123,10 @@
     context = jnp.concatenate([ctx_ref[pl.ds(i, n_ctx, stride=rows), :] for i in range(rows)], axis=1)
     h_ref[tok:, :] = modulated(context, shift_ctx, scale_ctx)
     h = h_ref[...]
-    loads[0].wait()
     mixed = jnp.dot(h, w_side_ref[...], preferred_element_type=F32)
-    loads[1].wait()
+    load.wait()
     inner = jnp.dot(h, w_down_ref[...], preferred_element_type=F32)
     inner = (inner * lax.rsqrt(jnp.mean(inner * inner, axis=1, keepdims=True) + EPS) * kv_gain_ref[...]).astype(BF16)
-    loads[2].wait()
     both = jnp.dot(inner, w_up_ref[...], preferred_element_type=F32).astype(BF16)
     q_ref[:tok, :] = mixed[:tok, :lanes].astype(BF16)
     pair = mixed[:, lanes:]
@@ -298,7 +292,7 @@
 
     project = pl.pallas_call(
         project_kernel,
-        in_specs=[smem] + [vmem] * 6 + [any_space] * 3,
+        in_specs=[smem] + [vmem] * 8 + [any_space],
         out_specs=[vmem, vmem, vmem],
         out_shape=[
             pltpu.VMEM((tok + tok // 2, lanes), BF16),
@@ -308,20 +302,18 @@
         scratch_shapes=[
             pltpu.VMEM((tok, lanes), F32),
             pltpu.VMEM((tok + n_tp, width), BF16),
-            pltpu.VMEM(w_side.shape, BF16),
             pltpu.VMEM(w_kv_down.shape, BF16),
-            pltpu.VMEM(w_up.shape, BF16),
-            pltpu.SemaphoreType.DMA,
-            pltpu.SemaphoreType.DMA,
             pltpu.SemaphoreType.DMA,
         ],
         name="project",
     )
     q_own, kv_copies, gate = project(
-        at, near(mine), near(other), norm_gain.reshape(1, width), kv_gain.reshape(1, -1), cosine, sine, w_side, w_kv_down, w_up
-    )
-
-    queries = [q_own] + [shifted(q_own, Q_AXIS, k) for k in range(1, n_q)]
+        at, near(mine), near(other), norm_gain.reshape(1, width), kv_gain.reshape(1, -1), near(cosine), near(sine), near(w_side),
+        near(w_up), w_kv_down,
+    )
+
+    far = shifted(q_own, Q_AXIS, n_q // 2)
+    queries = [q_own, shifted(q_own, Q_AXIS, 1), far, shifted(q_own, Q_AXIS, n_q - 1)]
     kv = exchanged(kv_copies, KV_AXES)
     n_kv = kv.shape[0]
     attend = pl.pallas_call(

time: 132 us -> 132 us (level)
  transfers between devices with their start and end apart: 11 -> 11, of which waited for: 6 -> 6; matrix products, arithmetic and copies ran while one was open for 5% -> 4% of each run, Pallas kernels for 3% -> 3%
where the time goes in v12:
time: 132 us; the launch traced here: 130 us
  starting transfers between devices  53.5 us (41%)
  waiting for transfers between devices  41.4 us (31%)
  Pallas kernels  14.7 us (11%)
  blocking collectives  13.2 us (10%)
  other arithmetic  5.1 us (4%)
  local copies, waits for them, and re-layouts  1.33 us (1%)
    all_to_all x4, starting transfers between devices, exchanged(): return lax.all_to_all(array, axes, 0, 0, tiled=True)  31.8 us
    all_to_all x4, waiting for transfers between devices, exchanged(): return lax.all_to_all(array, axes, 0, 0, tiled=True)  29.4 us
    ppermute x7, starting transfers between devices, shifted(): return lax.ppermute(array, axis, [(i, (i + k) % n) for i in range(n)])  21.7 us
    all_to_all x1, blocking collectives, exchanged(): return lax.all_to_all(array, axes, 0, 0, tiled=True)  13.2 us
    ppermute x7, waiting for transfers between devices, shifted(): return lax.ppermute(array, axis, [(i, (i + k) % n) for i in range(n)])  12.1 us
    pallas_call x1, Pallas kernels, step(): project(at, near(mine), near(other), norm_gain.reshape(1, width), kv_gain...  5.17 us
    pallas_call x1, Pallas kernels, step(): attend(to, ctx_bias.reshape(1, 1), *(near(q) for q in queries), near(kv))  4.03 us
    pallas_call x1, Pallas kernels, step(): pl.pallas_call(merge_kernel, in_specs=[smem, vmem] + [any_space] * 4, out...  2.71 us
  transfers between devices with their start and end apart: 11, of which 6 were waited for; matrix products, arithmetic and copies ran while one was open for 4% of the time, Pallas kernels for 3%

profile of v12, /device:TPU:1, one launch (start us, length us, event | category | flops | bytes accessed | tf_op | source)
XLA Modules:
  0.0 130.2 jit_solution(6580918911209604313)
XLA Ops:
  0.0 0.0 copy-start.4
  0.0 0.0 copy-start.5
  0.0 0.0 copy-start.7
  0.0 0.0 copy-start.8
  0.0 1.8 %front.1 = f32[32,5,128]{2,1,0:T(8,128)} custom-call(s32[1,1]{1,0:T(1,128)} %bitcast.3.at_ref, f32[16,128]{1,0:T(8,128)} %bitcast.20, f32[16,128]{1,0:T(8,128)} %bitcast.21, f32[64,128]{1,0:T(8,128)} %shift_ref.1, f32[64,128]{1,0:T(8,128)} %scale_ref.1, f32[64,128]{1,0:T(8,128)} %gate_ref.1), custom_call_target="tpu_custom_call" | custom-call | tf_op jit(solution)/shard_map/front/pallas_call | solution.py:259
  1.9 13.7 %all-to-all-start = ((f32[32,5,128]{2,1,0:T(8,128)}), f32[32,5,128]{2,1,0:T(8,128)S(1)}, u32[]{:S(2)}, u32[]{:S(2)}) async-start(f32[32,5,128]{2,1,0:T(8,128)} %front.1), calls=%async_computation | async-start | bytes 262144 | tf_op jit(solution)/shard_map/all_to_all | solution.py:30
  15.6 0.7 reduce
  16.3 0.8 pad_maximum_fusion.2.block_ref
  17.1 7.8 %all-to-all-done.sums_ref = f32[32,5,128]{2,1,0:T(8,128)S(1)} async-done(((f32[32,5,128]{2,1,0:T(8,128)}), f32[32,5,128]{2,1,0:T(8,128)S(1)}, u32[]{:S(2)}, u32[]{:S(2)}) %all-to-all-start) | async-done | bytes 81952 | tf_op jit(solution)/shard_map/all_to_all | solution.py:30
  24.9 0.9 pack.1
  25.8 6.8 %all-to-all-start.1 = ((bf16[8,16,2304]{2,1,0:T(8,128)(2,1)}), bf16[8,16,2304]{2,1,0:T(8,128)(2,1)S(1)}, u32[]{:S(2)}, u32[]{:S(2)}) async-start(bf16[8,16,2304]{2,1,0:T(8,128)(2,1)} %pack.1), calls=%async_computation.1 | async-start | bytes 1179648 | tf_op jit(solution)/shard_map/all_to_all | solution.py:30
  32.6 0.0 copy-done.4
  32.6 0.3 copy.18
  32.9 0.0 copy-done.5
  32.9 1.0 copy.19
  34.0 0.0 copy-done.7
  34.0 0.0 copy-done.8
  34.1 15.5 %all-to-all-done.1.own_ref = bf16[8,16,2304]{2,1,0:T(8,128)(2,1)S(1)} async-done(((bf16[8,16,2304]{2,1,0:T(8,128)(2,1)}), bf16[8,16,2304]{2,1,0:T(8,128)(2,1)S(1)}, u32[]{:S(2)}, u32[]{:S(2)}) %all-to-all-start.1) | async-done | bytes 589856 | tf_op jit(solution)/shard_map/all_to_all | solution.py:30
  49.6 4.8 %collective-permute-start = (bf16[8,16,2304]{2,1,0:T(8,128)(2,1)S(1)}, bf16[8,16,2304]{2,1,0:T(8,128)(2,1)S(1)}, u32[]{:S(2)}, u32[]{:S(2)}) collective-permute-start(bf16[8,16,2304]{2,1,0:T(8,128)(2,1)S(1)} %all-to-all-done.1.own_ref), channel_id=1, source_target_pairs={{0,1},{1,0},{2,3},{3,2},{4,5},{5,4},{6,7},{7,6},{8,9},{9,8},{10,11... | collective-permute-start | bytes 1769480 | tf_op jit(solution)/shard_map/ppermute | solution.py:48
  54.4 0.6 add_bitcast_fusion.at_ref
  55.0 0.6 sine_multiply_fusion
  55.6 1.5 %pad_maximum_fusion.w_side_ref = bf16[2048,256]{1,0:T(8,128)(2,1)S(1)} fusion(bf16[2048,64]{1,0:T(8,128)(2,1)} %copy.19, bf16[2048,64]{1,0:T(8,128)(2,1)S(1)} %copy.18, bf16[2048,128]{1,0:T(8,128)(2,1)} %param.25), kind=kLoop, calls=%fused_computation | loop fusion | flops 3145728 | bytes 2097152 | tf_op jit(solution)/shard_map/concatenate | solution.py:284
  57.2 0.0 collective-permute-done.other_ref
  57.2 5.2 %project.1 = (bf16[384,128]{1,0:T(8,128)(2,1)S(1)}, bf16[8,688,128]{2,1,0:T(8,128)(2,1)}, f32[1,2048]{1,0:T(1,128)}) custom-call(s32[1,2]{1,0:T(1,128)} %add_bitcast_fusion.at_ref, bf16[8,16,2304]{2,1,0:T(8,128)(2,1)S(1)} %all-to-all-done.1.own_ref, bf16[8,16,2304]{2,1,0:T(8,128)(2,1)S(1)} %collective-permute-done.other_ref, f32[1,2048]{1,0:T(1,128)} %bitcast.19, ...), custom_call_target="tpu_custom_call" | custom-call | tf_op jit(solution)/shard_map/project/pallas_call | solution.py:310
  62.3 0.0 copy-start
  62.3 3.7 %all-to-all-start.2 = ((bf16[8,688,128]{2,1,0:T(8,128)(2,1)}), bf16[8,688,128]{2,1,0:T(8,128)(2,1)S(1)}, u32[]{:S(2)}, u32[]{:S(2)}) async-start(bf16[8,688,128]{2,1,0:T(8,128)(2,1)} %get-tuple-element.10), calls=%async_computation.2 | async-start | bytes 2818048 | tf_op jit(solution)/shard_map/all_to_all | solution.py:30
  66.1 0.0 copy-done
  66.1 2.2 %collective-permute-start.5 = (bf16[128,2048]{1,0:T(8,128)(2,1)S(1)}, bf16[128,2048]{1,0:T(8,128)(2,1)S(1)}, u32[]{:S(2)}, u32[]{:S(2)}) collective-permute-start(bf16[128,2048]{1,0:T(8,128)(2,1)S(1)} %copy-done), channel_id=1, source_target_pairs={{0,2},{2,0},{1,3},{3,1},{4,6},{6,4},{5,7},{7,5},{8,10},{10,8},{9,1... | collective-permute-start | bytes 1572872 | tf_op jit(solution)/shard_map/ppermute | solution.py:48
  68.3 2.9 %collective-permute-start.1 = (bf16[384,128]{1,0:T(8,128)(2,1)S(1)}, bf16[384,128]{1,0:T(8,128)(2,1)S(1)}, u32[]{:S(2)}, u32[]{:S(2)}) collective-permute-start(bf16[384,128]{1,0:T(8,128)(2,1)S(1)} %get-tuple-element.9.q0), channel_id=1, source_target_pairs={{0,128},{128,256},{256,384},{384,0},{1,129},{129,257},{257,385},{3... | collective-permute-start | bytes 294920 | tf_op jit(solution)/shard_map/ppermute | solution.py:48
  71.2 3.5 %collective-permute-start.2 = (bf16[384,128]{1,0:T(8,128)(2,1)S(1)}, bf16[384,128]{1,0:T(8,128)(2,1)S(1)}, u32[]{:S(2)}, u32[]{:S(2)}) collective-permute-start(bf16[384,128]{1,0:T(8,128)(2,1)S(1)} %get-tuple-element.9.q0), channel_id=1, source_target_pairs={{0,256},{128,384},{256,0},{384,128},{1,257},{129,385},{257,1},{385... | collective-permute-start | bytes 294920 | tf_op jit(solution)/shard_map/ppermute | solution.py:48
  74.7 4.0 %collective-permute-start.3 = (bf16[384,128]{1,0:T(8,128)(2,1)S(1)}, bf16[384,128]{1,0:T(8,128)(2,1)S(1)}, u32[]{:S(2)}, u32[]{:S(2)}) collective-permute-start(bf16[384,128]{1,0:T(8,128)(2,1)S(1)} %get-tuple-element.9.q0), channel_id=1, source_target_pairs={{0,384},{128,0},{256,128},{384,256},{1,385},{129,1},{257,129},{385... | collective-permute-start | bytes 294920 | tf_op jit(solution)/shard_map/ppermute | solution.py:48
  79.4 7.9 %collective-permute-done.1.q1 = bf16[384,128]{1,0:T(8,128)(2,1)S(1)} collective-permute-done((bf16[384,128]{1,0:T(8,128)(2,1)S(1)}, bf16[384,128]{1,0:T(8,128)(2,1)S(1)}, u32[]{:S(2)}, u32[]{:S(2)}) %collective-permute-start.1) | collective-permute-done | bytes 98336 | tf_op jit(solution)/shard_map/ppermute | solution.py:48
  87.2 2.7 %collective-permute-done.2.q2 = bf16[384,128]{1,0:T(8,128)(2,1)S(1)} collective-permute-done((bf16[384,128]{1,0:T(8,128)(2,1)S(1)}, bf16[384,128]{1,0:T(8,128)(2,1)S(1)}, u32[]{:S(2)}, u32[]{:S(2)}) %collective-permute-start.2) | collective-permute-done | bytes 98336 | tf_op jit(solution)/shard_map/ppermute | solution.py:48
  90.0 0.0 collective-permute-done.3.q3
  90.0 0.0 all-to-all-done.2.kv_ref
  90.0 4.0 %attend.1 = bf16[4,4,72,128]{3,2,1,0:T(8,128)(2,1)} custom-call(s32[1,1]{1,0:T(1,128)} %bitcast.9.place_ref, f32[1,1]{1,0:T(1,128)} %bitcast.15.bias_ref, bf16[384,128]{1,0:T(8,128)(2,1)S(1)} %get-tuple-element.9.q0, bf16[384,128]{1,0:T(8,128)(2,1)S(1)} %collective-permute-done.1.q1, bf16[384,128]{1,0:T(8,128)(2,1)S(1)} %collective-permute-done.2.q2, ...), custom_call_target="tpu_custom_call" | custom-call | tf_op jit(solution)/shard_map/attend/pallas_call | solution.py:331
  94.0 0.0 copy-start.6
  94.0 0.0 copy-start.9
  94.0 7.6 %all-to-all-start.3 = ((bf16[16,72,128]{2,1,0:T(8,128)(2,1)}), bf16[16,72,128]{2,1,0:T(8,128)(2,1)S(1)}, u32[]{:S(2)}, u32[]{:S(2)}) async-start(bf16[16,72,128]{2,1,0:T(8,128)(2,1)} %bitcast.17), calls=%async_computation.3 | async-start | bytes 589824 | tf_op jit(solution)/shard_map/all_to_all | solution.py:30
  101.6 2.0 %collective-permute-start.4 = (bf16[128,2048]{1,0:T(8,128)(2,1)S(1)}, bf16[128,2048]{1,0:T(8,128)(2,1)S(1)}, u32[]{:S(2)}, u32[]{:S(2)}) collective-permute-start(bf16[128,2048]{1,0:T(8,128)(2,1)S(1)} %copy-done), channel_id=1, source_target_pairs={{0,1},{1,0},{2,3},{3,2},{4,5},{5,4},{6,7},{7,6},{8,9},{9,8},{10,11... | collective-permute-start | bytes 1572872 | tf_op jit(solution)/shard_map/ppermute | solution.py:48
  103.6 0.0 collective-permute-done.5.refs_2_
  103.6 0.0 copy-start.1
  103.6 2.3 %collective-permute-start.6 = (bf16[128,2048]{1,0:T(8,128)(2,1)S(1)}, bf16[128,2048]{1,0:T(8,128)(2,1)S(1)}, u32[]{:S(2)}, u32[]{:S(2)}) collective-permute-start(bf16[128,2048]{1,0:T(8,128)(2,1)S(1)} %collective-permute-done.5.refs_2_), channel_id=1, source_target_pairs={{0,1},{1,0},{2,3},{3,2},{4,5},{5,4},{6,7},{7,6},{8,9},{9,8},{10,11... | collective-permute-start | bytes 1572872 | tf_op jit(solution)/shard_map/ppermute | solution.py:48
  105.9 0.0 collective-permute-done.4.refs_1_
  105.9 0.0 copy-start.2
  105.9 1.5 %collective-permute-done.6.refs_3_ = bf16[128,2048]{1,0:T(8,128)(2,1)S(1)} collective-permute-done((bf16[128,2048]{1,0:T(8,128)(2,1)S(1)}, bf16[128,2048]{1,0:T(8,128)(2,1)S(1)}, u32[]{:S(2)}, u32[]{:S(2)}) %collective-permute-start.6) | collective-permute-done | bytes 524320 | tf_op jit(solution)/shard_map/ppermute | solution.py:48
  107.4 0.0 copy-start.3
  107.4 6.1 %all-to-all-done.3 = bf16[16,72,128]{2,1,0:T(8,128)(2,1)S(1)} async-done(((bf16[16,72,128]{2,1,0:T(8,128)(2,1)}), bf16[16,72,128]{2,1,0:T(8,128)(2,1)S(1)}, u32[]{:S(2)}, u32[]{:S(2)}) %all-to-all-start.3) | async-done | bytes 294944 | tf_op jit(solution)/shard_map/all_to_all | solution.py:30
  113.5 0.0 copy-done.1
  113.5 0.0 copy-done.2
  113.5 0.0 copy-done.3
  113.5 2.7 %merge.1 = bf16[4,16,2048]{2,1,0:T(8,128)(2,1)S(1)} custom-call(s32[1,2]{1,0:T(1,128)} %add_bitcast_fusion.at_ref, bf16[4,4,72,128]{3,2,1,0:T(8,128)(2,1)S(1)} %bitcast.16, bf16[128,2048]{1,0:T(8,128)(2,1)} %refs_0_.1, bf16[128,2048]{1,0:T(8,128)(2,1)} %copy-done.2, bf16[128,2048]{1,0:T(8,128)(2,1)} %copy-done.1, bf16[128,2048]{1,0:T(8,128)(2,1)} %copy-done.3), custom_call_target="tpu_custom_call" | custom-call | tf_op jit(solution)/shard_map/merge/pallas_call | solution.py:334
  116.3 13.2 %all_to_all.25 = bf16[4,16,2048]{2,1,0:T(8,128)(2,1)S(1)} all-to-all(bf16[4,16,2048]{2,1,0:T(8,128)(2,1)S(1)} %merge.1), channel_id=1, replica_groups=mesh['za'=4,'zb'=2,'x'=4,'ya'=4,'yb'=2,'c'=2] {'ya'}, dimensions={0} | all-to-all | bytes 524288 | tf_op jit(solution)/shard_map/all_to_all | solution.py:30
  129.5 0.0 copy-done.6
  129.6 0.0 copy-done.9
  129.6 0.7 add_convert_fusion
  (5 shorter events, 0.1 us)
Async XLA Ops:
  0.0 32.6 %copy-start.4 = (bf16[2048,64]{0,1:T(8,128)(2,1)S(1)}, bf16[2048,64]{0,1:T(8,128)(2,1)}, u32[]{:S(2)}) copy-start(bf16[2048,64]{0,1:T(8,128)(2,1)} %param.26) | copy-start | bytes 786436
  0.0 32.9 %copy-start.5 = (bf16[2048,64]{0,1:T(8,128)(2,1)S(1)}, bf16[2048,64]{0,1:T(8,128)(2,1)}, u32[]{:S(2)}) copy-start(bf16[2048,64]{0,1:T(8,128)(2,1)} %param.28) | copy-start | bytes 786436
  0.0 34.0 %copy-start.7 = (bf16[512,128]{1,0:T(8,128)(2,1)S(1)}, bf16[512,128]{1,0:T(8,128)(2,1)}, u32[]{:S(2)}) copy-start(bf16[512,128]{1,0:T(8,128)(2,1)} %param.31) | copy-start | bytes 393220
  0.0 34.0 %copy-start.8 = (bf16[512,128]{1,0:T(8,128)(2,1)S(1)}, bf16[512,128]{1,0:T(8,128)(2,1)}, u32[]{:S(2)}) copy-start(bf16[512,128]{1,0:T(8,128)(2,1)} %param.30) | copy-start | bytes 393220
  1.9 23.1 %all-to-all-start = ((f32[32,5,128]{2,1,0:T(8,128)}), f32[32,5,128]{2,1,0:T(8,128)S(1)}, u32[]{:S(2)}, u32[]{:S(2)}) async-start(f32[32,5,128]{2,1,0:T(8,128)} %front.1), calls=%async_computation | async-start | bytes 262144 | tf_op jit(solution)/shard_map/all_to_all | solution.py:30
  25.8 23.8 %all-to-all-start.1 = ((bf16[8,16,2304]{2,1,0:T(8,128)(2,1)}), bf16[8,16,2304]{2,1,0:T(8,128)(2,1)S(1)}, u32[]{:S(2)}, u32[]{:S(2)}) async-start(bf16[8,16,2304]{2,1,0:T(8,128)(2,1)} %pack.1), calls=%async_computation.1 | async-start | bytes 1179648 | tf_op jit(solution)/shard_map/all_to_all | solution.py:30
  49.6 7.5 %collective-permute-start = (bf16[8,16,2304]{2,1,0:T(8,128)(2,1)S(1)}, bf16[8,16,2304]{2,1,0:T(8,128)(2,1)S(1)}, u32[]{:S(2)}, u32[]{:S(2)}) collective-permute-start(bf16[8,16,2304]{2,1,0:T(8,128)(2,1)S(1)} %all-to-all-done.1.own_ref), channel_id=1, source_target_pairs={{0,1},{1,0},{2,3},{3,2},{4,5},{5,4},{6,7},{7,6},{8,9},{9,8},{10,11... | collective-permute-start | bytes 1769480 | tf_op jit(solution)/shard_map/ppermute | solution.py:48
  62.3 3.7 %copy-start = (bf16[128,2048]{1,0:T(8,128)(2,1)S(1)}, bf16[128,2048]{1,0:T(8,128)(2,1)}, u32[]{:S(2)}) copy-start(bf16[128,2048]{1,0:T(8,128)(2,1)} %refs_0_.1) | copy-start | bytes 1572868
  62.3 27.6 %all-to-all-start.2 = ((bf16[8,688,128]{2,1,0:T(8,128)(2,1)}), bf16[8,688,128]{2,1,0:T(8,128)(2,1)S(1)}, u32[]{:S(2)}, u32[]{:S(2)}) async-start(bf16[8,688,128]{2,1,0:T(8,128)(2,1)} %get-tuple-element.10), calls=%async_computation.2 | async-start | bytes 2818048 | tf_op jit(solution)/shard_map/all_to_all | solution.py:30
  66.1 37.5 %collective-permute-start.5 = (bf16[128,2048]{1,0:T(8,128)(2,1)S(1)}, bf16[128,2048]{1,0:T(8,128)(2,1)S(1)}, u32[]{:S(2)}, u32[]{:S(2)}) collective-permute-start(bf16[128,2048]{1,0:T(8,128)(2,1)S(1)} %copy-done), channel_id=1, source_target_pairs={{0,2},{2,0},{1,3},{3,1},{4,6},{6,4},{5,7},{7,5},{8,10},{10,8},{9,1... | collective-permute-start | bytes 1572872 | tf_op jit(solution)/shard_map/ppermute | solution.py:48
  68.3 19.0 %collective-permute-start.1 = (bf16[384,128]{1,0:T(8,128)(2,1)S(1)}, bf16[384,128]{1,0:T(8,128)(2,1)S(1)}, u32[]{:S(2)}, u32[]{:S(2)}) collective-permute-start(bf16[384,128]{1,0:T(8,128)(2,1)S(1)} %get-tuple-element.9.q0), channel_id=1, source_target_pairs={{0,128},{128,256},{256,384},{384,0},{1,129},{129,257},{257,385},{3... | collective-permute-start | bytes 294920 | tf_op jit(solution)/shard_map/ppermute | solution.py:48
  71.2 18.7 %collective-permute-start.2 = (bf16[384,128]{1,0:T(8,128)(2,1)S(1)}, bf16[384,128]{1,0:T(8,128)(2,1)S(1)}, u32[]{:S(2)}, u32[]{:S(2)}) collective-permute-start(bf16[384,128]{1,0:T(8,128)(2,1)S(1)} %get-tuple-element.9.q0), channel_id=1, source_target_pairs={{0,256},{128,384},{256,0},{384,128},{1,257},{129,385},{257,1},{385... | collective-permute-start | bytes 294920 | tf_op jit(solution)/shard_map/ppermute | solution.py:48
  74.7 15.2 %collective-permute-start.3 = (bf16[384,128]{1,0:T(8,128)(2,1)S(1)}, bf16[384,128]{1,0:T(8,128)(2,1)S(1)}, u32[]{:S(2)}, u32[]{:S(2)}) collective-permute-start(bf16[384,128]{1,0:T(8,128)(2,1)S(1)} %get-tuple-element.9.q0), channel_id=1, source_target_pairs={{0,384},{128,0},{256,128},{384,256},{1,385},{129,1},{257,129},{385... | collective-permute-start | bytes 294920 | tf_op jit(solution)/shard_map/ppermute | solution.py:48
  94.0 35.6 %copy-start.6 = (bf16[16,2048]{1,0:T(8,128)(2,1)S(1)}, bf16[16,2048]{1,0:T(8,128)(2,1)}, u32[]{:S(2)}) copy-start(bf16[16,2048]{1,0:T(8,128)(2,1)} %param.17) | copy-start | bytes 196612
  94.0 35.6 %copy-start.9 = (f32[1,2048]{1,0:T(1,128)S(1)}, f32[1,2048]{1,0:T(1,128)}, u32[]{:S(2)}) copy-start(f32[1,2048]{1,0:T(1,128)} %get-tuple-element.8) | copy-start | bytes 24580
  94.0 19.5 %all-to-all-start.3 = ((bf16[16,72,128]{2,1,0:T(8,128)(2,1)}), bf16[16,72,128]{2,1,0:T(8,128)(2,1)S(1)}, u32[]{:S(2)}, u32[]{:S(2)}) async-start(bf16[16,72,128]{2,1,0:T(8,128)(2,1)} %bitcast.17), calls=%async_computation.3 | async-start | bytes 589824 | tf_op jit(solution)/shard_map/all_to_all | solution.py:30
  101.6 4.4 %collective-permute-start.4 = (bf16[128,2048]{1,0:T(8,128)(2,1)S(1)}, bf16[128,2048]{1,0:T(8,128)(2,1)S(1)}, u32[]{:S(2)}, u32[]{:S(2)}) collective-permute-start(bf16[128,2048]{1,0:T(8,128)(2,1)S(1)} %copy-done), channel_id=1, source_target_pairs={{0,1},{1,0},{2,3},{3,2},{4,5},{5,4},{6,7},{7,6},{8,9},{9,8},{10,11... | collective-permute-start | bytes 1572872 | tf_op jit(solution)/shard_map/ppermute | solution.py:48
  103.6 9.9 %copy-start.1 = (bf16[128,2048]{1,0:T(8,128)(2,1)}, bf16[128,2048]{1,0:T(8,128)(2,1)S(1)}, u32[]{:S(2)}) copy-start(bf16[128,2048]{1,0:T(8,128)(2,1)S(1)} %collective-permute-done.5.refs_2_) | copy-start | bytes 1572868
  103.6 3.8 %collective-permute-start.6 = (bf16[128,2048]{1,0:T(8,128)(2,1)S(1)}, bf16[128,2048]{1,0:T(8,128)(2,1)S(1)}, u32[]{:S(2)}, u32[]{:S(2)}) collective-permute-start(bf16[128,2048]{1,0:T(8,128)(2,1)S(1)} %collective-permute-done.5.refs_2_), channel_id=1, source_target_pairs={{0,1},{1,0},{2,3},{3,2},{4,5},{5,4},{6,7},{7,6},{8,9},{9,8},{10,11... | collective-permute-start | bytes 1572872 | tf_op jit(solution)/shard_map/ppermute | solution.py:48
  105.9 7.6 %copy-start.2 = (bf16[128,2048]{1,0:T(8,128)(2,1)}, bf16[128,2048]{1,0:T(8,128)(2,1)S(1)}, u32[]{:S(2)}) copy-start(bf16[128,2048]{1,0:T(8,128)(2,1)S(1)} %collective-permute-done.4.refs_1_) | copy-start | bytes 1572868
  107.4 6.1 %copy-start.3 = (bf16[128,2048]{1,0:T(8,128)(2,1)}, bf16[128,2048]{1,0:T(8,128)(2,1)S(1)}, u32[]{:S(2)}) copy-start(bf16[128,2048]{1,0:T(8,128)(2,1)S(1)} %collective-permute-done.6.refs_3_) | copy-start | bytes 1572868
